TPU v7x, 128 devices: a whole 4x4x4 slice. The times are simulated.
128 devices in a mesh: kv: 16 (over z, y), tp: 8 (over x, core).
Axes of the slice: x: 4, y: 4, z: 4, core: 2. Of those that a mesh axis runs over, the one named last changes fastest.
Arguments:
- hidden_in: bfloat16 [16, 4096], P(None, ('kv', 'tp')), may hold values from -12 to 12
- attn_gain: float32 [4096], P('kv'), may hold values from 0.1 to 1.9
- query_weight: bfloat16 [4096, 4096], P('kv', 'tp'), may hold values from -0.09375 to 0.09375
- key_cache: bfloat16 [16, 16384, 8, 128], P(None, 'kv', 'tp'), may hold values from -600 to 600
- value_cache: bfloat16 [16, 16384, 8, 128], P(None, 'kv', 'tp'), may hold values from -6 to 6
- lambdas: float32 [32], P('tp'), may hold values from 0.3 to 0.8
- head_gain: float32 [128], replicated, may hold values from 0.1 to 1.9
- out_weight: bfloat16 [4096, 4096], P('tp', 'kv'), may hold values from -0.09375 to 0.09375
- mixer_gain: float32 [4096], P(('kv', 'tp')), may hold values from 0.1 to 1.9
- gate_weight: bfloat16 [4096, 11264], P('kv', 'tp'), may hold values from -0.09375 to 0.09375
- up_weight: bfloat16 [4096, 11264], P('kv', 'tp'), may hold values from -0.09375 to 0.09375
- down_weight: bfloat16 [11264, 4096], P('tp', 'kv'), may hold values from -0.0546875 to 0.0546875
Outputs:
- mixed: bfloat16 [16, 4096], P(None, ('kv', 'tp'))
All inputs are finite; a program needn't handle non-finite values.
Results may differ from a plain program's by a relative error of at most 0.017.
Values may be sent and summed in bfloat16 or wider, within the bound.
No kernel may reach another device: no remote copies, remote signals or barrier semaphores. Data moves between devices by JAX's collectives and lax.ppermute only.
A program may use at most 64 MiB of HBM per device.

v0:
```python
import functools
import math

import jax
import jax.numpy as jnp
from jax import lax
from jax.sharding import Mesh
from jax.sharding import PartitionSpec as P

D = 4096
HEAD_DIM = 64
TP = ("tp_0", "tp_1")
KV = ("kv_0", "kv_1")
KV_TP = ("kv_0", "kv_1", "tp_0", "tp_1")


eps = 1e-06


def from_everyone(shard, axis):
    length = lax.axis_size(axis)
    return lax.all_to_all(
        jnp.broadcast_to(shard[None], (length, *shard.shape)), axis, 0, 0, tiled=True
    )


def joined_along(tiles, dim):
    shape = list(tiles.shape[1:])
    shape[dim] *= tiles.shape[0]
    return jnp.moveaxis(tiles, 0, dim).reshape(shape)


def collect(shard, axis, dim):
    tiles = from_everyone(shard, axis)
    return joined_along(tiles, dim)


def over_copies(shard, axis):
    return from_everyone(shard, axis).sum(axis=0)


def in_one(arrays, axis):
    vector, at, gathered = (jnp.concatenate([a.reshape(-1) for a in arrays]), 0, [])
    subtotal = over_copies(vector, axis)
    for a in arrays:
        gathered.append(subtotal[at : at + a.size].reshape(a.shape))
        at += a.size
    return tuple(gathered)


def side_by_side(arrays, axis, split_dim, concat_dim, along):
    widths = [math.prod(a.shape[along:]) for a in arrays]
    both = jnp.concatenate(
        [a.reshape(*a.shape[:along], w) for a, w in zip(arrays, widths)], axis=along
    )
    whole = lax.all_to_all(both, axis, split_axis=split_dim, concat_axis=concat_dim, tiled=True)
    tiles = jnp.split(whole, [sum(widths[:k]) for k in range(1, len(widths))], axis=along)
    return tuple((b.reshape(*whole.shape[:along], *a.shape[along:]) for a, b in zip(arrays, tiles)))


def cut_along(shard, dim, length):
    before, after = (shard.shape[:dim], shard.shape[dim + 1 :])
    return jnp.moveaxis(shard.reshape(*before, length, -1, *after), dim, 0)


def summed_on_arrival(shard, axis, dim):
    tiles = cut_along(shard, dim, lax.axis_size(axis))
    arrived = lax.all_to_all(tiles, axis, split_axis=0, concat_axis=0, tiled=True)
    return arrived.astype(jnp.float32).sum(axis=0)


def by_axis(shard, axes):
    return functools.reduce(lax.psum, axes, shard)


def sent_and_summed(shard, axis, dim):
    length = lax.axis_size(axis)
    tiles = lax.all_to_all(cut_along(shard, dim, length), axis, 0, 0, tiled=True)
    return jnp.sum(tiles, axis=0)


def in_one_piece(arrays, axis, dim, along):
    widths = [a.shape[along] for a in arrays]
    both = jnp.concatenate(arrays, axis=along)
    whole = sent_and_summed(both, axis, dim)
    return tuple(jnp.split(whole, [sum(widths[:k]) for k in range(1, len(widths))], axis=along))


def finish_heads(totals, weighted, lambdas, head_gain, kv_dev, group_size):
    head_means = weighted / totals[..., None]
    mixing = lambdas.reshape(kv_dev, group_size)
    attended = head_means[0] - mixing[None, :, :, None] * head_means[1]
    norm_inv = lax.rsqrt(jnp.mean(attended * attended, axis=-1, keepdims=True) + eps)
    head_out = (attended * norm_inv * head_gain).astype(jnp.bfloat16)
    return head_out.reshape(head_out.shape[0], kv_dev * group_size * 2 * HEAD_DIM)


def per_device(
    hidden_in,
    attn_gain,
    query_weight,
    key_cache,
    value_cache,
    lambdas,
    head_gain,
    out_weight,
    mixer_gain,
    gate_weight,
    up_weight,
    down_weight,
):
    batch_rows = hidden_in.shape[0]
    rows_block = collect(hidden_in, TP, 1)
    block_f = rows_block.astype(jnp.float32)
    gained = (block_f * attn_gain).astype(jnp.bfloat16)
    partial_value = jnp.dot(gained, query_weight, preferred_element_type=jnp.float32)
    query_full, squares = in_one((partial_value, jnp.sum(block_f * block_f, axis=1)), KV)
    row_scale = lax.rsqrt(squares / D + eps)
    query_rows = (query_full * row_scale[:, None]).astype(jnp.bfloat16)
    positions = key_cache.shape[1]
    kv_dev = key_cache.shape[2]
    heads_dev = query_rows.shape[1] // (2 * HEAD_DIM)
    group_size = heads_dev // kv_dev
    query_heads = query_rows.reshape(batch_rows, kv_dev, group_size, 2, HEAD_DIM)
    key_rows = key_cache.reshape(batch_rows, positions, kv_dev, 2, HEAD_DIM)
    scores = jnp.einsum(
        "bkgcd,bpkcd->cbkgp", query_heads, key_rows, preferred_element_type=jnp.float32
    ) * HEAD_DIM ** (-0.5)
    maxima = jnp.max(scores, axis=-1)
    exponent = jnp.exp(scores - maxima[..., None])
    totals = jnp.sum(exponent, axis=-1)
    exp_weights = exponent.astype(jnp.bfloat16)
    weighted = jnp.einsum(
        "cbkgp,bpkv->cbkgv", exp_weights, value_cache, preferred_element_type=jnp.float32
    )
    parts_max, parts_tot, parts_acc = side_by_side(
        (maxima[None], totals[None], weighted[None]), KV, 2, 0, 5
    )
    top = jnp.max(parts_max, axis=0)
    factors = jnp.exp(parts_max - top[None])
    own_tot = jnp.sum(parts_tot * factors, axis=0)
    own_acc = jnp.sum(parts_acc * factors[..., None], axis=0)
    own_out = finish_heads(own_tot, own_acc, lambdas, head_gain, kv_dev, group_size)
    head_out = collect(own_out, KV, 0)
    projected = jnp.dot(head_out, out_weight, preferred_element_type=jnp.float32)
    attn_out = summed_on_arrival(projected.astype(jnp.bfloat16), TP, 1)
    after_attn = (hidden_in.astype(jnp.float32) + attn_out).astype(jnp.bfloat16)
    after_f = after_attn.astype(jnp.float32)
    squares_two = by_axis(jnp.sum(after_f * after_f, axis=1), KV_TP)
    mixer_in = (after_f * lax.rsqrt(squares_two / D + eps)[:, None] * mixer_gain).astype(
        jnp.bfloat16
    )
    gathered = collect(mixer_in, TP, 1)
    gate_part = jnp.dot(gathered, gate_weight, preferred_element_type=jnp.float32)
    up_part = jnp.dot(gathered, up_weight, preferred_element_type=jnp.float32)
    gate_sum, up_sum = in_one_piece((gate_part, up_part), KV, 1, 0)
    hidden_share = (jax.nn.silu(gate_sum) * up_sum).astype(jnp.bfloat16)
    hidden = collect(hidden_share, KV, 1)
    down_part = jnp.dot(hidden, down_weight, preferred_element_type=jnp.float32)
    mixer_out = summed_on_arrival(down_part.astype(jnp.bfloat16), TP, 1)
    return (after_f + mixer_out).astype(jnp.bfloat16)


def solution(mesh):
    split = Mesh(mesh.devices.reshape(4, 4, 4, 2), ("kv_0", "kv_1", "tp_0", "tp_1"))
    placed = (
        P(None, KV_TP),
        P(KV),
        P(KV, TP),
        P(None, KV, TP, None),
        P(None, KV, TP, None),
        P(TP),
        P(),
        P(TP, KV),
        P(KV_TP),
        P(KV, TP),
        P(KV, TP),
        P(TP, KV),
    )
    return jax.shard_map(
        per_device, mesh=split, in_specs=placed, out_specs=P(None, KV_TP), check_vma=False
    )
```

profile of v0, /device:TPU:1, one launch (start us, length us, event | category | flops | bytes accessed | tf_op | source)
XLA Modules:
  0.0 142.8 jit_solution(11357041819467350813)
XLA Ops:
  0.0 0.0 copy-start
  0.0 0.8 broadcast_in_dim.12
  0.8 0.1 reshape.255
  0.9 10.2 %all_to_all.59 = bf16[8,2,256]{2,1,0:T(2,128)(2,1)S(1)} all-to-all(bf16[8,2,256]{2,1,0:T(2,128)(2,1)S(1)} %reshape.255), channel_id=1, replica_groups=mesh['kv_0'=4,'kv_1'=4,'tp_0'=4,'tp_1'=2] {'tp_0','tp_1'}, dimensions={0} | all-to-all | bytes 16384 | tf_op jit(solution)/shard_map/all_to_all | solution.py:22
  11.1 0.1 reshape.256
  11.2 0.1 fusion.14
  11.3 0.1 reshape.253
  11.4 1.1 convolution_bitcast_fusion
  12.5 1.1 broadcast_in_dim.13
  13.6 7.8 %all-to-all-start.1 = ((f32[16,1,8208]{2,1,0:T(1,128)}), f32[16,1,8208]{2,1,0:T(1,128)S(1)}, u32[]{:S(2)}, u32[]{:S(2)}) async-start(f32[16,1,8208]{2,1,0:T(1,128)} %broadcast_in_dim.13), calls=%async_computation.1 | async-start | bytes 1064960 | tf_op jit(solution)/shard_map/all_to_all | solution.py:22
  21.4 6.4 %copy.135 = bf16[16,1024,1,128]{1,3,0,2:T(8,128)(2,1)} copy(bf16[16,1024,1,128]{3,1,2,0:T(8,128)(2,1)} %param.15) | data formatting | bytes 8388608 | tf_op args[3]
  27.8 4.1 %all-to-all-done.1 = f32[16,1,8208]{2,1,0:T(1,128)S(1)} async-done(((f32[16,1,8208]{2,1,0:T(1,128)}), f32[16,1,8208]{2,1,0:T(1,128)S(1)}, u32[]{:S(2)}, u32[]{:S(2)}) %all-to-all-start.1) | async-done | bytes 525344 | tf_op jit(solution)/shard_map/all_to_all | solution.py:22
  31.9 0.3 reduce_sum.93
  32.2 0.1 reshape.242
  32.3 0.1 fusion.18
  32.4 2.9 %fusion.36 = (f32[2,16,4]{2,1,0:T(8,128)S(1)}, f32[2,16,4,1024]{3,2,1,0:T(4,128)S(1)}) fusion(bf16[16,1024,2,64]{1,3,2,0:T(8,128)(2,1)} %bitcast.99, bf16[16,4,2,64]{3,0,2,1:T(8,128)(2,1)S(1)} %fusion.18), kind=kOutput, calls=%fused_computation.65 | convolution fusion | flops 17039232 | bytes 4735488 | tf_op jit(solution)/shard_map/bkgcd,bpkcd->cbkgp/dot_general | solution.py:126
  35.4 0.4 fusion.12
  35.7 0.3 copy.142
  36.0 0.3 copy.141
  36.4 3.0 %fusion.7 = f32[1,2,16,1,4,128]{5,4,1,2,3,0:T(4,128)S(1)} fusion(bf16[16,1024,1,128]{3,1,2,0:T(8,128)(2,1)} %param.16, bf16[2,16,4,1024]{3,2,1,0:T(4,128)(2,1)S(1)} %get-tuple-element.8), kind=kOutput, calls=%fused_computation.5 | convolution fusion | flops 33554432 | bytes 4521984 | tf_op jit(solution)/shard_map/cbkgp,bpkv->cbkgv/dot_general | solution.py:133
  39.3 0.2 maximum_bitcast_fusion
  39.5 10.1 %all_to_all.60 = f32[1,2,16,1,4,130]{5,4,1,3,0,2:T(4,128)S(1)} all-to-all(f32[1,2,16,1,4,130]{5,4,1,3,0,2:T(4,128)S(1)} %maximum_bitcast_fusion), channel_id=1, replica_groups=mesh['kv_0'=4,'kv_1'=4,'tp_0'=4,'tp_1'=2] {'kv_0','kv_1'}, dimensions={2} | all-to-all | bytes 133120 | tf_op jit(solution)/shard_map/all_to_all | solution.py:56
  49.7 0.4 copy.144
  50.1 0.1 slice_reduce_fusion
  50.1 0.1 exponential_bitcast_fusion
  50.2 0.2 fusion.29
  50.4 0.4 fusion.10
  50.8 0.1 copy.146
  50.9 0.0 copy-done.5
  50.9 0.1 copy.147
  51.0 0.1 mul.164
  51.1 0.1 mul.158
  51.1 0.0 copy-done.6
  51.2 0.5 broadcast.113
  51.7 0.7 reduce.12
  52.5 9.5 %all_to_all.61 = bf16[16,2,256]{2,1,0:T(2,128)(2,1)S(1)} all-to-all(bf16[16,2,256]{2,1,0:T(2,128)(2,1)S(1)} %reshape.257), channel_id=1, replica_groups=mesh['kv_0'=4,'kv_1'=4,'tp_0'=4,'tp_1'=2] {'kv_0','kv_1'}, dimensions={0} | all-to-all | bytes 32768 | tf_op jit(solution)/shard_map/all_to_all | solution.py:22
  62.0 0.1 convolution_convert_fusion.1
  62.2 0.1 reshape.248
  62.3 0.1 reshape.259
  62.4 11.0 %all_to_all.62 = bf16[8,2,256]{2,1,0:T(2,128)(2,1)S(1)} all-to-all(bf16[8,2,256]{2,1,0:T(2,128)(2,1)S(1)} %reshape.259), channel_id=1, replica_groups=mesh['kv_0'=4,'kv_1'=4,'tp_0'=4,'tp_1'=2] {'tp_0','tp_1'}, dimensions={0} | all-to-all | bytes 16384 | tf_op jit(solution)/shard_map/all_to_all | solution.py:68
  73.4 0.1 reshape.260
  73.5 0.1 fusion.22
  73.6 6.9 %psum.28 = f32[16]{0:T(128)S(1)} all-reduce(f32[16]{0:T(128)S(1)} %get-tuple-element.5), channel_id=1, replica_groups=mesh['kv_0'=4,'kv_1'=4,'tp_0'=4,'tp_1'=2] {'kv_0'}, use_global_device_ids=true, to_apply=%region_10.0 | all-reduce | flops 16 | bytes 128 | tf_op jit(solution)/shard_map/psum | solution.py:73
  80.5 6.9 %psum.29 = f32[16]{0:T(128)S(1)} all-reduce(f32[16]{0:T(128)S(1)} %psum.28), channel_id=1, replica_groups=mesh['kv_0'=4,'kv_1'=4,'tp_0'=4,'tp_1'=2] {'kv_1'}, use_global_device_ids=true, to_apply=%region_11.0 | all-reduce | flops 16 | bytes 128 | tf_op jit(solution)/shard_map/psum | solution.py:73
  87.4 6.9 %psum.30 = f32[16]{0:T(128)S(1)} all-reduce(f32[16]{0:T(128)S(1)} %psum.29), channel_id=1, replica_groups=mesh['kv_0'=4,'kv_1'=4,'tp_0'=4,'tp_1'=2] {'tp_0'}, use_global_device_ids=true, to_apply=%region_12.0 | all-reduce | flops 16 | bytes 128 | tf_op jit(solution)/shard_map/psum | solution.py:73
  94.3 8.9 %psum.31 = f32[16]{0:T(128)S(1)} all-reduce(f32[16]{0:T(128)S(1)} %psum.30), channel_id=1, replica_groups=mesh['kv_0'=4,'kv_1'=4,'tp_0'=4,'tp_1'=2] {'tp_1'}, use_global_device_ids=true, to_apply=%region_13.0 | all-reduce | flops 16 | bytes 128 | tf_op jit(solution)/shard_map/psum | solution.py:73
  103.1 0.1 fusion.24
  103.2 0.1 reshape.261
  103.3 7.3 %all_to_all.63 = bf16[8,2,256]{2,1,0:T(2,128)(2,1)S(1)} all-to-all(bf16[8,2,256]{2,1,0:T(2,128)(2,1)S(1)} %reshape.261), channel_id=1, replica_groups=mesh['kv_0'=4,'kv_1'=4,'tp_0'=4,'tp_1'=2] {'tp_0','tp_1'}, dimensions={0} | all-to-all | bytes 16384 | tf_op jit(solution)/shard_map/all_to_all | solution.py:22
  110.6 0.1 reshape.262
  110.7 0.1 reshape.249
  110.8 0.2 fusion.37
  111.0 0.2 fusion.38
  111.3 0.2 reshape.250
  111.5 0.1 copy.187
  111.6 10.7 %all_to_all.64 = f32[16,32,88]{2,1,0:T(8,128)S(1)} all-to-all(f32[16,32,88]{2,1,0:T(8,128)S(1)} %bitcast.104), channel_id=1, replica_groups=mesh['kv_0'=4,'kv_1'=4,'tp_0'=4,'tp_1'=2] {'kv_0','kv_1'}, dimensions={0} | all-to-all | bytes 360448 | tf_op jit(solution)/shard_map/all_to_all | solution.py:78
  122.4 9.1 %all_to_all.65 = bf16[16,16,88]{2,1,0:T(8,128)(2,1)S(1)} all-to-all(bf16[16,16,88]{2,1,0:T(8,128)(2,1)S(1)} %broadcast_in_dim.17), channel_id=1, replica_groups=mesh['kv_0'=4,'kv_1'=4,'tp_0'=4,'tp_1'=2] {'kv_0','kv_1'}, dimensions={0} | all-to-all | bytes 90112 | tf_op jit(solution)/shard_map/all_to_all | solution.py:22
  131.5 0.1 reshape.251
  131.7 0.2 convolution_convert_fusion
  131.9 0.1 reshape.252
  132.0 0.1 reshape.263
  132.1 10.0 %all_to_all.66 = bf16[8,2,256]{2,1,0:T(2,128)(2,1)S(1)} all-to-all(bf16[8,2,256]{2,1,0:T(2,128)(2,1)S(1)} %reshape.263), channel_id=1, replica_groups=mesh['kv_0'=4,'kv_1'=4,'tp_0'=4,'tp_1'=2] {'tp_0','tp_1'}, dimensions={0} | all-to-all | bytes 16384 | tf_op jit(solution)/shard_map/all_to_all | solution.py:68
  142.1 0.1 reshape.264
  142.2 0.6 fusion.25
  (41 shorter events, 0.4 us)
Async XLA Ops:
  0.0 110.8 %copy-start = (bf16[256,1408]{1,0:T(8,128)(2,1)S(1)}, bf16[256,1408]{1,0:T(8,128)(2,1)}, u32[]{:S(2)}) copy-start(bf16[256,1408]{1,0:T(8,128)(2,1)} %param.21) | copy-start | bytes 2162692
  13.6 18.3 %all-to-all-start.1 = ((f32[16,1,8208]{2,1,0:T(1,128)}), f32[16,1,8208]{2,1,0:T(1,128)S(1)}, u32[]{:S(2)}, u32[]{:S(2)}) async-start(f32[16,1,8208]{2,1,0:T(1,128)} %broadcast_in_dim.13), calls=%async_computation.1 | async-start | bytes 1064960 | tf_op jit(solution)/shard_map/all_to_all | solution.py:22
  35.3 15.5 %copy-start.5 = (f32[4]{0:T(128)S(1)}, f32[4]{0:T(128)}, u32[]{:S(2)}) copy-start(f32[4]{0:T(128)} %param.17) | copy-start | bytes 52
  35.4 15.8 %copy-start.6 = (f32[128]{0:T(128)S(1)}, f32[128]{0:T(128)}, u32[]{:S(2)}) copy-start(f32[128]{0:T(128)} %param.18) | copy-start | bytes 1540
  35.4 26.7 %copy-start.3 = (bf16[512,256]{1,0:T(8,128)(2,1)S(1)}, bf16[512,256]{1,0:T(8,128)(2,1)}, u32[]{:S(2)}) copy-start(bf16[512,256]{1,0:T(8,128)(2,1)} %param.19) | copy-start | bytes 786436
  36.0 37.5 %copy-start.4 = (bf16[16,32]{1,0:T(8,128)(2,1)S(1)}, bf16[16,32]{1,0:T(8,128)(2,1)}, u32[]{:S(2)}) copy-start(bf16[16,32]{1,0:T(8,128)(2,1)} %param.12) | copy-start | bytes 3076
  36.0 67.1 %copy-start.7 = (f32[32]{0:T(128)S(1)}, f32[32]{0:T(128)}, u32[]{:S(2)}) copy-start(f32[32]{0:T(128)} %param.20) | copy-start | bytes 388
  36.3 74.7 %copy-start.1 = (bf16[256,1408]{1,0:T(8,128)(2,1)S(1)}, bf16[256,1408]{1,0:T(8,128)(2,1)}, u32[]{:S(2)}) copy-start(bf16[256,1408]{1,0:T(8,128)(2,1)} %param.22) | copy-start | bytes 2162692
  39.3 92.3 %copy-start.2 = (bf16[1408,256]{1,0:T(8,128)(2,1)S(1)}, bf16[1408,256]{1,0:T(8,128)(2,1)}, u32[]{:S(2)}) copy-start(bf16[1408,256]{1,0:T(8,128)(2,1)} %param.23) | copy-start | bytes 2162692
where the time goes:
time: 144 us; the launch traced here: 143 us
  blocking collectives  107 us (74%)
  local copies, waits for them, and re-layouts  11.9 us (8%)
  matrix products  7.77 us (5%)
  starting transfers between devices  7.77 us (5%)
  waiting for transfers between devices  4.08 us (3%)
  other arithmetic  3.54 us (2%)
    all_to_all x4, blocking collectives, from_everyone(): lax.all_to_all(jnp.broadcast_to(shard[None], (length, *shard.shape)), axi...  36.2 us
    psum x4, blocking collectives, by_axis(): return functools.reduce(lax.psum, axes, shard)  29.5 us
    all_to_all x2, blocking collectives, summed_on_arrival(): lax.all_to_all(tiles, axis, split_axis=0, concat_axis=0, tiled=True)  21 us
    all_to_all x1, blocking collectives, sent_and_summed(): lax.all_to_all(cut_along(shard, dim, length), axis, 0, 0, tiled=True)  10.7 us
    all_to_all x1, blocking collectives, side_by_side(): lax.all_to_all(both, axis, split_axis=split_dim, concat_axis=concat_dim,...  10.1 us
    all_to_all x1, starting transfers between devices, from_everyone(): lax.all_to_all(jnp.broadcast_to(shard[None], (length, *shard.shape)), axi...  7.77 us
    unnamed x28, local copies, waits for them, and re-layouts  7.24 us
    all_to_all x1, waiting for transfers between devices, from_everyone(): lax.all_to_all(jnp.broadcast_to(shard[None], (length, *shard.shape)), axi...  4.08 us
  transfers between devices with their start and end apart: 1, of which 1 were waited for; matrix products, arithmetic and copies ran while one was open for 4% of the time, Pallas kernels for 0%

commit v1 on v0

v1 whole, which is shorter than its diff:
```python
import jax
import jax.numpy as jnp
from jax import lax
from jax.sharding import Mesh
from jax.sharding import PartitionSpec as P

D = 4096
HEAD_DIM = 64
TP = ("tp_0", "tp_1")
KV = ("kv_0", "kv_1")
KV_TP = ("kv_0", "kv_1", "tp_0", "tp_1")
LANES = 128

eps = 1e-06


def to_all(shard, axis):
    length = lax.axis_size(axis)
    return lax.all_to_all(
        jnp.broadcast_to(shard[None], (length, *shard.shape)), axis, 0, 0, tiled=True
    )


def peers(shard, axis):
    n = lax.axis_size(axis)
    return [
        lax.ppermute(shard, axis, [(i, (i + s) % n) for i in range(n)]) for s in range(1, n)
    ]


def merged(parts):
    tops = [p[0] for p in parts]
    top = tops[0]
    for t in tops[1:]:
        top = jnp.maximum(top, t)
    total, acc = 0.0, 0.0
    for m, t, a in parts:
        f = jnp.exp(m - top)
        total = total + t * f
        acc = acc + a * f[..., None]
    return top, total, acc


def per_device(
    hidden_in,
    attn_gain,
    query_weight,
    key_cache,
    value_cache,
    lambdas,
    head_gain,
    out_weight,
    mixer_gain,
    gate_weight,
    up_weight,
    down_weight,
):
    batch = hidden_in.shape[0]
    n_tp = lax.axis_size(TP)
    n_kv = lax.axis_size(KV)
    own = hidden_in.astype(jnp.float32)
    first = to_all(jnp.concatenate([own, mixer_gain[None]], axis=0), TP)
    first = jnp.moveaxis(first, 0, 1).reshape(batch + 1, -1)
    block_f, mix_gain = first[:batch], first[batch:]
    gained = (block_f * attn_gain).astype(jnp.bfloat16)
    partial = jnp.dot(gained, query_weight, preferred_element_type=jnp.float32)
    heads = partial.shape[1] // LANES
    squares = jnp.sum(block_f * block_f, axis=1)
    packed = jnp.concatenate(
        [
            jnp.moveaxis(partial.reshape(batch, heads, LANES), 1, 0).reshape(-1, LANES),
            jnp.pad(squares[None], ((0, 7), (0, LANES - batch))),
        ],
        axis=0,
    )
    summed = to_all(packed, KV).sum(axis=0)
    inv = lax.rsqrt(summed[heads * batch, :batch] / D + eps)
    query = (
        summed[: heads * batch].reshape(heads, batch, LANES) * inv[None, :, None]
    ).astype(jnp.bfloat16)
    half = lax.broadcasted_iota(jnp.int32, (2, 1, 1, LANES), 3) // HEAD_DIM
    which = lax.broadcasted_iota(jnp.int32, (2, 1, 1, LANES), 0)
    split = jnp.where(half == which, query[None], jnp.zeros((), jnp.bfloat16))
    split = jnp.transpose(split, (2, 0, 1, 3)).reshape(batch, 2 * heads, LANES)
    positions = key_cache.shape[1]
    keys = key_cache.reshape(batch, positions, LANES)
    values = value_cache.reshape(batch, positions, LANES)
    scores = jnp.einsum(
        "brd,bpd->brp", split, keys, preferred_element_type=jnp.float32
    ) * HEAD_DIM ** (-0.5)
    maxima = jnp.max(scores, axis=-1)
    exponent = jnp.exp(scores - maxima[..., None])
    totals = jnp.sum(exponent, axis=-1)
    weighted = jnp.einsum(
        "brp,bpv->brv",
        exponent.astype(jnp.bfloat16),
        values,
        preferred_element_type=jnp.float32,
    )
    state = (maxima, totals, weighted)
    rows = batch * 2 * heads
    for axis in KV[::-1]:
        pack = jnp.concatenate(
            [
                state[2].reshape(rows, LANES),
                state[0].reshape(-1, LANES),
                state[1].reshape(-1, LANES),
                jnp.zeros((8 - 2 * rows // LANES, LANES), jnp.float32),
            ],
            axis=0,
        )
        parts = [state]
        k = rows // LANES
        for got in peers(pack, axis):
            parts.append(
                (
                    got[rows : rows + k].reshape(maxima.shape),
                    got[rows + k : rows + 2 * k].reshape(maxima.shape),
                    got[:rows].reshape(weighted.shape),
                )
            )
        state = merged(parts)
    means = (state[2] / state[1][..., None]).reshape(batch, 2, heads, LANES)
    attended = means[:, 0] - lambdas[None, :, None] * means[:, 1]
    norm = lax.rsqrt(jnp.mean(attended * attended, axis=-1, keepdims=True) + eps)
    head_out = (attended * norm * head_gain).astype(jnp.bfloat16).reshape(batch, -1)
    projected = jnp.dot(head_out, out_weight, preferred_element_type=jnp.float32)
    attn_out = to_all(projected.astype(jnp.bfloat16), TP).astype(jnp.float32).sum(axis=0)
    after_attn = (block_f + attn_out).astype(jnp.bfloat16)
    after_f = after_attn.astype(jnp.float32)
    squares_two = jnp.sum(after_f * after_f, axis=1, keepdims=True)
    mixer_in = (after_f * mix_gain).astype(jnp.bfloat16)
    gate_part = jnp.dot(mixer_in, gate_weight, preferred_element_type=jnp.float32)
    up_part = jnp.dot(mixer_in, up_weight, preferred_element_type=jnp.float32)
    width = gate_part.shape[1]
    both = jnp.concatenate(
        [gate_part, up_part, jnp.broadcast_to(squares_two, (batch, LANES))], axis=1
    ).reshape(batch, -1, LANES)
    row = lax.all_to_all(both, KV, 0, 0, tiled=True).sum(axis=0)
    k = width // LANES
    inv_two = lax.rsqrt(row[2 * k :, :] / D + eps)
    gate_sum, up_sum = row[:k] * inv_two, row[k : 2 * k] * inv_two
    hidden_share = (jax.nn.silu(gate_sum) * up_sum).astype(jnp.bfloat16)
    hidden = to_all(hidden_share, KV).reshape(batch, width)
    down_part = jnp.dot(hidden, down_weight, preferred_element_type=jnp.float32)
    tiles = jnp.moveaxis(down_part.astype(jnp.bfloat16).reshape(batch, n_tp, -1), 1, 0)
    arrived = lax.all_to_all(tiles, TP, 0, 0, tiled=True)
    mixer_out = arrived.astype(jnp.float32).sum(axis=0)
    cols = own.shape[1]
    mine = lax.dynamic_slice_in_dim(after_f, lax.axis_index(TP) * cols, cols, 1)
    return (mine + mixer_out).astype(jnp.bfloat16)


def solution(mesh):
    split = Mesh(mesh.devices.reshape(4, 4, 4, 2), ("kv_0", "kv_1", "tp_0", "tp_1"))
    placed = (
        P(None, KV_TP),
        P(KV),
        P(KV, TP),
        P(None, KV, TP, None),
        P(None, KV, TP, None),
        P(TP),
        P(),
        P(TP, KV),
        P(KV_TP),
        P(KV, TP),
        P(KV, TP),
        P(TP, KV),
    )
    return jax.shard_map(
        per_device, mesh=split, in_specs=placed, out_specs=P(None, KV_TP), check_vma=False
    )
```

time: 144 us -> 104 us (0.72)
  blocking collectives: 107 us -> 19.6 us
  waiting for transfers between devices: 4.08 us -> 31.1 us
  starting transfers between devices: 7.77 us -> 32.7 us
  local copies, waits for them, and re-layouts: 11.9 us -> 7.5 us
    all_to_all x8 -> x2, blocking collectives: 77.9 us -> 19.6 us  [the longest x1 10.1 us: per_device(): row = lax.all_to_all(both, KV, 0, 0, tiled=True).sum(axis=0)]
    psum x4 -> x0, blocking collectives: 29.5 us -> none  [by_axis(): return functools.reduce(lax.psum, axes, shard)]
    all_to_all x1 -> x4, starting transfers between devices: 7.77 us -> 28.6 us  [the longest x3 22.1 us: to_all(): lax.all_to_all(jnp.broadcast_to(shard[None], (length, *shard.shape)), axi...]
    all_to_all x1 -> x4, waiting for transfers between devices: 4.08 us -> 23.1 us  [the longest x3 18.5 us: to_all(): lax.all_to_all(jnp.broadcast_to(shard[None], (length, *shard.shape)), axi...]
    ppermute x0 -> x6, waiting for transfers between devices: none -> 7.94 us  [peers(): lax.ppermute(shard, axis, [(i, (i + s) % n) for i in range(n)])]
    unnamed x28 -> x16, local copies, waits for them, and re-layouts: 7.24 us -> 1.58 us
    ppermute x0 -> x6, starting transfers between devices: none -> 4.03 us  [peers(): lax.ppermute(shard, axis, [(i, (i + s) % n) for i in range(n)])]
  transfers between devices with their start and end apart: 1 -> 10, of which waited for: 1 -> 10; matrix products, arithmetic and copies ran while one was open for 4% -> 3% of each run, Pallas kernels for 0% -> 0%
where the time goes in v1:
time: 104 us; the launch traced here: 103 us
  starting transfers between devices  32.7 us (31%)
  waiting for transfers between devices  31.1 us (30%)
  blocking collectives  19.6 us (19%)
  local copies, waits for them, and re-layouts  7.5 us (7%)
  matrix products  7.35 us (7%)
  other arithmetic  4.48 us (4%)
    all_to_all x3, starting transfers between devices, to_all(): lax.all_to_all(jnp.broadcast_to(shard[None], (length, *shard.shape)), axi...  22.1 us
    all_to_all x3, waiting for transfers between devices, to_all(): lax.all_to_all(jnp.broadcast_to(shard[None], (length, *shard.shape)), axi...  18.5 us
    all_to_all x1, blocking collectives, per_device(): row = lax.all_to_all(both, KV, 0, 0, tiled=True).sum(axis=0)  10.1 us
    all_to_all x1, blocking collectives, to_all(): lax.all_to_all(jnp.broadcast_to(shard[None], (length, *shard.shape)), axi...  9.48 us
    ppermute x6, waiting for transfers between devices, peers(): lax.ppermute(shard, axis, [(i, (i + s) % n) for i in range(n)])  7.94 us
    all_to_all x1, starting transfers between devices, per_device(): arrived = lax.all_to_all(tiles, TP, 0, 0, tiled=True)  6.58 us
    all_to_all x1, waiting for transfers between devices, per_device(): arrived = lax.all_to_all(tiles, TP, 0, 0, tiled=True)  4.64 us
    ppermute x6, starting transfers between devices, peers(): lax.ppermute(shard, axis, [(i, (i + s) % n) for i in range(n)])  4.03 us
  transfers between devices with their start and end apart: 10, of which 10 were waited for; matrix products, arithmetic and copies ran while one was open for 3% of the time, Pallas kernels for 0%

profile of v1, /device:TPU:1, one launch (start us, length us, event | category | flops | bytes accessed | tf_op | source)
XLA Modules:
  0.0 103.0 jit_solution(9003985251413843324)
XLA Ops:
  0.0 0.8 convert_element_type.58
  0.8 0.7 pad_maximum_fusion.1
  1.4 0.7 reshape.528
  2.1 5.8 %all-to-all-start = ((f32[8,1,544]{2,1,0:T(1,128)}), f32[8,1,544]{2,1,0:T(1,128)S(1)}, u32[]{:S(2)}, u32[]{:S(2)}) async-start(f32[8,1,544]{2,1,0:T(1,128)} %reshape.528), calls=%async_computation | async-start | bytes 40960 | tf_op jit(solution)/shard_map/all_to_all | solution.py:19
  7.9 0.8 mul.252
  8.7 1.1 %copy.33 = bf16[512,256]{1,0:T(8,128)(2,1)S(1)} copy(bf16[512,256]{0,1:T(8,128)(2,1)} %bitcast.150) | data formatting | bytes 524288 | tf_op jit(solution)/shard_map/dot_general | solution.py:66
  9.8 2.8 %all-to-all-done = f32[8,1,544]{2,1,0:T(1,128)S(1)} async-done(((f32[8,1,544]{2,1,0:T(1,128)}), f32[8,1,544]{2,1,0:T(1,128)S(1)}, u32[]{:S(2)}, u32[]{:S(2)}) %all-to-all-start) | async-done | bytes 17440 | tf_op jit(solution)/shard_map/all_to_all | solution.py:19
  12.6 0.5 broadcast.164
  13.1 0.7 reduce.50
  13.9 0.2 fusion.50
  14.1 0.1 reshape.464
  14.2 0.2 fusion.53
  14.4 0.9 broadcast_in_dim.48
  15.2 7.8 %all-to-all-start.1 = ((f32[16,72,128]{2,1,0:T(8,128)}), f32[16,72,128]{2,1,0:T(8,128)S(1)}, u32[]{:S(2)}, u32[]{:S(2)}) async-start(f32[16,72,128]{2,1,0:T(8,128)} %broadcast_in_dim.48), calls=%async_computation.1 | async-start | bytes 1179648 | tf_op jit(solution)/shard_map/all_to_all | solution.py:19
  23.1 11.0 %all-to-all-done.1 = f32[16,72,128]{2,1,0:T(8,128)S(1)} async-done(((f32[16,72,128]{2,1,0:T(8,128)}), f32[16,72,128]{2,1,0:T(8,128)S(1)}, u32[]{:S(2)}, u32[]{:S(2)}) %all-to-all-start.1) | async-done | bytes 589856 | tf_op jit(solution)/shard_map/all_to_all | solution.py:19
  34.3 3.5 %fusion.52 = (f32[16,8]{1,0:T(8,128)S(1)}, f32[16,8,1024]{2,1,0:T(8,128)S(1)}) fusion(bf16[16,1024,1,128]{3,1,2,0:T(8,128)(2,1)} %param.15, bf16[16,8,128]{2,1,0:T(8,128)(2,1)S(1)} %bitcast.152, pred[8,128]{1,0:T(8,128)(4,1)S(1)} %bitcast.160), kind=kOutput, calls=%fused_computation.117 | convolution fusion | flops 33832832 | bytes 4752896 | tf_op jit(solution)/shard_map/brd,bpd->brp/dot_general | solution.py:88
  37.8 0.1 reshape.439
  37.9 0.2 fusion.7
  38.1 3.0 %fusion = f32[16,8,128]{2,1,0:T(8,128)S(1)} fusion(bf16[16,1024,1,128]{3,1,2,0:T(8,128)(2,1)} %param.16, f32[16,8,1024]{2,1,0:T(8,128)S(1)} %get-tuple-element.41, f32[16,8]{1,0:T(8,128)S(1)} %get-tuple-element.40), kind=kOutput, calls=%fused_computation | convolution fusion | flops 33816576 | bytes 4784640 | tf_op jit(solution)/shard_map/brp,bpv->brv/dot_general | solution.py:94
  41.1 0.1 reshape.440
  41.2 0.1 maximum_maximum_fusion
  41.3 0.2 collective-permute-start.2
  41.5 1.9 %collective-permute-start.1 = (f32[136,128]{1,0:T(8,128)S(1)}, f32[136,128]{1,0:T(8,128)S(1)}, u32[]{:S(2)}, u32[]{:S(2)}) collective-permute-start(f32[136,128]{1,0:T(8,128)S(1)} %maximum_maximum_fusion), channel_id=1, source_target_pairs={{0,16},{8,24},{16,0},{24,8},{1,17},{9,25},{17,1},{25,9},{2,18},{10... | collective-permute-start | bytes 208904 | tf_op jit(solution)/shard_map/ppermute | solution.py:27
  43.4 1.1 %collective-permute-done.2 = f32[136,128]{1,0:T(8,128)S(1)} collective-permute-done((f32[136,128]{1,0:T(8,128)S(1)}, f32[136,128]{1,0:T(8,128)S(1)}, u32[]{:S(2)}, u32[]{:S(2)}) %collective-permute-start.2) | collective-permute-done | bytes 69664 | tf_op jit(solution)/shard_map/ppermute | solution.py:27
  44.5 1.6 %collective-permute-done.1 = f32[136,128]{1,0:T(8,128)S(1)} collective-permute-done((f32[136,128]{1,0:T(8,128)S(1)}, f32[136,128]{1,0:T(8,128)S(1)}, u32[]{:S(2)}, u32[]{:S(2)}) %collective-permute-start.1) | collective-permute-done | bytes 69664 | tf_op jit(solution)/shard_map/ppermute | solution.py:27
  46.1 1.6 %collective-permute-done = f32[136,128]{1,0:T(8,128)S(1)} collective-permute-done((f32[136,128]{1,0:T(8,128)S(1)}, f32[136,128]{1,0:T(8,128)S(1)}, u32[]{:S(2)}, u32[]{:S(2)}) %collective-permute-start) | collective-permute-done | bytes 69664 | tf_op jit(solution)/shard_map/ppermute | solution.py:27
  47.8 0.1 reshape.441
  47.9 0.1 reshape.442
  48.0 0.1 reshape.443
  48.1 0.1 fusion.60
  48.2 0.1 maximum_maximum_fusion.1
  48.3 0.6 collective-permute-start.5
  49.0 0.6 collective-permute-start.4
  49.6 0.6 collective-permute-start.3
  50.3 0.1 reshape.454
  50.4 0.1 reshape.456
  50.5 1.0 collective-permute-done.5
  51.6 0.1 reshape.450
  51.7 0.1 reshape.459
  51.7 2.0 %collective-permute-done.4 = f32[136,128]{1,0:T(8,128)S(1)} collective-permute-done((f32[136,128]{1,0:T(8,128)S(1)}, f32[136,128]{1,0:T(8,128)S(1)}, u32[]{:S(2)}, u32[]{:S(2)}) %collective-permute-start.4) | collective-permute-done | bytes 69664 | tf_op jit(solution)/shard_map/ppermute | solution.py:27
  53.8 0.1 reshape.458
  53.9 0.1 reshape.449
  54.0 0.5 collective-permute-done.3
  54.5 0.1 reshape.457
  54.7 0.2 fusion.13
  54.9 0.2 fusion.30
  55.2 0.2 convolution_convert_fusion.1
  55.4 0.6 broadcast_in_dim.91
  56.0 8.5 %all-to-all-start.2 = ((bf16[8,16,256]{2,1,0:T(8,128)(2,1)}), bf16[8,16,256]{2,1,0:T(8,128)(2,1)S(1)}, u32[]{:S(2)}, u32[]{:S(2)}) async-start(bf16[8,16,256]{2,1,0:T(8,128)(2,1)} %broadcast_in_dim.91), calls=%async_computation.2 | async-start | bytes 131072 | tf_op jit(solution)/shard_map/all_to_all | solution.py:19
  64.5 0.1 mul.304
  64.6 0.1 slice.86
  64.7 4.7 %all-to-all-done.2 = bf16[8,16,256]{2,1,0:T(8,128)(2,1)S(1)} async-done(((bf16[8,16,256]{2,1,0:T(8,128)(2,1)}), bf16[8,16,256]{2,1,0:T(8,128)(2,1)S(1)}, u32[]{:S(2)}, u32[]{:S(2)}) %all-to-all-start.2) | async-done | bytes 65568 | tf_op jit(solution)/shard_map/all_to_all | solution.py:19
  69.5 0.2 multiply_reduce_fusion
  69.7 0.2 fusion.41
  69.9 0.2 fusion.42
  70.3 10.1 %all_to_all.30 = f32[16,23,128]{2,1,0:T(8,128)S(1)} all-to-all(f32[16,23,128]{2,1,0:T(8,128)S(1)} %reshape.461), channel_id=1, replica_groups=mesh['kv_0'=4,'kv_1'=4,'tp_0'=4,'tp_1'=2] {'kv_0','kv_1'}, dimensions={0} | all-to-all | bytes 376832 | tf_op jit(solution)/shard_map/all_to_all | solution.py:139
  80.5 9.5 %all_to_all.31 = bf16[16,11,128]{2,1,0:T(8,128)(2,1)S(1)} all-to-all(bf16[16,11,128]{2,1,0:T(8,128)(2,1)S(1)} %broadcast_in_dim.93), channel_id=1, replica_groups=mesh['kv_0'=4,'kv_1'=4,'tp_0'=4,'tp_1'=2] {'kv_0','kv_1'}, dimensions={0} | all-to-all | bytes 90112 | tf_op jit(solution)/shard_map/all_to_all | solution.py:19
  89.9 0.2 convolution_convert_fusion
  90.1 0.1 reshape.463
  90.3 0.7 reshape.530
  91.0 6.6 %all-to-all-start.5 = ((bf16[8,2,256]{2,1,0:T(2,128)(2,1)}), bf16[8,2,256]{2,1,0:T(2,128)(2,1)S(1)}, u32[]{:S(2)}, u32[]{:S(2)}) async-start(bf16[8,2,256]{2,1,0:T(2,128)(2,1)} %reshape.530), calls=%async_computation.5 | async-start | bytes 16384 | tf_op jit(solution)/shard_map/all_to_all | solution.py:147
  97.5 4.6 %all-to-all-done.5 = bf16[8,2,256]{2,1,0:T(2,128)(2,1)S(1)} async-done(((bf16[8,2,256]{2,1,0:T(2,128)(2,1)}), bf16[8,2,256]{2,1,0:T(2,128)(2,1)S(1)}, u32[]{:S(2)}, u32[]{:S(2)}) %all-to-all-start.5) | async-done | bytes 8224 | tf_op jit(solution)/shard_map/all_to_all | solution.py:147
  102.2 0.1 reshape.531
  102.3 0.7 add_convert_fusion.2
  (55 shorter events, 1.2 us)
Async XLA Ops:
  0.0 69.7 %copy-start = (bf16[256,1408]{1,0:T(8,128)(2,1)S(1)}, bf16[256,1408]{1,0:T(8,128)(2,1)}, u32[]{:S(2)}) copy-start(bf16[256,1408]{1,0:T(8,128)(2,1)} %param.22) | copy-start | bytes 2162692
  2.1 10.5 %all-to-all-start = ((f32[8,1,544]{2,1,0:T(1,128)}), f32[8,1,544]{2,1,0:T(1,128)S(1)}, u32[]{:S(2)}, u32[]{:S(2)}) async-start(f32[8,1,544]{2,1,0:T(1,128)} %reshape.528), calls=%async_computation | async-start | bytes 40960 | tf_op jit(solution)/shard_map/all_to_all | solution.py:19
  15.2 18.9 %all-to-all-start.1 = ((f32[16,72,128]{2,1,0:T(8,128)}), f32[16,72,128]{2,1,0:T(8,128)S(1)}, u32[]{:S(2)}, u32[]{:S(2)}) async-start(f32[16,72,128]{2,1,0:T(8,128)} %broadcast_in_dim.48), calls=%async_computation.1 | async-start | bytes 1179648 | tf_op jit(solution)/shard_map/all_to_all | solution.py:19
  37.7 11.2 %copy-start.4 = (f32[4]{0:T(128)S(1)}, f32[4]{0:T(128)}, u32[]{:S(2)}) copy-start(f32[4]{0:T(128)} %param.17) | copy-start | bytes 52
  37.8 11.2 %copy-start.5 = (f32[128]{0:T(128)S(1)}, f32[128]{0:T(128)}, u32[]{:S(2)}) copy-start(f32[128]{0:T(128)} %param.18) | copy-start | bytes 1540
  37.8 17.5 %copy-start.3 = (bf16[512,256]{1,0:T(8,128)(2,1)S(1)}, bf16[512,256]{1,0:T(8,128)(2,1)}, u32[]{:S(2)}) copy-start(bf16[512,256]{1,0:T(8,128)(2,1)} %param.19) | copy-start | bytes 786436
  38.1 31.8 %copy-start.1 = (bf16[256,1408]{1,0:T(8,128)(2,1)S(1)}, bf16[256,1408]{1,0:T(8,128)(2,1)}, u32[]{:S(2)}) copy-start(bf16[256,1408]{1,0:T(8,128)(2,1)} %param.21) | copy-start | bytes 2162692
  41.1 48.9 %copy-start.2 = (bf16[1408,256]{1,0:T(8,128)(2,1)S(1)}, bf16[1408,256]{1,0:T(8,128)(2,1)}, u32[]{:S(2)}) copy-start(bf16[1408,256]{1,0:T(8,128)(2,1)} %param.23) | copy-start | bytes 2162692
  41.3 3.2 %collective-permute-start.2 = (f32[136,128]{1,0:T(8,128)S(1)}, f32[136,128]{1,0:T(8,128)S(1)}, u32[]{:S(2)}, u32[]{:S(2)}) collective-permute-start(f32[136,128]{1,0:T(8,128)S(1)} %maximum_maximum_fusion), channel_id=1, source_target_pairs={{0,24},{8,0},{16,8},{24,16},{1,25},{9,1},{17,9},{25,17},{2,26},{10... | collective-permute-start | bytes 208904 | tf_op jit(solution)/shard_map/ppermute | solution.py:27
  41.5 4.7 %collective-permute-start.1 = (f32[136,128]{1,0:T(8,128)S(1)}, f32[136,128]{1,0:T(8,128)S(1)}, u32[]{:S(2)}, u32[]{:S(2)}) collective-permute-start(f32[136,128]{1,0:T(8,128)S(1)} %maximum_maximum_fusion), channel_id=1, source_target_pairs={{0,16},{8,24},{16,0},{24,8},{1,17},{9,25},{17,1},{25,9},{2,18},{10... | collective-permute-start | bytes 208904 | tf_op jit(solution)/shard_map/ppermute | solution.py:27
  43.4 4.4 %collective-permute-start = (f32[136,128]{1,0:T(8,128)S(1)}, f32[136,128]{1,0:T(8,128)S(1)}, u32[]{:S(2)}, u32[]{:S(2)}) collective-permute-start(f32[136,128]{1,0:T(8,128)S(1)} %maximum_maximum_fusion), channel_id=1, source_target_pairs={{0,8},{8,16},{16,24},{24,0},{1,9},{9,17},{17,25},{25,1},{2,10},{10... | collective-permute-start | bytes 208904 | tf_op jit(solution)/shard_map/ppermute | solution.py:27
  48.3 3.2 %collective-permute-start.5 = (f32[136,128]{1,0:T(8,128)S(1)}, f32[136,128]{1,0:T(8,128)S(1)}, u32[]{:S(2)}, u32[]{:S(2)}) collective-permute-start(f32[136,128]{1,0:T(8,128)S(1)} %maximum_maximum_fusion.1), channel_id=1, source_target_pairs={{0,96},{32,0},{64,32},{96,64},{1,97},{33,1},{65,33},{97,65},{2,98}... | collective-permute-start | bytes 208904 | tf_op jit(solution)/shard_map/ppermute | solution.py:27
  49.0 4.7 %collective-permute-start.4 = (f32[136,128]{1,0:T(8,128)S(1)}, f32[136,128]{1,0:T(8,128)S(1)}, u32[]{:S(2)}, u32[]{:S(2)}) collective-permute-start(f32[136,128]{1,0:T(8,128)S(1)} %maximum_maximum_fusion.1), channel_id=1, source_target_pairs={{0,64},{32,96},{64,0},{96,32},{1,65},{33,97},{65,1},{97,33},{2,66}... | collective-permute-start | bytes 208904 | tf_op jit(solution)/shard_map/ppermute | solution.py:27
  49.6 4.8 %collective-permute-start.3 = (f32[136,128]{1,0:T(8,128)S(1)}, f32[136,128]{1,0:T(8,128)S(1)}, u32[]{:S(2)}, u32[]{:S(2)}) collective-permute-start(f32[136,128]{1,0:T(8,128)S(1)} %maximum_maximum_fusion.1), channel_id=1, source_target_pairs={{0,32},{32,64},{64,96},{96,0},{1,33},{33,65},{65,97},{97,1},{2,34}... | collective-permute-start | bytes 208904 | tf_op jit(solution)/shard_map/ppermute | solution.py:27
  56.0 13.4 %all-to-all-start.2 = ((bf16[8,16,256]{2,1,0:T(8,128)(2,1)}), bf16[8,16,256]{2,1,0:T(8,128)(2,1)S(1)}, u32[]{:S(2)}, u32[]{:S(2)}) async-start(bf16[8,16,256]{2,1,0:T(8,128)(2,1)} %broadcast_in_dim.91), calls=%async_computation.2 | async-start | bytes 131072 | tf_op jit(solution)/shard_map/all_to_all | solution.py:19
  91.0 11.2 %all-to-all-start.5 = ((bf16[8,2,256]{2,1,0:T(2,128)(2,1)}), bf16[8,2,256]{2,1,0:T(2,128)(2,1)S(1)}, u32[]{:S(2)}, u32[]{:S(2)}) async-start(bf16[8,2,256]{2,1,0:T(2,128)(2,1)} %reshape.530), calls=%async_computation.5 | async-start | bytes 16384 | tf_op jit(solution)/shard_map/all_to_all | solution.py:147

commit v2 on v1

--- a/solution.py
+++ b/solution.py
@@ -23,9 +23,14 @@
 
 def peers(shard, axis):
     n = lax.axis_size(axis)
-    return [
-        lax.ppermute(shard, axis, [(i, (i + s) % n) for i in range(n)]) for s in range(1, n)
-    ]
+    near = [1, 3, 2] if n == 4 else list(range(1, n))
+    return [lax.ppermute(shard, axis, [(i, i ^ s) for i in range(n)]) for s in near]
+
+
+def added(own, got):
+    for p in got:
+        own = own + p
+    return own
 
 
 def merged(parts):
@@ -57,27 +62,21 @@
 ):
     batch = hidden_in.shape[0]
     n_tp = lax.axis_size(TP)
-    n_kv = lax.axis_size(KV)
     own = hidden_in.astype(jnp.float32)
     first = to_all(jnp.concatenate([own, mixer_gain[None]], axis=0), TP)
     first = jnp.moveaxis(first, 0, 1).reshape(batch + 1, -1)
     block_f, mix_gain = first[:batch], first[batch:]
     gained = (block_f * attn_gain).astype(jnp.bfloat16)
     partial = jnp.dot(gained, query_weight, preferred_element_type=jnp.float32)
-    heads = partial.shape[1] // LANES
-    squares = jnp.sum(block_f * block_f, axis=1)
-    packed = jnp.concatenate(
-        [
-            jnp.moveaxis(partial.reshape(batch, heads, LANES), 1, 0).reshape(-1, LANES),
-            jnp.pad(squares[None], ((0, 7), (0, LANES - batch))),
-        ],
-        axis=0,
-    )
-    summed = to_all(packed, KV).sum(axis=0)
-    inv = lax.rsqrt(summed[heads * batch, :batch] / D + eps)
-    query = (
-        summed[: heads * batch].reshape(heads, batch, LANES) * inv[None, :, None]
-    ).astype(jnp.bfloat16)
+    width_q = partial.shape[1]
+    heads = width_q // LANES
+    squares = jnp.sum(block_f * block_f, axis=1, keepdims=True)
+    packed = jnp.concatenate([partial, jnp.broadcast_to(squares, (batch, LANES))], axis=1)
+    for axis in KV[::-1]:
+        packed = added(packed, peers(packed, axis))
+    inv = lax.rsqrt(packed[:, width_q : width_q + 1] / D + eps)
+    query = (packed[:, :width_q] * inv).astype(jnp.bfloat16)
+    query = jnp.moveaxis(query.reshape(batch, heads, LANES), 1, 0)
     half = lax.broadcasted_iota(jnp.int32, (2, 1, 1, LANES), 3) // HEAD_DIM
     which = lax.broadcasted_iota(jnp.int32, (2, 1, 1, LANES), 0)
     split = jnp.where(half == which, query[None], jnp.zeros((), jnp.bfloat16))
@@ -133,15 +132,20 @@
     gate_part = jnp.dot(mixer_in, gate_weight, preferred_element_type=jnp.float32)
     up_part = jnp.dot(mixer_in, up_weight, preferred_element_type=jnp.float32)
     width = gate_part.shape[1]
-    both = jnp.concatenate(
-        [gate_part, up_part, jnp.broadcast_to(squares_two, (batch, LANES))], axis=1
-    ).reshape(batch, -1, LANES)
-    row = lax.all_to_all(both, KV, 0, 0, tiled=True).sum(axis=0)
-    k = width // LANES
-    inv_two = lax.rsqrt(row[2 * k :, :] / D + eps)
-    gate_sum, up_sum = row[:k] * inv_two, row[k : 2 * k] * inv_two
-    hidden_share = (jax.nn.silu(gate_sum) * up_sum).astype(jnp.bfloat16)
-    hidden = to_all(hidden_share, KV).reshape(batch, width)
+    both = jnp.concatenate([gate_part, up_part], axis=1)
+    lane = lax.broadcasted_iota(jnp.int32, (batch, LANES), 1)
+    for axis in KV[::-1]:
+        head = lax.reduce_precision(squares_two, 8, 7)
+        tail = jnp.where(lane < LANES // 2, head, squares_two - head)
+        sent = jnp.concatenate([both, tail], axis=1).astype(jnp.bfloat16)
+        got = [p.astype(jnp.float32) for p in peers(sent, axis)]
+        both = added(both, [p[:, : 2 * width] for p in got])
+        squares_two = added(
+            squares_two, [p[:, 2 * width : 2 * width + 1] + p[:, -1:] for p in got]
+        )
+    inv_two = lax.rsqrt(squares_two / D + eps)
+    gate_sum, up_sum = both[:, :width] * inv_two, both[:, width:] * inv_two
+    hidden = (jax.nn.silu(gate_sum) * up_sum).astype(jnp.bfloat16)
     down_part = jnp.dot(hidden, down_weight, preferred_element_type=jnp.float32)
     tiles = jnp.moveaxis(down_part.astype(jnp.bfloat16).reshape(batch, n_tp, -1), 1, 0)
     arrived = lax.all_to_all(tiles, TP, 0, 0, tiled=True)

time: 104 us -> 99 us (0.952)
  blocking collectives: 19.6 us -> 0 us
  starting transfers between devices: 32.7 us -> 46.1 us
  local copies, waits for them, and re-layouts: 7.5 us -> 4.79 us
  waiting for transfers between devices: 31.1 us -> 33.8 us
    all_to_all x2 -> x0, blocking collectives: 19.6 us -> none  [the longest x1 10.1 us: per_device(): row = lax.all_to_all(both, KV, 0, 0, tiled=True).sum(axis=0)]
    ppermute x6 -> x18, starting transfers between devices: 4.03 us -> 22.9 us  [peers(): lax.ppermute(shard, axis, [(i, i ^ s) for i in range(n)])]
    ppermute x6 -> x18, waiting for transfers between devices: 7.94 us -> 19.7 us  [peers(): lax.ppermute(shard, axis, [(i, i ^ s) for i in range(n)])]
    all_to_all x3 -> x2, waiting for transfers between devices: 18.5 us -> 9.45 us  [to_all(): lax.all_to_all(jnp.broadcast_to(shard[None], (length, *shard.shape)), axi...]
    all_to_all x3 -> x2, starting transfers between devices: 22.1 us -> 15.9 us  [to_all(): lax.all_to_all(jnp.broadcast_to(shard[None], (length, *shard.shape)), axi...]
    dot_general x1 -> x0, local copies, waits for them, and re-layouts: 1.08 us -> none  [per_device(): partial = jnp.dot(gained, query_weight, preferred_element_type=jnp.float32)]
  transfers between devices with their start and end apart: 10 -> 21, of which waited for: 10 -> 15; matrix products, arithmetic and copies ran while one was open for 3% -> 1% of each run, Pallas kernels for 0% -> 0%
where the time goes in v2:
time: 99 us; the launch traced here: 98.6 us
  starting transfers between devices  46.1 us (47%)
  waiting for transfers between devices  33.8 us (34%)
  matrix products  8.36 us (8%)
  other arithmetic  5.28 us (5%)
  local copies, waits for them, and re-layouts  4.79 us (5%)
    ppermute x18, starting transfers between devices, peers(): lax.ppermute(shard, axis, [(i, i ^ s) for i in range(n)])  22.9 us
    ppermute x18, waiting for transfers between devices, peers(): lax.ppermute(shard, axis, [(i, i ^ s) for i in range(n)])  19.7 us
    all_to_all x2, starting transfers between devices, to_all(): lax.all_to_all(jnp.broadcast_to(shard[None], (length, *shard.shape)), axi...  15.9 us
    all_to_all x2, waiting for transfers between devices, to_all(): lax.all_to_all(jnp.broadcast_to(shard[None], (length, *shard.shape)), axi...  9.45 us
    all_to_all x1, starting transfers between devices, per_device(): arrived = lax.all_to_all(tiles, TP, 0, 0, tiled=True)  7.26 us
    all_to_all x1, waiting for transfers between devices, per_device(): arrived = lax.all_to_all(tiles, TP, 0, 0, tiled=True)  4.64 us
    dot_general x1, matrix products, per_device(): jnp.einsum('brd,bpd->brp', split, keys, preferred_element_type=jnp.float32)  3.45 us
    dot_general x1, matrix products, per_device(): jnp.einsum('brp,bpv->brv', exponent.astype(jnp.bfloat16), values, preferr...  2.96 us
  transfers between devices with their start and end apart: 21, of which 15 were waited for; matrix products, arithmetic and copies ran while one was open for 1% of the time, Pallas kernels for 0%

profile of v2, /device:TPU:1, one launch (start us, length us, event | category | flops | bytes accessed | tf_op | source)
XLA Modules:
  0.0 98.6 jit_solution(13398801978390485487)
XLA Ops:
  0.0 0.8 convert_element_type.69
  0.8 0.7 pad_maximum_fusion.3
  1.4 0.7 reshape.499
  2.1 5.8 %all-to-all-start = ((f32[8,1,544]{2,1,0:T(1,128)}), f32[8,1,544]{2,1,0:T(1,128)S(1)}, u32[]{:S(2)}, u32[]{:S(2)}) async-start(f32[8,1,544]{2,1,0:T(1,128)} %reshape.499), calls=%async_computation | async-start | bytes 40960 | tf_op jit(solution)/shard_map/all_to_all | solution.py:19
  7.9 4.7 %all-to-all-done = f32[8,1,544]{2,1,0:T(1,128)S(1)} async-done(((f32[8,1,544]{2,1,0:T(1,128)}), f32[8,1,544]{2,1,0:T(1,128)S(1)}, u32[]{:S(2)}, u32[]{:S(2)}) %all-to-all-start) | async-done | bytes 17440 | tf_op jit(solution)/shard_map/all_to_all | solution.py:19
  12.6 0.5 broadcast.152
  13.1 0.7 reduce.58
  13.9 0.2 fusion.64
  14.2 1.1 %fusion.42 = f32[16,512]{1,0:T(8,128)S(1)} fusion(bf16[256,512]{1,0:T(8,128)(2,1)} %param.14, f32[16,256]{1,0:T(8,128)S(1)} %slice.137, f32[256]{0:T(256)} %param.13), kind=kOutput, calls=%fused_computation.79 | convolution fusion | flops 4202496 | bytes 312320 | tf_op jit(solution)/shard_map/dot_general | solution.py:70
  15.4 1.3 %collective-permute-start = (f32[16,640]{1,0:T(8,128)S(1)}, f32[16,640]{1,0:T(8,128)S(1)}, u32[]{:S(2)}, u32[]{:S(2)}) collective-permute-start(f32[16,640]{1,0:T(8,128)S(1)} %pad_maximum_fusion.2), channel_id=1, source_target_pairs={{0,8},{8,0},{16,24},{24,16},{1,9},{9,1},{17,25},{25,17},{2,10},{10... | collective-permute-start | bytes 122888 | tf_op jit(solution)/shard_map/ppermute | solution.py:27
  16.7 1.9 %collective-permute-start.1 = (f32[16,640]{1,0:T(8,128)S(1)}, f32[16,640]{1,0:T(8,128)S(1)}, u32[]{:S(2)}, u32[]{:S(2)}) collective-permute-start(f32[16,640]{1,0:T(8,128)S(1)} %pad_maximum_fusion.2), channel_id=1, source_target_pairs={{0,24},{8,16},{16,8},{24,0},{1,25},{9,17},{17,9},{25,1},{2,26},{10... | collective-permute-start | bytes 122888 | tf_op jit(solution)/shard_map/ppermute | solution.py:27
  18.6 0.7 collective-permute-start.2
  19.3 1.4 %collective-permute-done.1 = f32[16,640]{1,0:T(8,128)S(1)} collective-permute-done((f32[16,640]{1,0:T(8,128)S(1)}, f32[16,640]{1,0:T(8,128)S(1)}, u32[]{:S(2)}, u32[]{:S(2)}) %collective-permute-start.1) | collective-permute-done | bytes 40992 | tf_op jit(solution)/shard_map/ppermute | solution.py:27
  20.8 2.2 %collective-permute-done.2 = f32[16,640]{1,0:T(8,128)S(1)} collective-permute-done((f32[16,640]{1,0:T(8,128)S(1)}, f32[16,640]{1,0:T(8,128)S(1)}, u32[]{:S(2)}, u32[]{:S(2)}) %collective-permute-start.2) | collective-permute-done | bytes 40992 | tf_op jit(solution)/shard_map/ppermute | solution.py:27
  23.0 1.7 %collective-permute-start.3 = (f32[16,640]{1,0:T(8,128)S(1)}, f32[16,640]{1,0:T(8,128)S(1)}, u32[]{:S(2)}, u32[]{:S(2)}) collective-permute-start(f32[16,640]{1,0:T(8,128)S(1)} %add_add_fusion.1), channel_id=1, source_target_pairs={{0,32},{32,0},{64,96},{96,64},{1,33},{33,1},{65,97},{97,65},{2,34}... | collective-permute-start | bytes 122888 | tf_op jit(solution)/shard_map/ppermute | solution.py:27
  24.7 2.2 %collective-permute-start.4 = (f32[16,640]{1,0:T(8,128)S(1)}, f32[16,640]{1,0:T(8,128)S(1)}, u32[]{:S(2)}, u32[]{:S(2)}) collective-permute-start(f32[16,640]{1,0:T(8,128)S(1)} %add_add_fusion.1), channel_id=1, source_target_pairs={{0,96},{32,64},{64,32},{96,0},{1,97},{33,65},{65,33},{97,1},{2,98}... | collective-permute-start | bytes 122888 | tf_op jit(solution)/shard_map/ppermute | solution.py:27
  26.9 1.1 %collective-permute-start.5 = (f32[16,640]{1,0:T(8,128)S(1)}, f32[16,640]{1,0:T(8,128)S(1)}, u32[]{:S(2)}, u32[]{:S(2)}) collective-permute-start(f32[16,640]{1,0:T(8,128)S(1)} %add_add_fusion.1), channel_id=1, source_target_pairs={{0,64},{32,96},{64,0},{96,32},{1,65},{33,97},{65,1},{97,33},{2,66}... | collective-permute-start | bytes 122888 | tf_op jit(solution)/shard_map/ppermute | solution.py:27
  28.1 0.7 collective-permute-done.4
  28.8 2.5 %collective-permute-done.5 = f32[16,640]{1,0:T(8,128)S(1)} collective-permute-done((f32[16,640]{1,0:T(8,128)S(1)}, f32[16,640]{1,0:T(8,128)S(1)}, u32[]{:S(2)}, u32[]{:S(2)}) %collective-permute-start.5) | collective-permute-done | bytes 40992 | tf_op jit(solution)/shard_map/ppermute | solution.py:27
  31.3 0.1 fusion.56
  31.6 3.5 %fusion.67 = (f32[16,8]{1,0:T(8,128)S(1)}, f32[16,8,1024]{2,1,0:T(8,128)S(1)}) fusion(bf16[16,1024,1,128]{3,1,2,0:T(8,128)(2,1)} %param.15, bf16[16,8,128]{2,1,0:T(8,128)(2,1)S(1)} %bitcast.132, pred[8,128]{1,0:T(8,128)(4,1)S(1)} %bitcast.138), kind=kOutput, calls=%fused_computation.149 | convolution fusion | flops 33832832 | bytes 4752896 | tf_op jit(solution)/shard_map/brd,bpd->brp/dot_general | solution.py:87
  35.0 0.1 reshape.410
  35.1 0.2 fusion.7
  35.4 3.0 %fusion = f32[16,8,128]{2,1,0:T(8,128)S(1)} fusion(bf16[16,1024,1,128]{3,1,2,0:T(8,128)(2,1)} %param.16, f32[16,8,1024]{2,1,0:T(8,128)S(1)} %get-tuple-element.47, f32[16,8]{1,0:T(8,128)S(1)} %get-tuple-element.46), kind=kOutput, calls=%fused_computation | convolution fusion | flops 33816576 | bytes 4784640 | tf_op jit(solution)/shard_map/brp,bpv->brv/dot_general | solution.py:93
  38.3 0.1 reshape.411
  38.5 0.5 collective-permute-start.6
  39.0 0.7 collective-permute-start.7
  39.7 2.1 %collective-permute-start.8 = (f32[136,128]{1,0:T(8,128)S(1)}, f32[136,128]{1,0:T(8,128)S(1)}, u32[]{:S(2)}, u32[]{:S(2)}) collective-permute-start(f32[136,128]{1,0:T(8,128)S(1)} %maximum_maximum_fusion), channel_id=1, source_target_pairs={{0,16},{8,24},{16,0},{24,8},{1,17},{9,25},{17,1},{25,9},{2,18},{10... | collective-permute-start | bytes 208904 | tf_op jit(solution)/shard_map/ppermute | solution.py:27
  41.9 1.5 %collective-permute-done.7 = f32[136,128]{1,0:T(8,128)S(1)} collective-permute-done((f32[136,128]{1,0:T(8,128)S(1)}, f32[136,128]{1,0:T(8,128)S(1)}, u32[]{:S(2)}, u32[]{:S(2)}) %collective-permute-start.7) | collective-permute-done | bytes 69664 | tf_op jit(solution)/shard_map/ppermute | solution.py:27
  43.4 1.0 %collective-permute-done.8 = f32[136,128]{1,0:T(8,128)S(1)} collective-permute-done((f32[136,128]{1,0:T(8,128)S(1)}, f32[136,128]{1,0:T(8,128)S(1)}, u32[]{:S(2)}, u32[]{:S(2)}) %collective-permute-start.8) | collective-permute-done | bytes 69664 | tf_op jit(solution)/shard_map/ppermute | solution.py:27
  44.7 0.1 fusion.75
  45.0 0.9 collective-permute-start.9
  45.9 0.6 collective-permute-start.10
  46.5 1.9 %collective-permute-start.11 = (f32[136,128]{1,0:T(8,128)S(1)}, f32[136,128]{1,0:T(8,128)S(1)}, u32[]{:S(2)}, u32[]{:S(2)}) collective-permute-start(f32[136,128]{1,0:T(8,128)S(1)} %maximum_maximum_fusion.1), channel_id=1, source_target_pairs={{0,64},{32,96},{64,0},{96,32},{1,65},{33,97},{65,1},{97,33},{2,66}... | collective-permute-start | bytes 208904 | tf_op jit(solution)/shard_map/ppermute | solution.py:27
  48.8 1.5 %collective-permute-done.10 = f32[136,128]{1,0:T(8,128)S(1)} collective-permute-done((f32[136,128]{1,0:T(8,128)S(1)}, f32[136,128]{1,0:T(8,128)S(1)}, u32[]{:S(2)}, u32[]{:S(2)}) %collective-permute-start.10) | collective-permute-done | bytes 69664 | tf_op jit(solution)/shard_map/ppermute | solution.py:27
  50.4 0.7 collective-permute-done.11
  51.5 0.2 fusion.15
  51.8 0.2 fusion.34
  52.1 0.2 convolution_convert_fusion.1
  52.2 0.6 broadcast_in_dim.102
  52.9 10.1 %all-to-all-start.1 = ((bf16[8,16,256]{2,1,0:T(8,128)(2,1)}), bf16[8,16,256]{2,1,0:T(8,128)(2,1)S(1)}, u32[]{:S(2)}, u32[]{:S(2)}) async-start(bf16[8,16,256]{2,1,0:T(8,128)(2,1)} %broadcast_in_dim.102), calls=%async_computation.1 | async-start | bytes 131072 | tf_op jit(solution)/shard_map/all_to_all | solution.py:19
  63.1 4.8 %all-to-all-done.1 = bf16[8,16,256]{2,1,0:T(8,128)(2,1)S(1)} async-done(((bf16[8,16,256]{2,1,0:T(8,128)(2,1)}), bf16[8,16,256]{2,1,0:T(8,128)(2,1)S(1)}, u32[]{:S(2)}, u32[]{:S(2)}) %all-to-all-start.1) | async-done | bytes 65568 | tf_op jit(solution)/shard_map/all_to_all | solution.py:19
  68.0 0.2 fusion.69
  68.2 0.2 fusion.68
  68.4 0.2 multiply_reduce_fusion
  68.7 1.0 %collective-permute-start.12 = (bf16[16,2944]{1,0:T(8,128)(2,1)S(1)}, bf16[16,2944]{1,0:T(8,128)(2,1)S(1)}, u32[]{:S(2)}, u32[]{:S(2)}) collective-permute-start(bf16[16,2944]{1,0:T(8,128)(2,1)S(1)} %pad_maximum_fusion), channel_id=1, source_target_pairs={{0,8},{8,0},{16,24},{24,16},{1,9},{9,1},{17,25},{25,17},{2,10},{10... | collective-permute-start | bytes 282632 | tf_op jit(solution)/shard_map/ppermute | solution.py:27
  69.7 1.9 %collective-permute-start.13 = (bf16[16,2944]{1,0:T(8,128)(2,1)S(1)}, bf16[16,2944]{1,0:T(8,128)(2,1)S(1)}, u32[]{:S(2)}, u32[]{:S(2)}) collective-permute-start(bf16[16,2944]{1,0:T(8,128)(2,1)S(1)} %pad_maximum_fusion), channel_id=1, source_target_pairs={{0,24},{8,16},{16,8},{24,0},{1,25},{9,17},{17,9},{25,1},{2,26},{10... | collective-permute-start | bytes 282632 | tf_op jit(solution)/shard_map/ppermute | solution.py:27
  71.6 0.7 collective-permute-start.14
  72.4 1.9 %collective-permute-done.13 = bf16[16,2944]{1,0:T(8,128)(2,1)S(1)} collective-permute-done((bf16[16,2944]{1,0:T(8,128)(2,1)S(1)}, bf16[16,2944]{1,0:T(8,128)(2,1)S(1)}, u32[]{:S(2)}, u32[]{:S(2)}) %collective-permute-start.13) | collective-permute-done | bytes 94240 | tf_op jit(solution)/shard_map/ppermute | solution.py:27
  74.4 2.3 %collective-permute-done.14 = bf16[16,2944]{1,0:T(8,128)(2,1)S(1)} collective-permute-done((bf16[16,2944]{1,0:T(8,128)(2,1)S(1)}, bf16[16,2944]{1,0:T(8,128)(2,1)S(1)}, u32[]{:S(2)}, u32[]{:S(2)}) %collective-permute-start.14) | collective-permute-done | bytes 94240 | tf_op jit(solution)/shard_map/ppermute | solution.py:27
  76.7 0.2 reduce-precision_reduce_fusion
  77.0 0.3 collective-permute-start.15
  77.3 2.2 %collective-permute-start.16 = (bf16[16,2944]{1,0:T(8,128)(2,1)S(1)}, bf16[16,2944]{1,0:T(8,128)(2,1)S(1)}, u32[]{:S(2)}, u32[]{:S(2)}) collective-permute-start(bf16[16,2944]{1,0:T(8,128)(2,1)S(1)} %pad_maximum_fusion.1), channel_id=1, source_target_pairs={{0,96},{32,64},{64,32},{96,0},{1,97},{33,65},{65,33},{97,1},{2,98}... | collective-permute-start | bytes 282632 | tf_op jit(solution)/shard_map/ppermute | solution.py:27
  79.6 1.1 %collective-permute-start.17 = (bf16[16,2944]{1,0:T(8,128)(2,1)S(1)}, bf16[16,2944]{1,0:T(8,128)(2,1)S(1)}, u32[]{:S(2)}, u32[]{:S(2)}) collective-permute-start(bf16[16,2944]{1,0:T(8,128)(2,1)S(1)} %pad_maximum_fusion.1), channel_id=1, source_target_pairs={{0,64},{32,96},{64,0},{96,32},{1,65},{33,97},{65,1},{97,33},{2,66}... | collective-permute-start | bytes 282632 | tf_op jit(solution)/shard_map/ppermute | solution.py:27
  80.6 1.3 %collective-permute-done.16 = bf16[16,2944]{1,0:T(8,128)(2,1)S(1)} collective-permute-done((bf16[16,2944]{1,0:T(8,128)(2,1)S(1)}, bf16[16,2944]{1,0:T(8,128)(2,1)S(1)}, u32[]{:S(2)}, u32[]{:S(2)}) %collective-permute-start.16) | collective-permute-done | bytes 94240 | tf_op jit(solution)/shard_map/ppermute | solution.py:27
  82.0 2.6 %collective-permute-done.17 = bf16[16,2944]{1,0:T(8,128)(2,1)S(1)} collective-permute-done((bf16[16,2944]{1,0:T(8,128)(2,1)S(1)}, bf16[16,2944]{1,0:T(8,128)(2,1)S(1)}, u32[]{:S(2)}, u32[]{:S(2)}) %collective-permute-start.17) | collective-permute-done | bytes 94240 | tf_op jit(solution)/shard_map/ppermute | solution.py:27
  84.6 0.2 fusion.48
  84.8 0.2 convolution_convert_fusion
  85.1 0.1 reshape.432
  85.2 0.7 reshape.501
  85.9 7.3 %all-to-all-start.2 = ((bf16[8,2,256]{2,1,0:T(2,128)(2,1)}), bf16[8,2,256]{2,1,0:T(2,128)(2,1)S(1)}, u32[]{:S(2)}, u32[]{:S(2)}) async-start(bf16[8,2,256]{2,1,0:T(2,128)(2,1)} %reshape.501), calls=%async_computation.2 | async-start | bytes 16384 | tf_op jit(solution)/shard_map/all_to_all | solution.py:151
  93.2 4.6 %all-to-all-done.2 = bf16[8,2,256]{2,1,0:T(2,128)(2,1)S(1)} async-done(((bf16[8,2,256]{2,1,0:T(2,128)(2,1)}), bf16[8,2,256]{2,1,0:T(2,128)(2,1)S(1)}, u32[]{:S(2)}, u32[]{:S(2)}) %all-to-all-start.2) | async-done | bytes 8224 | tf_op jit(solution)/shard_map/all_to_all | solution.py:151
  97.8 0.1 reshape.502
  97.9 0.7 add_convert_fusion.2
  (82 shorter events, 2.7 us)
Async XLA Ops:
  0.0 68.0 %copy-start = (bf16[256,1408]{1,0:T(8,128)(2,1)S(1)}, bf16[256,1408]{1,0:T(8,128)(2,1)}, u32[]{:S(2)}) copy-start(bf16[256,1408]{1,0:T(8,128)(2,1)} %param.21) | copy-start | bytes 2162692
  2.1 10.5 %all-to-all-start = ((f32[8,1,544]{2,1,0:T(1,128)}), f32[8,1,544]{2,1,0:T(1,128)S(1)}, u32[]{:S(2)}, u32[]{:S(2)}) async-start(f32[8,1,544]{2,1,0:T(1,128)} %reshape.499), calls=%async_computation | async-start | bytes 40960 | tf_op jit(solution)/shard_map/all_to_all | solution.py:19
  15.4 4.0 %collective-permute-start = (f32[16,640]{1,0:T(8,128)S(1)}, f32[16,640]{1,0:T(8,128)S(1)}, u32[]{:S(2)}, u32[]{:S(2)}) collective-permute-start(f32[16,640]{1,0:T(8,128)S(1)} %pad_maximum_fusion.2), channel_id=1, source_target_pairs={{0,8},{8,0},{16,24},{24,16},{1,9},{9,1},{17,25},{25,17},{2,10},{10... | collective-permute-start | bytes 122888 | tf_op jit(solution)/shard_map/ppermute | solution.py:27
  16.7 4.1 %collective-permute-start.1 = (f32[16,640]{1,0:T(8,128)S(1)}, f32[16,640]{1,0:T(8,128)S(1)}, u32[]{:S(2)}, u32[]{:S(2)}) collective-permute-start(f32[16,640]{1,0:T(8,128)S(1)} %pad_maximum_fusion.2), channel_id=1, source_target_pairs={{0,24},{8,16},{16,8},{24,0},{1,25},{9,17},{17,9},{25,1},{2,26},{10... | collective-permute-start | bytes 122888 | tf_op jit(solution)/shard_map/ppermute | solution.py:27
  18.6 4.4 %collective-permute-start.2 = (f32[16,640]{1,0:T(8,128)S(1)}, f32[16,640]{1,0:T(8,128)S(1)}, u32[]{:S(2)}, u32[]{:S(2)}) collective-permute-start(f32[16,640]{1,0:T(8,128)S(1)} %pad_maximum_fusion.2), channel_id=1, source_target_pairs={{0,16},{8,24},{16,0},{24,8},{1,17},{9,25},{17,1},{25,9},{2,18},{10... | collective-permute-start | bytes 122888 | tf_op jit(solution)/shard_map/ppermute | solution.py:27
  23.0 5.1 %collective-permute-start.3 = (f32[16,640]{1,0:T(8,128)S(1)}, f32[16,640]{1,0:T(8,128)S(1)}, u32[]{:S(2)}, u32[]{:S(2)}) collective-permute-start(f32[16,640]{1,0:T(8,128)S(1)} %add_add_fusion.1), channel_id=1, source_target_pairs={{0,32},{32,0},{64,96},{96,64},{1,33},{33,1},{65,97},{97,65},{2,34}... | collective-permute-start | bytes 122888 | tf_op jit(solution)/shard_map/ppermute | solution.py:27
  24.7 4.1 %collective-permute-start.4 = (f32[16,640]{1,0:T(8,128)S(1)}, f32[16,640]{1,0:T(8,128)S(1)}, u32[]{:S(2)}, u32[]{:S(2)}) collective-permute-start(f32[16,640]{1,0:T(8,128)S(1)} %add_add_fusion.1), channel_id=1, source_target_pairs={{0,96},{32,64},{64,32},{96,0},{1,97},{33,65},{65,33},{97,1},{2,98}... | collective-permute-start | bytes 122888 | tf_op jit(solution)/shard_map/ppermute | solution.py:27
  26.9 4.4 %collective-permute-start.5 = (f32[16,640]{1,0:T(8,128)S(1)}, f32[16,640]{1,0:T(8,128)S(1)}, u32[]{:S(2)}, u32[]{:S(2)}) collective-permute-start(f32[16,640]{1,0:T(8,128)S(1)} %add_add_fusion.1), channel_id=1, source_target_pairs={{0,64},{32,96},{64,0},{96,32},{1,65},{33,97},{65,1},{97,33},{2,66}... | collective-permute-start | bytes 122888 | tf_op jit(solution)/shard_map/ppermute | solution.py:27
  35.0 10.8 %copy-start.3 = (f32[4]{0:T(128)S(1)}, f32[4]{0:T(128)}, u32[]{:S(2)}) copy-start(f32[4]{0:T(128)} %param.17) | copy-start | bytes 52
  35.0 10.8 %copy-start.4 = (f32[128]{0:T(128)S(1)}, f32[128]{0:T(128)}, u32[]{:S(2)}) copy-start(f32[128]{0:T(128)} %param.18) | copy-start | bytes 1540
  35.0 17.0 %copy-start.2 = (bf16[512,256]{1,0:T(8,128)(2,1)S(1)}, bf16[512,256]{1,0:T(8,128)(2,1)}, u32[]{:S(2)}) copy-start(bf16[512,256]{1,0:T(8,128)(2,1)} %param.19) | copy-start | bytes 786436
  35.3 32.8 %copy-start.1 = (bf16[256,1408]{1,0:T(8,128)(2,1)S(1)}, bf16[256,1408]{1,0:T(8,128)(2,1)}, u32[]{:S(2)}) copy-start(bf16[256,1408]{1,0:T(8,128)(2,1)} %param.22) | copy-start | bytes 2162692
  38.5 3.3 %collective-permute-start.6 = (f32[136,128]{1,0:T(8,128)S(1)}, f32[136,128]{1,0:T(8,128)S(1)}, u32[]{:S(2)}, u32[]{:S(2)}) collective-permute-start(f32[136,128]{1,0:T(8,128)S(1)} %maximum_maximum_fusion), channel_id=1, source_target_pairs={{0,8},{8,0},{16,24},{24,16},{1,9},{9,1},{17,25},{25,17},{2,10},{10... | collective-permute-start | bytes 208904 | tf_op jit(solution)/shard_map/ppermute | solution.py:27
  39.0 4.4 %collective-permute-start.7 = (f32[136,128]{1,0:T(8,128)S(1)}, f32[136,128]{1,0:T(8,128)S(1)}, u32[]{:S(2)}, u32[]{:S(2)}) collective-permute-start(f32[136,128]{1,0:T(8,128)S(1)} %maximum_maximum_fusion), channel_id=1, source_target_pairs={{0,24},{8,16},{16,8},{24,0},{1,25},{9,17},{17,9},{25,1},{2,26},{10... | collective-permute-start | bytes 208904 | tf_op jit(solution)/shard_map/ppermute | solution.py:27
  39.7 4.7 %collective-permute-start.8 = (f32[136,128]{1,0:T(8,128)S(1)}, f32[136,128]{1,0:T(8,128)S(1)}, u32[]{:S(2)}, u32[]{:S(2)}) collective-permute-start(f32[136,128]{1,0:T(8,128)S(1)} %maximum_maximum_fusion), channel_id=1, source_target_pairs={{0,16},{8,24},{16,0},{24,8},{1,17},{9,25},{17,1},{25,9},{2,18},{10... | collective-permute-start | bytes 208904 | tf_op jit(solution)/shard_map/ppermute | solution.py:27
  44.7 40.1 %copy-start.5 = (bf16[1408,256]{1,0:T(8,128)(2,1)S(1)}, bf16[1408,256]{1,0:T(8,128)(2,1)}, u32[]{:S(2)}) copy-start(bf16[1408,256]{1,0:T(8,128)(2,1)} %param.23) | copy-start | bytes 2162692
  45.0 3.7 %collective-permute-start.9 = (f32[136,128]{1,0:T(8,128)S(1)}, f32[136,128]{1,0:T(8,128)S(1)}, u32[]{:S(2)}, u32[]{:S(2)}) collective-permute-start(f32[136,128]{1,0:T(8,128)S(1)} %maximum_maximum_fusion.1), channel_id=1, source_target_pairs={{0,32},{32,0},{64,96},{96,64},{1,33},{33,1},{65,97},{97,65},{2,34}... | collective-permute-start | bytes 208904 | tf_op jit(solution)/shard_map/ppermute | solution.py:27
  45.9 4.4 %collective-permute-start.10 = (f32[136,128]{1,0:T(8,128)S(1)}, f32[136,128]{1,0:T(8,128)S(1)}, u32[]{:S(2)}, u32[]{:S(2)}) collective-permute-start(f32[136,128]{1,0:T(8,128)S(1)} %maximum_maximum_fusion.1), channel_id=1, source_target_pairs={{0,96},{32,64},{64,32},{96,0},{1,97},{33,65},{65,33},{97,1},{2,98}... | collective-permute-start | bytes 208904 | tf_op jit(solution)/shard_map/ppermute | solution.py:27
  46.5 4.7 %collective-permute-start.11 = (f32[136,128]{1,0:T(8,128)S(1)}, f32[136,128]{1,0:T(8,128)S(1)}, u32[]{:S(2)}, u32[]{:S(2)}) collective-permute-start(f32[136,128]{1,0:T(8,128)S(1)} %maximum_maximum_fusion.1), channel_id=1, source_target_pairs={{0,64},{32,96},{64,0},{96,32},{1,65},{33,97},{65,1},{97,33},{2,66}... | collective-permute-start | bytes 208904 | tf_op jit(solution)/shard_map/ppermute | solution.py:27
  52.9 15.0 %all-to-all-start.1 = ((bf16[8,16,256]{2,1,0:T(8,128)(2,1)}), bf16[8,16,256]{2,1,0:T(8,128)(2,1)S(1)}, u32[]{:S(2)}, u32[]{:S(2)}) async-start(bf16[8,16,256]{2,1,0:T(8,128)(2,1)} %broadcast_in_dim.102), calls=%async_computation.1 | async-start | bytes 131072 | tf_op jit(solution)/shard_map/all_to_all | solution.py:19
  68.7 3.7 %collective-permute-start.12 = (bf16[16,2944]{1,0:T(8,128)(2,1)S(1)}, bf16[16,2944]{1,0:T(8,128)(2,1)S(1)}, u32[]{:S(2)}, u32[]{:S(2)}) collective-permute-start(bf16[16,2944]{1,0:T(8,128)(2,1)S(1)} %pad_maximum_fusion), channel_id=1, source_target_pairs={{0,8},{8,0},{16,24},{24,16},{1,9},{9,1},{17,25},{25,17},{2,10},{10... | collective-permute-start | bytes 282632 | tf_op jit(solution)/shard_map/ppermute | solution.py:27
  69.7 4.6 %collective-permute-start.13 = (bf16[16,2944]{1,0:T(8,128)(2,1)S(1)}, bf16[16,2944]{1,0:T(8,128)(2,1)S(1)}, u32[]{:S(2)}, u32[]{:S(2)}) collective-permute-start(bf16[16,2944]{1,0:T(8,128)(2,1)S(1)} %pad_maximum_fusion), channel_id=1, source_target_pairs={{0,24},{8,16},{16,8},{24,0},{1,25},{9,17},{17,9},{25,1},{2,26},{10... | collective-permute-start | bytes 282632 | tf_op jit(solution)/shard_map/ppermute | solution.py:27
  71.6 5.0 %collective-permute-start.14 = (bf16[16,2944]{1,0:T(8,128)(2,1)S(1)}, bf16[16,2944]{1,0:T(8,128)(2,1)S(1)}, u32[]{:S(2)}, u32[]{:S(2)}) collective-permute-start(bf16[16,2944]{1,0:T(8,128)(2,1)S(1)} %pad_maximum_fusion), channel_id=1, source_target_pairs={{0,16},{8,24},{16,0},{24,8},{1,17},{9,25},{17,1},{25,9},{2,18},{10... | collective-permute-start | bytes 282632 | tf_op jit(solution)/shard_map/ppermute | solution.py:27
  77.0 3.6 %collective-permute-start.15 = (bf16[16,2944]{1,0:T(8,128)(2,1)S(1)}, bf16[16,2944]{1,0:T(8,128)(2,1)S(1)}, u32[]{:S(2)}, u32[]{:S(2)}) collective-permute-start(bf16[16,2944]{1,0:T(8,128)(2,1)S(1)} %pad_maximum_fusion.1), channel_id=1, source_target_pairs={{0,32},{32,0},{64,96},{96,64},{1,33},{33,1},{65,97},{97,65},{2,34}... | collective-permute-start | bytes 282632 | tf_op jit(solution)/shard_map/ppermute | solution.py:27
  77.3 4.6 %collective-permute-start.16 = (bf16[16,2944]{1,0:T(8,128)(2,1)S(1)}, bf16[16,2944]{1,0:T(8,128)(2,1)S(1)}, u32[]{:S(2)}, u32[]{:S(2)}) collective-permute-start(bf16[16,2944]{1,0:T(8,128)(2,1)S(1)} %pad_maximum_fusion.1), channel_id=1, source_target_pairs={{0,96},{32,64},{64,32},{96,0},{1,97},{33,65},{65,33},{97,1},{2,98}... | collective-permute-start | bytes 282632 | tf_op jit(solution)/shard_map/ppermute | solution.py:27
  79.6 5.0 %collective-permute-start.17 = (bf16[16,2944]{1,0:T(8,128)(2,1)S(1)}, bf16[16,2944]{1,0:T(8,128)(2,1)S(1)}, u32[]{:S(2)}, u32[]{:S(2)}) collective-permute-start(bf16[16,2944]{1,0:T(8,128)(2,1)S(1)} %pad_maximum_fusion.1), channel_id=1, source_target_pairs={{0,64},{32,96},{64,0},{96,32},{1,65},{33,97},{65,1},{97,33},{2,66}... | collective-permute-start | bytes 282632 | tf_op jit(solution)/shard_map/ppermute | solution.py:27
  85.9 11.9 %all-to-all-start.2 = ((bf16[8,2,256]{2,1,0:T(2,128)(2,1)}), bf16[8,2,256]{2,1,0:T(2,128)(2,1)S(1)}, u32[]{:S(2)}, u32[]{:S(2)}) async-start(bf16[8,2,256]{2,1,0:T(2,128)(2,1)} %reshape.501), calls=%async_computation.2 | async-start | bytes 16384 | tf_op jit(solution)/shard_map/all_to_all | solution.py:151

commit v3 on v2

--- a/solution.py
+++ b/solution.py
@@ -3,6 +3,7 @@
 from jax import lax
 from jax.sharding import Mesh
 from jax.sharding import PartitionSpec as P
+
 
 D = 4096
 HEAD_DIM = 64
@@ -21,10 +22,15 @@
     )
 
 
+SHIFTS = (2, 3, 1)
+
+
 def peers(shard, axis):
     n = lax.axis_size(axis)
-    near = [1, 3, 2] if n == 4 else list(range(1, n))
-    return [lax.ppermute(shard, axis, [(i, i ^ s) for i in range(n)]) for s in near]
+    got = []
+    for s in SHIFTS:
+        got.append(lax.ppermute(shard, axis, [(i, i ^ s) for i in range(n)]))
+    return got
 
 
 def added(own, got):

time: 99 us -> 94.4 us (0.954)
  starting transfers between devices: 46.1 us -> 39 us
  waiting for transfers between devices: 33.8 us -> 36.3 us
    ppermute x18, starting transfers between devices: 22.9 us -> 19.3 us  [peers(): got.append(lax.ppermute(shard, axis, [(i, i ^ s) for i in range(n)]))]
    all_to_all x1, starting transfers between devices: 7.26 us -> 4.68 us  [per_device(): arrived = lax.all_to_all(tiles, TP, 0, 0, tiled=True)]
    ppermute x18, waiting for transfers between devices: 19.7 us -> 22.2 us  [peers(): got.append(lax.ppermute(shard, axis, [(i, i ^ s) for i in range(n)]))]
where the time goes in v3:
time: 94.4 us; the launch traced here: 94.1 us
  starting transfers between devices  39 us (41%)
  waiting for transfers between devices  36.3 us (38%)
  matrix products  8.36 us (9%)
  other arithmetic  5.28 us (6%)
  local copies, waits for them, and re-layouts  4.8 us (5%)
    ppermute x18, waiting for transfers between devices, peers(): got.append(lax.ppermute(shard, axis, [(i, i ^ s) for i in range(n)]))  22.2 us
    ppermute x18, starting transfers between devices, peers(): got.append(lax.ppermute(shard, axis, [(i, i ^ s) for i in range(n)]))  19.3 us
    all_to_all x2, starting transfers between devices, to_all(): lax.all_to_all(jnp.broadcast_to(shard[None], (length, *shard.shape)), axi...  15.1 us
    all_to_all x2, waiting for transfers between devices, to_all(): lax.all_to_all(jnp.broadcast_to(shard[None], (length, *shard.shape)), axi...  9.45 us
    all_to_all x1, starting transfers between devices, per_device(): arrived = lax.all_to_all(tiles, TP, 0, 0, tiled=True)  4.68 us
    all_to_all x1, waiting for transfers between devices, per_device(): arrived = lax.all_to_all(tiles, TP, 0, 0, tiled=True)  4.64 us
    dot_general x1, matrix products, per_device(): jnp.einsum('brd,bpd->brp', split, keys, preferred_element_type=jnp.float32)  3.45 us
    dot_general x1, matrix products, per_device(): jnp.einsum('brp,bpv->brv', exponent.astype(jnp.bfloat16), values, preferr...  2.96 us
  transfers between devices with their start and end apart: 21, of which 15 were waited for; matrix products, arithmetic and copies ran while one was open for 1% of the time, Pallas kernels for 0%

profile of v3, /device:TPU:1, one launch (start us, length us, event | category | flops | bytes accessed | tf_op | source)
XLA Modules:
  0.0 94.1 jit_solution(3935077646254285270)
XLA Ops:
  0.0 0.8 convert_element_type.69
  0.8 0.7 pad_maximum_fusion.3
  1.4 0.7 reshape.499
  2.1 5.8 %all-to-all-start = ((f32[8,1,544]{2,1,0:T(1,128)}), f32[8,1,544]{2,1,0:T(1,128)S(1)}, u32[]{:S(2)}, u32[]{:S(2)}) async-start(f32[8,1,544]{2,1,0:T(1,128)} %reshape.499), calls=%async_computation | async-start | bytes 40960 | tf_op jit(solution)/shard_map/all_to_all | solution.py:20
  7.9 4.7 %all-to-all-done = f32[8,1,544]{2,1,0:T(1,128)S(1)} async-done(((f32[8,1,544]{2,1,0:T(1,128)}), f32[8,1,544]{2,1,0:T(1,128)S(1)}, u32[]{:S(2)}, u32[]{:S(2)}) %all-to-all-start) | async-done | bytes 17440 | tf_op jit(solution)/shard_map/all_to_all | solution.py:20
  12.6 0.5 broadcast.152
  13.1 0.7 reduce.58
  13.9 0.2 fusion.64
  14.2 1.1 %fusion.42 = f32[16,512]{1,0:T(8,128)S(1)} fusion(bf16[256,512]{1,0:T(8,128)(2,1)} %param.14, f32[16,256]{1,0:T(8,128)S(1)} %slice.137, f32[256]{0:T(256)} %param.13), kind=kOutput, calls=%fused_computation.79 | convolution fusion | flops 4202496 | bytes 312320 | tf_op jit(solution)/shard_map/dot_general | solution.py:76
  15.4 2.9 %collective-permute-start = (f32[16,640]{1,0:T(8,128)S(1)}, f32[16,640]{1,0:T(8,128)S(1)}, u32[]{:S(2)}, u32[]{:S(2)}) collective-permute-start(f32[16,640]{1,0:T(8,128)S(1)} %pad_maximum_fusion.2), channel_id=1, source_target_pairs={{0,16},{8,24},{16,0},{24,8},{1,17},{9,25},{17,1},{25,9},{2,18},{10... | collective-permute-start | bytes 122888 | tf_op jit(solution)/shard_map/ppermute | solution.py:32
  18.3 0.8 collective-permute-start.1
  19.1 0.7 collective-permute-done
  19.8 2.6 %collective-permute-done.1 = f32[16,640]{1,0:T(8,128)S(1)} collective-permute-done((f32[16,640]{1,0:T(8,128)S(1)}, f32[16,640]{1,0:T(8,128)S(1)}, u32[]{:S(2)}, u32[]{:S(2)}) %collective-permute-start.1) | collective-permute-done | bytes 40992 | tf_op jit(solution)/shard_map/ppermute | solution.py:32
  22.4 3.7 %collective-permute-start.3 = (f32[16,640]{1,0:T(8,128)S(1)}, f32[16,640]{1,0:T(8,128)S(1)}, u32[]{:S(2)}, u32[]{:S(2)}) collective-permute-start(f32[16,640]{1,0:T(8,128)S(1)} %add_add_fusion.1), channel_id=1, source_target_pairs={{0,64},{32,96},{64,0},{96,32},{1,65},{33,97},{65,1},{97,33},{2,66}... | collective-permute-start | bytes 122888 | tf_op jit(solution)/shard_map/ppermute | solution.py:32
  26.1 0.4 collective-permute-start.4
  26.5 0.3 collective-permute-start.5
  26.9 0.6 collective-permute-done.3
  27.5 2.8 %collective-permute-done.4 = f32[16,640]{1,0:T(8,128)S(1)} collective-permute-done((f32[16,640]{1,0:T(8,128)S(1)}, f32[16,640]{1,0:T(8,128)S(1)}, u32[]{:S(2)}, u32[]{:S(2)}) %collective-permute-start.4) | collective-permute-done | bytes 40992 | tf_op jit(solution)/shard_map/ppermute | solution.py:32
  30.3 0.1 fusion.56
  30.5 3.5 %fusion.67 = (f32[16,8]{1,0:T(8,128)S(1)}, f32[16,8,1024]{2,1,0:T(8,128)S(1)}) fusion(bf16[16,1024,1,128]{3,1,2,0:T(8,128)(2,1)} %param.15, bf16[16,8,128]{2,1,0:T(8,128)(2,1)S(1)} %bitcast.132, pred[8,128]{1,0:T(8,128)(4,1)S(1)} %bitcast.138), kind=kOutput, calls=%fused_computation.149 | convolution fusion | flops 33832832 | bytes 4752896 | tf_op jit(solution)/shard_map/brd,bpd->brp/dot_general | solution.py:93
  34.0 0.1 reshape.410
  34.1 0.2 fusion.7
  34.3 3.0 %fusion = f32[16,8,128]{2,1,0:T(8,128)S(1)} fusion(bf16[16,1024,1,128]{3,1,2,0:T(8,128)(2,1)} %param.16, f32[16,8,1024]{2,1,0:T(8,128)S(1)} %get-tuple-element.47, f32[16,8]{1,0:T(8,128)S(1)} %get-tuple-element.46), kind=kOutput, calls=%fused_computation | convolution fusion | flops 33816576 | bytes 4784640 | tf_op jit(solution)/shard_map/brp,bpv->brv/dot_general | solution.py:99
  37.3 0.1 reshape.411
  37.5 1.5 %collective-permute-start.6 = (f32[136,128]{1,0:T(8,128)S(1)}, f32[136,128]{1,0:T(8,128)S(1)}, u32[]{:S(2)}, u32[]{:S(2)}) collective-permute-start(f32[136,128]{1,0:T(8,128)S(1)} %maximum_maximum_fusion), channel_id=1, source_target_pairs={{0,16},{8,24},{16,0},{24,8},{1,17},{9,25},{17,1},{25,9},{2,18},{10... | collective-permute-start | bytes 208904 | tf_op jit(solution)/shard_map/ppermute | solution.py:32
  38.9 0.8 collective-permute-start.7
  39.7 0.5 collective-permute-start.8
  40.2 2.0 %collective-permute-done.6 = f32[136,128]{1,0:T(8,128)S(1)} collective-permute-done((f32[136,128]{1,0:T(8,128)S(1)}, f32[136,128]{1,0:T(8,128)S(1)}, u32[]{:S(2)}, u32[]{:S(2)}) %collective-permute-start.6) | collective-permute-done | bytes 69664 | tf_op jit(solution)/shard_map/ppermute | solution.py:32
  42.2 1.1 %collective-permute-done.7 = f32[136,128]{1,0:T(8,128)S(1)} collective-permute-done((f32[136,128]{1,0:T(8,128)S(1)}, f32[136,128]{1,0:T(8,128)S(1)}, u32[]{:S(2)}, u32[]{:S(2)}) %collective-permute-start.7) | collective-permute-done | bytes 69664 | tf_op jit(solution)/shard_map/ppermute | solution.py:32
  43.5 0.1 reshape.414
  43.6 0.1 fusion.75
  43.9 1.8 %collective-permute-start.9 = (f32[136,128]{1,0:T(8,128)S(1)}, f32[136,128]{1,0:T(8,128)S(1)}, u32[]{:S(2)}, u32[]{:S(2)}) collective-permute-start(f32[136,128]{1,0:T(8,128)S(1)} %maximum_maximum_fusion.1), channel_id=1, source_target_pairs={{0,64},{32,96},{64,0},{96,32},{1,65},{33,97},{65,1},{97,33},{2,66}... | collective-permute-start | bytes 208904 | tf_op jit(solution)/shard_map/ppermute | solution.py:32
  45.8 0.2 collective-permute-start.10
  46.0 0.7 collective-permute-start.11
  47.0 1.7 %collective-permute-done.9 = f32[136,128]{1,0:T(8,128)S(1)} collective-permute-done((f32[136,128]{1,0:T(8,128)S(1)}, f32[136,128]{1,0:T(8,128)S(1)}, u32[]{:S(2)}, u32[]{:S(2)}) %collective-permute-start.9) | collective-permute-done | bytes 69664 | tf_op jit(solution)/shard_map/ppermute | solution.py:32
  48.7 1.4 %collective-permute-done.10 = f32[136,128]{1,0:T(8,128)S(1)} collective-permute-done((f32[136,128]{1,0:T(8,128)S(1)}, f32[136,128]{1,0:T(8,128)S(1)}, u32[]{:S(2)}, u32[]{:S(2)}) %collective-permute-start.10) | collective-permute-done | bytes 69664 | tf_op jit(solution)/shard_map/ppermute | solution.py:32
  50.5 0.1 reshape.429
  50.7 0.2 fusion.15
  51.0 0.2 fusion.34
  51.2 0.2 convolution_convert_fusion.1
  51.4 0.6 broadcast_in_dim.102
  52.0 9.3 %all-to-all-start.1 = ((bf16[8,16,256]{2,1,0:T(8,128)(2,1)}), bf16[8,16,256]{2,1,0:T(8,128)(2,1)S(1)}, u32[]{:S(2)}, u32[]{:S(2)}) async-start(bf16[8,16,256]{2,1,0:T(8,128)(2,1)} %broadcast_in_dim.102), calls=%async_computation.1 | async-start | bytes 131072 | tf_op jit(solution)/shard_map/all_to_all | solution.py:20
  61.4 4.8 %all-to-all-done.1 = bf16[8,16,256]{2,1,0:T(8,128)(2,1)S(1)} async-done(((bf16[8,16,256]{2,1,0:T(8,128)(2,1)}), bf16[8,16,256]{2,1,0:T(8,128)(2,1)S(1)}, u32[]{:S(2)}, u32[]{:S(2)}) %all-to-all-start.1) | async-done | bytes 65568 | tf_op jit(solution)/shard_map/all_to_all | solution.py:20
  66.3 0.2 fusion.69
  66.5 0.2 fusion.68
  66.7 0.2 multiply_reduce_fusion
  67.0 2.0 %collective-permute-start.12 = (bf16[16,2944]{1,0:T(8,128)(2,1)S(1)}, bf16[16,2944]{1,0:T(8,128)(2,1)S(1)}, u32[]{:S(2)}, u32[]{:S(2)}) collective-permute-start(bf16[16,2944]{1,0:T(8,128)(2,1)S(1)} %pad_maximum_fusion), channel_id=1, source_target_pairs={{0,16},{8,24},{16,0},{24,8},{1,17},{9,25},{17,1},{25,9},{2,18},{10... | collective-permute-start | bytes 282632 | tf_op jit(solution)/shard_map/ppermute | solution.py:32
  69.0 0.9 collective-permute-start.13
  70.1 2.0 %collective-permute-done.12 = bf16[16,2944]{1,0:T(8,128)(2,1)S(1)} collective-permute-done((bf16[16,2944]{1,0:T(8,128)(2,1)S(1)}, bf16[16,2944]{1,0:T(8,128)(2,1)S(1)}, u32[]{:S(2)}, u32[]{:S(2)}) %collective-permute-start.12) | collective-permute-done | bytes 94240 | tf_op jit(solution)/shard_map/ppermute | solution.py:32
  72.1 2.6 %collective-permute-done.13 = bf16[16,2944]{1,0:T(8,128)(2,1)S(1)} collective-permute-done((bf16[16,2944]{1,0:T(8,128)(2,1)S(1)}, bf16[16,2944]{1,0:T(8,128)(2,1)S(1)}, u32[]{:S(2)}, u32[]{:S(2)}) %collective-permute-start.13) | collective-permute-done | bytes 94240 | tf_op jit(solution)/shard_map/ppermute | solution.py:32
  74.8 0.2 reduce-precision_reduce_fusion
  75.1 1.5 %collective-permute-start.15 = (bf16[16,2944]{1,0:T(8,128)(2,1)S(1)}, bf16[16,2944]{1,0:T(8,128)(2,1)S(1)}, u32[]{:S(2)}, u32[]{:S(2)}) collective-permute-start(bf16[16,2944]{1,0:T(8,128)(2,1)S(1)} %pad_maximum_fusion.1), channel_id=1, source_target_pairs={{0,64},{32,96},{64,0},{96,32},{1,65},{33,97},{65,1},{97,33},{2,66}... | collective-permute-start | bytes 282632 | tf_op jit(solution)/shard_map/ppermute | solution.py:32
  76.6 0.9 collective-permute-start.16
  77.6 0.2 collective-permute-start.17
  77.8 2.3 %collective-permute-done.15 = bf16[16,2944]{1,0:T(8,128)(2,1)S(1)} collective-permute-done((bf16[16,2944]{1,0:T(8,128)(2,1)S(1)}, bf16[16,2944]{1,0:T(8,128)(2,1)S(1)}, u32[]{:S(2)}, u32[]{:S(2)}) %collective-permute-start.15) | collective-permute-done | bytes 94240 | tf_op jit(solution)/shard_map/ppermute | solution.py:32
  80.1 2.4 %collective-permute-done.16 = bf16[16,2944]{1,0:T(8,128)(2,1)S(1)} collective-permute-done((bf16[16,2944]{1,0:T(8,128)(2,1)S(1)}, bf16[16,2944]{1,0:T(8,128)(2,1)S(1)}, u32[]{:S(2)}, u32[]{:S(2)}) %collective-permute-start.16) | collective-permute-done | bytes 94240 | tf_op jit(solution)/shard_map/ppermute | solution.py:32
  82.6 0.2 fusion.48
  82.9 0.2 convolution_convert_fusion
  83.1 0.1 reshape.432
  83.3 0.7 reshape.501
  83.9 4.7 %all-to-all-start.2 = ((bf16[8,2,256]{2,1,0:T(2,128)(2,1)}), bf16[8,2,256]{2,1,0:T(2,128)(2,1)S(1)}, u32[]{:S(2)}, u32[]{:S(2)}) async-start(bf16[8,2,256]{2,1,0:T(2,128)(2,1)} %reshape.501), calls=%async_computation.2 | async-start | bytes 16384 | tf_op jit(solution)/shard_map/all_to_all | solution.py:157
  88.6 4.6 %all-to-all-done.2 = bf16[8,2,256]{2,1,0:T(2,128)(2,1)S(1)} async-done(((bf16[8,2,256]{2,1,0:T(2,128)(2,1)}), bf16[8,2,256]{2,1,0:T(2,128)(2,1)S(1)}, u32[]{:S(2)}, u32[]{:S(2)}) %all-to-all-start.2) | async-done | bytes 8224 | tf_op jit(solution)/shard_map/all_to_all | solution.py:157
  93.3 0.1 reshape.502
  93.4 0.7 add_convert_fusion.2
  (82 shorter events, 2.5 us)
Async XLA Ops:
  0.0 66.3 %copy-start = (bf16[256,1408]{1,0:T(8,128)(2,1)S(1)}, bf16[256,1408]{1,0:T(8,128)(2,1)}, u32[]{:S(2)}) copy-start(bf16[256,1408]{1,0:T(8,128)(2,1)} %param.21) | copy-start | bytes 2162692
  2.1 10.5 %all-to-all-start = ((f32[8,1,544]{2,1,0:T(1,128)}), f32[8,1,544]{2,1,0:T(1,128)S(1)}, u32[]{:S(2)}, u32[]{:S(2)}) async-start(f32[8,1,544]{2,1,0:T(1,128)} %reshape.499), calls=%async_computation | async-start | bytes 40960 | tf_op jit(solution)/shard_map/all_to_all | solution.py:20
  15.4 4.4 %collective-permute-start = (f32[16,640]{1,0:T(8,128)S(1)}, f32[16,640]{1,0:T(8,128)S(1)}, u32[]{:S(2)}, u32[]{:S(2)}) collective-permute-start(f32[16,640]{1,0:T(8,128)S(1)} %pad_maximum_fusion.2), channel_id=1, source_target_pairs={{0,16},{8,24},{16,0},{24,8},{1,17},{9,25},{17,1},{25,9},{2,18},{10... | collective-permute-start | bytes 122888 | tf_op jit(solution)/shard_map/ppermute | solution.py:32
  18.3 4.1 %collective-permute-start.1 = (f32[16,640]{1,0:T(8,128)S(1)}, f32[16,640]{1,0:T(8,128)S(1)}, u32[]{:S(2)}, u32[]{:S(2)}) collective-permute-start(f32[16,640]{1,0:T(8,128)S(1)} %pad_maximum_fusion.2), channel_id=1, source_target_pairs={{0,24},{8,16},{16,8},{24,0},{1,25},{9,17},{17,9},{25,1},{2,26},{10... | collective-permute-start | bytes 122888 | tf_op jit(solution)/shard_map/ppermute | solution.py:32
  19.1 3.3 %collective-permute-start.2 = (f32[16,640]{1,0:T(8,128)S(1)}, f32[16,640]{1,0:T(8,128)S(1)}, u32[]{:S(2)}, u32[]{:S(2)}) collective-permute-start(f32[16,640]{1,0:T(8,128)S(1)} %pad_maximum_fusion.2), channel_id=1, source_target_pairs={{0,8},{8,0},{16,24},{24,16},{1,9},{9,1},{17,25},{25,17},{2,10},{10... | collective-permute-start | bytes 122888 | tf_op jit(solution)/shard_map/ppermute | solution.py:32
  22.4 5.1 %collective-permute-start.3 = (f32[16,640]{1,0:T(8,128)S(1)}, f32[16,640]{1,0:T(8,128)S(1)}, u32[]{:S(2)}, u32[]{:S(2)}) collective-permute-start(f32[16,640]{1,0:T(8,128)S(1)} %add_add_fusion.1), channel_id=1, source_target_pairs={{0,64},{32,96},{64,0},{96,32},{1,65},{33,97},{65,1},{97,33},{2,66}... | collective-permute-start | bytes 122888 | tf_op jit(solution)/shard_map/ppermute | solution.py:32
  26.1 4.2 %collective-permute-start.4 = (f32[16,640]{1,0:T(8,128)S(1)}, f32[16,640]{1,0:T(8,128)S(1)}, u32[]{:S(2)}, u32[]{:S(2)}) collective-permute-start(f32[16,640]{1,0:T(8,128)S(1)} %add_add_fusion.1), channel_id=1, source_target_pairs={{0,96},{32,64},{64,32},{96,0},{1,97},{33,65},{65,33},{97,1},{2,98}... | collective-permute-start | bytes 122888 | tf_op jit(solution)/shard_map/ppermute | solution.py:32
  26.5 3.7 %collective-permute-start.5 = (f32[16,640]{1,0:T(8,128)S(1)}, f32[16,640]{1,0:T(8,128)S(1)}, u32[]{:S(2)}, u32[]{:S(2)}) collective-permute-start(f32[16,640]{1,0:T(8,128)S(1)} %add_add_fusion.1), channel_id=1, source_target_pairs={{0,32},{32,0},{64,96},{96,64},{1,33},{33,1},{65,97},{97,65},{2,34}... | collective-permute-start | bytes 122888 | tf_op jit(solution)/shard_map/ppermute | solution.py:32
  34.0 11.7 %copy-start.3 = (f32[4]{0:T(128)S(1)}, f32[4]{0:T(128)}, u32[]{:S(2)}) copy-start(f32[4]{0:T(128)} %param.17) | copy-start | bytes 52
  34.0 11.7 %copy-start.4 = (f32[128]{0:T(128)S(1)}, f32[128]{0:T(128)}, u32[]{:S(2)}) copy-start(f32[128]{0:T(128)} %param.18) | copy-start | bytes 1540
  34.0 17.2 %copy-start.2 = (bf16[512,256]{1,0:T(8,128)(2,1)S(1)}, bf16[512,256]{1,0:T(8,128)(2,1)}, u32[]{:S(2)}) copy-start(bf16[512,256]{1,0:T(8,128)(2,1)} %param.19) | copy-start | bytes 786436
  34.3 32.2 %copy-start.1 = (bf16[256,1408]{1,0:T(8,128)(2,1)S(1)}, bf16[256,1408]{1,0:T(8,128)(2,1)}, u32[]{:S(2)}) copy-start(bf16[256,1408]{1,0:T(8,128)(2,1)} %param.22) | copy-start | bytes 2162692
  37.5 4.7 %collective-permute-start.6 = (f32[136,128]{1,0:T(8,128)S(1)}, f32[136,128]{1,0:T(8,128)S(1)}, u32[]{:S(2)}, u32[]{:S(2)}) collective-permute-start(f32[136,128]{1,0:T(8,128)S(1)} %maximum_maximum_fusion), channel_id=1, source_target_pairs={{0,16},{8,24},{16,0},{24,8},{1,17},{9,25},{17,1},{25,9},{2,18},{10... | collective-permute-start | bytes 208904 | tf_op jit(solution)/shard_map/ppermute | solution.py:32
  38.9 4.4 %collective-permute-start.7 = (f32[136,128]{1,0:T(8,128)S(1)}, f32[136,128]{1,0:T(8,128)S(1)}, u32[]{:S(2)}, u32[]{:S(2)}) collective-permute-start(f32[136,128]{1,0:T(8,128)S(1)} %maximum_maximum_fusion), channel_id=1, source_target_pairs={{0,24},{8,16},{16,8},{24,0},{1,25},{9,17},{17,9},{25,1},{2,26},{10... | collective-permute-start | bytes 208904 | tf_op jit(solution)/shard_map/ppermute | solution.py:32
  39.7 3.6 %collective-permute-start.8 = (f32[136,128]{1,0:T(8,128)S(1)}, f32[136,128]{1,0:T(8,128)S(1)}, u32[]{:S(2)}, u32[]{:S(2)}) collective-permute-start(f32[136,128]{1,0:T(8,128)S(1)} %maximum_maximum_fusion), channel_id=1, source_target_pairs={{0,8},{8,0},{16,24},{24,16},{1,9},{9,1},{17,25},{25,17},{2,10},{10... | collective-permute-start | bytes 208904 | tf_op jit(solution)/shard_map/ppermute | solution.py:32
  43.6 39.2 %copy-start.5 = (bf16[1408,256]{1,0:T(8,128)(2,1)S(1)}, bf16[1408,256]{1,0:T(8,128)(2,1)}, u32[]{:S(2)}) copy-start(bf16[1408,256]{1,0:T(8,128)(2,1)} %param.23) | copy-start | bytes 2162692
  43.9 4.7 %collective-permute-start.9 = (f32[136,128]{1,0:T(8,128)S(1)}, f32[136,128]{1,0:T(8,128)S(1)}, u32[]{:S(2)}, u32[]{:S(2)}) collective-permute-start(f32[136,128]{1,0:T(8,128)S(1)} %maximum_maximum_fusion.1), channel_id=1, source_target_pairs={{0,64},{32,96},{64,0},{96,32},{1,65},{33,97},{65,1},{97,33},{2,66}... | collective-permute-start | bytes 208904 | tf_op jit(solution)/shard_map/ppermute | solution.py:32
  45.8 4.4 %collective-permute-start.10 = (f32[136,128]{1,0:T(8,128)S(1)}, f32[136,128]{1,0:T(8,128)S(1)}, u32[]{:S(2)}, u32[]{:S(2)}) collective-permute-start(f32[136,128]{1,0:T(8,128)S(1)} %maximum_maximum_fusion.1), channel_id=1, source_target_pairs={{0,96},{32,64},{64,32},{96,0},{1,97},{33,65},{65,33},{97,1},{2,98}... | collective-permute-start | bytes 208904 | tf_op jit(solution)/shard_map/ppermute | solution.py:32
  46.0 4.3 %collective-permute-start.11 = (f32[136,128]{1,0:T(8,128)S(1)}, f32[136,128]{1,0:T(8,128)S(1)}, u32[]{:S(2)}, u32[]{:S(2)}) collective-permute-start(f32[136,128]{1,0:T(8,128)S(1)} %maximum_maximum_fusion.1), channel_id=1, source_target_pairs={{0,32},{32,0},{64,96},{96,64},{1,33},{33,1},{65,97},{97,65},{2,34}... | collective-permute-start | bytes 208904 | tf_op jit(solution)/shard_map/ppermute | solution.py:32
  52.0 14.2 %all-to-all-start.1 = ((bf16[8,16,256]{2,1,0:T(8,128)(2,1)}), bf16[8,16,256]{2,1,0:T(8,128)(2,1)S(1)}, u32[]{:S(2)}, u32[]{:S(2)}) async-start(bf16[8,16,256]{2,1,0:T(8,128)(2,1)} %broadcast_in_dim.102), calls=%async_computation.1 | async-start | bytes 131072 | tf_op jit(solution)/shard_map/all_to_all | solution.py:20
  67.0 5.0 %collective-permute-start.12 = (bf16[16,2944]{1,0:T(8,128)(2,1)S(1)}, bf16[16,2944]{1,0:T(8,128)(2,1)S(1)}, u32[]{:S(2)}, u32[]{:S(2)}) collective-permute-start(bf16[16,2944]{1,0:T(8,128)(2,1)S(1)} %pad_maximum_fusion), channel_id=1, source_target_pairs={{0,16},{8,24},{16,0},{24,8},{1,17},{9,25},{17,1},{25,9},{2,18},{10... | collective-permute-start | bytes 282632 | tf_op jit(solution)/shard_map/ppermute | solution.py:32
  69.0 5.7 %collective-permute-start.13 = (bf16[16,2944]{1,0:T(8,128)(2,1)S(1)}, bf16[16,2944]{1,0:T(8,128)(2,1)S(1)}, u32[]{:S(2)}, u32[]{:S(2)}) collective-permute-start(bf16[16,2944]{1,0:T(8,128)(2,1)S(1)} %pad_maximum_fusion), channel_id=1, source_target_pairs={{0,24},{8,16},{16,8},{24,0},{1,25},{9,17},{17,9},{25,1},{2,26},{10... | collective-permute-start | bytes 282632 | tf_op jit(solution)/shard_map/ppermute | solution.py:32
  70.0 4.7 %collective-permute-start.14 = (bf16[16,2944]{1,0:T(8,128)(2,1)S(1)}, bf16[16,2944]{1,0:T(8,128)(2,1)S(1)}, u32[]{:S(2)}, u32[]{:S(2)}) collective-permute-start(bf16[16,2944]{1,0:T(8,128)(2,1)S(1)} %pad_maximum_fusion), channel_id=1, source_target_pairs={{0,8},{8,0},{16,24},{24,16},{1,9},{9,1},{17,25},{25,17},{2,10},{10... | collective-permute-start | bytes 282632 | tf_op jit(solution)/shard_map/ppermute | solution.py:32
  75.1 5.0 %collective-permute-start.15 = (bf16[16,2944]{1,0:T(8,128)(2,1)S(1)}, bf16[16,2944]{1,0:T(8,128)(2,1)S(1)}, u32[]{:S(2)}, u32[]{:S(2)}) collective-permute-start(bf16[16,2944]{1,0:T(8,128)(2,1)S(1)} %pad_maximum_fusion.1), channel_id=1, source_target_pairs={{0,64},{32,96},{64,0},{96,32},{1,65},{33,97},{65,1},{97,33},{2,66}... | collective-permute-start | bytes 282632 | tf_op jit(solution)/shard_map/ppermute | solution.py:32
  76.6 5.9 %collective-permute-start.16 = (bf16[16,2944]{1,0:T(8,128)(2,1)S(1)}, bf16[16,2944]{1,0:T(8,128)(2,1)S(1)}, u32[]{:S(2)}, u32[]{:S(2)}) collective-permute-start(bf16[16,2944]{1,0:T(8,128)(2,1)S(1)} %pad_maximum_fusion.1), channel_id=1, source_target_pairs={{0,96},{32,64},{64,32},{96,0},{1,97},{33,65},{65,33},{97,1},{2,98}... | collective-permute-start | bytes 282632 | tf_op jit(solution)/shard_map/ppermute | solution.py:32
  77.6 5.0 %collective-permute-start.17 = (bf16[16,2944]{1,0:T(8,128)(2,1)S(1)}, bf16[16,2944]{1,0:T(8,128)(2,1)S(1)}, u32[]{:S(2)}, u32[]{:S(2)}) collective-permute-start(bf16[16,2944]{1,0:T(8,128)(2,1)S(1)} %pad_maximum_fusion.1), channel_id=1, source_target_pairs={{0,32},{32,0},{64,96},{96,64},{1,33},{33,1},{65,97},{97,65},{2,34}... | collective-permute-start | bytes 282632 | tf_op jit(solution)/shard_map/ppermute | solution.py:32
  83.9 9.3 %all-to-all-start.2 = ((bf16[8,2,256]{2,1,0:T(2,128)(2,1)}), bf16[8,2,256]{2,1,0:T(2,128)(2,1)S(1)}, u32[]{:S(2)}, u32[]{:S(2)}) async-start(bf16[8,2,256]{2,1,0:T(2,128)(2,1)} %reshape.501), calls=%async_computation.2 | async-start | bytes 16384 | tf_op jit(solution)/shard_map/all_to_all | solution.py:157

commit v4 on v3

v4 whole, which is shorter than its diff:
```python
import functools

import jax
import jax.numpy as jnp
from jax import lax
from jax.experimental import pallas as pl
from jax.experimental.pallas import tpu as pltpu
from jax.sharding import Mesh
from jax.sharding import PartitionSpec as P


D = 4096
HEAD_DIM = 64
KV = ("kv_0", "kv_1")
KV_TP = ("kv_0", "kv_1", "tp_0", "tp_1")
TP = ("tp_0", "tp_1")
LANES = 128
F32 = jnp.float32
BF16 = jnp.bfloat16

eps = 1e-06

SHIFTS = (2, 3, 1)


def peers(shard, axis):
    n = lax.axis_size(axis)
    got = []
    for s in SHIFTS:
        got.append(lax.ppermute(shard, axis, [(i, i ^ s) for i in range(n)]))
    return got


def partner(shard):
    return lax.ppermute(shard, TP[1], [(0, 1), (1, 0)])


def added(own, got):
    for p in got:
        own = own + p
    return own


def lane_of(shape):
    return lax.broadcasted_iota(jnp.int32, shape, len(shape) - 1)


def kernel_call(body, outs, scratch=(), smem=0, n_in=1, mib=16):
    spec = [pl.BlockSpec(memory_space=pltpu.SMEM)] * smem
    spec += [pl.BlockSpec(memory_space=pltpu.VMEM)] * (n_in - smem)
    return pl.pallas_call(
        body,
        out_shape=outs,
        in_specs=spec,
        out_specs=[pl.BlockSpec(memory_space=pltpu.VMEM)] * len(outs),
        scratch_shapes=scratch,
        compiler_params=pltpu.CompilerParams(vmem_limit_bytes=mib * 2**20),
    )


def query_body(chip, own, a, b, c, gain, weight, packed, block, held):
    batch = packed.shape[0]
    x = chip[0]
    held[x] = own[...]
    for s, ref in zip(SHIFTS, (a, b, c)):
        held[x ^ s] = ref[...]
    left = lane_of(own.shape) < LANES // 2
    for t in range(2):
        block[:, t * LANES : (t + 1) * LANES] = jnp.where(left, held[2 * t], held[2 * t + 1])
    rows = block[:batch, :]
    gained = (rows * gain[...]).astype(BF16)
    width = weight.shape[1]
    packed[:, :width] = jnp.dot(gained, weight[...], preferred_element_type=F32)
    squares = jnp.sum(rows * rows, axis=1, keepdims=True)
    packed[:, width:] = jnp.broadcast_to(squares, (batch, LANES))


def attend_body(own, a, b, c, keys, values, out, query):
    batch, _, _ = keys.shape
    width = own.shape[1] - LANES
    heads = width // LANES
    whole = own[...] + a[...] + b[...] + c[...]
    inv = lax.rsqrt(whole[:, width:] / D + eps)
    for g in range(heads):
        part = whole[:, g * LANES : (g + 1) * LANES] * inv
        query[g * batch : (g + 1) * batch, :] = part.astype(BF16).astype(F32)
    shape = (2 * heads, LANES)
    half = lane_of(shape) // HEAD_DIM
    keep = half == lax.broadcasted_iota(jnp.int32, shape, 0) // heads
    lane = lane_of(shape)
    stats = jnp.zeros(shape, F32)
    for n in range(batch):
        q = query[pl.ds(n, heads, stride=batch), :]
        q = jnp.where(keep, jnp.concatenate([q, q], axis=0), 0.0).astype(BF16)
        scores = lax.dot_general(
            q, keys[n], (((1,), (1,)), ((), ())), preferred_element_type=F32
        ) * HEAD_DIM ** (-0.5)
        top = jnp.max(scores, axis=1, keepdims=True)
        exponent = jnp.exp(scores - top)
        total = jnp.sum(exponent, axis=1, keepdims=True)
        out[n * 2 * heads : (n + 1) * 2 * heads, :] = jnp.dot(
            exponent.astype(BF16), values[n], preferred_element_type=F32
        )
        stats = jnp.where(lane == n, top, stats)
        stats = jnp.where(lane == n + LANES // 2, total, stats)
    out[batch * 2 * heads :, :] = stats


def combined(parts, rows, high):
    n = rows * high
    stats = [p[n : n + high, :] for p in parts]
    top = functools.reduce(jnp.maximum, stats)
    factors = [jnp.exp(s - top) for s in stats]
    shifted = [pltpu.roll(f, LANES // 2, 1) for f in factors]
    total = sum(s * f for s, f in zip(stats, shifted))
    low = lane_of(top.shape) < LANES // 2
    accs = []
    for k in range(rows):
        acc = 0.0
        for p, f in zip(parts, factors):
            acc = acc + p[k * high : (k + 1) * high, :] * f[:, k : k + 1]
        accs.append(acc)
    return jnp.where(low, top, total), accs


def merge_body(own, a, b, c, out):
    high = 8
    rows = own.shape[0] // high - 1
    stats, accs = combined((own, a, b, c), rows, high)
    for k, acc in enumerate(accs):
        out[k * high : (k + 1) * high, :] = acc
    out[rows * high :, :] = stats


def project_body(lambdas, own, a, b, c, gain, weight, out, held):
    high = 8
    heads = high // 2
    rows = own.shape[0] // high - 1
    stats, accs = combined((own, a, b, c), rows, high)
    inverse = 1.0 / stats
    at = lax.broadcasted_iota(jnp.int32, (heads, LANES), 0)
    mixing = jnp.zeros((heads, LANES), F32)
    for g in range(heads):
        mixing = jnp.where(at == g, lambdas[g], mixing)
    for k, acc in enumerate(accs):
        at_lane = LANES // 2 + k
        means = acc * inverse[:, at_lane : at_lane + 1]
        attended = means[:heads] - mixing * means[heads:]
        norm = lax.rsqrt(jnp.mean(attended * attended, axis=1, keepdims=True) + eps)
        held[pl.ds(k, heads, stride=rows), :] = attended * norm * gain[...]
    projected = 0.0
    for g in range(heads):
        projected = projected + jnp.dot(
            held[g * rows : (g + 1) * rows, :].astype(BF16),
            weight[g * LANES : (g + 1) * LANES, :],
            preferred_element_type=F32,
        )
    out[...] = projected.astype(BF16)


def gate_body(attn, other, block, gate, up, both, sent, after):
    batch = attn.shape[0]
    rows = (block[:batch, :] + (attn[...] + other[...])).astype(BF16).astype(F32)
    after[...] = rows
    squares = jnp.sum(rows * rows, axis=1, keepdims=True)
    mixer_in = (rows * block[batch : batch + 1, :]).astype(BF16)
    width = gate.shape[1]
    for k, weight in enumerate((gate, up)):
        part = jnp.dot(mixer_in, weight[...], preferred_element_type=F32)
        both[:, k * width : (k + 1) * width] = part
        sent[:, k * width : (k + 1) * width] = part.astype(BF16)
    both[:, 2 * width :] = jnp.broadcast_to(squares, (batch, LANES))
    sent[:, 2 * width :] = high_and_low(squares, batch)


def high_and_low(squares, batch):
    high = squares.astype(BF16).astype(F32)
    low = lane_of((batch, LANES)) >= LANES // 2
    return jnp.where(low, squares - high, high).astype(BF16)


def gathered_sums(own, others):
    width = own.shape[1] - LANES
    sums = own[:, :width]
    squares = own[:, width : width + 1]
    for p in others:
        sums = sums + p[:, :width].astype(F32)
        tail = p[:, width:].astype(F32)
        squares = squares + (tail[:, :1] + tail[:, LANES // 2 : LANES // 2 + 1])
    return sums, squares


def middle_body(own, a, b, c, both, sent):
    sums, squares = gathered_sums(own, (a, b, c))
    batch, width = sums.shape
    both[:, :width] = sums
    sent[:, :width] = sums.astype(BF16)
    both[:, width:] = jnp.broadcast_to(squares, (batch, LANES))
    sent[:, width:] = high_and_low(squares, batch)


def down_body(own, a, b, c, weight, out):
    sums, squares = gathered_sums(own, (a, b, c))
    width = sums.shape[1] // 2
    inv = lax.rsqrt(squares / D + eps)
    gate, up = sums[:, :width] * inv, sums[:, width:] * inv
    hidden = (gate / (1.0 + jnp.exp(-gate)) * up).astype(BF16)
    out[...] = jnp.dot(hidden, weight[...], preferred_element_type=F32).astype(BF16)


def per_device(
    hidden_in,
    attn_gain,
    query_weight,
    key_cache,
    value_cache,
    lambdas,
    head_gain,
    out_weight,
    mixer_gain,
    gate_weight,
    up_weight,
    down_weight,
):
    batch, cols = hidden_in.shape
    width_q = query_weight.shape[1]
    heads = width_q // LANES
    wide = query_weight.shape[0]
    positions = key_cache.shape[1]
    shape = jax.ShapeDtypeStruct
    core = lax.axis_index(TP[1])
    chip = lax.axis_index(TP[0]).astype(jnp.int32)

    own = jnp.concatenate([hidden_in.astype(F32), mixer_gain[None]], axis=0)
    own = jnp.concatenate([own] * (LANES // cols), axis=1)
    own = jnp.pad(own, ((0, 7), (0, 0)))
    mine = lane_of(own.shape) // cols % 2 == core
    pair = jnp.where(mine, own, partner(own))
    packed, block = kernel_call(
        query_body,
        [shape((batch, width_q + LANES), F32), shape((own.shape[0], wide), F32)],
        [pltpu.VMEM((4, *own.shape), F32)],
        smem=1,
        n_in=7,
    )(chip[None], pair, *peers(pair, "tp_0"), attn_gain[None], query_weight)
    packed = added(packed, peers(packed, "kv_1"))
    state = kernel_call(
        attend_body,
        [shape(((batch + 1) * 2 * heads, LANES), F32)],
        [pltpu.VMEM((heads * batch, LANES), F32)],
        n_in=6,
    )(
        packed,
        *peers(packed, "kv_0"),
        key_cache.reshape(batch, positions, LANES),
        value_cache.reshape(batch, positions, LANES),
    )[0]
    state = kernel_call(merge_body, [shape(state.shape, F32)], n_in=4)(
        state, *peers(state, "kv_1")
    )[0]
    projected = kernel_call(
        project_body,
        [shape((batch, wide), BF16)],
        [pltpu.VMEM((heads * batch, LANES), F32)],
        smem=1,
        n_in=7,
    )(lambdas, state, *peers(state, "kv_0"), head_gain[None], out_weight)[0]
    attn = added(
        projected.astype(F32), [p.astype(F32) for p in peers(projected, "tp_0")]
    )
    width = gate_weight.shape[1]
    both_shape = (batch, 2 * width + LANES)
    both, sent, after = kernel_call(
        gate_body,
        [shape(both_shape, F32), shape(both_shape, BF16), shape((batch, wide), F32)],
        n_in=5,
    )(attn, partner(attn), block, gate_weight, up_weight)
    both, sent = kernel_call(
        middle_body, [shape(both_shape, F32), shape(both_shape, BF16)], n_in=4
    )(both, *peers(sent, "kv_1"))
    down = kernel_call(down_body, [shape((batch, wide), BF16)], n_in=5)(
        both, *peers(sent, "kv_0"), down_weight
    )[0]
    mix = added(down.astype(F32), [p.astype(F32) for p in peers(down, "tp_0")])
    mixed = after + (mix + partner(mix))
    return lax.dynamic_slice_in_dim(mixed, (chip * 2 + core) * cols, cols, 1).astype(BF16)


def solution(mesh):
    split = Mesh(mesh.devices.reshape(4, 4, 4, 2), ("kv_0", "kv_1", "tp_0", "tp_1"))
    placed = (
        P(None, KV_TP),
        P(KV),
        P(KV, TP),
        P(None, KV, TP, None),
        P(None, KV, TP, None),
        P(TP),
        P(),
        P(TP, KV),
        P(KV_TP),
        P(KV, TP),
        P(KV, TP),
        P(TP, KV),
    )
    return jax.shard_map(
        per_device, mesh=split, in_specs=placed, out_specs=P(None, KV_TP), check_vma=False
    )
```

time: 94.4 us -> 97.8 us (1.036)
  starting transfers between devices: 39 us -> 49.4 us
  matrix products: 8.36 us -> 0 us
  Pallas kernels: 0 us -> 6.93 us
  waiting for transfers between devices: 36.3 us -> 32 us
  other arithmetic: 5.28 us -> 3.16 us
  local copies, waits for them, and re-layouts: 4.8 us -> 6.03 us
    all_to_all x3 -> x0, starting transfers between devices: 19.8 us -> none  [the longest x2 15.1 us: to_all(): lax.all_to_all(jnp.broadcast_to(shard[None], (length, *shard.shape)), axi...]
    ppermute x0 -> x3, starting transfers between devices: none -> 16 us  [partner(): return lax.ppermute(shard, TP[1], [(0, 1), (1, 0)])]
    ppermute x18 -> x27, starting transfers between devices: 19.3 us -> 33.4 us  [peers(): got.append(lax.ppermute(shard, axis, [(i, i ^ s) for i in range(n)]))]
    all_to_all x3 -> x0, waiting for transfers between devices: 14.1 us -> none  [the longest x2 9.45 us: to_all(): lax.all_to_all(jnp.broadcast_to(shard[None], (length, *shard.shape)), axi...]
    dot_general x7 -> x0, matrix products: 8.36 us -> none  [the longest x1 3.45 us: per_device(): jnp.einsum('brd,bpd->brp', split, keys, preferred_element_type=jnp.float32)]
    ppermute x18 -> x27, waiting for transfers between devices: 22.2 us -> 29.5 us  [peers(): got.append(lax.ppermute(shard, axis, [(i, i ^ s) for i in range(n)]))]
    pallas_call x0 -> x7, Pallas kernels: none -> 6.93 us  [the longest x1 4.76 us: per_device(): kernel_call(attend_body, [shape(((batch + 1) * 2 * heads, LANES), F32)],...]
    unnamed x16 -> x20, local copies, waits for them, and re-layouts: 1.58 us -> 6.03 us
  transfers between devices with their start and end apart: 21 -> 30, of which waited for: 15 -> 22; matrix products, arithmetic and copies ran while one was open for 1% -> 0% of each run, Pallas kernels for 0% -> 0%
where the time goes in v4:
time: 97.8 us; the launch traced here: 97.5 us
  starting transfers between devices  49.4 us (51%)
  waiting for transfers between devices  32 us (33%)
  Pallas kernels  6.93 us (7%)
  local copies, waits for them, and re-layouts  6.03 us (6%)
  other arithmetic  3.16 us (3%)
    ppermute x27, starting transfers between devices, peers(): got.append(lax.ppermute(shard, axis, [(i, i ^ s) for i in range(n)]))  33.4 us
    ppermute x27, waiting for transfers between devices, peers(): got.append(lax.ppermute(shard, axis, [(i, i ^ s) for i in range(n)]))  29.5 us
    ppermute x3, starting transfers between devices, partner(): return lax.ppermute(shard, TP[1], [(0, 1), (1, 0)])  16 us
    unnamed x20, local copies, waits for them, and re-layouts  6.03 us
    pallas_call x1, Pallas kernels, per_device(): kernel_call(attend_body, [shape(((batch + 1) * 2 * heads, LANES), F32)],...  4.76 us
    ppermute x3, waiting for transfers between devices, partner(): return lax.ppermute(shard, TP[1], [(0, 1), (1, 0)])  2.5 us
  transfers between devices with their start and end apart: 30, of which 22 were waited for; matrix products, arithmetic and copies ran while one was open for 0% of the time, Pallas kernels for 0%

profile of v4, /device:TPU:1, one launch (start us, length us, event | category | flops | bytes accessed | tf_op | source)
XLA Modules:
  0.0 97.5 jit_solution(586448572941187495)
XLA Ops:
  0.0 0.7 convert_element_type.32
  0.7 0.9 fusion.2
  1.6 1.5 %collective-permute-start = (f32[24,128]{1,0:T(8,128)S(1)}, f32[24,128]{1,0:T(8,128)S(1)}, u32[]{:S(2)}, u32[]{:S(2)}) collective-permute-start(f32[24,128]{1,0:T(8,128)S(1)} %fusion.2), channel_id=1, source_target_pairs={{0,1},{1,0},{2,3},{3,2},{4,5},{5,4},{6,7},{7,6},{8,9},{9,8},{10,11... | collective-permute-start | bytes 36872 | tf_op jit(solution)/shard_map/ppermute | solution.py:35
  3.1 0.8 collective-permute-done
  3.9 0.9 fusion.5.own
  4.8 1.4 %collective-permute-start.3 = (f32[24,128]{1,0:T(8,128)S(1)}, f32[24,128]{1,0:T(8,128)S(1)}, u32[]{:S(2)}, u32[]{:S(2)}) collective-permute-start(f32[24,128]{1,0:T(8,128)S(1)} %fusion.5.own), channel_id=1, source_target_pairs={{0,2},{2,0},{4,6},{6,4},{1,3},{3,1},{5,7},{7,5},{8,10},{10,8},{12,... | collective-permute-start | bytes 36872 | tf_op jit(solution)/shard_map/ppermute | solution.py:30
  6.2 1.8 %collective-permute-start.2 = (f32[24,128]{1,0:T(8,128)S(1)}, f32[24,128]{1,0:T(8,128)S(1)}, u32[]{:S(2)}, u32[]{:S(2)}) collective-permute-start(f32[24,128]{1,0:T(8,128)S(1)} %fusion.5.own), channel_id=1, source_target_pairs={{0,6},{2,4},{4,2},{6,0},{1,7},{3,5},{5,3},{7,1},{8,14},{10,12},{12... | collective-permute-start | bytes 36872 | tf_op jit(solution)/shard_map/ppermute | solution.py:30
  8.0 0.6 collective-permute-start.1
  8.6 1.3 %collective-permute-done.2.b = f32[24,128]{1,0:T(8,128)S(1)} collective-permute-done((f32[24,128]{1,0:T(8,128)S(1)}, f32[24,128]{1,0:T(8,128)S(1)}, u32[]{:S(2)}, u32[]{:S(2)}) %collective-permute-start.2) | collective-permute-done | bytes 12320 | tf_op jit(solution)/shard_map/ppermute | solution.py:30
  9.9 2.1 %collective-permute-done.1.a = f32[24,128]{1,0:T(8,128)S(1)} collective-permute-done((f32[24,128]{1,0:T(8,128)S(1)}, f32[24,128]{1,0:T(8,128)S(1)}, u32[]{:S(2)}, u32[]{:S(2)}) %collective-permute-start.1) | collective-permute-done | bytes 12320 | tf_op jit(solution)/shard_map/ppermute | solution.py:30
  12.0 0.9 copy-done.5
  13.0 0.7 copy-done.7
  13.8 1.3 %collective-permute-start.6 = (f32[16,640]{1,0:T(8,128)S(1)}, f32[16,640]{1,0:T(8,128)S(1)}, u32[]{:S(2)}, u32[]{:S(2)}) collective-permute-start(f32[16,640]{1,0:T(8,128)S(1)} %get-tuple-element.12), channel_id=1, source_target_pairs={{0,8},{8,0},{16,24},{24,16},{1,9},{9,1},{17,25},{25,17},{2,10},{10... | collective-permute-start | bytes 122888 | tf_op jit(solution)/shard_map/ppermute | solution.py:30
  15.1 1.9 %collective-permute-start.5 = (f32[16,640]{1,0:T(8,128)S(1)}, f32[16,640]{1,0:T(8,128)S(1)}, u32[]{:S(2)}, u32[]{:S(2)}) collective-permute-start(f32[16,640]{1,0:T(8,128)S(1)} %get-tuple-element.12), channel_id=1, source_target_pairs={{0,24},{8,16},{16,8},{24,0},{1,25},{9,17},{17,9},{25,1},{2,26},{10... | collective-permute-start | bytes 122888 | tf_op jit(solution)/shard_map/ppermute | solution.py:30
  17.0 0.7 collective-permute-start.4
  17.7 1.4 %collective-permute-done.5 = f32[16,640]{1,0:T(8,128)S(1)} collective-permute-done((f32[16,640]{1,0:T(8,128)S(1)}, f32[16,640]{1,0:T(8,128)S(1)}, u32[]{:S(2)}, u32[]{:S(2)}) %collective-permute-start.5) | collective-permute-done | bytes 40992 | tf_op jit(solution)/shard_map/ppermute | solution.py:30
  19.2 2.4 %collective-permute-done.4 = f32[16,640]{1,0:T(8,128)S(1)} collective-permute-done((f32[16,640]{1,0:T(8,128)S(1)}, f32[16,640]{1,0:T(8,128)S(1)}, u32[]{:S(2)}, u32[]{:S(2)}) %collective-permute-start.4) | collective-permute-done | bytes 40992 | tf_op jit(solution)/shard_map/ppermute | solution.py:30
  21.6 1.7 %collective-permute-start.9 = (f32[16,640]{1,0:T(8,128)S(1)}, f32[16,640]{1,0:T(8,128)S(1)}, u32[]{:S(2)}, u32[]{:S(2)}) collective-permute-start(f32[16,640]{1,0:T(8,128)S(1)} %add_add_fusion.own), channel_id=1, source_target_pairs={{0,32},{32,0},{64,96},{96,64},{1,33},{33,1},{65,97},{97,65},{2,34}... | collective-permute-start | bytes 122888 | tf_op jit(solution)/shard_map/ppermute | solution.py:30
  23.3 2.2 %collective-permute-start.8 = (f32[16,640]{1,0:T(8,128)S(1)}, f32[16,640]{1,0:T(8,128)S(1)}, u32[]{:S(2)}, u32[]{:S(2)}) collective-permute-start(f32[16,640]{1,0:T(8,128)S(1)} %add_add_fusion.own), channel_id=1, source_target_pairs={{0,96},{32,64},{64,32},{96,0},{1,97},{33,65},{65,33},{97,1},{2,98}... | collective-permute-start | bytes 122888 | tf_op jit(solution)/shard_map/ppermute | solution.py:30
  25.5 1.1 %collective-permute-start.7 = (f32[16,640]{1,0:T(8,128)S(1)}, f32[16,640]{1,0:T(8,128)S(1)}, u32[]{:S(2)}, u32[]{:S(2)}) collective-permute-start(f32[16,640]{1,0:T(8,128)S(1)} %add_add_fusion.own), channel_id=1, source_target_pairs={{0,64},{32,96},{64,0},{96,32},{1,65},{33,97},{65,1},{97,33},{2,66}... | collective-permute-start | bytes 122888 | tf_op jit(solution)/shard_map/ppermute | solution.py:30
  26.6 0.8 collective-permute-done.8.b
  27.3 2.5 %collective-permute-done.7.a = f32[16,640]{1,0:T(8,128)S(1)} collective-permute-done((f32[16,640]{1,0:T(8,128)S(1)}, f32[16,640]{1,0:T(8,128)S(1)}, u32[]{:S(2)}, u32[]{:S(2)}) %collective-permute-start.7) | collective-permute-done | bytes 40992 | tf_op jit(solution)/shard_map/ppermute | solution.py:30
  29.9 2.2 %copy-done = bf16[16,1024,1,128]{3,1,2,0:T(8,128)(2,1)S(1)} copy-done((bf16[16,1024,1,128]{3,1,2,0:T(8,128)(2,1)S(1)}, bf16[16,1024,1,128]{3,1,2,0:T(8,128)(2,1)}, u32[]{:S(2)}) %copy-start) | copy-done | bytes 4194328
  32.1 2.2 %copy-done.1 = bf16[16,1024,1,128]{3,1,2,0:T(8,128)(2,1)S(1)} copy-done((bf16[16,1024,1,128]{3,1,2,0:T(8,128)(2,1)S(1)}, bf16[16,1024,1,128]{3,1,2,0:T(8,128)(2,1)}, u32[]{:S(2)}) %copy-start.1) | copy-done | bytes 4194328
  34.3 4.8 %shard_map.119.own = f32[136,128]{1,0:T(8,128)S(1)} custom-call(f32[16,640]{1,0:T(8,128)S(1)} %add_add_fusion.own, f32[16,640]{1,0:T(8,128)S(1)} %collective-permute-done.7.a, f32[16,640]{1,0:T(8,128)S(1)} %collective-permute-done.8.b, f32[16,640]{1,0:T(8,128)S(1)} %collective-permute-done.9.c, bf16[16,1024,128]{2,1,0:T(8,128)(2,1)S(1)} %bitcast.6, ...), custom_call_target="tpu_custom_call" | custom-call | tf_op jit(solution)/shard_map/pallas_call | solution.py:247
  39.1 0.4 collective-permute-start.12
  39.4 0.8 collective-permute-start.11
  40.2 2.1 %collective-permute-start.10 = (f32[136,128]{1,0:T(8,128)S(1)}, f32[136,128]{1,0:T(8,128)S(1)}, u32[]{:S(2)}, u32[]{:S(2)}) collective-permute-start(f32[136,128]{1,0:T(8,128)S(1)} %shard_map.119.own), channel_id=1, source_target_pairs={{0,16},{8,24},{16,0},{24,8},{1,17},{9,25},{17,1},{25,9},{2,18},{10... | collective-permute-start | bytes 208904 | tf_op jit(solution)/shard_map/ppermute | solution.py:30
  42.3 1.5 %collective-permute-done.11.b = f32[136,128]{1,0:T(8,128)S(1)} collective-permute-done((f32[136,128]{1,0:T(8,128)S(1)}, f32[136,128]{1,0:T(8,128)S(1)}, u32[]{:S(2)}, u32[]{:S(2)}) %collective-permute-start.11) | collective-permute-done | bytes 69664 | tf_op jit(solution)/shard_map/ppermute | solution.py:30
  43.8 1.1 %collective-permute-done.10.a = f32[136,128]{1,0:T(8,128)S(1)} collective-permute-done((f32[136,128]{1,0:T(8,128)S(1)}, f32[136,128]{1,0:T(8,128)S(1)}, u32[]{:S(2)}, u32[]{:S(2)}) %collective-permute-start.10) | collective-permute-done | bytes 69664 | tf_op jit(solution)/shard_map/ppermute | solution.py:30
  45.1 0.8 collective-permute-start.15
  45.9 0.7 collective-permute-start.14
  46.6 1.8 %collective-permute-start.13 = (f32[136,128]{1,0:T(8,128)S(1)}, f32[136,128]{1,0:T(8,128)S(1)}, u32[]{:S(2)}, u32[]{:S(2)}) collective-permute-start(f32[136,128]{1,0:T(8,128)S(1)} %shard_map.120.own), channel_id=1, source_target_pairs={{0,64},{32,96},{64,0},{96,32},{1,65},{33,97},{65,1},{97,33},{2,66}... | collective-permute-start | bytes 208904 | tf_op jit(solution)/shard_map/ppermute | solution.py:30
  48.4 2.1 %collective-permute-done.14.b = f32[136,128]{1,0:T(8,128)S(1)} collective-permute-done((f32[136,128]{1,0:T(8,128)S(1)}, f32[136,128]{1,0:T(8,128)S(1)}, u32[]{:S(2)}, u32[]{:S(2)}) %collective-permute-start.14) | collective-permute-done | bytes 69664 | tf_op jit(solution)/shard_map/ppermute | solution.py:30
  50.5 0.7 collective-permute-done.13.a
  51.3 1.0 %shard_map.121 = bf16[16,256]{1,0:T(8,128)(2,1)S(1)} custom-call(f32[4]{0:T(128)S(1)} %copy-done.8, f32[136,128]{1,0:T(8,128)S(1)} %shard_map.120.own, f32[136,128]{1,0:T(8,128)S(1)} %collective-permute-done.13.a, f32[136,128]{1,0:T(8,128)S(1)} %collective-permute-done.14.b, f32[136,128]{1,0:T(8,128)S(1)} %collective-permute-done.15.c, ...), custom_call_target="tpu_custom_call" | custom-call | tf_op jit(solution)/shard_map/pallas_call | solution.py:261
  52.3 0.3 collective-permute-start.18
  52.7 0.6 collective-permute-start.17
  53.3 2.3 %collective-permute-start.16 = (bf16[16,256]{1,0:T(8,128)(2,1)S(1)}, bf16[16,256]{1,0:T(8,128)(2,1)S(1)}, u32[]{:S(2)}, u32[]{:S(2)}) collective-permute-start(bf16[16,256]{1,0:T(8,128)(2,1)S(1)} %shard_map.121), channel_id=1, source_target_pairs={{0,4},{2,6},{4,0},{6,2},{1,5},{3,7},{5,1},{7,3},{8,12},{10,14},{12... | collective-permute-start | bytes 24584 | tf_op jit(solution)/shard_map/ppermute | solution.py:30
  55.6 0.8 collective-permute-done.17
  56.4 0.9 collective-permute-done.16
  57.3 9.4 %collective-permute-start.19 = (f32[16,256]{1,0:T(8,128)S(1)}, f32[16,256]{1,0:T(8,128)S(1)}, u32[]{:S(2)}, u32[]{:S(2)}) collective-permute-start(f32[16,256]{1,0:T(8,128)S(1)} %convert_add_fusion.1.attn), channel_id=1, source_target_pairs={{0,1},{1,0},{2,3},{3,2},{4,5},{5,4},{6,7},{7,6},{8,9},{9,8},{10,11... | collective-permute-start | bytes 49160 | tf_op jit(solution)/shard_map/ppermute | solution.py:35
  66.7 0.8 collective-permute-done.19.other
  67.5 0.3 shard_map.122
  67.8 1.0 %collective-permute-start.22 = (bf16[16,2944]{1,0:T(8,128)(2,1)S(1)}, bf16[16,2944]{1,0:T(8,128)(2,1)S(1)}, u32[]{:S(2)}, u32[]{:S(2)}) collective-permute-start(bf16[16,2944]{1,0:T(8,128)(2,1)S(1)} %get-tuple-element.16), channel_id=1, source_target_pairs={{0,8},{8,0},{16,24},{24,16},{1,9},{9,1},{17,25},{25,17},{2,10},{10... | collective-permute-start | bytes 282632 | tf_op jit(solution)/shard_map/ppermute | solution.py:30
  68.8 1.9 %collective-permute-start.21 = (bf16[16,2944]{1,0:T(8,128)(2,1)S(1)}, bf16[16,2944]{1,0:T(8,128)(2,1)S(1)}, u32[]{:S(2)}, u32[]{:S(2)}) collective-permute-start(bf16[16,2944]{1,0:T(8,128)(2,1)S(1)} %get-tuple-element.16), channel_id=1, source_target_pairs={{0,24},{8,16},{16,8},{24,0},{1,25},{9,17},{17,9},{25,1},{2,26},{10... | collective-permute-start | bytes 282632 | tf_op jit(solution)/shard_map/ppermute | solution.py:30
  70.7 0.7 collective-permute-start.20
  71.4 0.4 collective-permute-done.22.c
  71.8 1.6 %collective-permute-done.21.b = bf16[16,2944]{1,0:T(8,128)(2,1)S(1)} collective-permute-done((bf16[16,2944]{1,0:T(8,128)(2,1)S(1)}, bf16[16,2944]{1,0:T(8,128)(2,1)S(1)}, u32[]{:S(2)}, u32[]{:S(2)}) %collective-permute-start.21) | collective-permute-done | bytes 94240 | tf_op jit(solution)/shard_map/ppermute | solution.py:30
  73.4 2.2 %collective-permute-done.20.a = bf16[16,2944]{1,0:T(8,128)(2,1)S(1)} collective-permute-done((bf16[16,2944]{1,0:T(8,128)(2,1)S(1)}, bf16[16,2944]{1,0:T(8,128)(2,1)S(1)}, u32[]{:S(2)}, u32[]{:S(2)}) %collective-permute-start.20) | collective-permute-done | bytes 94240 | tf_op jit(solution)/shard_map/ppermute | solution.py:30
  75.8 0.2 collective-permute-start.25
  76.0 2.2 %collective-permute-start.24 = (bf16[16,2944]{1,0:T(8,128)(2,1)S(1)}, bf16[16,2944]{1,0:T(8,128)(2,1)S(1)}, u32[]{:S(2)}, u32[]{:S(2)}) collective-permute-start(bf16[16,2944]{1,0:T(8,128)(2,1)S(1)} %get-tuple-element.18), channel_id=1, source_target_pairs={{0,96},{32,64},{64,32},{96,0},{1,97},{33,65},{65,33},{97,1},{2,98}... | collective-permute-start | bytes 282632 | tf_op jit(solution)/shard_map/ppermute | solution.py:30
  78.3 1.1 %collective-permute-start.23 = (bf16[16,2944]{1,0:T(8,128)(2,1)S(1)}, bf16[16,2944]{1,0:T(8,128)(2,1)S(1)}, u32[]{:S(2)}, u32[]{:S(2)}) collective-permute-start(bf16[16,2944]{1,0:T(8,128)(2,1)S(1)} %get-tuple-element.18), channel_id=1, source_target_pairs={{0,64},{32,96},{64,0},{96,32},{1,65},{33,97},{65,1},{97,33},{2,66}... | collective-permute-start | bytes 282632 | tf_op jit(solution)/shard_map/ppermute | solution.py:30
  79.3 1.3 %collective-permute-done.24.b = bf16[16,2944]{1,0:T(8,128)(2,1)S(1)} collective-permute-done((bf16[16,2944]{1,0:T(8,128)(2,1)S(1)}, bf16[16,2944]{1,0:T(8,128)(2,1)S(1)}, u32[]{:S(2)}, u32[]{:S(2)}) %collective-permute-start.24) | collective-permute-done | bytes 94240 | tf_op jit(solution)/shard_map/ppermute | solution.py:30
  80.7 2.9 %collective-permute-done.23.a = bf16[16,2944]{1,0:T(8,128)(2,1)S(1)} collective-permute-done((bf16[16,2944]{1,0:T(8,128)(2,1)S(1)}, bf16[16,2944]{1,0:T(8,128)(2,1)S(1)}, u32[]{:S(2)}, u32[]{:S(2)}) %collective-permute-start.23) | collective-permute-done | bytes 94240 | tf_op jit(solution)/shard_map/ppermute | solution.py:30
  83.6 0.3 shard_map.124
  83.9 1.1 %collective-permute-start.28 = (bf16[16,256]{1,0:T(8,128)(2,1)S(1)}, bf16[16,256]{1,0:T(8,128)(2,1)S(1)}, u32[]{:S(2)}, u32[]{:S(2)}) collective-permute-start(bf16[16,256]{1,0:T(8,128)(2,1)S(1)} %shard_map.124), channel_id=1, source_target_pairs={{0,2},{2,0},{4,6},{6,4},{1,3},{3,1},{5,7},{7,5},{8,10},{10,8},{12,... | collective-permute-start | bytes 24584 | tf_op jit(solution)/shard_map/ppermute | solution.py:30
  85.1 1.8 %collective-permute-start.27 = (bf16[16,256]{1,0:T(8,128)(2,1)S(1)}, bf16[16,256]{1,0:T(8,128)(2,1)S(1)}, u32[]{:S(2)}, u32[]{:S(2)}) collective-permute-start(bf16[16,256]{1,0:T(8,128)(2,1)S(1)} %shard_map.124), channel_id=1, source_target_pairs={{0,6},{2,4},{4,2},{6,0},{1,7},{3,5},{5,3},{7,1},{8,14},{10,12},{12... | collective-permute-start | bytes 24584 | tf_op jit(solution)/shard_map/ppermute | solution.py:30
  86.9 0.6 collective-permute-start.26
  87.5 1.3 %collective-permute-done.27 = bf16[16,256]{1,0:T(8,128)(2,1)S(1)} collective-permute-done((bf16[16,256]{1,0:T(8,128)(2,1)S(1)}, bf16[16,256]{1,0:T(8,128)(2,1)S(1)}, u32[]{:S(2)}, u32[]{:S(2)}) %collective-permute-start.27) | collective-permute-done | bytes 8224 | tf_op jit(solution)/shard_map/ppermute | solution.py:30
  88.8 2.1 %collective-permute-done.26 = bf16[16,256]{1,0:T(8,128)(2,1)S(1)} collective-permute-done((bf16[16,256]{1,0:T(8,128)(2,1)S(1)}, bf16[16,256]{1,0:T(8,128)(2,1)S(1)}, u32[]{:S(2)}, u32[]{:S(2)}) %collective-permute-start.26) | collective-permute-done | bytes 8224 | tf_op jit(solution)/shard_map/ppermute | solution.py:30
  90.9 5.1 %collective-permute-start.29 = (f32[16,256]{1,0:T(8,128)S(1)}, f32[16,256]{1,0:T(8,128)S(1)}, u32[]{:S(2)}, u32[]{:S(2)}) collective-permute-start(f32[16,256]{1,0:T(8,128)S(1)} %convert_add_fusion), channel_id=1, source_target_pairs={{0,1},{1,0},{2,3},{3,2},{4,5},{5,4},{6,7},{7,6},{8,9},{9,8},{10,11... | collective-permute-start | bytes 49160 | tf_op jit(solution)/shard_map/ppermute | solution.py:35
  96.0 0.8 collective-permute-done.29
  96.9 0.7 fusion.6
  (32 shorter events, 0.6 us)
Async XLA Ops:
  1.6 2.3 %collective-permute-start = (f32[24,128]{1,0:T(8,128)S(1)}, f32[24,128]{1,0:T(8,128)S(1)}, u32[]{:S(2)}, u32[]{:S(2)}) collective-permute-start(f32[24,128]{1,0:T(8,128)S(1)} %fusion.2), channel_id=1, source_target_pairs={{0,1},{1,0},{2,3},{3,2},{4,5},{5,4},{6,7},{7,6},{8,9},{9,8},{10,11... | collective-permute-start | bytes 36872 | tf_op jit(solution)/shard_map/ppermute | solution.py:35
  4.8 3.9 %collective-permute-start.3 = (f32[24,128]{1,0:T(8,128)S(1)}, f32[24,128]{1,0:T(8,128)S(1)}, u32[]{:S(2)}, u32[]{:S(2)}) collective-permute-start(f32[24,128]{1,0:T(8,128)S(1)} %fusion.5.own), channel_id=1, source_target_pairs={{0,2},{2,0},{4,6},{6,4},{1,3},{3,1},{5,7},{7,5},{8,10},{10,8},{12,... | collective-permute-start | bytes 36872 | tf_op jit(solution)/shard_map/ppermute | solution.py:30
  6.2 3.8 %collective-permute-start.2 = (f32[24,128]{1,0:T(8,128)S(1)}, f32[24,128]{1,0:T(8,128)S(1)}, u32[]{:S(2)}, u32[]{:S(2)}) collective-permute-start(f32[24,128]{1,0:T(8,128)S(1)} %fusion.5.own), channel_id=1, source_target_pairs={{0,6},{2,4},{4,2},{6,0},{1,7},{3,5},{5,3},{7,1},{8,14},{10,12},{12... | collective-permute-start | bytes 36872 | tf_op jit(solution)/shard_map/ppermute | solution.py:30
  8.0 4.0 %collective-permute-start.1 = (f32[24,128]{1,0:T(8,128)S(1)}, f32[24,128]{1,0:T(8,128)S(1)}, u32[]{:S(2)}, u32[]{:S(2)}) collective-permute-start(f32[24,128]{1,0:T(8,128)S(1)} %fusion.5.own), channel_id=1, source_target_pairs={{0,4},{2,6},{4,0},{6,2},{1,5},{3,7},{5,1},{7,3},{8,12},{10,14},{12... | collective-permute-start | bytes 36872 | tf_op jit(solution)/shard_map/ppermute | solution.py:30
  12.0 1.0 copy-start.5
  13.0 0.7 copy-start.7
  13.8 3.9 %collective-permute-start.6 = (f32[16,640]{1,0:T(8,128)S(1)}, f32[16,640]{1,0:T(8,128)S(1)}, u32[]{:S(2)}, u32[]{:S(2)}) collective-permute-start(f32[16,640]{1,0:T(8,128)S(1)} %get-tuple-element.12), channel_id=1, source_target_pairs={{0,8},{8,0},{16,24},{24,16},{1,9},{9,1},{17,25},{25,17},{2,10},{10... | collective-permute-start | bytes 122888 | tf_op jit(solution)/shard_map/ppermute | solution.py:30
  15.1 4.1 %collective-permute-start.5 = (f32[16,640]{1,0:T(8,128)S(1)}, f32[16,640]{1,0:T(8,128)S(1)}, u32[]{:S(2)}, u32[]{:S(2)}) collective-permute-start(f32[16,640]{1,0:T(8,128)S(1)} %get-tuple-element.12), channel_id=1, source_target_pairs={{0,24},{8,16},{16,8},{24,0},{1,25},{9,17},{17,9},{25,1},{2,26},{10... | collective-permute-start | bytes 122888 | tf_op jit(solution)/shard_map/ppermute | solution.py:30
  17.0 4.5 %collective-permute-start.4 = (f32[16,640]{1,0:T(8,128)S(1)}, f32[16,640]{1,0:T(8,128)S(1)}, u32[]{:S(2)}, u32[]{:S(2)}) collective-permute-start(f32[16,640]{1,0:T(8,128)S(1)} %get-tuple-element.12), channel_id=1, source_target_pairs={{0,16},{8,24},{16,0},{24,8},{1,17},{9,25},{17,1},{25,9},{2,18},{10... | collective-permute-start | bytes 122888 | tf_op jit(solution)/shard_map/ppermute | solution.py:30
  21.6 5.0 %collective-permute-start.9 = (f32[16,640]{1,0:T(8,128)S(1)}, f32[16,640]{1,0:T(8,128)S(1)}, u32[]{:S(2)}, u32[]{:S(2)}) collective-permute-start(f32[16,640]{1,0:T(8,128)S(1)} %add_add_fusion.own), channel_id=1, source_target_pairs={{0,32},{32,0},{64,96},{96,64},{1,33},{33,1},{65,97},{97,65},{2,34}... | collective-permute-start | bytes 122888 | tf_op jit(solution)/shard_map/ppermute | solution.py:30
  23.3 4.1 %collective-permute-start.8 = (f32[16,640]{1,0:T(8,128)S(1)}, f32[16,640]{1,0:T(8,128)S(1)}, u32[]{:S(2)}, u32[]{:S(2)}) collective-permute-start(f32[16,640]{1,0:T(8,128)S(1)} %add_add_fusion.own), channel_id=1, source_target_pairs={{0,96},{32,64},{64,32},{96,0},{1,97},{33,65},{65,33},{97,1},{2,98}... | collective-permute-start | bytes 122888 | tf_op jit(solution)/shard_map/ppermute | solution.py:30
  25.5 4.4 %collective-permute-start.7 = (f32[16,640]{1,0:T(8,128)S(1)}, f32[16,640]{1,0:T(8,128)S(1)}, u32[]{:S(2)}, u32[]{:S(2)}) collective-permute-start(f32[16,640]{1,0:T(8,128)S(1)} %add_add_fusion.own), channel_id=1, source_target_pairs={{0,64},{32,96},{64,0},{96,32},{1,65},{33,97},{65,1},{97,33},{2,66}... | collective-permute-start | bytes 122888 | tf_op jit(solution)/shard_map/ppermute | solution.py:30
  29.9 2.2 %copy-start = (bf16[16,1024,1,128]{3,1,2,0:T(8,128)(2,1)S(1)}, bf16[16,1024,1,128]{3,1,2,0:T(8,128)(2,1)}, u32[]{:S(2)}) copy-start(bf16[16,1024,1,128]{3,1,2,0:T(8,128)(2,1)} %param.15) | copy-start | bytes 12582916
  32.1 2.2 %copy-start.1 = (bf16[16,1024,1,128]{3,1,2,0:T(8,128)(2,1)S(1)}, bf16[16,1024,1,128]{3,1,2,0:T(8,128)(2,1)}, u32[]{:S(2)}) copy-start(bf16[16,1024,1,128]{3,1,2,0:T(8,128)(2,1)} %param.16) | copy-start | bytes 12582916
  34.3 17.0 %copy-start.6 = (bf16[512,256]{1,0:T(8,128)(2,1)S(1)}, bf16[512,256]{1,0:T(8,128)(2,1)}, u32[]{:S(2)}) copy-start(bf16[512,256]{1,0:T(8,128)(2,1)} %weight.4) | copy-start | bytes 786436
  34.3 17.0 %copy-start.8 = (f32[4]{0:T(128)S(1)}, f32[4]{0:T(128)}, u32[]{:S(2)}) copy-start(f32[4]{0:T(128)} %lambdas.1) | copy-start | bytes 52
  34.3 17.0 %copy-start.9 = (f32[128]{0:T(128)S(1)}, f32[128]{0:T(128)}, u32[]{:S(2)}) copy-start(f32[128]{0:T(128)} %param.18) | copy-start | bytes 1540
  34.3 33.2 %copy-start.2 = (bf16[256,1408]{1,0:T(8,128)(2,1)S(1)}, bf16[256,1408]{1,0:T(8,128)(2,1)}, u32[]{:S(2)}) copy-start(bf16[256,1408]{1,0:T(8,128)(2,1)} %gate.1) | copy-start | bytes 2162692
  34.3 33.2 %copy-start.3 = (bf16[256,1408]{1,0:T(8,128)(2,1)S(1)}, bf16[256,1408]{1,0:T(8,128)(2,1)}, u32[]{:S(2)}) copy-start(bf16[256,1408]{1,0:T(8,128)(2,1)} %up.1) | copy-start | bytes 2162692
  34.3 49.3 %copy-start.4 = (bf16[1408,256]{1,0:T(8,128)(2,1)S(1)}, bf16[1408,256]{1,0:T(8,128)(2,1)}, u32[]{:S(2)}) copy-start(bf16[1408,256]{1,0:T(8,128)(2,1)} %weight.5) | copy-start | bytes 2162692
  39.1 3.3 %collective-permute-start.12 = (f32[136,128]{1,0:T(8,128)S(1)}, f32[136,128]{1,0:T(8,128)S(1)}, u32[]{:S(2)}, u32[]{:S(2)}) collective-permute-start(f32[136,128]{1,0:T(8,128)S(1)} %shard_map.119.own), channel_id=1, source_target_pairs={{0,8},{8,0},{16,24},{24,16},{1,9},{9,1},{17,25},{25,17},{2,10},{10... | collective-permute-start | bytes 208904 | tf_op jit(solution)/shard_map/ppermute | solution.py:30
  39.4 4.4 %collective-permute-start.11 = (f32[136,128]{1,0:T(8,128)S(1)}, f32[136,128]{1,0:T(8,128)S(1)}, u32[]{:S(2)}, u32[]{:S(2)}) collective-permute-start(f32[136,128]{1,0:T(8,128)S(1)} %shard_map.119.own), channel_id=1, source_target_pairs={{0,24},{8,16},{16,8},{24,0},{1,25},{9,17},{17,9},{25,1},{2,26},{10... | collective-permute-start | bytes 208904 | tf_op jit(solution)/shard_map/ppermute | solution.py:30
  40.2 4.7 %collective-permute-start.10 = (f32[136,128]{1,0:T(8,128)S(1)}, f32[136,128]{1,0:T(8,128)S(1)}, u32[]{:S(2)}, u32[]{:S(2)}) collective-permute-start(f32[136,128]{1,0:T(8,128)S(1)} %shard_map.119.own), channel_id=1, source_target_pairs={{0,16},{8,24},{16,0},{24,8},{1,17},{9,25},{17,1},{25,9},{2,18},{10... | collective-permute-start | bytes 208904 | tf_op jit(solution)/shard_map/ppermute | solution.py:30
  45.1 3.3 %collective-permute-start.15 = (f32[136,128]{1,0:T(8,128)S(1)}, f32[136,128]{1,0:T(8,128)S(1)}, u32[]{:S(2)}, u32[]{:S(2)}) collective-permute-start(f32[136,128]{1,0:T(8,128)S(1)} %shard_map.120.own), channel_id=1, source_target_pairs={{0,32},{32,0},{64,96},{96,64},{1,33},{33,1},{65,97},{97,65},{2,34}... | collective-permute-start | bytes 208904 | tf_op jit(solution)/shard_map/ppermute | solution.py:30
  45.9 4.7 %collective-permute-start.14 = (f32[136,128]{1,0:T(8,128)S(1)}, f32[136,128]{1,0:T(8,128)S(1)}, u32[]{:S(2)}, u32[]{:S(2)}) collective-permute-start(f32[136,128]{1,0:T(8,128)S(1)} %shard_map.120.own), channel_id=1, source_target_pairs={{0,96},{32,64},{64,32},{96,0},{1,97},{33,65},{65,33},{97,1},{2,98}... | collective-permute-start | bytes 208904 | tf_op jit(solution)/shard_map/ppermute | solution.py:30
  46.6 4.7 %collective-permute-start.13 = (f32[136,128]{1,0:T(8,128)S(1)}, f32[136,128]{1,0:T(8,128)S(1)}, u32[]{:S(2)}, u32[]{:S(2)}) collective-permute-start(f32[136,128]{1,0:T(8,128)S(1)} %shard_map.120.own), channel_id=1, source_target_pairs={{0,64},{32,96},{64,0},{96,32},{1,65},{33,97},{65,1},{97,33},{2,66}... | collective-permute-start | bytes 208904 | tf_op jit(solution)/shard_map/ppermute | solution.py:30
  52.3 3.3 %collective-permute-start.18 = (bf16[16,256]{1,0:T(8,128)(2,1)S(1)}, bf16[16,256]{1,0:T(8,128)(2,1)S(1)}, u32[]{:S(2)}, u32[]{:S(2)}) collective-permute-start(bf16[16,256]{1,0:T(8,128)(2,1)S(1)} %shard_map.121), channel_id=1, source_target_pairs={{0,2},{2,0},{4,6},{6,4},{1,3},{3,1},{5,7},{7,5},{8,10},{10,8},{12,... | collective-permute-start | bytes 24584 | tf_op jit(solution)/shard_map/ppermute | solution.py:30
  52.7 3.7 %collective-permute-start.17 = (bf16[16,256]{1,0:T(8,128)(2,1)S(1)}, bf16[16,256]{1,0:T(8,128)(2,1)S(1)}, u32[]{:S(2)}, u32[]{:S(2)}) collective-permute-start(bf16[16,256]{1,0:T(8,128)(2,1)S(1)} %shard_map.121), channel_id=1, source_target_pairs={{0,6},{2,4},{4,2},{6,0},{1,7},{3,5},{5,3},{7,1},{8,14},{10,12},{12... | collective-permute-start | bytes 24584 | tf_op jit(solution)/shard_map/ppermute | solution.py:30
  53.3 4.0 %collective-permute-start.16 = (bf16[16,256]{1,0:T(8,128)(2,1)S(1)}, bf16[16,256]{1,0:T(8,128)(2,1)S(1)}, u32[]{:S(2)}, u32[]{:S(2)}) collective-permute-start(bf16[16,256]{1,0:T(8,128)(2,1)S(1)} %shard_map.121), channel_id=1, source_target_pairs={{0,4},{2,6},{4,0},{6,2},{1,5},{3,7},{5,1},{7,3},{8,12},{10,14},{12... | collective-permute-start | bytes 24584 | tf_op jit(solution)/shard_map/ppermute | solution.py:30
  57.3 10.2 %collective-permute-start.19 = (f32[16,256]{1,0:T(8,128)S(1)}, f32[16,256]{1,0:T(8,128)S(1)}, u32[]{:S(2)}, u32[]{:S(2)}) collective-permute-start(f32[16,256]{1,0:T(8,128)S(1)} %convert_add_fusion.1.attn), channel_id=1, source_target_pairs={{0,1},{1,0},{2,3},{3,2},{4,5},{5,4},{6,7},{7,6},{8,9},{9,8},{10,11... | collective-permute-start | bytes 49160 | tf_op jit(solution)/shard_map/ppermute | solution.py:35
  67.8 4.0 %collective-permute-start.22 = (bf16[16,2944]{1,0:T(8,128)(2,1)S(1)}, bf16[16,2944]{1,0:T(8,128)(2,1)S(1)}, u32[]{:S(2)}, u32[]{:S(2)}) collective-permute-start(bf16[16,2944]{1,0:T(8,128)(2,1)S(1)} %get-tuple-element.16), channel_id=1, source_target_pairs={{0,8},{8,0},{16,24},{24,16},{1,9},{9,1},{17,25},{25,17},{2,10},{10... | collective-permute-start | bytes 282632 | tf_op jit(solution)/shard_map/ppermute | solution.py:30
  68.8 4.6 %collective-permute-start.21 = (bf16[16,2944]{1,0:T(8,128)(2,1)S(1)}, bf16[16,2944]{1,0:T(8,128)(2,1)S(1)}, u32[]{:S(2)}, u32[]{:S(2)}) collective-permute-start(bf16[16,2944]{1,0:T(8,128)(2,1)S(1)} %get-tuple-element.16), channel_id=1, source_target_pairs={{0,24},{8,16},{16,8},{24,0},{1,25},{9,17},{17,9},{25,1},{2,26},{10... | collective-permute-start | bytes 282632 | tf_op jit(solution)/shard_map/ppermute | solution.py:30
  70.7 4.9 %collective-permute-start.20 = (bf16[16,2944]{1,0:T(8,128)(2,1)S(1)}, bf16[16,2944]{1,0:T(8,128)(2,1)S(1)}, u32[]{:S(2)}, u32[]{:S(2)}) collective-permute-start(bf16[16,2944]{1,0:T(8,128)(2,1)S(1)} %get-tuple-element.16), channel_id=1, source_target_pairs={{0,16},{8,24},{16,0},{24,8},{1,17},{9,25},{17,1},{25,9},{2,18},{10... | collective-permute-start | bytes 282632 | tf_op jit(solution)/shard_map/ppermute | solution.py:30
  75.8 3.6 %collective-permute-start.25 = (bf16[16,2944]{1,0:T(8,128)(2,1)S(1)}, bf16[16,2944]{1,0:T(8,128)(2,1)S(1)}, u32[]{:S(2)}, u32[]{:S(2)}) collective-permute-start(bf16[16,2944]{1,0:T(8,128)(2,1)S(1)} %get-tuple-element.18), channel_id=1, source_target_pairs={{0,32},{32,0},{64,96},{96,64},{1,33},{33,1},{65,97},{97,65},{2,34}... | collective-permute-start | bytes 282632 | tf_op jit(solution)/shard_map/ppermute | solution.py:30
  76.0 4.6 %collective-permute-start.24 = (bf16[16,2944]{1,0:T(8,128)(2,1)S(1)}, bf16[16,2944]{1,0:T(8,128)(2,1)S(1)}, u32[]{:S(2)}, u32[]{:S(2)}) collective-permute-start(bf16[16,2944]{1,0:T(8,128)(2,1)S(1)} %get-tuple-element.18), channel_id=1, source_target_pairs={{0,96},{32,64},{64,32},{96,0},{1,97},{33,65},{65,33},{97,1},{2,98}... | collective-permute-start | bytes 282632 | tf_op jit(solution)/shard_map/ppermute | solution.py:30
  78.3 5.3 %collective-permute-start.23 = (bf16[16,2944]{1,0:T(8,128)(2,1)S(1)}, bf16[16,2944]{1,0:T(8,128)(2,1)S(1)}, u32[]{:S(2)}, u32[]{:S(2)}) collective-permute-start(bf16[16,2944]{1,0:T(8,128)(2,1)S(1)} %get-tuple-element.18), channel_id=1, source_target_pairs={{0,64},{32,96},{64,0},{96,32},{1,65},{33,97},{65,1},{97,33},{2,66}... | collective-permute-start | bytes 282632 | tf_op jit(solution)/shard_map/ppermute | solution.py:30
  83.9 3.6 %collective-permute-start.28 = (bf16[16,256]{1,0:T(8,128)(2,1)S(1)}, bf16[16,256]{1,0:T(8,128)(2,1)S(1)}, u32[]{:S(2)}, u32[]{:S(2)}) collective-permute-start(bf16[16,256]{1,0:T(8,128)(2,1)S(1)} %shard_map.124), channel_id=1, source_target_pairs={{0,2},{2,0},{4,6},{6,4},{1,3},{3,1},{5,7},{7,5},{8,10},{10,8},{12,... | collective-permute-start | bytes 24584 | tf_op jit(solution)/shard_map/ppermute | solution.py:30
  85.1 3.7 %collective-permute-start.27 = (bf16[16,256]{1,0:T(8,128)(2,1)S(1)}, bf16[16,256]{1,0:T(8,128)(2,1)S(1)}, u32[]{:S(2)}, u32[]{:S(2)}) collective-permute-start(bf16[16,256]{1,0:T(8,128)(2,1)S(1)} %shard_map.124), channel_id=1, source_target_pairs={{0,6},{2,4},{4,2},{6,0},{1,7},{3,5},{5,3},{7,1},{8,14},{10,12},{12... | collective-permute-start | bytes 24584 | tf_op jit(solution)/shard_map/ppermute | solution.py:30
  86.9 4.0 %collective-permute-start.26 = (bf16[16,256]{1,0:T(8,128)(2,1)S(1)}, bf16[16,256]{1,0:T(8,128)(2,1)S(1)}, u32[]{:S(2)}, u32[]{:S(2)}) collective-permute-start(bf16[16,256]{1,0:T(8,128)(2,1)S(1)} %shard_map.124), channel_id=1, source_target_pairs={{0,4},{2,6},{4,0},{6,2},{1,5},{3,7},{5,1},{7,3},{8,12},{10,14},{12... | collective-permute-start | bytes 24584 | tf_op jit(solution)/shard_map/ppermute | solution.py:30
  90.9 6.0 %collective-permute-start.29 = (f32[16,256]{1,0:T(8,128)S(1)}, f32[16,256]{1,0:T(8,128)S(1)}, u32[]{:S(2)}, u32[]{:S(2)}) collective-permute-start(f32[16,256]{1,0:T(8,128)S(1)} %convert_add_fusion), channel_id=1, source_target_pairs={{0,1},{1,0},{2,3},{3,2},{4,5},{5,4},{6,7},{7,6},{8,9},{9,8},{10,11... | collective-permute-start | bytes 49160 | tf_op jit(solution)/shard_map/ppermute | solution.py:35

commit v5 on v4

--- a/solution.py
+++ b/solution.py
@@ -19,6 +19,7 @@
 BF16 = jnp.bfloat16
 
 eps = 1e-06
+COST = 2**40
 
 SHIFTS = (2, 3, 1)
 
@@ -45,7 +46,7 @@
     return lax.broadcasted_iota(jnp.int32, shape, len(shape) - 1)
 
 
-def kernel_call(body, outs, scratch=(), smem=0, n_in=1, mib=16):
+def kernel_call(body, outs, scratch=(), smem=0, n_in=1, mib=16, cost=0):
     spec = [pl.BlockSpec(memory_space=pltpu.SMEM)] * smem
     spec += [pl.BlockSpec(memory_space=pltpu.VMEM)] * (n_in - smem)
     return pl.pallas_call(
@@ -55,7 +56,25 @@
         out_specs=[pl.BlockSpec(memory_space=pltpu.VMEM)] * len(outs),
         scratch_shapes=scratch,
         compiler_params=pltpu.CompilerParams(vmem_limit_bytes=mib * 2**20),
-    )
+        cost_estimate=pl.CostEstimate(flops=cost, bytes_accessed=cost, transcendentals=0)
+        if cost
+        else None,
+    )
+
+
+def pack_body(hidden, gain, out, rows, scale, sems):
+    loads = [
+        pltpu.make_async_copy(hidden, rows, sems.at[0]),
+        pltpu.make_async_copy(gain, scale, sems.at[1]),
+    ]
+    for load in loads:
+        load.start()
+    for load in loads:
+        load.wait()
+    batch, cols = hidden.shape
+    out[:batch, :] = jnp.concatenate([rows[...].astype(F32)] * (LANES // cols), axis=1)
+    row = jnp.concatenate([scale[...]] * (LANES // cols), axis=1)
+    out[batch:, :] = jnp.broadcast_to(row, (out.shape[0] - batch, LANES))
 
 
 def query_body(chip, own, a, b, c, gain, weight, packed, block, held):
@@ -75,7 +94,7 @@
     packed[:, width:] = jnp.broadcast_to(squares, (batch, LANES))
 
 
-def attend_body(own, a, b, c, keys, values, out, query):
+def attend_body(own, a, b, c, keys, values, out, query, scores, weights):
     batch, _, _ = keys.shape
     width = own.shape[1] - LANES
     heads = width // LANES
@@ -88,22 +107,27 @@
     half = lane_of(shape) // HEAD_DIM
     keep = half == lax.broadcasted_iota(jnp.int32, shape, 0) // heads
     lane = lane_of(shape)
-    stats = jnp.zeros(shape, F32)
+    high = 2 * heads
     for n in range(batch):
         q = query[pl.ds(n, heads, stride=batch), :]
         q = jnp.where(keep, jnp.concatenate([q, q], axis=0), 0.0).astype(BF16)
-        scores = lax.dot_general(
+        scores[n * high : (n + 1) * high, :] = lax.dot_general(
             q, keys[n], (((1,), (1,)), ((), ())), preferred_element_type=F32
-        ) * HEAD_DIM ** (-0.5)
-        top = jnp.max(scores, axis=1, keepdims=True)
-        exponent = jnp.exp(scores - top)
+        )
+    stats = jnp.zeros(shape, F32)
+    for n in range(batch):
+        score = scores[n * high : (n + 1) * high, :] * HEAD_DIM ** (-0.5)
+        top = jnp.max(score, axis=1, keepdims=True)
+        exponent = jnp.exp(score - top)
         total = jnp.sum(exponent, axis=1, keepdims=True)
-        out[n * 2 * heads : (n + 1) * 2 * heads, :] = jnp.dot(
-            exponent.astype(BF16), values[n], preferred_element_type=F32
-        )
+        weights[n] = exponent.astype(BF16)
         stats = jnp.where(lane == n, top, stats)
         stats = jnp.where(lane == n + LANES // 2, total, stats)
-    out[batch * 2 * heads :, :] = stats
+    out[batch * high :, :] = stats
+    for n in range(batch):
+        out[n * high : (n + 1) * high, :] = jnp.dot(
+            weights[n], values[n], preferred_element_type=F32
+        )
 
 
 def combined(parts, rows, high):
@@ -138,20 +162,17 @@
     rows = own.shape[0] // high - 1
     stats, accs = combined((own, a, b, c), rows, high)
     inverse = 1.0 / stats
-    at = lax.broadcasted_iota(jnp.int32, (heads, LANES), 0)
-    mixing = jnp.zeros((heads, LANES), F32)
-    for g in range(heads):
-        mixing = jnp.where(at == g, lambdas[g], mixing)
     for k, acc in enumerate(accs):
         at_lane = LANES // 2 + k
-        means = acc * inverse[:, at_lane : at_lane + 1]
-        attended = means[:heads] - mixing * means[heads:]
-        norm = lax.rsqrt(jnp.mean(attended * attended, axis=1, keepdims=True) + eps)
-        held[pl.ds(k, heads, stride=rows), :] = attended * norm * gain[...]
+        held[k * high : (k + 1) * high, :] = acc * inverse[:, at_lane : at_lane + 1]
     projected = 0.0
     for g in range(heads):
+        first = held[pl.ds(g, rows, stride=high), :]
+        second = held[pl.ds(heads + g, rows, stride=high), :]
+        attended = first - lambdas[:, g : g + 1] * second
+        norm = lax.rsqrt(jnp.mean(attended * attended, axis=1, keepdims=True) + eps)
         projected = projected + jnp.dot(
-            held[g * rows : (g + 1) * rows, :].astype(BF16),
+            (attended * norm * gain[...]).astype(BF16),
             weight[g * LANES : (g + 1) * LANES, :],
             preferred_element_type=F32,
         )
@@ -231,9 +252,22 @@
     core = lax.axis_index(TP[1])
     chip = lax.axis_index(TP[0]).astype(jnp.int32)
 
-    own = jnp.concatenate([hidden_in.astype(F32), mixer_gain[None]], axis=0)
-    own = jnp.concatenate([own] * (LANES // cols), axis=1)
-    own = jnp.pad(own, ((0, 7), (0, 0)))
+    own = pl.pallas_call(
+        pack_body,
+        out_shape=shape((batch + 8, LANES), F32),
+        in_specs=[pl.BlockSpec(memory_space=pltpu.HBM)] * 2,
+        out_specs=pl.BlockSpec(memory_space=pltpu.VMEM),
+        scratch_shapes=[
+            pltpu.VMEM((batch, cols), BF16),
+            pltpu.VMEM((1, cols), F32),
+            pltpu.SemaphoreType.DMA((2,)),
+        ],
+        compiler_params=pltpu.CompilerParams(vmem_limit_bytes=4 * 2**20),
+        cost_estimate=pl.CostEstimate(flops=COST, bytes_accessed=COST, transcendentals=0),
+    )(
+        pltpu.with_memory_space_constraint(hidden_in, pltpu.HBM),
+        pltpu.with_memory_space_constraint(mixer_gain[None], pltpu.HBM),
+    )
     mine = lane_of(own.shape) // cols % 2 == core
     pair = jnp.where(mine, own, partner(own))
     packed, block = kernel_call(
@@ -242,12 +276,17 @@
         [pltpu.VMEM((4, *own.shape), F32)],
         smem=1,
         n_in=7,
+        cost=COST,
     )(chip[None], pair, *peers(pair, "tp_0"), attn_gain[None], query_weight)
     packed = added(packed, peers(packed, "kv_1"))
     state = kernel_call(
         attend_body,
         [shape(((batch + 1) * 2 * heads, LANES), F32)],
-        [pltpu.VMEM((heads * batch, LANES), F32)],
+        [
+            pltpu.VMEM((heads * batch, LANES), F32),
+            pltpu.VMEM((2 * heads * batch, positions), F32),
+            pltpu.VMEM((batch, 2 * heads, positions), BF16),
+        ],
         n_in=6,
     )(
         packed,
@@ -261,10 +300,9 @@
     projected = kernel_call(
         project_body,
         [shape((batch, wide), BF16)],
-        [pltpu.VMEM((heads * batch, LANES), F32)],
-        smem=1,
+        [pltpu.VMEM((2 * heads * batch, LANES), F32)],
         n_in=7,
-    )(lambdas, state, *peers(state, "kv_0"), head_gain[None], out_weight)[0]
+    )(lambdas[None], state, *peers(state, "kv_0"), head_gain[None], out_weight)[0]
     attn = added(
         projected.astype(F32), [p.astype(F32) for p in peers(projected, "tp_0")]
     )

time: 97.8 us -> 86.5 us (0.88)
  local copies, waits for them, and re-layouts: 6.03 us -> 0.05 us
  Pallas kernels: 6.93 us -> 4.17 us
  other arithmetic: 3.16 us -> 0.72 us
    unnamed x20, local copies, waits for them, and re-layouts: 6.03 us -> 0.05 us
    pallas_call x1, Pallas kernels: 4.76 us -> 1.77 us  [per_device(): kernel_call(attend_body, [shape(((batch + 1) * 2 * heads, LANES), F32)],...]
where the time goes in v5:
time: 86.5 us; the launch traced here: 86.4 us
  starting transfers between devices  49.4 us (57%)
  waiting for transfers between devices  32 us (37%)
  Pallas kernels  4.17 us (5%)
    ppermute x27, starting transfers between devices, peers(): got.append(lax.ppermute(shard, axis, [(i, i ^ s) for i in range(n)]))  33.4 us
    ppermute x27, waiting for transfers between devices, peers(): got.append(lax.ppermute(shard, axis, [(i, i ^ s) for i in range(n)]))  29.5 us
    ppermute x3, starting transfers between devices, partner(): return lax.ppermute(shard, TP[1], [(0, 1), (1, 0)])  16 us
    ppermute x3, waiting for transfers between devices, partner(): return lax.ppermute(shard, TP[1], [(0, 1), (1, 0)])  2.5 us
    pallas_call x1, Pallas kernels, per_device(): kernel_call(attend_body, [shape(((batch + 1) * 2 * heads, LANES), F32)],...  1.77 us
  transfers between devices with their start and end apart: 30, of which 22 were waited for; matrix products, arithmetic and copies ran while one was open for 0% of the time, Pallas kernels for 0%

profile of v5, /device:TPU:1, one launch (start us, length us, event | category | flops | bytes accessed | tf_op | source)
XLA Modules:
  0.0 86.4 jit_solution(15743509582047722461)
XLA Ops:
  0.0 0.8 shard_map.118
  0.8 1.5 %collective-permute-start = (f32[24,128]{1,0:T(8,128)S(1)}, f32[24,128]{1,0:T(8,128)S(1)}, u32[]{:S(2)}, u32[]{:S(2)}) collective-permute-start(f32[24,128]{1,0:T(8,128)S(1)} %shard_map.118), channel_id=1, source_target_pairs={{0,1},{1,0},{2,3},{3,2},{4,5},{5,4},{6,7},{7,6},{8,9},{9,8},{10,11... | collective-permute-start | bytes 36872 | tf_op jit(solution)/shard_map/ppermute | solution.py:36
  2.3 0.8 collective-permute-done
  3.1 1.4 %collective-permute-start.3 = (f32[24,128]{1,0:T(8,128)S(1)}, f32[24,128]{1,0:T(8,128)S(1)}, u32[]{:S(2)}, u32[]{:S(2)}) collective-permute-start(f32[24,128]{1,0:T(8,128)S(1)} %fusion.2.own), channel_id=1, source_target_pairs={{0,2},{2,0},{4,6},{6,4},{1,3},{3,1},{5,7},{7,5},{8,10},{10,8},{12,... | collective-permute-start | bytes 36872 | tf_op jit(solution)/shard_map/ppermute | solution.py:31
  4.5 1.8 %collective-permute-start.2 = (f32[24,128]{1,0:T(8,128)S(1)}, f32[24,128]{1,0:T(8,128)S(1)}, u32[]{:S(2)}, u32[]{:S(2)}) collective-permute-start(f32[24,128]{1,0:T(8,128)S(1)} %fusion.2.own), channel_id=1, source_target_pairs={{0,6},{2,4},{4,2},{6,0},{1,7},{3,5},{5,3},{7,1},{8,14},{10,12},{12... | collective-permute-start | bytes 36872 | tf_op jit(solution)/shard_map/ppermute | solution.py:31
  6.4 0.6 collective-permute-start.1
  7.0 1.3 %collective-permute-done.2.b = f32[24,128]{1,0:T(8,128)S(1)} collective-permute-done((f32[24,128]{1,0:T(8,128)S(1)}, f32[24,128]{1,0:T(8,128)S(1)}, u32[]{:S(2)}, u32[]{:S(2)}) %collective-permute-start.2) | collective-permute-done | bytes 12320 | tf_op jit(solution)/shard_map/ppermute | solution.py:31
  8.3 2.1 %collective-permute-done.1.a = f32[24,128]{1,0:T(8,128)S(1)} collective-permute-done((f32[24,128]{1,0:T(8,128)S(1)}, f32[24,128]{1,0:T(8,128)S(1)}, u32[]{:S(2)}, u32[]{:S(2)}) %collective-permute-start.1) | collective-permute-done | bytes 12320 | tf_op jit(solution)/shard_map/ppermute | solution.py:31
  10.4 0.2 shard_map.119
  10.6 1.3 %collective-permute-start.6 = (f32[16,640]{1,0:T(8,128)S(1)}, f32[16,640]{1,0:T(8,128)S(1)}, u32[]{:S(2)}, u32[]{:S(2)}) collective-permute-start(f32[16,640]{1,0:T(8,128)S(1)} %get-tuple-element.12), channel_id=1, source_target_pairs={{0,8},{8,0},{16,24},{24,16},{1,9},{9,1},{17,25},{25,17},{2,10},{10... | collective-permute-start | bytes 122888 | tf_op jit(solution)/shard_map/ppermute | solution.py:31
  11.9 1.9 %collective-permute-start.5 = (f32[16,640]{1,0:T(8,128)S(1)}, f32[16,640]{1,0:T(8,128)S(1)}, u32[]{:S(2)}, u32[]{:S(2)}) collective-permute-start(f32[16,640]{1,0:T(8,128)S(1)} %get-tuple-element.12), channel_id=1, source_target_pairs={{0,24},{8,16},{16,8},{24,0},{1,25},{9,17},{17,9},{25,1},{2,26},{10... | collective-permute-start | bytes 122888 | tf_op jit(solution)/shard_map/ppermute | solution.py:31
  13.8 0.7 collective-permute-start.4
  14.5 1.4 %collective-permute-done.5 = f32[16,640]{1,0:T(8,128)S(1)} collective-permute-done((f32[16,640]{1,0:T(8,128)S(1)}, f32[16,640]{1,0:T(8,128)S(1)}, u32[]{:S(2)}, u32[]{:S(2)}) %collective-permute-start.5) | collective-permute-done | bytes 40992 | tf_op jit(solution)/shard_map/ppermute | solution.py:31
  15.9 2.4 %collective-permute-done.4 = f32[16,640]{1,0:T(8,128)S(1)} collective-permute-done((f32[16,640]{1,0:T(8,128)S(1)}, f32[16,640]{1,0:T(8,128)S(1)}, u32[]{:S(2)}, u32[]{:S(2)}) %collective-permute-start.4) | collective-permute-done | bytes 40992 | tf_op jit(solution)/shard_map/ppermute | solution.py:31
  18.3 1.7 %collective-permute-start.9 = (f32[16,640]{1,0:T(8,128)S(1)}, f32[16,640]{1,0:T(8,128)S(1)}, u32[]{:S(2)}, u32[]{:S(2)}) collective-permute-start(f32[16,640]{1,0:T(8,128)S(1)} %add_add_fusion.own), channel_id=1, source_target_pairs={{0,32},{32,0},{64,96},{96,64},{1,33},{33,1},{65,97},{97,65},{2,34}... | collective-permute-start | bytes 122888 | tf_op jit(solution)/shard_map/ppermute | solution.py:31
  20.0 2.2 %collective-permute-start.8 = (f32[16,640]{1,0:T(8,128)S(1)}, f32[16,640]{1,0:T(8,128)S(1)}, u32[]{:S(2)}, u32[]{:S(2)}) collective-permute-start(f32[16,640]{1,0:T(8,128)S(1)} %add_add_fusion.own), channel_id=1, source_target_pairs={{0,96},{32,64},{64,32},{96,0},{1,97},{33,65},{65,33},{97,1},{2,98}... | collective-permute-start | bytes 122888 | tf_op jit(solution)/shard_map/ppermute | solution.py:31
  22.3 1.1 %collective-permute-start.7 = (f32[16,640]{1,0:T(8,128)S(1)}, f32[16,640]{1,0:T(8,128)S(1)}, u32[]{:S(2)}, u32[]{:S(2)}) collective-permute-start(f32[16,640]{1,0:T(8,128)S(1)} %add_add_fusion.own), channel_id=1, source_target_pairs={{0,64},{32,96},{64,0},{96,32},{1,65},{33,97},{65,1},{97,33},{2,66}... | collective-permute-start | bytes 122888 | tf_op jit(solution)/shard_map/ppermute | solution.py:31
  23.4 0.8 collective-permute-done.8.b
  24.1 2.5 %collective-permute-done.7.a = f32[16,640]{1,0:T(8,128)S(1)} collective-permute-done((f32[16,640]{1,0:T(8,128)S(1)}, f32[16,640]{1,0:T(8,128)S(1)}, u32[]{:S(2)}, u32[]{:S(2)}) %collective-permute-start.7) | collective-permute-done | bytes 40992 | tf_op jit(solution)/shard_map/ppermute | solution.py:31
  26.7 0.0 copy-start.7
  26.7 0.0 copy-start.2
  26.7 0.0 copy-start.4
  26.7 1.8 %shard_map.120.own = f32[136,128]{1,0:T(8,128)S(1)} custom-call(f32[16,640]{1,0:T(8,128)S(1)} %add_add_fusion.own, f32[16,640]{1,0:T(8,128)S(1)} %collective-permute-done.7.a, f32[16,640]{1,0:T(8,128)S(1)} %collective-permute-done.8.b, f32[16,640]{1,0:T(8,128)S(1)} %collective-permute-done.9.c, bf16[16,1024,128]{2,1,0:T(8,128)(2,1)S(1)} %bitcast.7, ...), custom_call_target="tpu_custom_call" | custom-call | tf_op jit(solution)/shard_map/pallas_call | solution.py:282
  28.5 0.5 collective-permute-start.12
  28.9 0.8 collective-permute-start.11
  29.7 2.1 %collective-permute-start.10 = (f32[136,128]{1,0:T(8,128)S(1)}, f32[136,128]{1,0:T(8,128)S(1)}, u32[]{:S(2)}, u32[]{:S(2)}) collective-permute-start(f32[136,128]{1,0:T(8,128)S(1)} %shard_map.120.own), channel_id=1, source_target_pairs={{0,16},{8,24},{16,0},{24,8},{1,17},{9,25},{17,1},{25,9},{2,18},{10... | collective-permute-start | bytes 208904 | tf_op jit(solution)/shard_map/ppermute | solution.py:31
  31.8 1.5 %collective-permute-done.11.b = f32[136,128]{1,0:T(8,128)S(1)} collective-permute-done((f32[136,128]{1,0:T(8,128)S(1)}, f32[136,128]{1,0:T(8,128)S(1)}, u32[]{:S(2)}, u32[]{:S(2)}) %collective-permute-start.11) | collective-permute-done | bytes 69664 | tf_op jit(solution)/shard_map/ppermute | solution.py:31
  33.3 1.1 %collective-permute-done.10.a = f32[136,128]{1,0:T(8,128)S(1)} collective-permute-done((f32[136,128]{1,0:T(8,128)S(1)}, f32[136,128]{1,0:T(8,128)S(1)}, u32[]{:S(2)}, u32[]{:S(2)}) %collective-permute-start.10) | collective-permute-done | bytes 69664 | tf_op jit(solution)/shard_map/ppermute | solution.py:31
  34.4 0.2 shard_map.121.own
  34.6 0.8 collective-permute-start.15
  35.4 0.7 collective-permute-start.14
  36.1 1.8 %collective-permute-start.13 = (f32[136,128]{1,0:T(8,128)S(1)}, f32[136,128]{1,0:T(8,128)S(1)}, u32[]{:S(2)}, u32[]{:S(2)}) collective-permute-start(f32[136,128]{1,0:T(8,128)S(1)} %shard_map.121.own), channel_id=1, source_target_pairs={{0,64},{32,96},{64,0},{96,32},{1,65},{33,97},{65,1},{97,33},{2,66}... | collective-permute-start | bytes 208904 | tf_op jit(solution)/shard_map/ppermute | solution.py:31
  37.9 2.1 %collective-permute-done.14.b = f32[136,128]{1,0:T(8,128)S(1)} collective-permute-done((f32[136,128]{1,0:T(8,128)S(1)}, f32[136,128]{1,0:T(8,128)S(1)}, u32[]{:S(2)}, u32[]{:S(2)}) %collective-permute-start.14) | collective-permute-done | bytes 69664 | tf_op jit(solution)/shard_map/ppermute | solution.py:31
  40.0 0.7 collective-permute-done.13.a
  40.8 0.4 shard_map.122
  41.2 0.3 collective-permute-start.18
  41.6 0.6 collective-permute-start.17
  42.2 2.3 %collective-permute-start.16 = (bf16[16,256]{1,0:T(8,128)(2,1)S(1)}, bf16[16,256]{1,0:T(8,128)(2,1)S(1)}, u32[]{:S(2)}, u32[]{:S(2)}) collective-permute-start(bf16[16,256]{1,0:T(8,128)(2,1)S(1)} %shard_map.122), channel_id=1, source_target_pairs={{0,4},{2,6},{4,0},{6,2},{1,5},{3,7},{5,1},{7,3},{8,12},{10,14},{12... | collective-permute-start | bytes 24584 | tf_op jit(solution)/shard_map/ppermute | solution.py:31
  44.5 0.8 collective-permute-done.17
  45.3 0.9 %collective-permute-done.16 = bf16[16,256]{1,0:T(8,128)(2,1)S(1)} collective-permute-done((bf16[16,256]{1,0:T(8,128)(2,1)S(1)}, bf16[16,256]{1,0:T(8,128)(2,1)S(1)}, u32[]{:S(2)}, u32[]{:S(2)}) %collective-permute-start.16) | collective-permute-done | bytes 8224 | tf_op jit(solution)/shard_map/ppermute | solution.py:31
  46.2 9.4 %collective-permute-start.19 = (f32[16,256]{1,0:T(8,128)S(1)}, f32[16,256]{1,0:T(8,128)S(1)}, u32[]{:S(2)}, u32[]{:S(2)}) collective-permute-start(f32[16,256]{1,0:T(8,128)S(1)} %convert_add_fusion.1.attn), channel_id=1, source_target_pairs={{0,1},{1,0},{2,3},{3,2},{4,5},{5,4},{6,7},{7,6},{8,9},{9,8},{10,11... | collective-permute-start | bytes 49160 | tf_op jit(solution)/shard_map/ppermute | solution.py:36
  55.6 0.8 collective-permute-done.19.other
  56.4 0.3 shard_map.123
  56.7 1.0 %collective-permute-start.22 = (bf16[16,2944]{1,0:T(8,128)(2,1)S(1)}, bf16[16,2944]{1,0:T(8,128)(2,1)S(1)}, u32[]{:S(2)}, u32[]{:S(2)}) collective-permute-start(bf16[16,2944]{1,0:T(8,128)(2,1)S(1)} %get-tuple-element.16), channel_id=1, source_target_pairs={{0,8},{8,0},{16,24},{24,16},{1,9},{9,1},{17,25},{25,17},{2,10},{10... | collective-permute-start | bytes 282632 | tf_op jit(solution)/shard_map/ppermute | solution.py:31
  57.7 1.9 %collective-permute-start.21 = (bf16[16,2944]{1,0:T(8,128)(2,1)S(1)}, bf16[16,2944]{1,0:T(8,128)(2,1)S(1)}, u32[]{:S(2)}, u32[]{:S(2)}) collective-permute-start(bf16[16,2944]{1,0:T(8,128)(2,1)S(1)} %get-tuple-element.16), channel_id=1, source_target_pairs={{0,24},{8,16},{16,8},{24,0},{1,25},{9,17},{17,9},{25,1},{2,26},{10... | collective-permute-start | bytes 282632 | tf_op jit(solution)/shard_map/ppermute | solution.py:31
  59.6 0.7 collective-permute-start.20
  60.3 0.4 collective-permute-done.22.c
  60.7 1.6 %collective-permute-done.21.b = bf16[16,2944]{1,0:T(8,128)(2,1)S(1)} collective-permute-done((bf16[16,2944]{1,0:T(8,128)(2,1)S(1)}, bf16[16,2944]{1,0:T(8,128)(2,1)S(1)}, u32[]{:S(2)}, u32[]{:S(2)}) %collective-permute-start.21) | collective-permute-done | bytes 94240 | tf_op jit(solution)/shard_map/ppermute | solution.py:31
  62.3 2.2 %collective-permute-done.20.a = bf16[16,2944]{1,0:T(8,128)(2,1)S(1)} collective-permute-done((bf16[16,2944]{1,0:T(8,128)(2,1)S(1)}, bf16[16,2944]{1,0:T(8,128)(2,1)S(1)}, u32[]{:S(2)}, u32[]{:S(2)}) %collective-permute-start.20) | collective-permute-done | bytes 94240 | tf_op jit(solution)/shard_map/ppermute | solution.py:31
  64.5 0.2 shard_map.124
  64.7 0.2 collective-permute-start.25
  64.9 2.2 %collective-permute-start.24 = (bf16[16,2944]{1,0:T(8,128)(2,1)S(1)}, bf16[16,2944]{1,0:T(8,128)(2,1)S(1)}, u32[]{:S(2)}, u32[]{:S(2)}) collective-permute-start(bf16[16,2944]{1,0:T(8,128)(2,1)S(1)} %get-tuple-element.18), channel_id=1, source_target_pairs={{0,96},{32,64},{64,32},{96,0},{1,97},{33,65},{65,33},{97,1},{2,98}... | collective-permute-start | bytes 282632 | tf_op jit(solution)/shard_map/ppermute | solution.py:31
  67.2 1.1 %collective-permute-start.23 = (bf16[16,2944]{1,0:T(8,128)(2,1)S(1)}, bf16[16,2944]{1,0:T(8,128)(2,1)S(1)}, u32[]{:S(2)}, u32[]{:S(2)}) collective-permute-start(bf16[16,2944]{1,0:T(8,128)(2,1)S(1)} %get-tuple-element.18), channel_id=1, source_target_pairs={{0,64},{32,96},{64,0},{96,32},{1,65},{33,97},{65,1},{97,33},{2,66}... | collective-permute-start | bytes 282632 | tf_op jit(solution)/shard_map/ppermute | solution.py:31
  68.2 1.3 %collective-permute-done.24.b = bf16[16,2944]{1,0:T(8,128)(2,1)S(1)} collective-permute-done((bf16[16,2944]{1,0:T(8,128)(2,1)S(1)}, bf16[16,2944]{1,0:T(8,128)(2,1)S(1)}, u32[]{:S(2)}, u32[]{:S(2)}) %collective-permute-start.24) | collective-permute-done | bytes 94240 | tf_op jit(solution)/shard_map/ppermute | solution.py:31
  69.6 2.9 %collective-permute-done.23.a = bf16[16,2944]{1,0:T(8,128)(2,1)S(1)} collective-permute-done((bf16[16,2944]{1,0:T(8,128)(2,1)S(1)}, bf16[16,2944]{1,0:T(8,128)(2,1)S(1)}, u32[]{:S(2)}, u32[]{:S(2)}) %collective-permute-start.23) | collective-permute-done | bytes 94240 | tf_op jit(solution)/shard_map/ppermute | solution.py:31
  72.5 0.3 shard_map.125
  72.9 1.1 %collective-permute-start.28 = (bf16[16,256]{1,0:T(8,128)(2,1)S(1)}, bf16[16,256]{1,0:T(8,128)(2,1)S(1)}, u32[]{:S(2)}, u32[]{:S(2)}) collective-permute-start(bf16[16,256]{1,0:T(8,128)(2,1)S(1)} %shard_map.125), channel_id=1, source_target_pairs={{0,2},{2,0},{4,6},{6,4},{1,3},{3,1},{5,7},{7,5},{8,10},{10,8},{12,... | collective-permute-start | bytes 24584 | tf_op jit(solution)/shard_map/ppermute | solution.py:31
  74.0 1.8 %collective-permute-start.27 = (bf16[16,256]{1,0:T(8,128)(2,1)S(1)}, bf16[16,256]{1,0:T(8,128)(2,1)S(1)}, u32[]{:S(2)}, u32[]{:S(2)}) collective-permute-start(bf16[16,256]{1,0:T(8,128)(2,1)S(1)} %shard_map.125), channel_id=1, source_target_pairs={{0,6},{2,4},{4,2},{6,0},{1,7},{3,5},{5,3},{7,1},{8,14},{10,12},{12... | collective-permute-start | bytes 24584 | tf_op jit(solution)/shard_map/ppermute | solution.py:31
  75.8 0.6 collective-permute-start.26
  76.4 1.3 %collective-permute-done.27 = bf16[16,256]{1,0:T(8,128)(2,1)S(1)} collective-permute-done((bf16[16,256]{1,0:T(8,128)(2,1)S(1)}, bf16[16,256]{1,0:T(8,128)(2,1)S(1)}, u32[]{:S(2)}, u32[]{:S(2)}) %collective-permute-start.27) | collective-permute-done | bytes 8224 | tf_op jit(solution)/shard_map/ppermute | solution.py:31
  77.7 2.1 %collective-permute-done.26 = bf16[16,256]{1,0:T(8,128)(2,1)S(1)} collective-permute-done((bf16[16,256]{1,0:T(8,128)(2,1)S(1)}, bf16[16,256]{1,0:T(8,128)(2,1)S(1)}, u32[]{:S(2)}, u32[]{:S(2)}) %collective-permute-start.26) | collective-permute-done | bytes 8224 | tf_op jit(solution)/shard_map/ppermute | solution.py:31
  79.8 5.1 %collective-permute-start.29 = (f32[16,256]{1,0:T(8,128)S(1)}, f32[16,256]{1,0:T(8,128)S(1)}, u32[]{:S(2)}, u32[]{:S(2)}) collective-permute-start(f32[16,256]{1,0:T(8,128)S(1)} %convert_add_fusion), channel_id=1, source_target_pairs={{0,1},{1,0},{2,3},{3,2},{4,5},{5,4},{6,7},{7,6},{8,9},{9,8},{10,11... | collective-permute-start | bytes 49160 | tf_op jit(solution)/shard_map/ppermute | solution.py:36
  84.9 0.8 collective-permute-done.29
  85.8 0.7 fusion.3
  (31 shorter events, 0.1 us)
Async XLA Ops:
  0.0 10.4 %copy-start.8 = (bf16[256,512]{1,0:T(8,128)(2,1)S(1)}, bf16[256,512]{1,0:T(8,128)(2,1)}, u32[]{:S(2)}) copy-start(bf16[256,512]{1,0:T(8,128)(2,1)} %weight.3) | copy-start | bytes 786436
  0.0 10.4 %copy-start.9 = (f32[256]{0:T(256)S(1)}, f32[256]{0:T(256)}, u32[]{:S(2)}) copy-start(f32[256]{0:T(256)} %param.13) | copy-start | bytes 3076
  0.8 2.3 %collective-permute-start = (f32[24,128]{1,0:T(8,128)S(1)}, f32[24,128]{1,0:T(8,128)S(1)}, u32[]{:S(2)}, u32[]{:S(2)}) collective-permute-start(f32[24,128]{1,0:T(8,128)S(1)} %shard_map.118), channel_id=1, source_target_pairs={{0,1},{1,0},{2,3},{3,2},{4,5},{5,4},{6,7},{7,6},{8,9},{9,8},{10,11... | collective-permute-start | bytes 36872 | tf_op jit(solution)/shard_map/ppermute | solution.py:36
  3.1 3.9 %collective-permute-start.3 = (f32[24,128]{1,0:T(8,128)S(1)}, f32[24,128]{1,0:T(8,128)S(1)}, u32[]{:S(2)}, u32[]{:S(2)}) collective-permute-start(f32[24,128]{1,0:T(8,128)S(1)} %fusion.2.own), channel_id=1, source_target_pairs={{0,2},{2,0},{4,6},{6,4},{1,3},{3,1},{5,7},{7,5},{8,10},{10,8},{12,... | collective-permute-start | bytes 36872 | tf_op jit(solution)/shard_map/ppermute | solution.py:31
  4.5 3.8 %collective-permute-start.2 = (f32[24,128]{1,0:T(8,128)S(1)}, f32[24,128]{1,0:T(8,128)S(1)}, u32[]{:S(2)}, u32[]{:S(2)}) collective-permute-start(f32[24,128]{1,0:T(8,128)S(1)} %fusion.2.own), channel_id=1, source_target_pairs={{0,6},{2,4},{4,2},{6,0},{1,7},{3,5},{5,3},{7,1},{8,14},{10,12},{12... | collective-permute-start | bytes 36872 | tf_op jit(solution)/shard_map/ppermute | solution.py:31
  6.4 4.0 %collective-permute-start.1 = (f32[24,128]{1,0:T(8,128)S(1)}, f32[24,128]{1,0:T(8,128)S(1)}, u32[]{:S(2)}, u32[]{:S(2)}) collective-permute-start(f32[24,128]{1,0:T(8,128)S(1)} %fusion.2.own), channel_id=1, source_target_pairs={{0,4},{2,6},{4,0},{6,2},{1,5},{3,7},{5,1},{7,3},{8,12},{10,14},{12... | collective-permute-start | bytes 36872 | tf_op jit(solution)/shard_map/ppermute | solution.py:31
  10.4 16.2 %copy-start = (bf16[16,1024,1,128]{3,1,2,0:T(8,128)(2,1)S(1)}, bf16[16,1024,1,128]{3,1,2,0:T(8,128)(2,1)}, u32[]{:S(2)}) copy-start(bf16[16,1024,1,128]{3,1,2,0:T(8,128)(2,1)} %param.15) | copy-start | bytes 12582916
  10.4 16.2 %copy-start.1 = (bf16[16,1024,1,128]{3,1,2,0:T(8,128)(2,1)S(1)}, bf16[16,1024,1,128]{3,1,2,0:T(8,128)(2,1)}, u32[]{:S(2)}) copy-start(bf16[16,1024,1,128]{3,1,2,0:T(8,128)(2,1)} %param.16) | copy-start | bytes 12582916
  10.6 3.9 %collective-permute-start.6 = (f32[16,640]{1,0:T(8,128)S(1)}, f32[16,640]{1,0:T(8,128)S(1)}, u32[]{:S(2)}, u32[]{:S(2)}) collective-permute-start(f32[16,640]{1,0:T(8,128)S(1)} %get-tuple-element.12), channel_id=1, source_target_pairs={{0,8},{8,0},{16,24},{24,16},{1,9},{9,1},{17,25},{25,17},{2,10},{10... | collective-permute-start | bytes 122888 | tf_op jit(solution)/shard_map/ppermute | solution.py:31
  11.9 4.1 %collective-permute-start.5 = (f32[16,640]{1,0:T(8,128)S(1)}, f32[16,640]{1,0:T(8,128)S(1)}, u32[]{:S(2)}, u32[]{:S(2)}) collective-permute-start(f32[16,640]{1,0:T(8,128)S(1)} %get-tuple-element.12), channel_id=1, source_target_pairs={{0,24},{8,16},{16,8},{24,0},{1,25},{9,17},{17,9},{25,1},{2,26},{10... | collective-permute-start | bytes 122888 | tf_op jit(solution)/shard_map/ppermute | solution.py:31
  13.8 4.5 %collective-permute-start.4 = (f32[16,640]{1,0:T(8,128)S(1)}, f32[16,640]{1,0:T(8,128)S(1)}, u32[]{:S(2)}, u32[]{:S(2)}) collective-permute-start(f32[16,640]{1,0:T(8,128)S(1)} %get-tuple-element.12), channel_id=1, source_target_pairs={{0,16},{8,24},{16,0},{24,8},{1,17},{9,25},{17,1},{25,9},{2,18},{10... | collective-permute-start | bytes 122888 | tf_op jit(solution)/shard_map/ppermute | solution.py:31
  18.3 5.0 %collective-permute-start.9 = (f32[16,640]{1,0:T(8,128)S(1)}, f32[16,640]{1,0:T(8,128)S(1)}, u32[]{:S(2)}, u32[]{:S(2)}) collective-permute-start(f32[16,640]{1,0:T(8,128)S(1)} %add_add_fusion.own), channel_id=1, source_target_pairs={{0,32},{32,0},{64,96},{96,64},{1,33},{33,1},{65,97},{97,65},{2,34}... | collective-permute-start | bytes 122888 | tf_op jit(solution)/shard_map/ppermute | solution.py:31
  20.0 4.1 %collective-permute-start.8 = (f32[16,640]{1,0:T(8,128)S(1)}, f32[16,640]{1,0:T(8,128)S(1)}, u32[]{:S(2)}, u32[]{:S(2)}) collective-permute-start(f32[16,640]{1,0:T(8,128)S(1)} %add_add_fusion.own), channel_id=1, source_target_pairs={{0,96},{32,64},{64,32},{96,0},{1,97},{33,65},{65,33},{97,1},{2,98}... | collective-permute-start | bytes 122888 | tf_op jit(solution)/shard_map/ppermute | solution.py:31
  22.3 4.4 %collective-permute-start.7 = (f32[16,640]{1,0:T(8,128)S(1)}, f32[16,640]{1,0:T(8,128)S(1)}, u32[]{:S(2)}, u32[]{:S(2)}) collective-permute-start(f32[16,640]{1,0:T(8,128)S(1)} %add_add_fusion.own), channel_id=1, source_target_pairs={{0,64},{32,96},{64,0},{96,32},{1,65},{33,97},{65,1},{97,33},{2,66}... | collective-permute-start | bytes 122888 | tf_op jit(solution)/shard_map/ppermute | solution.py:31
  26.7 14.1 %copy-start.5 = (bf16[512,256]{1,0:T(8,128)(2,1)S(1)}, bf16[512,256]{1,0:T(8,128)(2,1)}, u32[]{:S(2)}) copy-start(bf16[512,256]{1,0:T(8,128)(2,1)} %weight.4) | copy-start | bytes 786436
  26.7 14.1 %copy-start.6 = (f32[4]{0:T(128)S(1)}, f32[4]{0:T(128)}, u32[]{:S(2)}) copy-start(f32[4]{0:T(128)} %param.17) | copy-start | bytes 52
  26.7 14.1 %copy-start.7 = (f32[128]{0:T(128)S(1)}, f32[128]{0:T(128)}, u32[]{:S(2)}) copy-start(f32[128]{0:T(128)} %param.18) | copy-start | bytes 1540
  26.7 29.7 %copy-start.2 = (bf16[256,1408]{1,0:T(8,128)(2,1)S(1)}, bf16[256,1408]{1,0:T(8,128)(2,1)}, u32[]{:S(2)}) copy-start(bf16[256,1408]{1,0:T(8,128)(2,1)} %gate.1) | copy-start | bytes 2162692
  26.7 29.7 %copy-start.3 = (bf16[256,1408]{1,0:T(8,128)(2,1)S(1)}, bf16[256,1408]{1,0:T(8,128)(2,1)}, u32[]{:S(2)}) copy-start(bf16[256,1408]{1,0:T(8,128)(2,1)} %up.1) | copy-start | bytes 2162692
  26.7 45.8 %copy-start.4 = (bf16[1408,256]{1,0:T(8,128)(2,1)S(1)}, bf16[1408,256]{1,0:T(8,128)(2,1)}, u32[]{:S(2)}) copy-start(bf16[1408,256]{1,0:T(8,128)(2,1)} %weight.5) | copy-start | bytes 2162692
  28.5 3.3 %collective-permute-start.12 = (f32[136,128]{1,0:T(8,128)S(1)}, f32[136,128]{1,0:T(8,128)S(1)}, u32[]{:S(2)}, u32[]{:S(2)}) collective-permute-start(f32[136,128]{1,0:T(8,128)S(1)} %shard_map.120.own), channel_id=1, source_target_pairs={{0,8},{8,0},{16,24},{24,16},{1,9},{9,1},{17,25},{25,17},{2,10},{10... | collective-permute-start | bytes 208904 | tf_op jit(solution)/shard_map/ppermute | solution.py:31
  28.9 4.4 %collective-permute-start.11 = (f32[136,128]{1,0:T(8,128)S(1)}, f32[136,128]{1,0:T(8,128)S(1)}, u32[]{:S(2)}, u32[]{:S(2)}) collective-permute-start(f32[136,128]{1,0:T(8,128)S(1)} %shard_map.120.own), channel_id=1, source_target_pairs={{0,24},{8,16},{16,8},{24,0},{1,25},{9,17},{17,9},{25,1},{2,26},{10... | collective-permute-start | bytes 208904 | tf_op jit(solution)/shard_map/ppermute | solution.py:31
  29.7 4.7 %collective-permute-start.10 = (f32[136,128]{1,0:T(8,128)S(1)}, f32[136,128]{1,0:T(8,128)S(1)}, u32[]{:S(2)}, u32[]{:S(2)}) collective-permute-start(f32[136,128]{1,0:T(8,128)S(1)} %shard_map.120.own), channel_id=1, source_target_pairs={{0,16},{8,24},{16,0},{24,8},{1,17},{9,25},{17,1},{25,9},{2,18},{10... | collective-permute-start | bytes 208904 | tf_op jit(solution)/shard_map/ppermute | solution.py:31
  34.6 3.3 %collective-permute-start.15 = (f32[136,128]{1,0:T(8,128)S(1)}, f32[136,128]{1,0:T(8,128)S(1)}, u32[]{:S(2)}, u32[]{:S(2)}) collective-permute-start(f32[136,128]{1,0:T(8,128)S(1)} %shard_map.121.own), channel_id=1, source_target_pairs={{0,32},{32,0},{64,96},{96,64},{1,33},{33,1},{65,97},{97,65},{2,34}... | collective-permute-start | bytes 208904 | tf_op jit(solution)/shard_map/ppermute | solution.py:31
  35.4 4.7 %collective-permute-start.14 = (f32[136,128]{1,0:T(8,128)S(1)}, f32[136,128]{1,0:T(8,128)S(1)}, u32[]{:S(2)}, u32[]{:S(2)}) collective-permute-start(f32[136,128]{1,0:T(8,128)S(1)} %shard_map.121.own), channel_id=1, source_target_pairs={{0,96},{32,64},{64,32},{96,0},{1,97},{33,65},{65,33},{97,1},{2,98}... | collective-permute-start | bytes 208904 | tf_op jit(solution)/shard_map/ppermute | solution.py:31
  36.1 4.7 %collective-permute-start.13 = (f32[136,128]{1,0:T(8,128)S(1)}, f32[136,128]{1,0:T(8,128)S(1)}, u32[]{:S(2)}, u32[]{:S(2)}) collective-permute-start(f32[136,128]{1,0:T(8,128)S(1)} %shard_map.121.own), channel_id=1, source_target_pairs={{0,64},{32,96},{64,0},{96,32},{1,65},{33,97},{65,1},{97,33},{2,66}... | collective-permute-start | bytes 208904 | tf_op jit(solution)/shard_map/ppermute | solution.py:31
  41.2 3.3 %collective-permute-start.18 = (bf16[16,256]{1,0:T(8,128)(2,1)S(1)}, bf16[16,256]{1,0:T(8,128)(2,1)S(1)}, u32[]{:S(2)}, u32[]{:S(2)}) collective-permute-start(bf16[16,256]{1,0:T(8,128)(2,1)S(1)} %shard_map.122), channel_id=1, source_target_pairs={{0,2},{2,0},{4,6},{6,4},{1,3},{3,1},{5,7},{7,5},{8,10},{10,8},{12,... | collective-permute-start | bytes 24584 | tf_op jit(solution)/shard_map/ppermute | solution.py:31
  41.6 3.7 %collective-permute-start.17 = (bf16[16,256]{1,0:T(8,128)(2,1)S(1)}, bf16[16,256]{1,0:T(8,128)(2,1)S(1)}, u32[]{:S(2)}, u32[]{:S(2)}) collective-permute-start(bf16[16,256]{1,0:T(8,128)(2,1)S(1)} %shard_map.122), channel_id=1, source_target_pairs={{0,6},{2,4},{4,2},{6,0},{1,7},{3,5},{5,3},{7,1},{8,14},{10,12},{12... | collective-permute-start | bytes 24584 | tf_op jit(solution)/shard_map/ppermute | solution.py:31
  42.2 4.0 %collective-permute-start.16 = (bf16[16,256]{1,0:T(8,128)(2,1)S(1)}, bf16[16,256]{1,0:T(8,128)(2,1)S(1)}, u32[]{:S(2)}, u32[]{:S(2)}) collective-permute-start(bf16[16,256]{1,0:T(8,128)(2,1)S(1)} %shard_map.122), channel_id=1, source_target_pairs={{0,4},{2,6},{4,0},{6,2},{1,5},{3,7},{5,1},{7,3},{8,12},{10,14},{12... | collective-permute-start | bytes 24584 | tf_op jit(solution)/shard_map/ppermute | solution.py:31
  46.2 10.2 %collective-permute-start.19 = (f32[16,256]{1,0:T(8,128)S(1)}, f32[16,256]{1,0:T(8,128)S(1)}, u32[]{:S(2)}, u32[]{:S(2)}) collective-permute-start(f32[16,256]{1,0:T(8,128)S(1)} %convert_add_fusion.1.attn), channel_id=1, source_target_pairs={{0,1},{1,0},{2,3},{3,2},{4,5},{5,4},{6,7},{7,6},{8,9},{9,8},{10,11... | collective-permute-start | bytes 49160 | tf_op jit(solution)/shard_map/ppermute | solution.py:36
  56.7 4.0 %collective-permute-start.22 = (bf16[16,2944]{1,0:T(8,128)(2,1)S(1)}, bf16[16,2944]{1,0:T(8,128)(2,1)S(1)}, u32[]{:S(2)}, u32[]{:S(2)}) collective-permute-start(bf16[16,2944]{1,0:T(8,128)(2,1)S(1)} %get-tuple-element.16), channel_id=1, source_target_pairs={{0,8},{8,0},{16,24},{24,16},{1,9},{9,1},{17,25},{25,17},{2,10},{10... | collective-permute-start | bytes 282632 | tf_op jit(solution)/shard_map/ppermute | solution.py:31
  57.7 4.6 %collective-permute-start.21 = (bf16[16,2944]{1,0:T(8,128)(2,1)S(1)}, bf16[16,2944]{1,0:T(8,128)(2,1)S(1)}, u32[]{:S(2)}, u32[]{:S(2)}) collective-permute-start(bf16[16,2944]{1,0:T(8,128)(2,1)S(1)} %get-tuple-element.16), channel_id=1, source_target_pairs={{0,24},{8,16},{16,8},{24,0},{1,25},{9,17},{17,9},{25,1},{2,26},{10... | collective-permute-start | bytes 282632 | tf_op jit(solution)/shard_map/ppermute | solution.py:31
  59.6 4.9 %collective-permute-start.20 = (bf16[16,2944]{1,0:T(8,128)(2,1)S(1)}, bf16[16,2944]{1,0:T(8,128)(2,1)S(1)}, u32[]{:S(2)}, u32[]{:S(2)}) collective-permute-start(bf16[16,2944]{1,0:T(8,128)(2,1)S(1)} %get-tuple-element.16), channel_id=1, source_target_pairs={{0,16},{8,24},{16,0},{24,8},{1,17},{9,25},{17,1},{25,9},{2,18},{10... | collective-permute-start | bytes 282632 | tf_op jit(solution)/shard_map/ppermute | solution.py:31
  64.7 3.6 %collective-permute-start.25 = (bf16[16,2944]{1,0:T(8,128)(2,1)S(1)}, bf16[16,2944]{1,0:T(8,128)(2,1)S(1)}, u32[]{:S(2)}, u32[]{:S(2)}) collective-permute-start(bf16[16,2944]{1,0:T(8,128)(2,1)S(1)} %get-tuple-element.18), channel_id=1, source_target_pairs={{0,32},{32,0},{64,96},{96,64},{1,33},{33,1},{65,97},{97,65},{2,34}... | collective-permute-start | bytes 282632 | tf_op jit(solution)/shard_map/ppermute | solution.py:31
  64.9 4.6 %collective-permute-start.24 = (bf16[16,2944]{1,0:T(8,128)(2,1)S(1)}, bf16[16,2944]{1,0:T(8,128)(2,1)S(1)}, u32[]{:S(2)}, u32[]{:S(2)}) collective-permute-start(bf16[16,2944]{1,0:T(8,128)(2,1)S(1)} %get-tuple-element.18), channel_id=1, source_target_pairs={{0,96},{32,64},{64,32},{96,0},{1,97},{33,65},{65,33},{97,1},{2,98}... | collective-permute-start | bytes 282632 | tf_op jit(solution)/shard_map/ppermute | solution.py:31
  67.2 5.3 %collective-permute-start.23 = (bf16[16,2944]{1,0:T(8,128)(2,1)S(1)}, bf16[16,2944]{1,0:T(8,128)(2,1)S(1)}, u32[]{:S(2)}, u32[]{:S(2)}) collective-permute-start(bf16[16,2944]{1,0:T(8,128)(2,1)S(1)} %get-tuple-element.18), channel_id=1, source_target_pairs={{0,64},{32,96},{64,0},{96,32},{1,65},{33,97},{65,1},{97,33},{2,66}... | collective-permute-start | bytes 282632 | tf_op jit(solution)/shard_map/ppermute | solution.py:31
  72.9 3.6 %collective-permute-start.28 = (bf16[16,256]{1,0:T(8,128)(2,1)S(1)}, bf16[16,256]{1,0:T(8,128)(2,1)S(1)}, u32[]{:S(2)}, u32[]{:S(2)}) collective-permute-start(bf16[16,256]{1,0:T(8,128)(2,1)S(1)} %shard_map.125), channel_id=1, source_target_pairs={{0,2},{2,0},{4,6},{6,4},{1,3},{3,1},{5,7},{7,5},{8,10},{10,8},{12,... | collective-permute-start | bytes 24584 | tf_op jit(solution)/shard_map/ppermute | solution.py:31
  74.0 3.7 %collective-permute-start.27 = (bf16[16,256]{1,0:T(8,128)(2,1)S(1)}, bf16[16,256]{1,0:T(8,128)(2,1)S(1)}, u32[]{:S(2)}, u32[]{:S(2)}) collective-permute-start(bf16[16,256]{1,0:T(8,128)(2,1)S(1)} %shard_map.125), channel_id=1, source_target_pairs={{0,6},{2,4},{4,2},{6,0},{1,7},{3,5},{5,3},{7,1},{8,14},{10,12},{12... | collective-permute-start | bytes 24584 | tf_op jit(solution)/shard_map/ppermute | solution.py:31
  75.8 4.0 %collective-permute-start.26 = (bf16[16,256]{1,0:T(8,128)(2,1)S(1)}, bf16[16,256]{1,0:T(8,128)(2,1)S(1)}, u32[]{:S(2)}, u32[]{:S(2)}) collective-permute-start(bf16[16,256]{1,0:T(8,128)(2,1)S(1)} %shard_map.125), channel_id=1, source_target_pairs={{0,4},{2,6},{4,0},{6,2},{1,5},{3,7},{5,1},{7,3},{8,12},{10,14},{12... | collective-permute-start | bytes 24584 | tf_op jit(solution)/shard_map/ppermute | solution.py:31
  79.8 6.0 %collective-permute-start.29 = (f32[16,256]{1,0:T(8,128)S(1)}, f32[16,256]{1,0:T(8,128)S(1)}, u32[]{:S(2)}, u32[]{:S(2)}) collective-permute-start(f32[16,256]{1,0:T(8,128)S(1)} %convert_add_fusion), channel_id=1, source_target_pairs={{0,1},{1,0},{2,3},{3,2},{4,5},{5,4},{6,7},{7,6},{8,9},{9,8},{10,11... | collective-permute-start | bytes 49160 | tf_op jit(solution)/shard_map/ppermute | solution.py:36

commit v6 on v5

--- a/solution.py
+++ b/solution.py
@@ -22,13 +22,16 @@
 COST = 2**40
 
 SHIFTS = (2, 3, 1)
-
-
-def peers(shard, axis):
-    n = lax.axis_size(axis)
+STRAIGHT = ("gates", "heads")
+
+
+def peers(shard, axis, what):
+    across, wide = (axis, 1) if what in STRAIGHT else ((axis, TP[1]), 2)
+    n = lax.axis_size(across)
     got = []
     for s in SHIFTS:
-        got.append(lax.ppermute(shard, axis, [(i, i ^ s) for i in range(n)]))
+        pairs = [(i, i ^ (wide * s + wide - 1)) for i in range(n)]
+        got.append(lax.ppermute(shard, across, pairs))
     return got
 
 
@@ -277,8 +280,8 @@
         smem=1,
         n_in=7,
         cost=COST,
-    )(chip[None], pair, *peers(pair, "tp_0"), attn_gain[None], query_weight)
-    packed = added(packed, peers(packed, "kv_1"))
+    )(chip[None], pair, *peers(pair, "tp_0", "rows"), attn_gain[None], query_weight)
+    packed = added(partner(packed), peers(packed, "kv_1", "query"))
     state = kernel_call(
         attend_body,
         [shape(((batch + 1) * 2 * heads, LANES), F32)],
@@ -289,22 +292,28 @@
         ],
         n_in=6,
     )(
-        packed,
-        *peers(packed, "kv_0"),
+        partner(packed),
+        *peers(packed, "kv_0", "query"),
         key_cache.reshape(batch, positions, LANES),
         value_cache.reshape(batch, positions, LANES),
     )[0]
     state = kernel_call(merge_body, [shape(state.shape, F32)], n_in=4)(
-        state, *peers(state, "kv_1")
+        state, *peers(state, "kv_1", "heads")
     )[0]
     projected = kernel_call(
         project_body,
         [shape((batch, wide), BF16)],
         [pltpu.VMEM((2 * heads * batch, LANES), F32)],
         n_in=7,
-    )(lambdas[None], state, *peers(state, "kv_0"), head_gain[None], out_weight)[0]
+    )(
+        lambdas[None],
+        state,
+        *peers(state, "kv_0", "heads"),
+        head_gain[None],
+        out_weight,
+    )[0]
     attn = added(
-        projected.astype(F32), [p.astype(F32) for p in peers(projected, "tp_0")]
+        projected.astype(F32), [p.astype(F32) for p in peers(projected, "tp_0", "attn")]
     )
     width = gate_weight.shape[1]
     both_shape = (batch, 2 * width + LANES)
@@ -315,11 +324,11 @@
     )(attn, partner(attn), block, gate_weight, up_weight)
     both, sent = kernel_call(
         middle_body, [shape(both_shape, F32), shape(both_shape, BF16)], n_in=4
-    )(both, *peers(sent, "kv_1"))
+    )(both, *peers(sent, "kv_1", "gates"))
     down = kernel_call(down_body, [shape((batch, wide), BF16)], n_in=5)(
-        both, *peers(sent, "kv_0"), down_weight
+        both, *peers(sent, "kv_0", "gates"), down_weight
     )[0]
-    mix = added(down.astype(F32), [p.astype(F32) for p in peers(down, "tp_0")])
+    mix = added(down.astype(F32), [p.astype(F32) for p in peers(down, "tp_0", "mix")])
     mixed = after + (mix + partner(mix))
     return lax.dynamic_slice_in_dim(mixed, (chip * 2 + core) * cols, cols, 1).astype(BF16)
 

time: 86.5 us -> 82.5 us (0.954)
  starting transfers between devices: 49.4 us -> 43.6 us
  waiting for transfers between devices: 32 us -> 33.7 us
    ppermute x3 -> x5, starting transfers between devices: 16 us -> 3.39 us  [partner(): return lax.ppermute(shard, TP[1], [(0, 1), (1, 0)])]
    ppermute x27, starting transfers between devices: 33.4 us -> 40.2 us  [peers(): got.append(lax.ppermute(shard, across, pairs))]
    ppermute x27, waiting for transfers between devices: 29.5 us -> 31.1 us  [peers(): got.append(lax.ppermute(shard, across, pairs))]
    ppermute x3 -> x5, waiting for transfers between devices: 2.5 us -> 2.61 us  [partner(): return lax.ppermute(shard, TP[1], [(0, 1), (1, 0)])]
  transfers between devices with their start and end apart: 30 -> 32, of which waited for: 22 -> 22; matrix products, arithmetic and copies ran while one was open for 0% -> 0% of each run, Pallas kernels for 0% -> 0%
where the time goes in v6:
time: 82.5 us; the launch traced here: 82.4 us
  starting transfers between devices  43.6 us (53%)
  waiting for transfers between devices  33.7 us (41%)
  Pallas kernels  4.17 us (5%)
    ppermute x27, starting transfers between devices, peers(): got.append(lax.ppermute(shard, across, pairs))  40.2 us
    ppermute x27, waiting for transfers between devices, peers(): got.append(lax.ppermute(shard, across, pairs))  31.1 us
    ppermute x5, starting transfers between devices, partner(): return lax.ppermute(shard, TP[1], [(0, 1), (1, 0)])  3.39 us
    ppermute x5, waiting for transfers between devices, partner(): return lax.ppermute(shard, TP[1], [(0, 1), (1, 0)])  2.61 us
    pallas_call x1, Pallas kernels, per_device(): kernel_call(attend_body, [shape(((batch + 1) * 2 * heads, LANES), F32)],...  1.77 us
  transfers between devices with their start and end apart: 32, of which 22 were waited for; matrix products, arithmetic and copies ran while one was open for 0% of the time, Pallas kernels for 0%

profile of v6, /device:TPU:1, one launch (start us, length us, event | category | flops | bytes accessed | tf_op | source)
XLA Modules:
  0.0 82.4 jit_solution(15236803139509853508)
XLA Ops:
  0.0 0.8 shard_map.118
  0.8 1.5 %collective-permute-start = (f32[24,128]{1,0:T(8,128)S(1)}, f32[24,128]{1,0:T(8,128)S(1)}, u32[]{:S(2)}, u32[]{:S(2)}) collective-permute-start(f32[24,128]{1,0:T(8,128)S(1)} %shard_map.118), channel_id=1, source_target_pairs={{0,1},{1,0},{2,3},{3,2},{4,5},{5,4},{6,7},{7,6},{8,9},{9,8},{10,11... | collective-permute-start | bytes 36872 | tf_op jit(solution)/shard_map/ppermute | solution.py:39
  2.3 0.8 collective-permute-done
  3.1 1.6 %collective-permute-start.3 = (f32[24,128]{1,0:T(8,128)S(1)}, f32[24,128]{1,0:T(8,128)S(1)}, u32[]{:S(2)}, u32[]{:S(2)}) collective-permute-start(f32[24,128]{1,0:T(8,128)S(1)} %fusion.2.own), channel_id=1, source_target_pairs={{0,3},{1,2},{2,1},{3,0},{4,7},{5,6},{6,5},{7,4},{8,11},{9,10},{10,... | collective-permute-start | bytes 36872 | tf_op jit(solution)/shard_map/ppermute | solution.py:34
  4.8 1.9 %collective-permute-start.2 = (f32[24,128]{1,0:T(8,128)S(1)}, f32[24,128]{1,0:T(8,128)S(1)}, u32[]{:S(2)}, u32[]{:S(2)}) collective-permute-start(f32[24,128]{1,0:T(8,128)S(1)} %fusion.2.own), channel_id=1, source_target_pairs={{0,7},{1,6},{2,5},{3,4},{4,3},{5,2},{6,1},{7,0},{8,15},{9,14},{10,... | collective-permute-start | bytes 36872 | tf_op jit(solution)/shard_map/ppermute | solution.py:34
  6.6 0.6 collective-permute-start.1
  7.3 1.8 %collective-permute-done.2.b = f32[24,128]{1,0:T(8,128)S(1)} collective-permute-done((f32[24,128]{1,0:T(8,128)S(1)}, f32[24,128]{1,0:T(8,128)S(1)}, u32[]{:S(2)}, u32[]{:S(2)}) %collective-permute-start.2) | collective-permute-done | bytes 12320 | tf_op jit(solution)/shard_map/ppermute | solution.py:34
  9.1 2.2 %collective-permute-done.1.a = f32[24,128]{1,0:T(8,128)S(1)} collective-permute-done((f32[24,128]{1,0:T(8,128)S(1)}, f32[24,128]{1,0:T(8,128)S(1)}, u32[]{:S(2)}, u32[]{:S(2)}) %collective-permute-start.1) | collective-permute-done | bytes 12320 | tf_op jit(solution)/shard_map/ppermute | solution.py:34
  11.3 0.2 shard_map.119
  11.4 1.5 %collective-permute-start.7 = (f32[16,640]{1,0:T(8,128)S(1)}, f32[16,640]{1,0:T(8,128)S(1)}, u32[]{:S(2)}, u32[]{:S(2)}) collective-permute-start(f32[16,640]{1,0:T(8,128)S(1)} %get-tuple-element.12), channel_id=1, source_target_pairs={{0,9},{1,8},{8,1},{9,0},{16,25},{17,24},{24,17},{25,16},{2,11},{3,... | collective-permute-start | bytes 122888 | tf_op jit(solution)/shard_map/ppermute | solution.py:34
  13.0 2.0 %collective-permute-start.6 = (f32[16,640]{1,0:T(8,128)S(1)}, f32[16,640]{1,0:T(8,128)S(1)}, u32[]{:S(2)}, u32[]{:S(2)}) collective-permute-start(f32[16,640]{1,0:T(8,128)S(1)} %get-tuple-element.12), channel_id=1, source_target_pairs={{0,25},{1,24},{8,17},{9,16},{16,9},{17,8},{24,1},{25,0},{2,27},{3,... | collective-permute-start | bytes 122888 | tf_op jit(solution)/shard_map/ppermute | solution.py:34
  14.9 0.7 collective-permute-start.5
  15.6 0.3 collective-permute-start.4
  16.0 1.6 %collective-permute-done.6 = f32[16,640]{1,0:T(8,128)S(1)} collective-permute-done((f32[16,640]{1,0:T(8,128)S(1)}, f32[16,640]{1,0:T(8,128)S(1)}, u32[]{:S(2)}, u32[]{:S(2)}) %collective-permute-start.6) | collective-permute-done | bytes 40992 | tf_op jit(solution)/shard_map/ppermute | solution.py:34
  17.6 2.3 %collective-permute-done.5 = f32[16,640]{1,0:T(8,128)S(1)} collective-permute-done((f32[16,640]{1,0:T(8,128)S(1)}, f32[16,640]{1,0:T(8,128)S(1)}, u32[]{:S(2)}, u32[]{:S(2)}) %collective-permute-start.5) | collective-permute-done | bytes 40992 | tf_op jit(solution)/shard_map/ppermute | solution.py:34
  20.0 1.9 %collective-permute-start.11 = (f32[16,640]{1,0:T(8,128)S(1)}, f32[16,640]{1,0:T(8,128)S(1)}, u32[]{:S(2)}, u32[]{:S(2)}) collective-permute-start(f32[16,640]{1,0:T(8,128)S(1)} %add_add_fusion), channel_id=1, source_target_pairs={{0,33},{1,32},{32,1},{33,0},{64,97},{65,96},{96,65},{97,64},{2,35}... | collective-permute-start | bytes 122888 | tf_op jit(solution)/shard_map/ppermute | solution.py:34
  21.9 2.3 %collective-permute-start.10 = (f32[16,640]{1,0:T(8,128)S(1)}, f32[16,640]{1,0:T(8,128)S(1)}, u32[]{:S(2)}, u32[]{:S(2)}) collective-permute-start(f32[16,640]{1,0:T(8,128)S(1)} %add_add_fusion), channel_id=1, source_target_pairs={{0,97},{1,96},{32,65},{33,64},{64,33},{65,32},{96,1},{97,0},{2,99}... | collective-permute-start | bytes 122888 | tf_op jit(solution)/shard_map/ppermute | solution.py:34
  24.2 1.1 %collective-permute-start.9 = (f32[16,640]{1,0:T(8,128)S(1)}, f32[16,640]{1,0:T(8,128)S(1)}, u32[]{:S(2)}, u32[]{:S(2)}) collective-permute-start(f32[16,640]{1,0:T(8,128)S(1)} %add_add_fusion), channel_id=1, source_target_pairs={{0,65},{1,64},{32,97},{33,96},{64,1},{65,0},{96,33},{97,32},{2,67}... | collective-permute-start | bytes 122888 | tf_op jit(solution)/shard_map/ppermute | solution.py:34
  25.3 0.3 collective-permute-start.8
  25.6 0.9 %collective-permute-done.10.b = f32[16,640]{1,0:T(8,128)S(1)} collective-permute-done((f32[16,640]{1,0:T(8,128)S(1)}, f32[16,640]{1,0:T(8,128)S(1)}, u32[]{:S(2)}, u32[]{:S(2)}) %collective-permute-start.10) | collective-permute-done | bytes 40992 | tf_op jit(solution)/shard_map/ppermute | solution.py:34
  26.5 2.7 %collective-permute-done.9.a = f32[16,640]{1,0:T(8,128)S(1)} collective-permute-done((f32[16,640]{1,0:T(8,128)S(1)}, f32[16,640]{1,0:T(8,128)S(1)}, u32[]{:S(2)}, u32[]{:S(2)}) %collective-permute-start.9) | collective-permute-done | bytes 40992 | tf_op jit(solution)/shard_map/ppermute | solution.py:34
  29.2 0.0 copy-start.5
  29.3 1.8 %shard_map.120.own = f32[136,128]{1,0:T(8,128)S(1)} custom-call(f32[16,640]{1,0:T(8,128)S(1)} %collective-permute-done.8.own, f32[16,640]{1,0:T(8,128)S(1)} %collective-permute-done.9.a, f32[16,640]{1,0:T(8,128)S(1)} %collective-permute-done.10.b, f32[16,640]{1,0:T(8,128)S(1)} %collective-permute-done.11.c, bf16[16,1024,128]{2,1,0:T(8,128)(2,1)S(1)} %bitcast.7, ...), custom_call_target="tpu_custom_call" | custom-call | tf_op jit(solution)/shard_map/pallas_call | solution.py:285
  31.1 0.5 collective-permute-start.14
  31.6 0.5 collective-permute-start.13
  32.0 2.4 %collective-permute-start.12 = (f32[136,128]{1,0:T(8,128)S(1)}, f32[136,128]{1,0:T(8,128)S(1)}, u32[]{:S(2)}, u32[]{:S(2)}) collective-permute-start(f32[136,128]{1,0:T(8,128)S(1)} %shard_map.120.own), channel_id=1, source_target_pairs={{0,16},{8,24},{16,0},{24,8},{1,17},{9,25},{17,1},{25,9},{2,18},{10... | collective-permute-start | bytes 208904 | tf_op jit(solution)/shard_map/ppermute | solution.py:34
  34.4 1.5 %collective-permute-done.13.b = f32[136,128]{1,0:T(8,128)S(1)} collective-permute-done((f32[136,128]{1,0:T(8,128)S(1)}, f32[136,128]{1,0:T(8,128)S(1)}, u32[]{:S(2)}, u32[]{:S(2)}) %collective-permute-start.13) | collective-permute-done | bytes 69664 | tf_op jit(solution)/shard_map/ppermute | solution.py:34
  35.9 0.8 collective-permute-done.12.a
  36.7 0.2 shard_map.121.own
  36.9 0.8 collective-permute-start.17
  37.7 0.5 collective-permute-start.16
  38.2 2.0 %collective-permute-start.15 = (f32[136,128]{1,0:T(8,128)S(1)}, f32[136,128]{1,0:T(8,128)S(1)}, u32[]{:S(2)}, u32[]{:S(2)}) collective-permute-start(f32[136,128]{1,0:T(8,128)S(1)} %shard_map.121.own), channel_id=1, source_target_pairs={{0,64},{32,96},{64,0},{96,32},{1,65},{33,97},{65,1},{97,33},{2,66}... | collective-permute-start | bytes 208904 | tf_op jit(solution)/shard_map/ppermute | solution.py:34
  40.2 1.9 %collective-permute-done.16.b = f32[136,128]{1,0:T(8,128)S(1)} collective-permute-done((f32[136,128]{1,0:T(8,128)S(1)}, f32[136,128]{1,0:T(8,128)S(1)}, u32[]{:S(2)}, u32[]{:S(2)}) %collective-permute-start.16) | collective-permute-done | bytes 69664 | tf_op jit(solution)/shard_map/ppermute | solution.py:34
  42.1 1.5 %collective-permute-done.15.a = f32[136,128]{1,0:T(8,128)S(1)} collective-permute-done((f32[136,128]{1,0:T(8,128)S(1)}, f32[136,128]{1,0:T(8,128)S(1)}, u32[]{:S(2)}, u32[]{:S(2)}) %collective-permute-start.15) | collective-permute-done | bytes 69664 | tf_op jit(solution)/shard_map/ppermute | solution.py:34
  43.6 0.4 shard_map.122
  44.0 3.3 %collective-permute-start.20 = (bf16[16,256]{1,0:T(8,128)(2,1)S(1)}, bf16[16,256]{1,0:T(8,128)(2,1)S(1)}, u32[]{:S(2)}, u32[]{:S(2)}) collective-permute-start(bf16[16,256]{1,0:T(8,128)(2,1)S(1)} %shard_map.122), channel_id=1, source_target_pairs={{0,3},{1,2},{2,1},{3,0},{4,7},{5,6},{6,5},{7,4},{8,11},{9,10},{10,... | collective-permute-start | bytes 24584 | tf_op jit(solution)/shard_map/ppermute | solution.py:34
  47.4 0.6 collective-permute-start.19
  48.0 2.6 %collective-permute-start.18 = (bf16[16,256]{1,0:T(8,128)(2,1)S(1)}, bf16[16,256]{1,0:T(8,128)(2,1)S(1)}, u32[]{:S(2)}, u32[]{:S(2)}) collective-permute-start(bf16[16,256]{1,0:T(8,128)(2,1)S(1)} %shard_map.122), channel_id=1, source_target_pairs={{0,5},{1,4},{2,7},{3,6},{4,1},{5,0},{6,3},{7,2},{8,13},{9,12},{10,... | collective-permute-start | bytes 24584 | tf_op jit(solution)/shard_map/ppermute | solution.py:34
  50.6 1.1 %collective-permute-done.19 = bf16[16,256]{1,0:T(8,128)(2,1)S(1)} collective-permute-done((bf16[16,256]{1,0:T(8,128)(2,1)S(1)}, bf16[16,256]{1,0:T(8,128)(2,1)S(1)}, u32[]{:S(2)}, u32[]{:S(2)}) %collective-permute-start.19) | collective-permute-done | bytes 8224 | tf_op jit(solution)/shard_map/ppermute | solution.py:34
  51.7 0.9 %collective-permute-done.18 = bf16[16,256]{1,0:T(8,128)(2,1)S(1)} collective-permute-done((bf16[16,256]{1,0:T(8,128)(2,1)S(1)}, bf16[16,256]{1,0:T(8,128)(2,1)S(1)}, u32[]{:S(2)}, u32[]{:S(2)}) %collective-permute-start.18) | collective-permute-done | bytes 8224 | tf_op jit(solution)/shard_map/ppermute | solution.py:34
  52.6 0.3 collective-permute-start.21
  52.9 0.9 %collective-permute-done.21.other = f32[16,256]{1,0:T(8,128)S(1)} collective-permute-done((f32[16,256]{1,0:T(8,128)S(1)}, f32[16,256]{1,0:T(8,128)S(1)}, u32[]{:S(2)}, u32[]{:S(2)}) %collective-permute-start.21) | collective-permute-done | bytes 16416 | tf_op jit(solution)/shard_map/ppermute | solution.py:39
  53.8 0.3 shard_map.123
  54.1 0.5 collective-permute-start.24
  54.7 1.9 %collective-permute-start.23 = (bf16[16,2944]{1,0:T(8,128)(2,1)S(1)}, bf16[16,2944]{1,0:T(8,128)(2,1)S(1)}, u32[]{:S(2)}, u32[]{:S(2)}) collective-permute-start(bf16[16,2944]{1,0:T(8,128)(2,1)S(1)} %get-tuple-element.16), channel_id=1, source_target_pairs={{0,24},{8,16},{16,8},{24,0},{1,25},{9,17},{17,9},{25,1},{2,26},{10... | collective-permute-start | bytes 282632 | tf_op jit(solution)/shard_map/ppermute | solution.py:34
  56.6 0.9 %collective-permute-start.22 = (bf16[16,2944]{1,0:T(8,128)(2,1)S(1)}, bf16[16,2944]{1,0:T(8,128)(2,1)S(1)}, u32[]{:S(2)}, u32[]{:S(2)}) collective-permute-start(bf16[16,2944]{1,0:T(8,128)(2,1)S(1)} %get-tuple-element.16), channel_id=1, source_target_pairs={{0,16},{8,24},{16,0},{24,8},{1,17},{9,25},{17,1},{25,9},{2,18},{10... | collective-permute-start | bytes 282632 | tf_op jit(solution)/shard_map/ppermute | solution.py:34
  57.5 0.8 collective-permute-done.24.c
  58.2 1.1 %collective-permute-done.23.b = bf16[16,2944]{1,0:T(8,128)(2,1)S(1)} collective-permute-done((bf16[16,2944]{1,0:T(8,128)(2,1)S(1)}, bf16[16,2944]{1,0:T(8,128)(2,1)S(1)}, u32[]{:S(2)}, u32[]{:S(2)}) %collective-permute-start.23) | collective-permute-done | bytes 94240 | tf_op jit(solution)/shard_map/ppermute | solution.py:34
  59.3 2.2 %collective-permute-done.22.a = bf16[16,2944]{1,0:T(8,128)(2,1)S(1)} collective-permute-done((bf16[16,2944]{1,0:T(8,128)(2,1)S(1)}, bf16[16,2944]{1,0:T(8,128)(2,1)S(1)}, u32[]{:S(2)}, u32[]{:S(2)}) %collective-permute-start.22) | collective-permute-done | bytes 94240 | tf_op jit(solution)/shard_map/ppermute | solution.py:34
  61.5 0.2 shard_map.124
  61.7 0.3 collective-permute-start.27
  62.0 2.2 %collective-permute-start.26 = (bf16[16,2944]{1,0:T(8,128)(2,1)S(1)}, bf16[16,2944]{1,0:T(8,128)(2,1)S(1)}, u32[]{:S(2)}, u32[]{:S(2)}) collective-permute-start(bf16[16,2944]{1,0:T(8,128)(2,1)S(1)} %get-tuple-element.18), channel_id=1, source_target_pairs={{0,96},{32,64},{64,32},{96,0},{1,97},{33,65},{65,33},{97,1},{2,98}... | collective-permute-start | bytes 282632 | tf_op jit(solution)/shard_map/ppermute | solution.py:34
  64.2 1.1 %collective-permute-start.25 = (bf16[16,2944]{1,0:T(8,128)(2,1)S(1)}, bf16[16,2944]{1,0:T(8,128)(2,1)S(1)}, u32[]{:S(2)}, u32[]{:S(2)}) collective-permute-start(bf16[16,2944]{1,0:T(8,128)(2,1)S(1)} %get-tuple-element.18), channel_id=1, source_target_pairs={{0,64},{32,96},{64,0},{96,32},{1,65},{33,97},{65,1},{97,33},{2,66}... | collective-permute-start | bytes 282632 | tf_op jit(solution)/shard_map/ppermute | solution.py:34
  65.3 1.3 %collective-permute-done.26.b = bf16[16,2944]{1,0:T(8,128)(2,1)S(1)} collective-permute-done((bf16[16,2944]{1,0:T(8,128)(2,1)S(1)}, bf16[16,2944]{1,0:T(8,128)(2,1)S(1)}, u32[]{:S(2)}, u32[]{:S(2)}) %collective-permute-start.26) | collective-permute-done | bytes 94240 | tf_op jit(solution)/shard_map/ppermute | solution.py:34
  66.6 3.1 %collective-permute-done.25.a = bf16[16,2944]{1,0:T(8,128)(2,1)S(1)} collective-permute-done((bf16[16,2944]{1,0:T(8,128)(2,1)S(1)}, bf16[16,2944]{1,0:T(8,128)(2,1)S(1)}, u32[]{:S(2)}, u32[]{:S(2)}) %collective-permute-start.25) | collective-permute-done | bytes 94240 | tf_op jit(solution)/shard_map/ppermute | solution.py:34
  69.7 0.3 shard_map.125
  70.1 4.0 %collective-permute-start.30 = (bf16[16,256]{1,0:T(8,128)(2,1)S(1)}, bf16[16,256]{1,0:T(8,128)(2,1)S(1)}, u32[]{:S(2)}, u32[]{:S(2)}) collective-permute-start(bf16[16,256]{1,0:T(8,128)(2,1)S(1)} %shard_map.125), channel_id=1, source_target_pairs={{0,3},{1,2},{2,1},{3,0},{4,7},{5,6},{6,5},{7,4},{8,11},{9,10},{10,... | collective-permute-start | bytes 24584 | tf_op jit(solution)/shard_map/ppermute | solution.py:34
  74.0 1.3 %collective-permute-start.29 = (bf16[16,256]{1,0:T(8,128)(2,1)S(1)}, bf16[16,256]{1,0:T(8,128)(2,1)S(1)}, u32[]{:S(2)}, u32[]{:S(2)}) collective-permute-start(bf16[16,256]{1,0:T(8,128)(2,1)S(1)} %shard_map.125), channel_id=1, source_target_pairs={{0,7},{1,6},{2,5},{3,4},{4,3},{5,2},{6,1},{7,0},{8,15},{9,14},{10,... | collective-permute-start | bytes 24584 | tf_op jit(solution)/shard_map/ppermute | solution.py:34
  75.4 1.2 %collective-permute-start.28 = (bf16[16,256]{1,0:T(8,128)(2,1)S(1)}, bf16[16,256]{1,0:T(8,128)(2,1)S(1)}, u32[]{:S(2)}, u32[]{:S(2)}) collective-permute-start(bf16[16,256]{1,0:T(8,128)(2,1)S(1)} %shard_map.125), channel_id=1, source_target_pairs={{0,5},{1,4},{2,7},{3,6},{4,1},{5,0},{6,3},{7,2},{8,13},{9,12},{10,... | collective-permute-start | bytes 24584 | tf_op jit(solution)/shard_map/ppermute | solution.py:34
  76.5 1.8 %collective-permute-done.29 = bf16[16,256]{1,0:T(8,128)(2,1)S(1)} collective-permute-done((bf16[16,256]{1,0:T(8,128)(2,1)S(1)}, bf16[16,256]{1,0:T(8,128)(2,1)S(1)}, u32[]{:S(2)}, u32[]{:S(2)}) %collective-permute-start.29) | collective-permute-done | bytes 8224 | tf_op jit(solution)/shard_map/ppermute | solution.py:34
  78.3 1.6 %collective-permute-done.28 = bf16[16,256]{1,0:T(8,128)(2,1)S(1)} collective-permute-done((bf16[16,256]{1,0:T(8,128)(2,1)S(1)}, bf16[16,256]{1,0:T(8,128)(2,1)S(1)}, u32[]{:S(2)}, u32[]{:S(2)}) %collective-permute-start.28) | collective-permute-done | bytes 8224 | tf_op jit(solution)/shard_map/ppermute | solution.py:34
  79.9 0.9 %collective-permute-start.31 = (f32[16,256]{1,0:T(8,128)S(1)}, f32[16,256]{1,0:T(8,128)S(1)}, u32[]{:S(2)}, u32[]{:S(2)}) collective-permute-start(f32[16,256]{1,0:T(8,128)S(1)} %convert_add_fusion), channel_id=1, source_target_pairs={{0,1},{1,0},{2,3},{3,2},{4,5},{5,4},{6,7},{7,6},{8,9},{9,8},{10,11... | collective-permute-start | bytes 49160 | tf_op jit(solution)/shard_map/ppermute | solution.py:39
  80.9 0.8 %collective-permute-done.31 = f32[16,256]{1,0:T(8,128)S(1)} collective-permute-done((f32[16,256]{1,0:T(8,128)S(1)}, f32[16,256]{1,0:T(8,128)S(1)}, u32[]{:S(2)}, u32[]{:S(2)}) %collective-permute-start.31) | collective-permute-done | bytes 16416 | tf_op jit(solution)/shard_map/ppermute | solution.py:39
  81.7 0.7 fusion.3
  (35 shorter events, 0.1 us)
Async XLA Ops:
  0.0 11.3 %copy-start.8 = (bf16[256,512]{1,0:T(8,128)(2,1)S(1)}, bf16[256,512]{1,0:T(8,128)(2,1)}, u32[]{:S(2)}) copy-start(bf16[256,512]{1,0:T(8,128)(2,1)} %weight.3) | copy-start | bytes 786436
  0.0 11.3 %copy-start.9 = (f32[256]{0:T(256)S(1)}, f32[256]{0:T(256)}, u32[]{:S(2)}) copy-start(f32[256]{0:T(256)} %param.13) | copy-start | bytes 3076
  0.8 2.3 %collective-permute-start = (f32[24,128]{1,0:T(8,128)S(1)}, f32[24,128]{1,0:T(8,128)S(1)}, u32[]{:S(2)}, u32[]{:S(2)}) collective-permute-start(f32[24,128]{1,0:T(8,128)S(1)} %shard_map.118), channel_id=1, source_target_pairs={{0,1},{1,0},{2,3},{3,2},{4,5},{5,4},{6,7},{7,6},{8,9},{9,8},{10,11... | collective-permute-start | bytes 36872 | tf_op jit(solution)/shard_map/ppermute | solution.py:39
  3.1 4.1 %collective-permute-start.3 = (f32[24,128]{1,0:T(8,128)S(1)}, f32[24,128]{1,0:T(8,128)S(1)}, u32[]{:S(2)}, u32[]{:S(2)}) collective-permute-start(f32[24,128]{1,0:T(8,128)S(1)} %fusion.2.own), channel_id=1, source_target_pairs={{0,3},{1,2},{2,1},{3,0},{4,7},{5,6},{6,5},{7,4},{8,11},{9,10},{10,... | collective-permute-start | bytes 36872 | tf_op jit(solution)/shard_map/ppermute | solution.py:34
  4.8 4.3 %collective-permute-start.2 = (f32[24,128]{1,0:T(8,128)S(1)}, f32[24,128]{1,0:T(8,128)S(1)}, u32[]{:S(2)}, u32[]{:S(2)}) collective-permute-start(f32[24,128]{1,0:T(8,128)S(1)} %fusion.2.own), channel_id=1, source_target_pairs={{0,7},{1,6},{2,5},{3,4},{4,3},{5,2},{6,1},{7,0},{8,15},{9,14},{10,... | collective-permute-start | bytes 36872 | tf_op jit(solution)/shard_map/ppermute | solution.py:34
  6.6 4.6 %collective-permute-start.1 = (f32[24,128]{1,0:T(8,128)S(1)}, f32[24,128]{1,0:T(8,128)S(1)}, u32[]{:S(2)}, u32[]{:S(2)}) collective-permute-start(f32[24,128]{1,0:T(8,128)S(1)} %fusion.2.own), channel_id=1, source_target_pairs={{0,5},{1,4},{2,7},{3,6},{4,1},{5,0},{6,3},{7,2},{8,13},{9,12},{10,... | collective-permute-start | bytes 36872 | tf_op jit(solution)/shard_map/ppermute | solution.py:34
  11.3 18.0 %copy-start = (bf16[16,1024,1,128]{3,1,2,0:T(8,128)(2,1)S(1)}, bf16[16,1024,1,128]{3,1,2,0:T(8,128)(2,1)}, u32[]{:S(2)}) copy-start(bf16[16,1024,1,128]{3,1,2,0:T(8,128)(2,1)} %param.15) | copy-start | bytes 12582916
  11.3 18.0 %copy-start.1 = (bf16[16,1024,1,128]{3,1,2,0:T(8,128)(2,1)S(1)}, bf16[16,1024,1,128]{3,1,2,0:T(8,128)(2,1)}, u32[]{:S(2)}) copy-start(bf16[16,1024,1,128]{3,1,2,0:T(8,128)(2,1)} %param.16) | copy-start | bytes 12582916
  11.4 4.6 %collective-permute-start.7 = (f32[16,640]{1,0:T(8,128)S(1)}, f32[16,640]{1,0:T(8,128)S(1)}, u32[]{:S(2)}, u32[]{:S(2)}) collective-permute-start(f32[16,640]{1,0:T(8,128)S(1)} %get-tuple-element.12), channel_id=1, source_target_pairs={{0,9},{1,8},{8,1},{9,0},{16,25},{17,24},{24,17},{25,16},{2,11},{3,... | collective-permute-start | bytes 122888 | tf_op jit(solution)/shard_map/ppermute | solution.py:34
  13.0 4.6 %collective-permute-start.6 = (f32[16,640]{1,0:T(8,128)S(1)}, f32[16,640]{1,0:T(8,128)S(1)}, u32[]{:S(2)}, u32[]{:S(2)}) collective-permute-start(f32[16,640]{1,0:T(8,128)S(1)} %get-tuple-element.12), channel_id=1, source_target_pairs={{0,25},{1,24},{8,17},{9,16},{16,9},{17,8},{24,1},{25,0},{2,27},{3,... | collective-permute-start | bytes 122888 | tf_op jit(solution)/shard_map/ppermute | solution.py:34
  14.9 5.0 %collective-permute-start.5 = (f32[16,640]{1,0:T(8,128)S(1)}, f32[16,640]{1,0:T(8,128)S(1)}, u32[]{:S(2)}, u32[]{:S(2)}) collective-permute-start(f32[16,640]{1,0:T(8,128)S(1)} %get-tuple-element.12), channel_id=1, source_target_pairs={{0,17},{1,16},{8,25},{9,24},{16,1},{17,0},{24,9},{25,8},{2,19},{3,... | collective-permute-start | bytes 122888 | tf_op jit(solution)/shard_map/ppermute | solution.py:34
  15.6 4.3 %collective-permute-start.4 = (f32[16,640]{1,0:T(8,128)S(1)}, f32[16,640]{1,0:T(8,128)S(1)}, u32[]{:S(2)}, u32[]{:S(2)}) collective-permute-start(f32[16,640]{1,0:T(8,128)S(1)} %get-tuple-element.12), channel_id=1, source_target_pairs={{0,1},{1,0},{2,3},{3,2},{4,5},{5,4},{6,7},{7,6},{8,9},{9,8},{10,11... | collective-permute-start | bytes 122888 | tf_op jit(solution)/shard_map/ppermute | solution.py:39
  20.0 5.7 %collective-permute-start.11 = (f32[16,640]{1,0:T(8,128)S(1)}, f32[16,640]{1,0:T(8,128)S(1)}, u32[]{:S(2)}, u32[]{:S(2)}) collective-permute-start(f32[16,640]{1,0:T(8,128)S(1)} %add_add_fusion), channel_id=1, source_target_pairs={{0,33},{1,32},{32,1},{33,0},{64,97},{65,96},{96,65},{97,64},{2,35}... | collective-permute-start | bytes 122888 | tf_op jit(solution)/shard_map/ppermute | solution.py:34
  21.9 4.6 %collective-permute-start.10 = (f32[16,640]{1,0:T(8,128)S(1)}, f32[16,640]{1,0:T(8,128)S(1)}, u32[]{:S(2)}, u32[]{:S(2)}) collective-permute-start(f32[16,640]{1,0:T(8,128)S(1)} %add_add_fusion), channel_id=1, source_target_pairs={{0,97},{1,96},{32,65},{33,64},{64,33},{65,32},{96,1},{97,0},{2,99}... | collective-permute-start | bytes 122888 | tf_op jit(solution)/shard_map/ppermute | solution.py:34
  24.2 5.0 %collective-permute-start.9 = (f32[16,640]{1,0:T(8,128)S(1)}, f32[16,640]{1,0:T(8,128)S(1)}, u32[]{:S(2)}, u32[]{:S(2)}) collective-permute-start(f32[16,640]{1,0:T(8,128)S(1)} %add_add_fusion), channel_id=1, source_target_pairs={{0,65},{1,64},{32,97},{33,96},{64,1},{65,0},{96,33},{97,32},{2,67}... | collective-permute-start | bytes 122888 | tf_op jit(solution)/shard_map/ppermute | solution.py:34
  25.3 4.0 %collective-permute-start.8 = (f32[16,640]{1,0:T(8,128)S(1)}, f32[16,640]{1,0:T(8,128)S(1)}, u32[]{:S(2)}, u32[]{:S(2)}) collective-permute-start(f32[16,640]{1,0:T(8,128)S(1)} %add_add_fusion), channel_id=1, source_target_pairs={{0,1},{1,0},{2,3},{3,2},{4,5},{5,4},{6,7},{7,6},{8,9},{9,8},{10,11... | collective-permute-start | bytes 122888 | tf_op jit(solution)/shard_map/ppermute | solution.py:39
  29.2 14.4 %copy-start.5 = (bf16[512,256]{1,0:T(8,128)(2,1)S(1)}, bf16[512,256]{1,0:T(8,128)(2,1)}, u32[]{:S(2)}) copy-start(bf16[512,256]{1,0:T(8,128)(2,1)} %weight.4) | copy-start | bytes 786436
  29.3 14.3 %copy-start.6 = (f32[4]{0:T(128)S(1)}, f32[4]{0:T(128)}, u32[]{:S(2)}) copy-start(f32[4]{0:T(128)} %param.17) | copy-start | bytes 52
  29.3 14.3 %copy-start.7 = (f32[128]{0:T(128)S(1)}, f32[128]{0:T(128)}, u32[]{:S(2)}) copy-start(f32[128]{0:T(128)} %param.18) | copy-start | bytes 1540
  29.3 24.6 %copy-start.2 = (bf16[256,1408]{1,0:T(8,128)(2,1)S(1)}, bf16[256,1408]{1,0:T(8,128)(2,1)}, u32[]{:S(2)}) copy-start(bf16[256,1408]{1,0:T(8,128)(2,1)} %gate.1) | copy-start | bytes 2162692
  29.3 24.6 %copy-start.3 = (bf16[256,1408]{1,0:T(8,128)(2,1)S(1)}, bf16[256,1408]{1,0:T(8,128)(2,1)}, u32[]{:S(2)}) copy-start(bf16[256,1408]{1,0:T(8,128)(2,1)} %up.1) | copy-start | bytes 2162692
  29.3 40.4 %copy-start.4 = (bf16[1408,256]{1,0:T(8,128)(2,1)S(1)}, bf16[1408,256]{1,0:T(8,128)(2,1)}, u32[]{:S(2)}) copy-start(bf16[1408,256]{1,0:T(8,128)(2,1)} %weight.5) | copy-start | bytes 2162692
  31.1 3.3 %collective-permute-start.14 = (f32[136,128]{1,0:T(8,128)S(1)}, f32[136,128]{1,0:T(8,128)S(1)}, u32[]{:S(2)}, u32[]{:S(2)}) collective-permute-start(f32[136,128]{1,0:T(8,128)S(1)} %shard_map.120.own), channel_id=1, source_target_pairs={{0,8},{8,0},{16,24},{24,16},{1,9},{9,1},{17,25},{25,17},{2,10},{10... | collective-permute-start | bytes 208904 | tf_op jit(solution)/shard_map/ppermute | solution.py:34
  31.6 4.4 %collective-permute-start.13 = (f32[136,128]{1,0:T(8,128)S(1)}, f32[136,128]{1,0:T(8,128)S(1)}, u32[]{:S(2)}, u32[]{:S(2)}) collective-permute-start(f32[136,128]{1,0:T(8,128)S(1)} %shard_map.120.own), channel_id=1, source_target_pairs={{0,24},{8,16},{16,8},{24,0},{1,25},{9,17},{17,9},{25,1},{2,26},{10... | collective-permute-start | bytes 208904 | tf_op jit(solution)/shard_map/ppermute | solution.py:34
  32.0 4.7 %collective-permute-start.12 = (f32[136,128]{1,0:T(8,128)S(1)}, f32[136,128]{1,0:T(8,128)S(1)}, u32[]{:S(2)}, u32[]{:S(2)}) collective-permute-start(f32[136,128]{1,0:T(8,128)S(1)} %shard_map.120.own), channel_id=1, source_target_pairs={{0,16},{8,24},{16,0},{24,8},{1,17},{9,25},{17,1},{25,9},{2,18},{10... | collective-permute-start | bytes 208904 | tf_op jit(solution)/shard_map/ppermute | solution.py:34
  36.9 3.3 %collective-permute-start.17 = (f32[136,128]{1,0:T(8,128)S(1)}, f32[136,128]{1,0:T(8,128)S(1)}, u32[]{:S(2)}, u32[]{:S(2)}) collective-permute-start(f32[136,128]{1,0:T(8,128)S(1)} %shard_map.121.own), channel_id=1, source_target_pairs={{0,32},{32,0},{64,96},{96,64},{1,33},{33,1},{65,97},{97,65},{2,34}... | collective-permute-start | bytes 208904 | tf_op jit(solution)/shard_map/ppermute | solution.py:34
  37.7 4.4 %collective-permute-start.16 = (f32[136,128]{1,0:T(8,128)S(1)}, f32[136,128]{1,0:T(8,128)S(1)}, u32[]{:S(2)}, u32[]{:S(2)}) collective-permute-start(f32[136,128]{1,0:T(8,128)S(1)} %shard_map.121.own), channel_id=1, source_target_pairs={{0,96},{32,64},{64,32},{96,0},{1,97},{33,65},{65,33},{97,1},{2,98}... | collective-permute-start | bytes 208904 | tf_op jit(solution)/shard_map/ppermute | solution.py:34
  38.2 5.4 %collective-permute-start.15 = (f32[136,128]{1,0:T(8,128)S(1)}, f32[136,128]{1,0:T(8,128)S(1)}, u32[]{:S(2)}, u32[]{:S(2)}) collective-permute-start(f32[136,128]{1,0:T(8,128)S(1)} %shard_map.121.own), channel_id=1, source_target_pairs={{0,64},{32,96},{64,0},{96,32},{1,65},{33,97},{65,1},{97,33},{2,66}... | collective-permute-start | bytes 208904 | tf_op jit(solution)/shard_map/ppermute | solution.py:34
  44.0 6.6 %collective-permute-start.20 = (bf16[16,256]{1,0:T(8,128)(2,1)S(1)}, bf16[16,256]{1,0:T(8,128)(2,1)S(1)}, u32[]{:S(2)}, u32[]{:S(2)}) collective-permute-start(bf16[16,256]{1,0:T(8,128)(2,1)S(1)} %shard_map.122), channel_id=1, source_target_pairs={{0,3},{1,2},{2,1},{3,0},{4,7},{5,6},{6,5},{7,4},{8,11},{9,10},{10,... | collective-permute-start | bytes 24584 | tf_op jit(solution)/shard_map/ppermute | solution.py:34
  47.4 4.3 %collective-permute-start.19 = (bf16[16,256]{1,0:T(8,128)(2,1)S(1)}, bf16[16,256]{1,0:T(8,128)(2,1)S(1)}, u32[]{:S(2)}, u32[]{:S(2)}) collective-permute-start(bf16[16,256]{1,0:T(8,128)(2,1)S(1)} %shard_map.122), channel_id=1, source_target_pairs={{0,7},{1,6},{2,5},{3,4},{4,3},{5,2},{6,1},{7,0},{8,15},{9,14},{10,... | collective-permute-start | bytes 24584 | tf_op jit(solution)/shard_map/ppermute | solution.py:34
  48.0 4.6 %collective-permute-start.18 = (bf16[16,256]{1,0:T(8,128)(2,1)S(1)}, bf16[16,256]{1,0:T(8,128)(2,1)S(1)}, u32[]{:S(2)}, u32[]{:S(2)}) collective-permute-start(bf16[16,256]{1,0:T(8,128)(2,1)S(1)} %shard_map.122), channel_id=1, source_target_pairs={{0,5},{1,4},{2,7},{3,6},{4,1},{5,0},{6,3},{7,2},{8,13},{9,12},{10,... | collective-permute-start | bytes 24584 | tf_op jit(solution)/shard_map/ppermute | solution.py:34
  52.6 1.3 %collective-permute-start.21 = (f32[16,256]{1,0:T(8,128)S(1)}, f32[16,256]{1,0:T(8,128)S(1)}, u32[]{:S(2)}, u32[]{:S(2)}) collective-permute-start(f32[16,256]{1,0:T(8,128)S(1)} %convert_add_fusion.1.attn), channel_id=1, source_target_pairs={{0,1},{1,0},{2,3},{3,2},{4,5},{5,4},{6,7},{7,6},{8,9},{9,8},{10,11... | collective-permute-start | bytes 49160 | tf_op jit(solution)/shard_map/ppermute | solution.py:39
  54.1 4.1 %collective-permute-start.24 = (bf16[16,2944]{1,0:T(8,128)(2,1)S(1)}, bf16[16,2944]{1,0:T(8,128)(2,1)S(1)}, u32[]{:S(2)}, u32[]{:S(2)}) collective-permute-start(bf16[16,2944]{1,0:T(8,128)(2,1)S(1)} %get-tuple-element.16), channel_id=1, source_target_pairs={{0,8},{8,0},{16,24},{24,16},{1,9},{9,1},{17,25},{25,17},{2,10},{10... | collective-permute-start | bytes 282632 | tf_op jit(solution)/shard_map/ppermute | solution.py:34
  54.7 4.6 %collective-permute-start.23 = (bf16[16,2944]{1,0:T(8,128)(2,1)S(1)}, bf16[16,2944]{1,0:T(8,128)(2,1)S(1)}, u32[]{:S(2)}, u32[]{:S(2)}) collective-permute-start(bf16[16,2944]{1,0:T(8,128)(2,1)S(1)} %get-tuple-element.16), channel_id=1, source_target_pairs={{0,24},{8,16},{16,8},{24,0},{1,25},{9,17},{17,9},{25,1},{2,26},{10... | collective-permute-start | bytes 282632 | tf_op jit(solution)/shard_map/ppermute | solution.py:34
  56.6 4.9 %collective-permute-start.22 = (bf16[16,2944]{1,0:T(8,128)(2,1)S(1)}, bf16[16,2944]{1,0:T(8,128)(2,1)S(1)}, u32[]{:S(2)}, u32[]{:S(2)}) collective-permute-start(bf16[16,2944]{1,0:T(8,128)(2,1)S(1)} %get-tuple-element.16), channel_id=1, source_target_pairs={{0,16},{8,24},{16,0},{24,8},{1,17},{9,25},{17,1},{25,9},{2,18},{10... | collective-permute-start | bytes 282632 | tf_op jit(solution)/shard_map/ppermute | solution.py:34
  61.7 3.6 %collective-permute-start.27 = (bf16[16,2944]{1,0:T(8,128)(2,1)S(1)}, bf16[16,2944]{1,0:T(8,128)(2,1)S(1)}, u32[]{:S(2)}, u32[]{:S(2)}) collective-permute-start(bf16[16,2944]{1,0:T(8,128)(2,1)S(1)} %get-tuple-element.18), channel_id=1, source_target_pairs={{0,32},{32,0},{64,96},{96,64},{1,33},{33,1},{65,97},{97,65},{2,34}... | collective-permute-start | bytes 282632 | tf_op jit(solution)/shard_map/ppermute | solution.py:34
  62.0 4.6 %collective-permute-start.26 = (bf16[16,2944]{1,0:T(8,128)(2,1)S(1)}, bf16[16,2944]{1,0:T(8,128)(2,1)S(1)}, u32[]{:S(2)}, u32[]{:S(2)}) collective-permute-start(bf16[16,2944]{1,0:T(8,128)(2,1)S(1)} %get-tuple-element.18), channel_id=1, source_target_pairs={{0,96},{32,64},{64,32},{96,0},{1,97},{33,65},{65,33},{97,1},{2,98}... | collective-permute-start | bytes 282632 | tf_op jit(solution)/shard_map/ppermute | solution.py:34
  64.2 5.5 %collective-permute-start.25 = (bf16[16,2944]{1,0:T(8,128)(2,1)S(1)}, bf16[16,2944]{1,0:T(8,128)(2,1)S(1)}, u32[]{:S(2)}, u32[]{:S(2)}) collective-permute-start(bf16[16,2944]{1,0:T(8,128)(2,1)S(1)} %get-tuple-element.18), channel_id=1, source_target_pairs={{0,64},{32,96},{64,0},{96,32},{1,65},{33,97},{65,1},{97,33},{2,66}... | collective-permute-start | bytes 282632 | tf_op jit(solution)/shard_map/ppermute | solution.py:34
  70.1 6.4 %collective-permute-start.30 = (bf16[16,256]{1,0:T(8,128)(2,1)S(1)}, bf16[16,256]{1,0:T(8,128)(2,1)S(1)}, u32[]{:S(2)}, u32[]{:S(2)}) collective-permute-start(bf16[16,256]{1,0:T(8,128)(2,1)S(1)} %shard_map.125), channel_id=1, source_target_pairs={{0,3},{1,2},{2,1},{3,0},{4,7},{5,6},{6,5},{7,4},{8,11},{9,10},{10,... | collective-permute-start | bytes 24584 | tf_op jit(solution)/shard_map/ppermute | solution.py:34
  74.0 4.3 %collective-permute-start.29 = (bf16[16,256]{1,0:T(8,128)(2,1)S(1)}, bf16[16,256]{1,0:T(8,128)(2,1)S(1)}, u32[]{:S(2)}, u32[]{:S(2)}) collective-permute-start(bf16[16,256]{1,0:T(8,128)(2,1)S(1)} %shard_map.125), channel_id=1, source_target_pairs={{0,7},{1,6},{2,5},{3,4},{4,3},{5,2},{6,1},{7,0},{8,15},{9,14},{10,... | collective-permute-start | bytes 24584 | tf_op jit(solution)/shard_map/ppermute | solution.py:34
  75.4 4.6 %collective-permute-start.28 = (bf16[16,256]{1,0:T(8,128)(2,1)S(1)}, bf16[16,256]{1,0:T(8,128)(2,1)S(1)}, u32[]{:S(2)}, u32[]{:S(2)}) collective-permute-start(bf16[16,256]{1,0:T(8,128)(2,1)S(1)} %shard_map.125), channel_id=1, source_target_pairs={{0,5},{1,4},{2,7},{3,6},{4,1},{5,0},{6,3},{7,2},{8,13},{9,12},{10,... | collective-permute-start | bytes 24584 | tf_op jit(solution)/shard_map/ppermute | solution.py:34
  79.9 1.8 %collective-permute-start.31 = (f32[16,256]{1,0:T(8,128)S(1)}, f32[16,256]{1,0:T(8,128)S(1)}, u32[]{:S(2)}, u32[]{:S(2)}) collective-permute-start(f32[16,256]{1,0:T(8,128)S(1)} %convert_add_fusion), channel_id=1, source_target_pairs={{0,1},{1,0},{2,3},{3,2},{4,5},{5,4},{6,7},{7,6},{8,9},{9,8},{10,11... | collective-permute-start | bytes 49160 | tf_op jit(solution)/shard_map/ppermute | solution.py:39

commit v7 on v6

--- a/solution.py
+++ b/solution.py
@@ -22,7 +22,7 @@
 COST = 2**40
 
 SHIFTS = (2, 3, 1)
-STRAIGHT = ("gates", "heads")
+STRAIGHT = ("gates",)
 
 
 def peers(shard, axis, what):
@@ -97,7 +97,7 @@
     packed[:, width:] = jnp.broadcast_to(squares, (batch, LANES))
 
 
-def attend_body(own, a, b, c, keys, values, out, query, scores, weights):
+def attend_body(own, a, b, c, keys, values, out, sent, query, scores, weights):
     batch, _, _ = keys.shape
     width = own.shape[1] - LANES
     heads = width // LANES
@@ -131,39 +131,59 @@
         out[n * high : (n + 1) * high, :] = jnp.dot(
             weights[n], values[n], preferred_element_type=F32
         )
-
-
-def combined(parts, rows, high):
-    n = rows * high
-    stats = [p[n : n + high, :] for p in parts]
+    write_sent(sent, out[: batch * high, :], stats)
+
+
+def three_parts(stats):
+    high = stats.astype(BF16).astype(F32)
+    rest = stats - high
+    middle = rest.astype(BF16).astype(F32)
+    low = rest - middle
+    return high + pltpu.roll(middle, 16, 1) + pltpu.roll(low, 32, 1)
+
+
+def from_parts(parts):
+    whole = (parts + pltpu.roll(parts, LANES - 16, 1)) + pltpu.roll(parts, LANES - 32, 1)
+    return jnp.where(lane_of(parts.shape) % (LANES // 2) < 16, whole, 0.0)
+
+
+def write_sent(sent, accs, stats):
+    n = accs.shape[0]
+    sent[:n, :] = accs.astype(BF16)
+    sent[n:, :] = jnp.concatenate([three_parts(stats)] * 2, axis=0).astype(BF16)
+
+
+def combined(own, others, high):
+    n = own.shape[0] - high
+    stats = [own[n:, :]] + [from_parts(p[n:, :].astype(F32)[:high]) for p in others]
+    values = [own[:n, :]] + [p[:n, :].astype(F32) for p in others]
     top = functools.reduce(jnp.maximum, stats)
     factors = [jnp.exp(s - top) for s in stats]
     shifted = [pltpu.roll(f, LANES // 2, 1) for f in factors]
     total = sum(s * f for s, f in zip(stats, shifted))
     low = lane_of(top.shape) < LANES // 2
     accs = []
-    for k in range(rows):
+    for k in range(n // high):
         acc = 0.0
-        for p, f in zip(parts, factors):
-            acc = acc + p[k * high : (k + 1) * high, :] * f[:, k : k + 1]
+        for v, f in zip(values, factors):
+            acc = acc + v[k * high : (k + 1) * high] * f[:, k : k + 1]
         accs.append(acc)
     return jnp.where(low, top, total), accs
 
 
-def merge_body(own, a, b, c, out):
-    high = 8
-    rows = own.shape[0] // high - 1
-    stats, accs = combined((own, a, b, c), rows, high)
-    for k, acc in enumerate(accs):
-        out[k * high : (k + 1) * high, :] = acc
-    out[rows * high :, :] = stats
+def merge_body(own, a, b, c, out, sent):
+    stats, accs = combined(own, (a, b, c), 8)
+    accs = jnp.concatenate(accs, axis=0)
+    out[: accs.shape[0], :] = accs
+    out[accs.shape[0] :, :] = stats
+    write_sent(sent, accs, stats)
 
 
 def project_body(lambdas, own, a, b, c, gain, weight, out, held):
     high = 8
     heads = high // 2
     rows = own.shape[0] // high - 1
-    stats, accs = combined((own, a, b, c), rows, high)
+    stats, accs = combined(own, (a, b, c), high)
     inverse = 1.0 / stats
     for k, acc in enumerate(accs):
         at_lane = LANES // 2 + k
@@ -282,9 +302,11 @@
         cost=COST,
     )(chip[None], pair, *peers(pair, "tp_0", "rows"), attn_gain[None], query_weight)
     packed = added(partner(packed), peers(packed, "kv_1", "query"))
-    state = kernel_call(
+    rows = batch * 2 * heads
+    states = [shape((rows + 8, LANES), F32), shape((rows + 16, LANES), BF16)]
+    state, sent = kernel_call(
         attend_body,
-        [shape(((batch + 1) * 2 * heads, LANES), F32)],
+        states,
         [
             pltpu.VMEM((heads * batch, LANES), F32),
             pltpu.VMEM((2 * heads * batch, positions), F32),
@@ -296,22 +318,16 @@
         *peers(packed, "kv_0", "query"),
         key_cache.reshape(batch, positions, LANES),
         value_cache.reshape(batch, positions, LANES),
-    )[0]
-    state = kernel_call(merge_body, [shape(state.shape, F32)], n_in=4)(
-        state, *peers(state, "kv_1", "heads")
-    )[0]
+    )
+    state, sent = kernel_call(merge_body, states, n_in=4)(
+        partner(state), *peers(sent, "kv_1", "heads")
+    )
     projected = kernel_call(
         project_body,
         [shape((batch, wide), BF16)],
         [pltpu.VMEM((2 * heads * batch, LANES), F32)],
         n_in=7,
-    )(
-        lambdas[None],
-        state,
-        *peers(state, "kv_0", "heads"),
-        head_gain[None],
-        out_weight,
-    )[0]
+    )(lambdas[None], partner(state), *peers(sent, "kv_0", "heads"), head_gain[None], out_weight)[0]
     attn = added(
         projected.astype(F32), [p.astype(F32) for p in peers(projected, "tp_0", "attn")]
     )

time: 82.5 us -> 80.8 us (0.979)
  starting transfers between devices: 43.6 us -> 42.2 us
    ppermute x27, starting transfers between devices: 40.2 us -> 38 us  [peers(): got.append(lax.ppermute(shard, across, pairs))]
    ppermute x5 -> x7, starting transfers between devices: 3.39 us -> 4.25 us  [partner(): return lax.ppermute(shard, TP[1], [(0, 1), (1, 0)])]
    ppermute x5 -> x7, waiting for transfers between devices: 2.61 us -> 2.63 us  [partner(): return lax.ppermute(shard, TP[1], [(0, 1), (1, 0)])]
  transfers between devices with their start and end apart: 32 -> 34, of which waited for: 22 -> 22; matrix products, arithmetic and copies ran while one was open for 0% -> 0% of each run, Pallas kernels for 0% -> 0%
where the time goes in v7:
time: 80.8 us; the launch traced here: 80.7 us
  starting transfers between devices  42.2 us (52%)
  waiting for transfers between devices  33.2 us (41%)
  Pallas kernels  4.32 us (5%)
    ppermute x27, starting transfers between devices, peers(): got.append(lax.ppermute(shard, across, pairs))  38 us
    ppermute x27, waiting for transfers between devices, peers(): got.append(lax.ppermute(shard, across, pairs))  30.6 us
    ppermute x7, starting transfers between devices, partner(): return lax.ppermute(shard, TP[1], [(0, 1), (1, 0)])  4.25 us
    ppermute x7, waiting for transfers between devices, partner(): return lax.ppermute(shard, TP[1], [(0, 1), (1, 0)])  2.63 us
    pallas_call x1, Pallas kernels, per_device(): kernel_call(attend_body, states, [pltpu.VMEM((heads * batch, LANES), F32)...  1.77 us
  transfers between devices with their start and end apart: 34, of which 22 were waited for; matrix products, arithmetic and copies ran while one was open for 0% of the time, Pallas kernels for 0%

profile of v7, /device:TPU:1, one launch (start us, length us, event | category | flops | bytes accessed | tf_op | source)
XLA Modules:
  0.0 80.7 jit_solution(8655481877884558210)
XLA Ops:
  0.0 0.8 %shard_map.118 = f32[24,128]{1,0:T(8,128)S(1)} custom-call(bf16[16,32]{1,0:T(8,128)(2,1)} %hidden.1, f32[1,32]{1,0:T(1,128)} %bitcast.12), custom_call_target="tpu_custom_call" | custom-call | flops 1099511627776 | bytes 1099511627776 | tf_op jit(solution)/shard_map/pallas_call | solution.py:278
  0.8 1.5 %collective-permute-start = (f32[24,128]{1,0:T(8,128)S(1)}, f32[24,128]{1,0:T(8,128)S(1)}, u32[]{:S(2)}, u32[]{:S(2)}) collective-permute-start(f32[24,128]{1,0:T(8,128)S(1)} %shard_map.118), channel_id=1, source_target_pairs={{0,1},{1,0},{2,3},{3,2},{4,5},{5,4},{6,7},{7,6},{8,9},{9,8},{10,11... | collective-permute-start | bytes 36872 | tf_op jit(solution)/shard_map/ppermute | solution.py:39
  2.3 0.8 %collective-permute-done = f32[24,128]{1,0:T(8,128)S(1)} collective-permute-done((f32[24,128]{1,0:T(8,128)S(1)}, f32[24,128]{1,0:T(8,128)S(1)}, u32[]{:S(2)}, u32[]{:S(2)}) %collective-permute-start) | collective-permute-done | bytes 12320 | tf_op jit(solution)/shard_map/ppermute | solution.py:39
  3.1 1.6 %collective-permute-start.3 = (f32[24,128]{1,0:T(8,128)S(1)}, f32[24,128]{1,0:T(8,128)S(1)}, u32[]{:S(2)}, u32[]{:S(2)}) collective-permute-start(f32[24,128]{1,0:T(8,128)S(1)} %fusion.2.own), channel_id=1, source_target_pairs={{0,3},{1,2},{2,1},{3,0},{4,7},{5,6},{6,5},{7,4},{8,11},{9,10},{10,... | collective-permute-start | bytes 36872 | tf_op jit(solution)/shard_map/ppermute | solution.py:34
  4.8 1.9 %collective-permute-start.2 = (f32[24,128]{1,0:T(8,128)S(1)}, f32[24,128]{1,0:T(8,128)S(1)}, u32[]{:S(2)}, u32[]{:S(2)}) collective-permute-start(f32[24,128]{1,0:T(8,128)S(1)} %fusion.2.own), channel_id=1, source_target_pairs={{0,7},{1,6},{2,5},{3,4},{4,3},{5,2},{6,1},{7,0},{8,15},{9,14},{10,... | collective-permute-start | bytes 36872 | tf_op jit(solution)/shard_map/ppermute | solution.py:34
  6.6 0.6 collective-permute-start.1
  7.3 1.8 %collective-permute-done.2.b = f32[24,128]{1,0:T(8,128)S(1)} collective-permute-done((f32[24,128]{1,0:T(8,128)S(1)}, f32[24,128]{1,0:T(8,128)S(1)}, u32[]{:S(2)}, u32[]{:S(2)}) %collective-permute-start.2) | collective-permute-done | bytes 12320 | tf_op jit(solution)/shard_map/ppermute | solution.py:34
  9.1 2.2 %collective-permute-done.1.a = f32[24,128]{1,0:T(8,128)S(1)} collective-permute-done((f32[24,128]{1,0:T(8,128)S(1)}, f32[24,128]{1,0:T(8,128)S(1)}, u32[]{:S(2)}, u32[]{:S(2)}) %collective-permute-start.1) | collective-permute-done | bytes 12320 | tf_op jit(solution)/shard_map/ppermute | solution.py:34
  11.4 1.5 %collective-permute-start.7 = (f32[16,640]{1,0:T(8,128)S(1)}, f32[16,640]{1,0:T(8,128)S(1)}, u32[]{:S(2)}, u32[]{:S(2)}) collective-permute-start(f32[16,640]{1,0:T(8,128)S(1)} %get-tuple-element.16), channel_id=1, source_target_pairs={{0,9},{1,8},{8,1},{9,0},{16,25},{17,24},{24,17},{25,16},{2,11},{3,... | collective-permute-start | bytes 122888 | tf_op jit(solution)/shard_map/ppermute | solution.py:34
  13.0 2.0 %collective-permute-start.6 = (f32[16,640]{1,0:T(8,128)S(1)}, f32[16,640]{1,0:T(8,128)S(1)}, u32[]{:S(2)}, u32[]{:S(2)}) collective-permute-start(f32[16,640]{1,0:T(8,128)S(1)} %get-tuple-element.16), channel_id=1, source_target_pairs={{0,25},{1,24},{8,17},{9,16},{16,9},{17,8},{24,1},{25,0},{2,27},{3,... | collective-permute-start | bytes 122888 | tf_op jit(solution)/shard_map/ppermute | solution.py:34
  14.9 0.7 collective-permute-start.5
  15.6 0.3 collective-permute-start.4
  16.0 1.6 %collective-permute-done.6 = f32[16,640]{1,0:T(8,128)S(1)} collective-permute-done((f32[16,640]{1,0:T(8,128)S(1)}, f32[16,640]{1,0:T(8,128)S(1)}, u32[]{:S(2)}, u32[]{:S(2)}) %collective-permute-start.6) | collective-permute-done | bytes 40992 | tf_op jit(solution)/shard_map/ppermute | solution.py:34
  17.6 2.3 %collective-permute-done.5 = f32[16,640]{1,0:T(8,128)S(1)} collective-permute-done((f32[16,640]{1,0:T(8,128)S(1)}, f32[16,640]{1,0:T(8,128)S(1)}, u32[]{:S(2)}, u32[]{:S(2)}) %collective-permute-start.5) | collective-permute-done | bytes 40992 | tf_op jit(solution)/shard_map/ppermute | solution.py:34
  20.0 1.9 %collective-permute-start.11 = (f32[16,640]{1,0:T(8,128)S(1)}, f32[16,640]{1,0:T(8,128)S(1)}, u32[]{:S(2)}, u32[]{:S(2)}) collective-permute-start(f32[16,640]{1,0:T(8,128)S(1)} %add_add_fusion), channel_id=1, source_target_pairs={{0,33},{1,32},{32,1},{33,0},{64,97},{65,96},{96,65},{97,64},{2,35}... | collective-permute-start | bytes 122888 | tf_op jit(solution)/shard_map/ppermute | solution.py:34
  21.9 2.3 %collective-permute-start.10 = (f32[16,640]{1,0:T(8,128)S(1)}, f32[16,640]{1,0:T(8,128)S(1)}, u32[]{:S(2)}, u32[]{:S(2)}) collective-permute-start(f32[16,640]{1,0:T(8,128)S(1)} %add_add_fusion), channel_id=1, source_target_pairs={{0,97},{1,96},{32,65},{33,64},{64,33},{65,32},{96,1},{97,0},{2,99}... | collective-permute-start | bytes 122888 | tf_op jit(solution)/shard_map/ppermute | solution.py:34
  24.2 1.1 %collective-permute-start.9 = (f32[16,640]{1,0:T(8,128)S(1)}, f32[16,640]{1,0:T(8,128)S(1)}, u32[]{:S(2)}, u32[]{:S(2)}) collective-permute-start(f32[16,640]{1,0:T(8,128)S(1)} %add_add_fusion), channel_id=1, source_target_pairs={{0,65},{1,64},{32,97},{33,96},{64,1},{65,0},{96,33},{97,32},{2,67}... | collective-permute-start | bytes 122888 | tf_op jit(solution)/shard_map/ppermute | solution.py:34
  25.3 0.3 collective-permute-start.8
  25.6 0.9 %collective-permute-done.10.b = f32[16,640]{1,0:T(8,128)S(1)} collective-permute-done((f32[16,640]{1,0:T(8,128)S(1)}, f32[16,640]{1,0:T(8,128)S(1)}, u32[]{:S(2)}, u32[]{:S(2)}) %collective-permute-start.10) | collective-permute-done | bytes 40992 | tf_op jit(solution)/shard_map/ppermute | solution.py:34
  26.5 2.7 %collective-permute-done.9.a = f32[16,640]{1,0:T(8,128)S(1)} collective-permute-done((f32[16,640]{1,0:T(8,128)S(1)}, f32[16,640]{1,0:T(8,128)S(1)}, u32[]{:S(2)}, u32[]{:S(2)}) %collective-permute-start.9) | collective-permute-done | bytes 40992 | tf_op jit(solution)/shard_map/ppermute | solution.py:34
  29.3 1.8 %shard_map.120 = (f32[136,128]{1,0:T(8,128)S(1)}, bf16[144,128]{1,0:T(8,128)(2,1)S(1)}) custom-call(f32[16,640]{1,0:T(8,128)S(1)} %collective-permute-done.8.own, f32[16,640]{1,0:T(8,128)S(1)} %collective-permute-done.9.a, f32[16,640]{1,0:T(8,128)S(1)} %collective-permute-done.10.b, f32[16,640]{1,0:T(8,128)S(1)} %collective-permute-done.11.c, ...), custom_call_target="tpu_custom_call" | custom-call | tf_op jit(solution)/shard_map/pallas_call | solution.py:307
  31.1 0.4 collective-permute-start.12
  31.5 0.4 collective-permute-start.15
  31.9 0.4 collective-permute-start.14
  32.4 2.7 %collective-permute-start.13 = (bf16[144,128]{1,0:T(8,128)(2,1)S(1)}, bf16[144,128]{1,0:T(8,128)(2,1)S(1)}, u32[]{:S(2)}, u32[]{:S(2)}) collective-permute-start(bf16[144,128]{1,0:T(8,128)(2,1)S(1)} %get-tuple-element.18), channel_id=1, source_target_pairs={{0,17},{1,16},{8,25},{9,24},{16,1},{17,0},{24,9},{25,8},{2,19},{3,... | collective-permute-start | bytes 110600 | tf_op jit(solution)/shard_map/ppermute | solution.py:34
  35.1 1.8 %collective-permute-done.14.b = bf16[144,128]{1,0:T(8,128)(2,1)S(1)} collective-permute-done((bf16[144,128]{1,0:T(8,128)(2,1)S(1)}, bf16[144,128]{1,0:T(8,128)(2,1)S(1)}, u32[]{:S(2)}, u32[]{:S(2)}) %collective-permute-start.14) | collective-permute-done | bytes 36896 | tf_op jit(solution)/shard_map/ppermute | solution.py:34
  36.9 0.5 collective-permute-done.13.a
  37.4 0.3 shard_map.121
  37.6 0.4 collective-permute-start.16
  38.1 0.8 collective-permute-start.19
  38.9 0.6 collective-permute-start.18
  39.5 2.2 %collective-permute-start.17 = (bf16[144,128]{1,0:T(8,128)(2,1)S(1)}, bf16[144,128]{1,0:T(8,128)(2,1)S(1)}, u32[]{:S(2)}, u32[]{:S(2)}) collective-permute-start(bf16[144,128]{1,0:T(8,128)(2,1)S(1)} %get-tuple-element.20), channel_id=1, source_target_pairs={{0,65},{1,64},{32,97},{33,96},{64,1},{65,0},{96,33},{97,32},{2,67}... | collective-permute-start | bytes 110600 | tf_op jit(solution)/shard_map/ppermute | solution.py:34
  41.7 1.8 %collective-permute-done.18.b = bf16[144,128]{1,0:T(8,128)(2,1)S(1)} collective-permute-done((bf16[144,128]{1,0:T(8,128)(2,1)S(1)}, bf16[144,128]{1,0:T(8,128)(2,1)S(1)}, u32[]{:S(2)}, u32[]{:S(2)}) %collective-permute-start.18) | collective-permute-done | bytes 36896 | tf_op jit(solution)/shard_map/ppermute | solution.py:34
  43.5 0.9 %collective-permute-done.17.a = bf16[144,128]{1,0:T(8,128)(2,1)S(1)} collective-permute-done((bf16[144,128]{1,0:T(8,128)(2,1)S(1)}, bf16[144,128]{1,0:T(8,128)(2,1)S(1)}, u32[]{:S(2)}, u32[]{:S(2)}) %collective-permute-start.17) | collective-permute-done | bytes 36896 | tf_op jit(solution)/shard_map/ppermute | solution.py:34
  44.4 0.5 shard_map.122
  44.9 0.5 collective-permute-start.22
  45.5 0.6 collective-permute-start.21
  46.1 2.6 %collective-permute-start.20 = (bf16[16,256]{1,0:T(8,128)(2,1)S(1)}, bf16[16,256]{1,0:T(8,128)(2,1)S(1)}, u32[]{:S(2)}, u32[]{:S(2)}) collective-permute-start(bf16[16,256]{1,0:T(8,128)(2,1)S(1)} %shard_map.122), channel_id=1, source_target_pairs={{0,5},{1,4},{2,7},{3,6},{4,1},{5,0},{6,3},{7,2},{8,13},{9,12},{10,... | collective-permute-start | bytes 24584 | tf_op jit(solution)/shard_map/ppermute | solution.py:34
  48.7 1.1 %collective-permute-done.21 = bf16[16,256]{1,0:T(8,128)(2,1)S(1)} collective-permute-done((bf16[16,256]{1,0:T(8,128)(2,1)S(1)}, bf16[16,256]{1,0:T(8,128)(2,1)S(1)}, u32[]{:S(2)}, u32[]{:S(2)}) %collective-permute-start.21) | collective-permute-done | bytes 8224 | tf_op jit(solution)/shard_map/ppermute | solution.py:34
  49.7 0.9 %collective-permute-done.20 = bf16[16,256]{1,0:T(8,128)(2,1)S(1)} collective-permute-done((bf16[16,256]{1,0:T(8,128)(2,1)S(1)}, bf16[16,256]{1,0:T(8,128)(2,1)S(1)}, u32[]{:S(2)}, u32[]{:S(2)}) %collective-permute-start.20) | collective-permute-done | bytes 8224 | tf_op jit(solution)/shard_map/ppermute | solution.py:34
  50.7 0.3 collective-permute-start.23
  51.0 1.0 %collective-permute-done.23.other = f32[16,256]{1,0:T(8,128)S(1)} collective-permute-done((f32[16,256]{1,0:T(8,128)S(1)}, f32[16,256]{1,0:T(8,128)S(1)}, u32[]{:S(2)}, u32[]{:S(2)}) %collective-permute-start.23) | collective-permute-done | bytes 16416 | tf_op jit(solution)/shard_map/ppermute | solution.py:39
  51.9 0.3 shard_map.123
  52.2 0.8 %collective-permute-start.26 = (bf16[16,2944]{1,0:T(8,128)(2,1)S(1)}, bf16[16,2944]{1,0:T(8,128)(2,1)S(1)}, u32[]{:S(2)}, u32[]{:S(2)}) collective-permute-start(bf16[16,2944]{1,0:T(8,128)(2,1)S(1)} %get-tuple-element.24), channel_id=1, source_target_pairs={{0,8},{8,0},{16,24},{24,16},{1,9},{9,1},{17,25},{25,17},{2,10},{10... | collective-permute-start | bytes 282632 | tf_op jit(solution)/shard_map/ppermute | solution.py:34
  53.0 1.9 %collective-permute-start.25 = (bf16[16,2944]{1,0:T(8,128)(2,1)S(1)}, bf16[16,2944]{1,0:T(8,128)(2,1)S(1)}, u32[]{:S(2)}, u32[]{:S(2)}) collective-permute-start(bf16[16,2944]{1,0:T(8,128)(2,1)S(1)} %get-tuple-element.24), channel_id=1, source_target_pairs={{0,24},{8,16},{16,8},{24,0},{1,25},{9,17},{17,9},{25,1},{2,26},{10... | collective-permute-start | bytes 282632 | tf_op jit(solution)/shard_map/ppermute | solution.py:34
  55.0 0.7 collective-permute-start.24
  55.7 0.7 collective-permute-done.26.c
  56.3 1.4 %collective-permute-done.25.b = bf16[16,2944]{1,0:T(8,128)(2,1)S(1)} collective-permute-done((bf16[16,2944]{1,0:T(8,128)(2,1)S(1)}, bf16[16,2944]{1,0:T(8,128)(2,1)S(1)}, u32[]{:S(2)}, u32[]{:S(2)}) %collective-permute-start.25) | collective-permute-done | bytes 94240 | tf_op jit(solution)/shard_map/ppermute | solution.py:34
  57.7 2.2 %collective-permute-done.24.a = bf16[16,2944]{1,0:T(8,128)(2,1)S(1)} collective-permute-done((bf16[16,2944]{1,0:T(8,128)(2,1)S(1)}, bf16[16,2944]{1,0:T(8,128)(2,1)S(1)}, u32[]{:S(2)}, u32[]{:S(2)}) %collective-permute-start.24) | collective-permute-done | bytes 94240 | tf_op jit(solution)/shard_map/ppermute | solution.py:34
  59.9 0.2 shard_map.124
  60.0 0.2 collective-permute-start.29
  60.2 2.3 %collective-permute-start.28 = (bf16[16,2944]{1,0:T(8,128)(2,1)S(1)}, bf16[16,2944]{1,0:T(8,128)(2,1)S(1)}, u32[]{:S(2)}, u32[]{:S(2)}) collective-permute-start(bf16[16,2944]{1,0:T(8,128)(2,1)S(1)} %get-tuple-element.26), channel_id=1, source_target_pairs={{0,96},{32,64},{64,32},{96,0},{1,97},{33,65},{65,33},{97,1},{2,98}... | collective-permute-start | bytes 282632 | tf_op jit(solution)/shard_map/ppermute | solution.py:34
  62.5 1.1 %collective-permute-start.27 = (bf16[16,2944]{1,0:T(8,128)(2,1)S(1)}, bf16[16,2944]{1,0:T(8,128)(2,1)S(1)}, u32[]{:S(2)}, u32[]{:S(2)}) collective-permute-start(bf16[16,2944]{1,0:T(8,128)(2,1)S(1)} %get-tuple-element.26), channel_id=1, source_target_pairs={{0,64},{32,96},{64,0},{96,32},{1,65},{33,97},{65,1},{97,33},{2,66}... | collective-permute-start | bytes 282632 | tf_op jit(solution)/shard_map/ppermute | solution.py:34
  63.6 1.3 %collective-permute-done.28.b = bf16[16,2944]{1,0:T(8,128)(2,1)S(1)} collective-permute-done((bf16[16,2944]{1,0:T(8,128)(2,1)S(1)}, bf16[16,2944]{1,0:T(8,128)(2,1)S(1)}, u32[]{:S(2)}, u32[]{:S(2)}) %collective-permute-start.28) | collective-permute-done | bytes 94240 | tf_op jit(solution)/shard_map/ppermute | solution.py:34
  64.9 3.2 %collective-permute-done.27.a = bf16[16,2944]{1,0:T(8,128)(2,1)S(1)} collective-permute-done((bf16[16,2944]{1,0:T(8,128)(2,1)S(1)}, bf16[16,2944]{1,0:T(8,128)(2,1)S(1)}, u32[]{:S(2)}, u32[]{:S(2)}) %collective-permute-start.27) | collective-permute-done | bytes 94240 | tf_op jit(solution)/shard_map/ppermute | solution.py:34
  68.0 0.3 shard_map.125
  68.4 3.9 %collective-permute-start.32 = (bf16[16,256]{1,0:T(8,128)(2,1)S(1)}, bf16[16,256]{1,0:T(8,128)(2,1)S(1)}, u32[]{:S(2)}, u32[]{:S(2)}) collective-permute-start(bf16[16,256]{1,0:T(8,128)(2,1)S(1)} %shard_map.125), channel_id=1, source_target_pairs={{0,3},{1,2},{2,1},{3,0},{4,7},{5,6},{6,5},{7,4},{8,11},{9,10},{10,... | collective-permute-start | bytes 24584 | tf_op jit(solution)/shard_map/ppermute | solution.py:34
  72.3 1.3 %collective-permute-start.31 = (bf16[16,256]{1,0:T(8,128)(2,1)S(1)}, bf16[16,256]{1,0:T(8,128)(2,1)S(1)}, u32[]{:S(2)}, u32[]{:S(2)}) collective-permute-start(bf16[16,256]{1,0:T(8,128)(2,1)S(1)} %shard_map.125), channel_id=1, source_target_pairs={{0,7},{1,6},{2,5},{3,4},{4,3},{5,2},{6,1},{7,0},{8,15},{9,14},{10,... | collective-permute-start | bytes 24584 | tf_op jit(solution)/shard_map/ppermute | solution.py:34
  73.6 1.2 %collective-permute-start.30 = (bf16[16,256]{1,0:T(8,128)(2,1)S(1)}, bf16[16,256]{1,0:T(8,128)(2,1)S(1)}, u32[]{:S(2)}, u32[]{:S(2)}) collective-permute-start(bf16[16,256]{1,0:T(8,128)(2,1)S(1)} %shard_map.125), channel_id=1, source_target_pairs={{0,5},{1,4},{2,7},{3,6},{4,1},{5,0},{6,3},{7,2},{8,13},{9,12},{10,... | collective-permute-start | bytes 24584 | tf_op jit(solution)/shard_map/ppermute | solution.py:34
  74.8 1.8 %collective-permute-done.31 = bf16[16,256]{1,0:T(8,128)(2,1)S(1)} collective-permute-done((bf16[16,256]{1,0:T(8,128)(2,1)S(1)}, bf16[16,256]{1,0:T(8,128)(2,1)S(1)}, u32[]{:S(2)}, u32[]{:S(2)}) %collective-permute-start.31) | collective-permute-done | bytes 8224 | tf_op jit(solution)/shard_map/ppermute | solution.py:34
  76.6 1.6 %collective-permute-done.30 = bf16[16,256]{1,0:T(8,128)(2,1)S(1)} collective-permute-done((bf16[16,256]{1,0:T(8,128)(2,1)S(1)}, bf16[16,256]{1,0:T(8,128)(2,1)S(1)}, u32[]{:S(2)}, u32[]{:S(2)}) %collective-permute-start.30) | collective-permute-done | bytes 8224 | tf_op jit(solution)/shard_map/ppermute | solution.py:34
  78.2 1.0 %collective-permute-start.33 = (f32[16,256]{1,0:T(8,128)S(1)}, f32[16,256]{1,0:T(8,128)S(1)}, u32[]{:S(2)}, u32[]{:S(2)}) collective-permute-start(f32[16,256]{1,0:T(8,128)S(1)} %convert_add_fusion), channel_id=1, source_target_pairs={{0,1},{1,0},{2,3},{3,2},{4,5},{5,4},{6,7},{7,6},{8,9},{9,8},{10,11... | collective-permute-start | bytes 49160 | tf_op jit(solution)/shard_map/ppermute | solution.py:39
  79.2 0.8 %collective-permute-done.33 = f32[16,256]{1,0:T(8,128)S(1)} collective-permute-done((f32[16,256]{1,0:T(8,128)S(1)}, f32[16,256]{1,0:T(8,128)S(1)}, u32[]{:S(2)}, u32[]{:S(2)}) %collective-permute-start.33) | collective-permute-done | bytes 16416 | tf_op jit(solution)/shard_map/ppermute | solution.py:39
  80.0 0.7 fusion.3
  (39 shorter events, 0.3 us)
Async XLA Ops:
  0.0 11.3 %copy-start.8 = (bf16[256,512]{1,0:T(8,128)(2,1)S(1)}, bf16[256,512]{1,0:T(8,128)(2,1)}, u32[]{:S(2)}) copy-start(bf16[256,512]{1,0:T(8,128)(2,1)} %weight.3) | copy-start | bytes 786436
  0.0 11.3 %copy-start.9 = (f32[256]{0:T(256)S(1)}, f32[256]{0:T(256)}, u32[]{:S(2)}) copy-start(f32[256]{0:T(256)} %param.13) | copy-start | bytes 3076
  0.8 2.3 %collective-permute-start = (f32[24,128]{1,0:T(8,128)S(1)}, f32[24,128]{1,0:T(8,128)S(1)}, u32[]{:S(2)}, u32[]{:S(2)}) collective-permute-start(f32[24,128]{1,0:T(8,128)S(1)} %shard_map.118), channel_id=1, source_target_pairs={{0,1},{1,0},{2,3},{3,2},{4,5},{5,4},{6,7},{7,6},{8,9},{9,8},{10,11... | collective-permute-start | bytes 36872 | tf_op jit(solution)/shard_map/ppermute | solution.py:39
  3.1 4.1 %collective-permute-start.3 = (f32[24,128]{1,0:T(8,128)S(1)}, f32[24,128]{1,0:T(8,128)S(1)}, u32[]{:S(2)}, u32[]{:S(2)}) collective-permute-start(f32[24,128]{1,0:T(8,128)S(1)} %fusion.2.own), channel_id=1, source_target_pairs={{0,3},{1,2},{2,1},{3,0},{4,7},{5,6},{6,5},{7,4},{8,11},{9,10},{10,... | collective-permute-start | bytes 36872 | tf_op jit(solution)/shard_map/ppermute | solution.py:34
  4.8 4.3 %collective-permute-start.2 = (f32[24,128]{1,0:T(8,128)S(1)}, f32[24,128]{1,0:T(8,128)S(1)}, u32[]{:S(2)}, u32[]{:S(2)}) collective-permute-start(f32[24,128]{1,0:T(8,128)S(1)} %fusion.2.own), channel_id=1, source_target_pairs={{0,7},{1,6},{2,5},{3,4},{4,3},{5,2},{6,1},{7,0},{8,15},{9,14},{10,... | collective-permute-start | bytes 36872 | tf_op jit(solution)/shard_map/ppermute | solution.py:34
  6.6 4.6 %collective-permute-start.1 = (f32[24,128]{1,0:T(8,128)S(1)}, f32[24,128]{1,0:T(8,128)S(1)}, u32[]{:S(2)}, u32[]{:S(2)}) collective-permute-start(f32[24,128]{1,0:T(8,128)S(1)} %fusion.2.own), channel_id=1, source_target_pairs={{0,5},{1,4},{2,7},{3,6},{4,1},{5,0},{6,3},{7,2},{8,13},{9,12},{10,... | collective-permute-start | bytes 36872 | tf_op jit(solution)/shard_map/ppermute | solution.py:34
  11.3 18.0 %copy-start = (bf16[16,1024,1,128]{3,1,2,0:T(8,128)(2,1)S(1)}, bf16[16,1024,1,128]{3,1,2,0:T(8,128)(2,1)}, u32[]{:S(2)}) copy-start(bf16[16,1024,1,128]{3,1,2,0:T(8,128)(2,1)} %param.15) | copy-start | bytes 12582916
  11.3 18.0 %copy-start.1 = (bf16[16,1024,1,128]{3,1,2,0:T(8,128)(2,1)S(1)}, bf16[16,1024,1,128]{3,1,2,0:T(8,128)(2,1)}, u32[]{:S(2)}) copy-start(bf16[16,1024,1,128]{3,1,2,0:T(8,128)(2,1)} %param.16) | copy-start | bytes 12582916
  11.4 4.6 %collective-permute-start.7 = (f32[16,640]{1,0:T(8,128)S(1)}, f32[16,640]{1,0:T(8,128)S(1)}, u32[]{:S(2)}, u32[]{:S(2)}) collective-permute-start(f32[16,640]{1,0:T(8,128)S(1)} %get-tuple-element.16), channel_id=1, source_target_pairs={{0,9},{1,8},{8,1},{9,0},{16,25},{17,24},{24,17},{25,16},{2,11},{3,... | collective-permute-start | bytes 122888 | tf_op jit(solution)/shard_map/ppermute | solution.py:34
  13.0 4.6 %collective-permute-start.6 = (f32[16,640]{1,0:T(8,128)S(1)}, f32[16,640]{1,0:T(8,128)S(1)}, u32[]{:S(2)}, u32[]{:S(2)}) collective-permute-start(f32[16,640]{1,0:T(8,128)S(1)} %get-tuple-element.16), channel_id=1, source_target_pairs={{0,25},{1,24},{8,17},{9,16},{16,9},{17,8},{24,1},{25,0},{2,27},{3,... | collective-permute-start | bytes 122888 | tf_op jit(solution)/shard_map/ppermute | solution.py:34
  14.9 5.0 %collective-permute-start.5 = (f32[16,640]{1,0:T(8,128)S(1)}, f32[16,640]{1,0:T(8,128)S(1)}, u32[]{:S(2)}, u32[]{:S(2)}) collective-permute-start(f32[16,640]{1,0:T(8,128)S(1)} %get-tuple-element.16), channel_id=1, source_target_pairs={{0,17},{1,16},{8,25},{9,24},{16,1},{17,0},{24,9},{25,8},{2,19},{3,... | collective-permute-start | bytes 122888 | tf_op jit(solution)/shard_map/ppermute | solution.py:34
  15.6 4.3 %collective-permute-start.4 = (f32[16,640]{1,0:T(8,128)S(1)}, f32[16,640]{1,0:T(8,128)S(1)}, u32[]{:S(2)}, u32[]{:S(2)}) collective-permute-start(f32[16,640]{1,0:T(8,128)S(1)} %get-tuple-element.16), channel_id=1, source_target_pairs={{0,1},{1,0},{2,3},{3,2},{4,5},{5,4},{6,7},{7,6},{8,9},{9,8},{10,11... | collective-permute-start | bytes 122888 | tf_op jit(solution)/shard_map/ppermute | solution.py:39
  20.0 5.7 %collective-permute-start.11 = (f32[16,640]{1,0:T(8,128)S(1)}, f32[16,640]{1,0:T(8,128)S(1)}, u32[]{:S(2)}, u32[]{:S(2)}) collective-permute-start(f32[16,640]{1,0:T(8,128)S(1)} %add_add_fusion), channel_id=1, source_target_pairs={{0,33},{1,32},{32,1},{33,0},{64,97},{65,96},{96,65},{97,64},{2,35}... | collective-permute-start | bytes 122888 | tf_op jit(solution)/shard_map/ppermute | solution.py:34
  21.9 4.6 %collective-permute-start.10 = (f32[16,640]{1,0:T(8,128)S(1)}, f32[16,640]{1,0:T(8,128)S(1)}, u32[]{:S(2)}, u32[]{:S(2)}) collective-permute-start(f32[16,640]{1,0:T(8,128)S(1)} %add_add_fusion), channel_id=1, source_target_pairs={{0,97},{1,96},{32,65},{33,64},{64,33},{65,32},{96,1},{97,0},{2,99}... | collective-permute-start | bytes 122888 | tf_op jit(solution)/shard_map/ppermute | solution.py:34
  24.2 5.0 %collective-permute-start.9 = (f32[16,640]{1,0:T(8,128)S(1)}, f32[16,640]{1,0:T(8,128)S(1)}, u32[]{:S(2)}, u32[]{:S(2)}) collective-permute-start(f32[16,640]{1,0:T(8,128)S(1)} %add_add_fusion), channel_id=1, source_target_pairs={{0,65},{1,64},{32,97},{33,96},{64,1},{65,0},{96,33},{97,32},{2,67}... | collective-permute-start | bytes 122888 | tf_op jit(solution)/shard_map/ppermute | solution.py:34
  25.3 4.0 %collective-permute-start.8 = (f32[16,640]{1,0:T(8,128)S(1)}, f32[16,640]{1,0:T(8,128)S(1)}, u32[]{:S(2)}, u32[]{:S(2)}) collective-permute-start(f32[16,640]{1,0:T(8,128)S(1)} %add_add_fusion), channel_id=1, source_target_pairs={{0,1},{1,0},{2,3},{3,2},{4,5},{5,4},{6,7},{7,6},{8,9},{9,8},{10,11... | collective-permute-start | bytes 122888 | tf_op jit(solution)/shard_map/ppermute | solution.py:39
  29.2 15.1 %copy-start.5 = (bf16[512,256]{1,0:T(8,128)(2,1)S(1)}, bf16[512,256]{1,0:T(8,128)(2,1)}, u32[]{:S(2)}) copy-start(bf16[512,256]{1,0:T(8,128)(2,1)} %weight.4) | copy-start | bytes 786436
  29.3 15.1 %copy-start.6 = (f32[4]{0:T(128)S(1)}, f32[4]{0:T(128)}, u32[]{:S(2)}) copy-start(f32[4]{0:T(128)} %param.17) | copy-start | bytes 52
  29.3 15.1 %copy-start.7 = (f32[128]{0:T(128)S(1)}, f32[128]{0:T(128)}, u32[]{:S(2)}) copy-start(f32[128]{0:T(128)} %param.18) | copy-start | bytes 1540
  29.3 22.6 %copy-start.2 = (bf16[256,1408]{1,0:T(8,128)(2,1)S(1)}, bf16[256,1408]{1,0:T(8,128)(2,1)}, u32[]{:S(2)}) copy-start(bf16[256,1408]{1,0:T(8,128)(2,1)} %gate.1) | copy-start | bytes 2162692
  29.3 22.6 %copy-start.3 = (bf16[256,1408]{1,0:T(8,128)(2,1)S(1)}, bf16[256,1408]{1,0:T(8,128)(2,1)}, u32[]{:S(2)}) copy-start(bf16[256,1408]{1,0:T(8,128)(2,1)} %up.1) | copy-start | bytes 2162692
  29.3 38.7 %copy-start.4 = (bf16[1408,256]{1,0:T(8,128)(2,1)S(1)}, bf16[1408,256]{1,0:T(8,128)(2,1)}, u32[]{:S(2)}) copy-start(bf16[1408,256]{1,0:T(8,128)(2,1)} %weight.5) | copy-start | bytes 2162692
  31.1 6.3 %collective-permute-start.12 = (f32[136,128]{1,0:T(8,128)S(1)}, f32[136,128]{1,0:T(8,128)S(1)}, u32[]{:S(2)}, u32[]{:S(2)}) collective-permute-start(f32[136,128]{1,0:T(8,128)S(1)} %get-tuple-element.17), channel_id=1, source_target_pairs={{0,1},{1,0},{2,3},{3,2},{4,5},{5,4},{6,7},{7,6},{8,9},{9,8},{10,11... | collective-permute-start | bytes 208904 | tf_op jit(solution)/shard_map/ppermute | solution.py:39
  31.5 3.6 %collective-permute-start.15 = (bf16[144,128]{1,0:T(8,128)(2,1)S(1)}, bf16[144,128]{1,0:T(8,128)(2,1)S(1)}, u32[]{:S(2)}, u32[]{:S(2)}) collective-permute-start(bf16[144,128]{1,0:T(8,128)(2,1)S(1)} %get-tuple-element.18), channel_id=1, source_target_pairs={{0,9},{1,8},{8,1},{9,0},{16,25},{17,24},{24,17},{25,16},{2,11},{3,... | collective-permute-start | bytes 110600 | tf_op jit(solution)/shard_map/ppermute | solution.py:34
  31.9 4.9 %collective-permute-start.14 = (bf16[144,128]{1,0:T(8,128)(2,1)S(1)}, bf16[144,128]{1,0:T(8,128)(2,1)S(1)}, u32[]{:S(2)}, u32[]{:S(2)}) collective-permute-start(bf16[144,128]{1,0:T(8,128)(2,1)S(1)} %get-tuple-element.18), channel_id=1, source_target_pairs={{0,25},{1,24},{8,17},{9,16},{16,9},{17,8},{24,1},{25,0},{2,27},{3,... | collective-permute-start | bytes 110600 | tf_op jit(solution)/shard_map/ppermute | solution.py:34
  32.4 5.0 %collective-permute-start.13 = (bf16[144,128]{1,0:T(8,128)(2,1)S(1)}, bf16[144,128]{1,0:T(8,128)(2,1)S(1)}, u32[]{:S(2)}, u32[]{:S(2)}) collective-permute-start(bf16[144,128]{1,0:T(8,128)(2,1)S(1)} %get-tuple-element.18), channel_id=1, source_target_pairs={{0,17},{1,16},{8,25},{9,24},{16,1},{17,0},{24,9},{25,8},{2,19},{3,... | collective-permute-start | bytes 110600 | tf_op jit(solution)/shard_map/ppermute | solution.py:34
  37.6 6.7 %collective-permute-start.16 = (f32[136,128]{1,0:T(8,128)S(1)}, f32[136,128]{1,0:T(8,128)S(1)}, u32[]{:S(2)}, u32[]{:S(2)}) collective-permute-start(f32[136,128]{1,0:T(8,128)S(1)} %get-tuple-element.19), channel_id=1, source_target_pairs={{0,1},{1,0},{2,3},{3,2},{4,5},{5,4},{6,7},{7,6},{8,9},{9,8},{10,11... | collective-permute-start | bytes 208904 | tf_op jit(solution)/shard_map/ppermute | solution.py:39
  38.1 3.6 %collective-permute-start.19 = (bf16[144,128]{1,0:T(8,128)(2,1)S(1)}, bf16[144,128]{1,0:T(8,128)(2,1)S(1)}, u32[]{:S(2)}, u32[]{:S(2)}) collective-permute-start(bf16[144,128]{1,0:T(8,128)(2,1)S(1)} %get-tuple-element.20), channel_id=1, source_target_pairs={{0,33},{1,32},{32,1},{33,0},{64,97},{65,96},{96,65},{97,64},{2,35}... | collective-permute-start | bytes 110600 | tf_op jit(solution)/shard_map/ppermute | solution.py:34
  38.9 4.6 %collective-permute-start.18 = (bf16[144,128]{1,0:T(8,128)(2,1)S(1)}, bf16[144,128]{1,0:T(8,128)(2,1)S(1)}, u32[]{:S(2)}, u32[]{:S(2)}) collective-permute-start(bf16[144,128]{1,0:T(8,128)(2,1)S(1)} %get-tuple-element.20), channel_id=1, source_target_pairs={{0,97},{1,96},{32,65},{33,64},{64,33},{65,32},{96,1},{97,0},{2,99}... | collective-permute-start | bytes 110600 | tf_op jit(solution)/shard_map/ppermute | solution.py:34
  39.5 4.9 %collective-permute-start.17 = (bf16[144,128]{1,0:T(8,128)(2,1)S(1)}, bf16[144,128]{1,0:T(8,128)(2,1)S(1)}, u32[]{:S(2)}, u32[]{:S(2)}) collective-permute-start(bf16[144,128]{1,0:T(8,128)(2,1)S(1)} %get-tuple-element.20), channel_id=1, source_target_pairs={{0,65},{1,64},{32,97},{33,96},{64,1},{65,0},{96,33},{97,32},{2,67}... | collective-permute-start | bytes 110600 | tf_op jit(solution)/shard_map/ppermute | solution.py:34
  44.9 3.8 %collective-permute-start.22 = (bf16[16,256]{1,0:T(8,128)(2,1)S(1)}, bf16[16,256]{1,0:T(8,128)(2,1)S(1)}, u32[]{:S(2)}, u32[]{:S(2)}) collective-permute-start(bf16[16,256]{1,0:T(8,128)(2,1)S(1)} %shard_map.122), channel_id=1, source_target_pairs={{0,3},{1,2},{2,1},{3,0},{4,7},{5,6},{6,5},{7,4},{8,11},{9,10},{10,... | collective-permute-start | bytes 24584 | tf_op jit(solution)/shard_map/ppermute | solution.py:34
  45.5 4.3 %collective-permute-start.21 = (bf16[16,256]{1,0:T(8,128)(2,1)S(1)}, bf16[16,256]{1,0:T(8,128)(2,1)S(1)}, u32[]{:S(2)}, u32[]{:S(2)}) collective-permute-start(bf16[16,256]{1,0:T(8,128)(2,1)S(1)} %shard_map.122), channel_id=1, source_target_pairs={{0,7},{1,6},{2,5},{3,4},{4,3},{5,2},{6,1},{7,0},{8,15},{9,14},{10,... | collective-permute-start | bytes 24584 | tf_op jit(solution)/shard_map/ppermute | solution.py:34
  46.1 4.6 %collective-permute-start.20 = (bf16[16,256]{1,0:T(8,128)(2,1)S(1)}, bf16[16,256]{1,0:T(8,128)(2,1)S(1)}, u32[]{:S(2)}, u32[]{:S(2)}) collective-permute-start(bf16[16,256]{1,0:T(8,128)(2,1)S(1)} %shard_map.122), channel_id=1, source_target_pairs={{0,5},{1,4},{2,7},{3,6},{4,1},{5,0},{6,3},{7,2},{8,13},{9,12},{10,... | collective-permute-start | bytes 24584 | tf_op jit(solution)/shard_map/ppermute | solution.py:34
  50.7 1.3 %collective-permute-start.23 = (f32[16,256]{1,0:T(8,128)S(1)}, f32[16,256]{1,0:T(8,128)S(1)}, u32[]{:S(2)}, u32[]{:S(2)}) collective-permute-start(f32[16,256]{1,0:T(8,128)S(1)} %convert_add_fusion.1.attn), channel_id=1, source_target_pairs={{0,1},{1,0},{2,3},{3,2},{4,5},{5,4},{6,7},{7,6},{8,9},{9,8},{10,11... | collective-permute-start | bytes 49160 | tf_op jit(solution)/shard_map/ppermute | solution.py:39
  52.2 4.1 %collective-permute-start.26 = (bf16[16,2944]{1,0:T(8,128)(2,1)S(1)}, bf16[16,2944]{1,0:T(8,128)(2,1)S(1)}, u32[]{:S(2)}, u32[]{:S(2)}) collective-permute-start(bf16[16,2944]{1,0:T(8,128)(2,1)S(1)} %get-tuple-element.24), channel_id=1, source_target_pairs={{0,8},{8,0},{16,24},{24,16},{1,9},{9,1},{17,25},{25,17},{2,10},{10... | collective-permute-start | bytes 282632 | tf_op jit(solution)/shard_map/ppermute | solution.py:34
  53.0 4.6 %collective-permute-start.25 = (bf16[16,2944]{1,0:T(8,128)(2,1)S(1)}, bf16[16,2944]{1,0:T(8,128)(2,1)S(1)}, u32[]{:S(2)}, u32[]{:S(2)}) collective-permute-start(bf16[16,2944]{1,0:T(8,128)(2,1)S(1)} %get-tuple-element.24), channel_id=1, source_target_pairs={{0,24},{8,16},{16,8},{24,0},{1,25},{9,17},{17,9},{25,1},{2,26},{10... | collective-permute-start | bytes 282632 | tf_op jit(solution)/shard_map/ppermute | solution.py:34
  55.0 4.9 %collective-permute-start.24 = (bf16[16,2944]{1,0:T(8,128)(2,1)S(1)}, bf16[16,2944]{1,0:T(8,128)(2,1)S(1)}, u32[]{:S(2)}, u32[]{:S(2)}) collective-permute-start(bf16[16,2944]{1,0:T(8,128)(2,1)S(1)} %get-tuple-element.24), channel_id=1, source_target_pairs={{0,16},{8,24},{16,0},{24,8},{1,17},{9,25},{17,1},{25,9},{2,18},{10... | collective-permute-start | bytes 282632 | tf_op jit(solution)/shard_map/ppermute | solution.py:34
  60.0 3.5 %collective-permute-start.29 = (bf16[16,2944]{1,0:T(8,128)(2,1)S(1)}, bf16[16,2944]{1,0:T(8,128)(2,1)S(1)}, u32[]{:S(2)}, u32[]{:S(2)}) collective-permute-start(bf16[16,2944]{1,0:T(8,128)(2,1)S(1)} %get-tuple-element.26), channel_id=1, source_target_pairs={{0,32},{32,0},{64,96},{96,64},{1,33},{33,1},{65,97},{97,65},{2,34}... | collective-permute-start | bytes 282632 | tf_op jit(solution)/shard_map/ppermute | solution.py:34
  60.2 4.6 %collective-permute-start.28 = (bf16[16,2944]{1,0:T(8,128)(2,1)S(1)}, bf16[16,2944]{1,0:T(8,128)(2,1)S(1)}, u32[]{:S(2)}, u32[]{:S(2)}) collective-permute-start(bf16[16,2944]{1,0:T(8,128)(2,1)S(1)} %get-tuple-element.26), channel_id=1, source_target_pairs={{0,96},{32,64},{64,32},{96,0},{1,97},{33,65},{65,33},{97,1},{2,98}... | collective-permute-start | bytes 282632 | tf_op jit(solution)/shard_map/ppermute | solution.py:34
  62.5 5.5 %collective-permute-start.27 = (bf16[16,2944]{1,0:T(8,128)(2,1)S(1)}, bf16[16,2944]{1,0:T(8,128)(2,1)S(1)}, u32[]{:S(2)}, u32[]{:S(2)}) collective-permute-start(bf16[16,2944]{1,0:T(8,128)(2,1)S(1)} %get-tuple-element.26), channel_id=1, source_target_pairs={{0,64},{32,96},{64,0},{96,32},{1,65},{33,97},{65,1},{97,33},{2,66}... | collective-permute-start | bytes 282632 | tf_op jit(solution)/shard_map/ppermute | solution.py:34
  68.4 6.4 %collective-permute-start.32 = (bf16[16,256]{1,0:T(8,128)(2,1)S(1)}, bf16[16,256]{1,0:T(8,128)(2,1)S(1)}, u32[]{:S(2)}, u32[]{:S(2)}) collective-permute-start(bf16[16,256]{1,0:T(8,128)(2,1)S(1)} %shard_map.125), channel_id=1, source_target_pairs={{0,3},{1,2},{2,1},{3,0},{4,7},{5,6},{6,5},{7,4},{8,11},{9,10},{10,... | collective-permute-start | bytes 24584 | tf_op jit(solution)/shard_map/ppermute | solution.py:34
  72.3 4.3 %collective-permute-start.31 = (bf16[16,256]{1,0:T(8,128)(2,1)S(1)}, bf16[16,256]{1,0:T(8,128)(2,1)S(1)}, u32[]{:S(2)}, u32[]{:S(2)}) collective-permute-start(bf16[16,256]{1,0:T(8,128)(2,1)S(1)} %shard_map.125), channel_id=1, source_target_pairs={{0,7},{1,6},{2,5},{3,4},{4,3},{5,2},{6,1},{7,0},{8,15},{9,14},{10,... | collective-permute-start | bytes 24584 | tf_op jit(solution)/shard_map/ppermute | solution.py:34
  73.6 4.6 %collective-permute-start.30 = (bf16[16,256]{1,0:T(8,128)(2,1)S(1)}, bf16[16,256]{1,0:T(8,128)(2,1)S(1)}, u32[]{:S(2)}, u32[]{:S(2)}) collective-permute-start(bf16[16,256]{1,0:T(8,128)(2,1)S(1)} %shard_map.125), channel_id=1, source_target_pairs={{0,5},{1,4},{2,7},{3,6},{4,1},{5,0},{6,3},{7,2},{8,13},{9,12},{10,... | collective-permute-start | bytes 24584 | tf_op jit(solution)/shard_map/ppermute | solution.py:34
  78.2 1.8 %collective-permute-start.33 = (f32[16,256]{1,0:T(8,128)S(1)}, f32[16,256]{1,0:T(8,128)S(1)}, u32[]{:S(2)}, u32[]{:S(2)}) collective-permute-start(f32[16,256]{1,0:T(8,128)S(1)} %convert_add_fusion), channel_id=1, source_target_pairs={{0,1},{1,0},{2,3},{3,2},{4,5},{5,4},{6,7},{7,6},{8,9},{9,8},{10,11... | collective-permute-start | bytes 49160 | tf_op jit(solution)/shard_map/ppermute | solution.py:39

commit v8 on v7

--- a/solution.py
+++ b/solution.py
@@ -26,12 +26,31 @@
 
 
 def peers(shard, axis, what):
+    if what in STRAIGHT:
+        return kv_peers(shard, axis, what)
     across, wide = (axis, 1) if what in STRAIGHT else ((axis, TP[1]), 2)
     n = lax.axis_size(across)
     got = []
     for s in SHIFTS:
         pairs = [(i, i ^ (wide * s + wide - 1)) for i in range(n)]
         got.append(lax.ppermute(shard, across, pairs))
+    return got
+
+
+def kv_peers(shard, axis, what):
+    n = lax.axis_size(KV[0])
+    got = []
+    for s in SHIFTS:
+        pairs = []
+        for z in range(n):
+            for y in range(n):
+                for c in range(2):
+                    straight = what in STRAIGHT
+                    inner = c == 0 if not straight or axis == KV[1] else c == 1
+                    to_z, to_y = (z, y ^ s) if inner else (z ^ s, y)
+                    to_c = c if straight else 1 - c
+                    pairs.append(((z * n + y) * 2 + c, (to_z * n + to_y) * 2 + to_c))
+        got.append(lax.ppermute(shard, (*KV, TP[1]), pairs))
     return got
 
 

time: 80.8 us -> 80.8 us (level)
  starting transfers between devices: 42.2 us -> 43.1 us
    ppermute x27 -> x21, waiting for transfers between devices: 30.6 us -> 22 us  [peers(): got.append(lax.ppermute(shard, across, pairs))]
    ppermute x0 -> x6, waiting for transfers between devices: none -> 7.77 us  [kv_peers(): got.append(lax.ppermute(shard, (*KV, TP[1]), pairs))]
    ppermute x0 -> x6, starting transfers between devices: none -> 7.27 us  [kv_peers(): got.append(lax.ppermute(shard, (*KV, TP[1]), pairs))]
    ppermute x27 -> x21, starting transfers between devices: 38 us -> 31.6 us  [peers(): got.append(lax.ppermute(shard, across, pairs))]
where the time goes in v8:
time: 80.8 us; the launch traced here: 80.7 us
  starting transfers between devices  43.1 us (53%)
  waiting for transfers between devices  32.4 us (40%)
  Pallas kernels  4.32 us (5%)
    ppermute x21, starting transfers between devices, peers(): got.append(lax.ppermute(shard, across, pairs))  31.6 us
    ppermute x21, waiting for transfers between devices, peers(): got.append(lax.ppermute(shard, across, pairs))  22 us
    ppermute x6, waiting for transfers between devices, kv_peers(): got.append(lax.ppermute(shard, (*KV, TP[1]), pairs))  7.77 us
    ppermute x6, starting transfers between devices, kv_peers(): got.append(lax.ppermute(shard, (*KV, TP[1]), pairs))  7.27 us
    ppermute x7, starting transfers between devices, partner(): return lax.ppermute(shard, TP[1], [(0, 1), (1, 0)])  4.25 us
    ppermute x7, waiting for transfers between devices, partner(): return lax.ppermute(shard, TP[1], [(0, 1), (1, 0)])  2.63 us
    pallas_call x1, Pallas kernels, per_device(): kernel_call(attend_body, states, [pltpu.VMEM((heads * batch, LANES), F32)...  1.77 us
  transfers between devices with their start and end apart: 34, of which 22 were waited for; matrix products, arithmetic and copies ran while one was open for 0% of the time, Pallas kernels for 0%

profile of v8, /device:TPU:1, one launch (start us, length us, event | category | flops | bytes accessed | tf_op | source)
XLA Modules:
  0.0 80.7 jit_solution(12244924696295714923)
XLA Ops:
  0.0 0.8 %shard_map.118 = f32[24,128]{1,0:T(8,128)S(1)} custom-call(bf16[16,32]{1,0:T(8,128)(2,1)} %hidden.1, f32[1,32]{1,0:T(1,128)} %bitcast.12), custom_call_target="tpu_custom_call" | custom-call | flops 1099511627776 | bytes 1099511627776 | tf_op jit(solution)/shard_map/pallas_call | solution.py:297
  0.8 1.5 %collective-permute-start = (f32[24,128]{1,0:T(8,128)S(1)}, f32[24,128]{1,0:T(8,128)S(1)}, u32[]{:S(2)}, u32[]{:S(2)}) collective-permute-start(f32[24,128]{1,0:T(8,128)S(1)} %shard_map.118), channel_id=1, source_target_pairs={{0,1},{1,0},{2,3},{3,2},{4,5},{5,4},{6,7},{7,6},{8,9},{9,8},{10,11... | collective-permute-start | bytes 36872 | tf_op jit(solution)/shard_map/ppermute | solution.py:58
  2.3 0.8 %collective-permute-done = f32[24,128]{1,0:T(8,128)S(1)} collective-permute-done((f32[24,128]{1,0:T(8,128)S(1)}, f32[24,128]{1,0:T(8,128)S(1)}, u32[]{:S(2)}, u32[]{:S(2)}) %collective-permute-start) | collective-permute-done | bytes 12320 | tf_op jit(solution)/shard_map/ppermute | solution.py:58
  3.1 1.6 %collective-permute-start.3 = (f32[24,128]{1,0:T(8,128)S(1)}, f32[24,128]{1,0:T(8,128)S(1)}, u32[]{:S(2)}, u32[]{:S(2)}) collective-permute-start(f32[24,128]{1,0:T(8,128)S(1)} %fusion.2.own), channel_id=1, source_target_pairs={{0,3},{1,2},{2,1},{3,0},{4,7},{5,6},{6,5},{7,4},{8,11},{9,10},{10,... | collective-permute-start | bytes 36872 | tf_op jit(solution)/shard_map/ppermute | solution.py:36
  4.8 1.9 %collective-permute-start.2 = (f32[24,128]{1,0:T(8,128)S(1)}, f32[24,128]{1,0:T(8,128)S(1)}, u32[]{:S(2)}, u32[]{:S(2)}) collective-permute-start(f32[24,128]{1,0:T(8,128)S(1)} %fusion.2.own), channel_id=1, source_target_pairs={{0,7},{1,6},{2,5},{3,4},{4,3},{5,2},{6,1},{7,0},{8,15},{9,14},{10,... | collective-permute-start | bytes 36872 | tf_op jit(solution)/shard_map/ppermute | solution.py:36
  6.6 0.6 collective-permute-start.1
  7.3 1.8 %collective-permute-done.2.b = f32[24,128]{1,0:T(8,128)S(1)} collective-permute-done((f32[24,128]{1,0:T(8,128)S(1)}, f32[24,128]{1,0:T(8,128)S(1)}, u32[]{:S(2)}, u32[]{:S(2)}) %collective-permute-start.2) | collective-permute-done | bytes 12320 | tf_op jit(solution)/shard_map/ppermute | solution.py:36
  9.1 2.2 %collective-permute-done.1.a = f32[24,128]{1,0:T(8,128)S(1)} collective-permute-done((f32[24,128]{1,0:T(8,128)S(1)}, f32[24,128]{1,0:T(8,128)S(1)}, u32[]{:S(2)}, u32[]{:S(2)}) %collective-permute-start.1) | collective-permute-done | bytes 12320 | tf_op jit(solution)/shard_map/ppermute | solution.py:36
  11.4 1.5 %collective-permute-start.7 = (f32[16,640]{1,0:T(8,128)S(1)}, f32[16,640]{1,0:T(8,128)S(1)}, u32[]{:S(2)}, u32[]{:S(2)}) collective-permute-start(f32[16,640]{1,0:T(8,128)S(1)} %get-tuple-element.16), channel_id=1, source_target_pairs={{0,9},{1,8},{8,1},{9,0},{16,25},{17,24},{24,17},{25,16},{2,11},{3,... | collective-permute-start | bytes 122888 | tf_op jit(solution)/shard_map/ppermute | solution.py:36
  13.0 2.0 %collective-permute-start.6 = (f32[16,640]{1,0:T(8,128)S(1)}, f32[16,640]{1,0:T(8,128)S(1)}, u32[]{:S(2)}, u32[]{:S(2)}) collective-permute-start(f32[16,640]{1,0:T(8,128)S(1)} %get-tuple-element.16), channel_id=1, source_target_pairs={{0,25},{1,24},{8,17},{9,16},{16,9},{17,8},{24,1},{25,0},{2,27},{3,... | collective-permute-start | bytes 122888 | tf_op jit(solution)/shard_map/ppermute | solution.py:36
  14.9 0.7 collective-permute-start.5
  15.6 0.3 collective-permute-start.4
  16.0 1.6 %collective-permute-done.6 = f32[16,640]{1,0:T(8,128)S(1)} collective-permute-done((f32[16,640]{1,0:T(8,128)S(1)}, f32[16,640]{1,0:T(8,128)S(1)}, u32[]{:S(2)}, u32[]{:S(2)}) %collective-permute-start.6) | collective-permute-done | bytes 40992 | tf_op jit(solution)/shard_map/ppermute | solution.py:36
  17.6 2.3 %collective-permute-done.5 = f32[16,640]{1,0:T(8,128)S(1)} collective-permute-done((f32[16,640]{1,0:T(8,128)S(1)}, f32[16,640]{1,0:T(8,128)S(1)}, u32[]{:S(2)}, u32[]{:S(2)}) %collective-permute-start.5) | collective-permute-done | bytes 40992 | tf_op jit(solution)/shard_map/ppermute | solution.py:36
  20.0 1.9 %collective-permute-start.11 = (f32[16,640]{1,0:T(8,128)S(1)}, f32[16,640]{1,0:T(8,128)S(1)}, u32[]{:S(2)}, u32[]{:S(2)}) collective-permute-start(f32[16,640]{1,0:T(8,128)S(1)} %add_add_fusion), channel_id=1, source_target_pairs={{0,33},{1,32},{32,1},{33,0},{64,97},{65,96},{96,65},{97,64},{2,35}... | collective-permute-start | bytes 122888 | tf_op jit(solution)/shard_map/ppermute | solution.py:36
  21.9 2.3 %collective-permute-start.10 = (f32[16,640]{1,0:T(8,128)S(1)}, f32[16,640]{1,0:T(8,128)S(1)}, u32[]{:S(2)}, u32[]{:S(2)}) collective-permute-start(f32[16,640]{1,0:T(8,128)S(1)} %add_add_fusion), channel_id=1, source_target_pairs={{0,97},{1,96},{32,65},{33,64},{64,33},{65,32},{96,1},{97,0},{2,99}... | collective-permute-start | bytes 122888 | tf_op jit(solution)/shard_map/ppermute | solution.py:36
  24.2 1.1 %collective-permute-start.9 = (f32[16,640]{1,0:T(8,128)S(1)}, f32[16,640]{1,0:T(8,128)S(1)}, u32[]{:S(2)}, u32[]{:S(2)}) collective-permute-start(f32[16,640]{1,0:T(8,128)S(1)} %add_add_fusion), channel_id=1, source_target_pairs={{0,65},{1,64},{32,97},{33,96},{64,1},{65,0},{96,33},{97,32},{2,67}... | collective-permute-start | bytes 122888 | tf_op jit(solution)/shard_map/ppermute | solution.py:36
  25.3 0.3 collective-permute-start.8
  25.6 0.9 %collective-permute-done.10.b = f32[16,640]{1,0:T(8,128)S(1)} collective-permute-done((f32[16,640]{1,0:T(8,128)S(1)}, f32[16,640]{1,0:T(8,128)S(1)}, u32[]{:S(2)}, u32[]{:S(2)}) %collective-permute-start.10) | collective-permute-done | bytes 40992 | tf_op jit(solution)/shard_map/ppermute | solution.py:36
  26.5 2.7 %collective-permute-done.9.a = f32[16,640]{1,0:T(8,128)S(1)} collective-permute-done((f32[16,640]{1,0:T(8,128)S(1)}, f32[16,640]{1,0:T(8,128)S(1)}, u32[]{:S(2)}, u32[]{:S(2)}) %collective-permute-start.9) | collective-permute-done | bytes 40992 | tf_op jit(solution)/shard_map/ppermute | solution.py:36
  29.3 1.8 %shard_map.120 = (f32[136,128]{1,0:T(8,128)S(1)}, bf16[144,128]{1,0:T(8,128)(2,1)S(1)}) custom-call(f32[16,640]{1,0:T(8,128)S(1)} %collective-permute-done.8.own, f32[16,640]{1,0:T(8,128)S(1)} %collective-permute-done.9.a, f32[16,640]{1,0:T(8,128)S(1)} %collective-permute-done.10.b, f32[16,640]{1,0:T(8,128)S(1)} %collective-permute-done.11.c, ...), custom_call_target="tpu_custom_call" | custom-call | tf_op jit(solution)/shard_map/pallas_call | solution.py:326
  31.1 0.4 collective-permute-start.12
  31.5 0.4 collective-permute-start.15
  31.9 0.4 collective-permute-start.14
  32.4 2.7 %collective-permute-start.13 = (bf16[144,128]{1,0:T(8,128)(2,1)S(1)}, bf16[144,128]{1,0:T(8,128)(2,1)S(1)}, u32[]{:S(2)}, u32[]{:S(2)}) collective-permute-start(bf16[144,128]{1,0:T(8,128)(2,1)S(1)} %get-tuple-element.18), channel_id=1, source_target_pairs={{0,17},{1,16},{8,25},{9,24},{16,1},{17,0},{24,9},{25,8},{2,19},{3,... | collective-permute-start | bytes 110600 | tf_op jit(solution)/shard_map/ppermute | solution.py:36
  35.1 1.8 %collective-permute-done.14.b = bf16[144,128]{1,0:T(8,128)(2,1)S(1)} collective-permute-done((bf16[144,128]{1,0:T(8,128)(2,1)S(1)}, bf16[144,128]{1,0:T(8,128)(2,1)S(1)}, u32[]{:S(2)}, u32[]{:S(2)}) %collective-permute-start.14) | collective-permute-done | bytes 36896 | tf_op jit(solution)/shard_map/ppermute | solution.py:36
  36.9 0.5 collective-permute-done.13.a
  37.4 0.3 shard_map.121
  37.6 0.4 collective-permute-start.16
  38.1 0.8 collective-permute-start.19
  38.9 0.6 collective-permute-start.18
  39.5 2.2 %collective-permute-start.17 = (bf16[144,128]{1,0:T(8,128)(2,1)S(1)}, bf16[144,128]{1,0:T(8,128)(2,1)S(1)}, u32[]{:S(2)}, u32[]{:S(2)}) collective-permute-start(bf16[144,128]{1,0:T(8,128)(2,1)S(1)} %get-tuple-element.20), channel_id=1, source_target_pairs={{0,65},{1,64},{32,97},{33,96},{64,1},{65,0},{96,33},{97,32},{2,67}... | collective-permute-start | bytes 110600 | tf_op jit(solution)/shard_map/ppermute | solution.py:36
  41.7 1.8 %collective-permute-done.18.b = bf16[144,128]{1,0:T(8,128)(2,1)S(1)} collective-permute-done((bf16[144,128]{1,0:T(8,128)(2,1)S(1)}, bf16[144,128]{1,0:T(8,128)(2,1)S(1)}, u32[]{:S(2)}, u32[]{:S(2)}) %collective-permute-start.18) | collective-permute-done | bytes 36896 | tf_op jit(solution)/shard_map/ppermute | solution.py:36
  43.5 0.9 %collective-permute-done.17.a = bf16[144,128]{1,0:T(8,128)(2,1)S(1)} collective-permute-done((bf16[144,128]{1,0:T(8,128)(2,1)S(1)}, bf16[144,128]{1,0:T(8,128)(2,1)S(1)}, u32[]{:S(2)}, u32[]{:S(2)}) %collective-permute-start.17) | collective-permute-done | bytes 36896 | tf_op jit(solution)/shard_map/ppermute | solution.py:36
  44.4 0.5 shard_map.122
  44.9 0.5 collective-permute-start.22
  45.5 0.6 collective-permute-start.21
  46.1 2.6 %collective-permute-start.20 = (bf16[16,256]{1,0:T(8,128)(2,1)S(1)}, bf16[16,256]{1,0:T(8,128)(2,1)S(1)}, u32[]{:S(2)}, u32[]{:S(2)}) collective-permute-start(bf16[16,256]{1,0:T(8,128)(2,1)S(1)} %shard_map.122), channel_id=1, source_target_pairs={{0,5},{1,4},{2,7},{3,6},{4,1},{5,0},{6,3},{7,2},{8,13},{9,12},{10,... | collective-permute-start | bytes 24584 | tf_op jit(solution)/shard_map/ppermute | solution.py:36
  48.7 1.1 %collective-permute-done.21 = bf16[16,256]{1,0:T(8,128)(2,1)S(1)} collective-permute-done((bf16[16,256]{1,0:T(8,128)(2,1)S(1)}, bf16[16,256]{1,0:T(8,128)(2,1)S(1)}, u32[]{:S(2)}, u32[]{:S(2)}) %collective-permute-start.21) | collective-permute-done | bytes 8224 | tf_op jit(solution)/shard_map/ppermute | solution.py:36
  49.7 0.9 %collective-permute-done.20 = bf16[16,256]{1,0:T(8,128)(2,1)S(1)} collective-permute-done((bf16[16,256]{1,0:T(8,128)(2,1)S(1)}, bf16[16,256]{1,0:T(8,128)(2,1)S(1)}, u32[]{:S(2)}, u32[]{:S(2)}) %collective-permute-start.20) | collective-permute-done | bytes 8224 | tf_op jit(solution)/shard_map/ppermute | solution.py:36
  50.7 0.3 collective-permute-start.23
  51.0 1.0 %collective-permute-done.23.other = f32[16,256]{1,0:T(8,128)S(1)} collective-permute-done((f32[16,256]{1,0:T(8,128)S(1)}, f32[16,256]{1,0:T(8,128)S(1)}, u32[]{:S(2)}, u32[]{:S(2)}) %collective-permute-start.23) | collective-permute-done | bytes 16416 | tf_op jit(solution)/shard_map/ppermute | solution.py:58
  51.9 0.3 shard_map.123
  52.2 0.2 collective-permute-start.26
  52.5 2.2 %collective-permute-start.25 = (bf16[16,2944]{1,0:T(8,128)(2,1)S(1)}, bf16[16,2944]{1,0:T(8,128)(2,1)S(1)}, u32[]{:S(2)}, u32[]{:S(2)}) collective-permute-start(bf16[16,2944]{1,0:T(8,128)(2,1)S(1)} %get-tuple-element.24), channel_id=1, source_target_pairs={{0,24},{1,97},{8,16},{9,105},{16,8},{17,113},{24,0},{25,121},{32,5... | collective-permute-start | bytes 282632 | tf_op jit(solution)/shard_map/ppermute | solution.py:53
  54.6 1.1 %collective-permute-start.24 = (bf16[16,2944]{1,0:T(8,128)(2,1)S(1)}, bf16[16,2944]{1,0:T(8,128)(2,1)S(1)}, u32[]{:S(2)}, u32[]{:S(2)}) collective-permute-start(bf16[16,2944]{1,0:T(8,128)(2,1)S(1)} %get-tuple-element.24), channel_id=1, source_target_pairs={{0,16},{1,65},{8,24},{9,73},{16,0},{17,81},{24,8},{25,89},{32,48},... | collective-permute-start | bytes 282632 | tf_op jit(solution)/shard_map/ppermute | solution.py:53
  55.7 0.3 collective-permute-done.26.c
  56.0 1.1 %collective-permute-done.25.b = bf16[16,2944]{1,0:T(8,128)(2,1)S(1)} collective-permute-done((bf16[16,2944]{1,0:T(8,128)(2,1)S(1)}, bf16[16,2944]{1,0:T(8,128)(2,1)S(1)}, u32[]{:S(2)}, u32[]{:S(2)}) %collective-permute-start.25) | collective-permute-done | bytes 94240 | tf_op jit(solution)/shard_map/ppermute | solution.py:53
  57.1 2.5 %collective-permute-done.24.a = bf16[16,2944]{1,0:T(8,128)(2,1)S(1)} collective-permute-done((bf16[16,2944]{1,0:T(8,128)(2,1)S(1)}, bf16[16,2944]{1,0:T(8,128)(2,1)S(1)}, u32[]{:S(2)}, u32[]{:S(2)}) %collective-permute-start.24) | collective-permute-done | bytes 94240 | tf_op jit(solution)/shard_map/ppermute | solution.py:53
  59.6 0.2 shard_map.124
  59.7 0.9 %collective-permute-start.29 = (bf16[16,2944]{1,0:T(8,128)(2,1)S(1)}, bf16[16,2944]{1,0:T(8,128)(2,1)S(1)}, u32[]{:S(2)}, u32[]{:S(2)}) collective-permute-start(bf16[16,2944]{1,0:T(8,128)(2,1)S(1)} %get-tuple-element.26), channel_id=1, source_target_pairs={{0,32},{1,9},{8,40},{9,1},{16,48},{17,25},{24,56},{25,17},{32,0},{... | collective-permute-start | bytes 282632 | tf_op jit(solution)/shard_map/ppermute | solution.py:53
  60.6 1.9 %collective-permute-start.28 = (bf16[16,2944]{1,0:T(8,128)(2,1)S(1)}, bf16[16,2944]{1,0:T(8,128)(2,1)S(1)}, u32[]{:S(2)}, u32[]{:S(2)}) collective-permute-start(bf16[16,2944]{1,0:T(8,128)(2,1)S(1)} %get-tuple-element.26), channel_id=1, source_target_pairs={{0,96},{1,25},{8,104},{9,17},{16,112},{17,9},{24,120},{25,1},{32,6... | collective-permute-start | bytes 282632 | tf_op jit(solution)/shard_map/ppermute | solution.py:53
  62.5 1.0 %collective-permute-start.27 = (bf16[16,2944]{1,0:T(8,128)(2,1)S(1)}, bf16[16,2944]{1,0:T(8,128)(2,1)S(1)}, u32[]{:S(2)}, u32[]{:S(2)}) collective-permute-start(bf16[16,2944]{1,0:T(8,128)(2,1)S(1)} %get-tuple-element.26), channel_id=1, source_target_pairs={{0,64},{1,17},{8,72},{9,25},{16,80},{17,1},{24,88},{25,9},{32,96},... | collective-permute-start | bytes 282632 | tf_op jit(solution)/shard_map/ppermute | solution.py:53
  63.5 1.7 %collective-permute-done.28.b = bf16[16,2944]{1,0:T(8,128)(2,1)S(1)} collective-permute-done((bf16[16,2944]{1,0:T(8,128)(2,1)S(1)}, bf16[16,2944]{1,0:T(8,128)(2,1)S(1)}, u32[]{:S(2)}, u32[]{:S(2)}) %collective-permute-start.28) | collective-permute-done | bytes 94240 | tf_op jit(solution)/shard_map/ppermute | solution.py:53
  65.3 2.2 %collective-permute-done.27.a = bf16[16,2944]{1,0:T(8,128)(2,1)S(1)} collective-permute-done((bf16[16,2944]{1,0:T(8,128)(2,1)S(1)}, bf16[16,2944]{1,0:T(8,128)(2,1)S(1)}, u32[]{:S(2)}, u32[]{:S(2)}) %collective-permute-start.27) | collective-permute-done | bytes 94240 | tf_op jit(solution)/shard_map/ppermute | solution.py:53
  67.5 0.3 shard_map.125
  67.8 4.5 %collective-permute-start.32 = (bf16[16,256]{1,0:T(8,128)(2,1)S(1)}, bf16[16,256]{1,0:T(8,128)(2,1)S(1)}, u32[]{:S(2)}, u32[]{:S(2)}) collective-permute-start(bf16[16,256]{1,0:T(8,128)(2,1)S(1)} %shard_map.125), channel_id=1, source_target_pairs={{0,3},{1,2},{2,1},{3,0},{4,7},{5,6},{6,5},{7,4},{8,11},{9,10},{10,... | collective-permute-start | bytes 24584 | tf_op jit(solution)/shard_map/ppermute | solution.py:36
  72.3 1.3 %collective-permute-start.31 = (bf16[16,256]{1,0:T(8,128)(2,1)S(1)}, bf16[16,256]{1,0:T(8,128)(2,1)S(1)}, u32[]{:S(2)}, u32[]{:S(2)}) collective-permute-start(bf16[16,256]{1,0:T(8,128)(2,1)S(1)} %shard_map.125), channel_id=1, source_target_pairs={{0,7},{1,6},{2,5},{3,4},{4,3},{5,2},{6,1},{7,0},{8,15},{9,14},{10,... | collective-permute-start | bytes 24584 | tf_op jit(solution)/shard_map/ppermute | solution.py:36
  73.6 1.2 %collective-permute-start.30 = (bf16[16,256]{1,0:T(8,128)(2,1)S(1)}, bf16[16,256]{1,0:T(8,128)(2,1)S(1)}, u32[]{:S(2)}, u32[]{:S(2)}) collective-permute-start(bf16[16,256]{1,0:T(8,128)(2,1)S(1)} %shard_map.125), channel_id=1, source_target_pairs={{0,5},{1,4},{2,7},{3,6},{4,1},{5,0},{6,3},{7,2},{8,13},{9,12},{10,... | collective-permute-start | bytes 24584 | tf_op jit(solution)/shard_map/ppermute | solution.py:36
  74.8 1.8 %collective-permute-done.31 = bf16[16,256]{1,0:T(8,128)(2,1)S(1)} collective-permute-done((bf16[16,256]{1,0:T(8,128)(2,1)S(1)}, bf16[16,256]{1,0:T(8,128)(2,1)S(1)}, u32[]{:S(2)}, u32[]{:S(2)}) %collective-permute-start.31) | collective-permute-done | bytes 8224 | tf_op jit(solution)/shard_map/ppermute | solution.py:36
  76.6 1.6 %collective-permute-done.30 = bf16[16,256]{1,0:T(8,128)(2,1)S(1)} collective-permute-done((bf16[16,256]{1,0:T(8,128)(2,1)S(1)}, bf16[16,256]{1,0:T(8,128)(2,1)S(1)}, u32[]{:S(2)}, u32[]{:S(2)}) %collective-permute-start.30) | collective-permute-done | bytes 8224 | tf_op jit(solution)/shard_map/ppermute | solution.py:36
  78.2 1.0 %collective-permute-start.33 = (f32[16,256]{1,0:T(8,128)S(1)}, f32[16,256]{1,0:T(8,128)S(1)}, u32[]{:S(2)}, u32[]{:S(2)}) collective-permute-start(f32[16,256]{1,0:T(8,128)S(1)} %convert_add_fusion), channel_id=1, source_target_pairs={{0,1},{1,0},{2,3},{3,2},{4,5},{5,4},{6,7},{7,6},{8,9},{9,8},{10,11... | collective-permute-start | bytes 49160 | tf_op jit(solution)/shard_map/ppermute | solution.py:58
  79.2 0.8 %collective-permute-done.33 = f32[16,256]{1,0:T(8,128)S(1)} collective-permute-done((f32[16,256]{1,0:T(8,128)S(1)}, f32[16,256]{1,0:T(8,128)S(1)}, u32[]{:S(2)}, u32[]{:S(2)}) %collective-permute-start.33) | collective-permute-done | bytes 16416 | tf_op jit(solution)/shard_map/ppermute | solution.py:58
  80.0 0.7 fusion.3
  (39 shorter events, 0.3 us)
Async XLA Ops:
  0.0 11.3 %copy-start.8 = (bf16[256,512]{1,0:T(8,128)(2,1)S(1)}, bf16[256,512]{1,0:T(8,128)(2,1)}, u32[]{:S(2)}) copy-start(bf16[256,512]{1,0:T(8,128)(2,1)} %weight.3) | copy-start | bytes 786436
  0.0 11.3 %copy-start.9 = (f32[256]{0:T(256)S(1)}, f32[256]{0:T(256)}, u32[]{:S(2)}) copy-start(f32[256]{0:T(256)} %param.13) | copy-start | bytes 3076
  0.8 2.3 %collective-permute-start = (f32[24,128]{1,0:T(8,128)S(1)}, f32[24,128]{1,0:T(8,128)S(1)}, u32[]{:S(2)}, u32[]{:S(2)}) collective-permute-start(f32[24,128]{1,0:T(8,128)S(1)} %shard_map.118), channel_id=1, source_target_pairs={{0,1},{1,0},{2,3},{3,2},{4,5},{5,4},{6,7},{7,6},{8,9},{9,8},{10,11... | collective-permute-start | bytes 36872 | tf_op jit(solution)/shard_map/ppermute | solution.py:58
  3.1 4.1 %collective-permute-start.3 = (f32[24,128]{1,0:T(8,128)S(1)}, f32[24,128]{1,0:T(8,128)S(1)}, u32[]{:S(2)}, u32[]{:S(2)}) collective-permute-start(f32[24,128]{1,0:T(8,128)S(1)} %fusion.2.own), channel_id=1, source_target_pairs={{0,3},{1,2},{2,1},{3,0},{4,7},{5,6},{6,5},{7,4},{8,11},{9,10},{10,... | collective-permute-start | bytes 36872 | tf_op jit(solution)/shard_map/ppermute | solution.py:36
  4.8 4.3 %collective-permute-start.2 = (f32[24,128]{1,0:T(8,128)S(1)}, f32[24,128]{1,0:T(8,128)S(1)}, u32[]{:S(2)}, u32[]{:S(2)}) collective-permute-start(f32[24,128]{1,0:T(8,128)S(1)} %fusion.2.own), channel_id=1, source_target_pairs={{0,7},{1,6},{2,5},{3,4},{4,3},{5,2},{6,1},{7,0},{8,15},{9,14},{10,... | collective-permute-start | bytes 36872 | tf_op jit(solution)/shard_map/ppermute | solution.py:36
  6.6 4.6 %collective-permute-start.1 = (f32[24,128]{1,0:T(8,128)S(1)}, f32[24,128]{1,0:T(8,128)S(1)}, u32[]{:S(2)}, u32[]{:S(2)}) collective-permute-start(f32[24,128]{1,0:T(8,128)S(1)} %fusion.2.own), channel_id=1, source_target_pairs={{0,5},{1,4},{2,7},{3,6},{4,1},{5,0},{6,3},{7,2},{8,13},{9,12},{10,... | collective-permute-start | bytes 36872 | tf_op jit(solution)/shard_map/ppermute | solution.py:36
  11.3 18.0 %copy-start = (bf16[16,1024,1,128]{3,1,2,0:T(8,128)(2,1)S(1)}, bf16[16,1024,1,128]{3,1,2,0:T(8,128)(2,1)}, u32[]{:S(2)}) copy-start(bf16[16,1024,1,128]{3,1,2,0:T(8,128)(2,1)} %param.15) | copy-start | bytes 12582916
  11.3 18.0 %copy-start.1 = (bf16[16,1024,1,128]{3,1,2,0:T(8,128)(2,1)S(1)}, bf16[16,1024,1,128]{3,1,2,0:T(8,128)(2,1)}, u32[]{:S(2)}) copy-start(bf16[16,1024,1,128]{3,1,2,0:T(8,128)(2,1)} %param.16) | copy-start | bytes 12582916
  11.4 4.6 %collective-permute-start.7 = (f32[16,640]{1,0:T(8,128)S(1)}, f32[16,640]{1,0:T(8,128)S(1)}, u32[]{:S(2)}, u32[]{:S(2)}) collective-permute-start(f32[16,640]{1,0:T(8,128)S(1)} %get-tuple-element.16), channel_id=1, source_target_pairs={{0,9},{1,8},{8,1},{9,0},{16,25},{17,24},{24,17},{25,16},{2,11},{3,... | collective-permute-start | bytes 122888 | tf_op jit(solution)/shard_map/ppermute | solution.py:36
  13.0 4.6 %collective-permute-start.6 = (f32[16,640]{1,0:T(8,128)S(1)}, f32[16,640]{1,0:T(8,128)S(1)}, u32[]{:S(2)}, u32[]{:S(2)}) collective-permute-start(f32[16,640]{1,0:T(8,128)S(1)} %get-tuple-element.16), channel_id=1, source_target_pairs={{0,25},{1,24},{8,17},{9,16},{16,9},{17,8},{24,1},{25,0},{2,27},{3,... | collective-permute-start | bytes 122888 | tf_op jit(solution)/shard_map/ppermute | solution.py:36
  14.9 5.0 %collective-permute-start.5 = (f32[16,640]{1,0:T(8,128)S(1)}, f32[16,640]{1,0:T(8,128)S(1)}, u32[]{:S(2)}, u32[]{:S(2)}) collective-permute-start(f32[16,640]{1,0:T(8,128)S(1)} %get-tuple-element.16), channel_id=1, source_target_pairs={{0,17},{1,16},{8,25},{9,24},{16,1},{17,0},{24,9},{25,8},{2,19},{3,... | collective-permute-start | bytes 122888 | tf_op jit(solution)/shard_map/ppermute | solution.py:36
  15.6 4.3 %collective-permute-start.4 = (f32[16,640]{1,0:T(8,128)S(1)}, f32[16,640]{1,0:T(8,128)S(1)}, u32[]{:S(2)}, u32[]{:S(2)}) collective-permute-start(f32[16,640]{1,0:T(8,128)S(1)} %get-tuple-element.16), channel_id=1, source_target_pairs={{0,1},{1,0},{2,3},{3,2},{4,5},{5,4},{6,7},{7,6},{8,9},{9,8},{10,11... | collective-permute-start | bytes 122888 | tf_op jit(solution)/shard_map/ppermute | solution.py:58
  20.0 5.7 %collective-permute-start.11 = (f32[16,640]{1,0:T(8,128)S(1)}, f32[16,640]{1,0:T(8,128)S(1)}, u32[]{:S(2)}, u32[]{:S(2)}) collective-permute-start(f32[16,640]{1,0:T(8,128)S(1)} %add_add_fusion), channel_id=1, source_target_pairs={{0,33},{1,32},{32,1},{33,0},{64,97},{65,96},{96,65},{97,64},{2,35}... | collective-permute-start | bytes 122888 | tf_op jit(solution)/shard_map/ppermute | solution.py:36
  21.9 4.6 %collective-permute-start.10 = (f32[16,640]{1,0:T(8,128)S(1)}, f32[16,640]{1,0:T(8,128)S(1)}, u32[]{:S(2)}, u32[]{:S(2)}) collective-permute-start(f32[16,640]{1,0:T(8,128)S(1)} %add_add_fusion), channel_id=1, source_target_pairs={{0,97},{1,96},{32,65},{33,64},{64,33},{65,32},{96,1},{97,0},{2,99}... | collective-permute-start | bytes 122888 | tf_op jit(solution)/shard_map/ppermute | solution.py:36
  24.2 5.0 %collective-permute-start.9 = (f32[16,640]{1,0:T(8,128)S(1)}, f32[16,640]{1,0:T(8,128)S(1)}, u32[]{:S(2)}, u32[]{:S(2)}) collective-permute-start(f32[16,640]{1,0:T(8,128)S(1)} %add_add_fusion), channel_id=1, source_target_pairs={{0,65},{1,64},{32,97},{33,96},{64,1},{65,0},{96,33},{97,32},{2,67}... | collective-permute-start | bytes 122888 | tf_op jit(solution)/shard_map/ppermute | solution.py:36
  25.3 4.0 %collective-permute-start.8 = (f32[16,640]{1,0:T(8,128)S(1)}, f32[16,640]{1,0:T(8,128)S(1)}, u32[]{:S(2)}, u32[]{:S(2)}) collective-permute-start(f32[16,640]{1,0:T(8,128)S(1)} %add_add_fusion), channel_id=1, source_target_pairs={{0,1},{1,0},{2,3},{3,2},{4,5},{5,4},{6,7},{7,6},{8,9},{9,8},{10,11... | collective-permute-start | bytes 122888 | tf_op jit(solution)/shard_map/ppermute | solution.py:58
  29.2 15.1 %copy-start.5 = (bf16[512,256]{1,0:T(8,128)(2,1)S(1)}, bf16[512,256]{1,0:T(8,128)(2,1)}, u32[]{:S(2)}) copy-start(bf16[512,256]{1,0:T(8,128)(2,1)} %weight.4) | copy-start | bytes 786436
  29.3 15.1 %copy-start.6 = (f32[4]{0:T(128)S(1)}, f32[4]{0:T(128)}, u32[]{:S(2)}) copy-start(f32[4]{0:T(128)} %param.17) | copy-start | bytes 52
  29.3 15.1 %copy-start.7 = (f32[128]{0:T(128)S(1)}, f32[128]{0:T(128)}, u32[]{:S(2)}) copy-start(f32[128]{0:T(128)} %param.18) | copy-start | bytes 1540
  29.3 22.6 %copy-start.2 = (bf16[256,1408]{1,0:T(8,128)(2,1)S(1)}, bf16[256,1408]{1,0:T(8,128)(2,1)}, u32[]{:S(2)}) copy-start(bf16[256,1408]{1,0:T(8,128)(2,1)} %gate.1) | copy-start | bytes 2162692
  29.3 22.6 %copy-start.3 = (bf16[256,1408]{1,0:T(8,128)(2,1)S(1)}, bf16[256,1408]{1,0:T(8,128)(2,1)}, u32[]{:S(2)}) copy-start(bf16[256,1408]{1,0:T(8,128)(2,1)} %up.1) | copy-start | bytes 2162692
  29.3 38.1 %copy-start.4 = (bf16[1408,256]{1,0:T(8,128)(2,1)S(1)}, bf16[1408,256]{1,0:T(8,128)(2,1)}, u32[]{:S(2)}) copy-start(bf16[1408,256]{1,0:T(8,128)(2,1)} %weight.5) | copy-start | bytes 2162692
  31.1 6.3 %collective-permute-start.12 = (f32[136,128]{1,0:T(8,128)S(1)}, f32[136,128]{1,0:T(8,128)S(1)}, u32[]{:S(2)}, u32[]{:S(2)}) collective-permute-start(f32[136,128]{1,0:T(8,128)S(1)} %get-tuple-element.17), channel_id=1, source_target_pairs={{0,1},{1,0},{2,3},{3,2},{4,5},{5,4},{6,7},{7,6},{8,9},{9,8},{10,11... | collective-permute-start | bytes 208904 | tf_op jit(solution)/shard_map/ppermute | solution.py:58
  31.5 3.6 %collective-permute-start.15 = (bf16[144,128]{1,0:T(8,128)(2,1)S(1)}, bf16[144,128]{1,0:T(8,128)(2,1)S(1)}, u32[]{:S(2)}, u32[]{:S(2)}) collective-permute-start(bf16[144,128]{1,0:T(8,128)(2,1)S(1)} %get-tuple-element.18), channel_id=1, source_target_pairs={{0,9},{1,8},{8,1},{9,0},{16,25},{17,24},{24,17},{25,16},{2,11},{3,... | collective-permute-start | bytes 110600 | tf_op jit(solution)/shard_map/ppermute | solution.py:36
  31.9 4.9 %collective-permute-start.14 = (bf16[144,128]{1,0:T(8,128)(2,1)S(1)}, bf16[144,128]{1,0:T(8,128)(2,1)S(1)}, u32[]{:S(2)}, u32[]{:S(2)}) collective-permute-start(bf16[144,128]{1,0:T(8,128)(2,1)S(1)} %get-tuple-element.18), channel_id=1, source_target_pairs={{0,25},{1,24},{8,17},{9,16},{16,9},{17,8},{24,1},{25,0},{2,27},{3,... | collective-permute-start | bytes 110600 | tf_op jit(solution)/shard_map/ppermute | solution.py:36
  32.4 5.0 %collective-permute-start.13 = (bf16[144,128]{1,0:T(8,128)(2,1)S(1)}, bf16[144,128]{1,0:T(8,128)(2,1)S(1)}, u32[]{:S(2)}, u32[]{:S(2)}) collective-permute-start(bf16[144,128]{1,0:T(8,128)(2,1)S(1)} %get-tuple-element.18), channel_id=1, source_target_pairs={{0,17},{1,16},{8,25},{9,24},{16,1},{17,0},{24,9},{25,8},{2,19},{3,... | collective-permute-start | bytes 110600 | tf_op jit(solution)/shard_map/ppermute | solution.py:36
  37.6 6.7 %collective-permute-start.16 = (f32[136,128]{1,0:T(8,128)S(1)}, f32[136,128]{1,0:T(8,128)S(1)}, u32[]{:S(2)}, u32[]{:S(2)}) collective-permute-start(f32[136,128]{1,0:T(8,128)S(1)} %get-tuple-element.19), channel_id=1, source_target_pairs={{0,1},{1,0},{2,3},{3,2},{4,5},{5,4},{6,7},{7,6},{8,9},{9,8},{10,11... | collective-permute-start | bytes 208904 | tf_op jit(solution)/shard_map/ppermute | solution.py:58
  38.1 3.6 %collective-permute-start.19 = (bf16[144,128]{1,0:T(8,128)(2,1)S(1)}, bf16[144,128]{1,0:T(8,128)(2,1)S(1)}, u32[]{:S(2)}, u32[]{:S(2)}) collective-permute-start(bf16[144,128]{1,0:T(8,128)(2,1)S(1)} %get-tuple-element.20), channel_id=1, source_target_pairs={{0,33},{1,32},{32,1},{33,0},{64,97},{65,96},{96,65},{97,64},{2,35}... | collective-permute-start | bytes 110600 | tf_op jit(solution)/shard_map/ppermute | solution.py:36
  38.9 4.6 %collective-permute-start.18 = (bf16[144,128]{1,0:T(8,128)(2,1)S(1)}, bf16[144,128]{1,0:T(8,128)(2,1)S(1)}, u32[]{:S(2)}, u32[]{:S(2)}) collective-permute-start(bf16[144,128]{1,0:T(8,128)(2,1)S(1)} %get-tuple-element.20), channel_id=1, source_target_pairs={{0,97},{1,96},{32,65},{33,64},{64,33},{65,32},{96,1},{97,0},{2,99}... | collective-permute-start | bytes 110600 | tf_op jit(solution)/shard_map/ppermute | solution.py:36
  39.5 4.9 %collective-permute-start.17 = (bf16[144,128]{1,0:T(8,128)(2,1)S(1)}, bf16[144,128]{1,0:T(8,128)(2,1)S(1)}, u32[]{:S(2)}, u32[]{:S(2)}) collective-permute-start(bf16[144,128]{1,0:T(8,128)(2,1)S(1)} %get-tuple-element.20), channel_id=1, source_target_pairs={{0,65},{1,64},{32,97},{33,96},{64,1},{65,0},{96,33},{97,32},{2,67}... | collective-permute-start | bytes 110600 | tf_op jit(solution)/shard_map/ppermute | solution.py:36
  44.9 3.8 %collective-permute-start.22 = (bf16[16,256]{1,0:T(8,128)(2,1)S(1)}, bf16[16,256]{1,0:T(8,128)(2,1)S(1)}, u32[]{:S(2)}, u32[]{:S(2)}) collective-permute-start(bf16[16,256]{1,0:T(8,128)(2,1)S(1)} %shard_map.122), channel_id=1, source_target_pairs={{0,3},{1,2},{2,1},{3,0},{4,7},{5,6},{6,5},{7,4},{8,11},{9,10},{10,... | collective-permute-start | bytes 24584 | tf_op jit(solution)/shard_map/ppermute | solution.py:36
  45.5 4.3 %collective-permute-start.21 = (bf16[16,256]{1,0:T(8,128)(2,1)S(1)}, bf16[16,256]{1,0:T(8,128)(2,1)S(1)}, u32[]{:S(2)}, u32[]{:S(2)}) collective-permute-start(bf16[16,256]{1,0:T(8,128)(2,1)S(1)} %shard_map.122), channel_id=1, source_target_pairs={{0,7},{1,6},{2,5},{3,4},{4,3},{5,2},{6,1},{7,0},{8,15},{9,14},{10,... | collective-permute-start | bytes 24584 | tf_op jit(solution)/shard_map/ppermute | solution.py:36
  46.1 4.6 %collective-permute-start.20 = (bf16[16,256]{1,0:T(8,128)(2,1)S(1)}, bf16[16,256]{1,0:T(8,128)(2,1)S(1)}, u32[]{:S(2)}, u32[]{:S(2)}) collective-permute-start(bf16[16,256]{1,0:T(8,128)(2,1)S(1)} %shard_map.122), channel_id=1, source_target_pairs={{0,5},{1,4},{2,7},{3,6},{4,1},{5,0},{6,3},{7,2},{8,13},{9,12},{10,... | collective-permute-start | bytes 24584 | tf_op jit(solution)/shard_map/ppermute | solution.py:36
  50.7 1.3 %collective-permute-start.23 = (f32[16,256]{1,0:T(8,128)S(1)}, f32[16,256]{1,0:T(8,128)S(1)}, u32[]{:S(2)}, u32[]{:S(2)}) collective-permute-start(f32[16,256]{1,0:T(8,128)S(1)} %convert_add_fusion.1.attn), channel_id=1, source_target_pairs={{0,1},{1,0},{2,3},{3,2},{4,5},{5,4},{6,7},{7,6},{8,9},{9,8},{10,11... | collective-permute-start | bytes 49160 | tf_op jit(solution)/shard_map/ppermute | solution.py:58
  52.2 3.8 %collective-permute-start.26 = (bf16[16,2944]{1,0:T(8,128)(2,1)S(1)}, bf16[16,2944]{1,0:T(8,128)(2,1)S(1)}, u32[]{:S(2)}, u32[]{:S(2)}) collective-permute-start(bf16[16,2944]{1,0:T(8,128)(2,1)S(1)} %get-tuple-element.24), channel_id=1, source_target_pairs={{0,8},{1,33},{8,0},{9,41},{16,24},{17,49},{24,16},{25,57},{32,40},... | collective-permute-start | bytes 282632 | tf_op jit(solution)/shard_map/ppermute | solution.py:53
  52.5 4.6 %collective-permute-start.25 = (bf16[16,2944]{1,0:T(8,128)(2,1)S(1)}, bf16[16,2944]{1,0:T(8,128)(2,1)S(1)}, u32[]{:S(2)}, u32[]{:S(2)}) collective-permute-start(bf16[16,2944]{1,0:T(8,128)(2,1)S(1)} %get-tuple-element.24), channel_id=1, source_target_pairs={{0,24},{1,97},{8,16},{9,105},{16,8},{17,113},{24,0},{25,121},{32,5... | collective-permute-start | bytes 282632 | tf_op jit(solution)/shard_map/ppermute | solution.py:53
  54.6 4.9 %collective-permute-start.24 = (bf16[16,2944]{1,0:T(8,128)(2,1)S(1)}, bf16[16,2944]{1,0:T(8,128)(2,1)S(1)}, u32[]{:S(2)}, u32[]{:S(2)}) collective-permute-start(bf16[16,2944]{1,0:T(8,128)(2,1)S(1)} %get-tuple-element.24), channel_id=1, source_target_pairs={{0,16},{1,65},{8,24},{9,73},{16,0},{17,81},{24,8},{25,89},{32,48},... | collective-permute-start | bytes 282632 | tf_op jit(solution)/shard_map/ppermute | solution.py:53
  59.7 3.8 %collective-permute-start.29 = (bf16[16,2944]{1,0:T(8,128)(2,1)S(1)}, bf16[16,2944]{1,0:T(8,128)(2,1)S(1)}, u32[]{:S(2)}, u32[]{:S(2)}) collective-permute-start(bf16[16,2944]{1,0:T(8,128)(2,1)S(1)} %get-tuple-element.26), channel_id=1, source_target_pairs={{0,32},{1,9},{8,40},{9,1},{16,48},{17,25},{24,56},{25,17},{32,0},{... | collective-permute-start | bytes 282632 | tf_op jit(solution)/shard_map/ppermute | solution.py:53
  60.6 4.6 %collective-permute-start.28 = (bf16[16,2944]{1,0:T(8,128)(2,1)S(1)}, bf16[16,2944]{1,0:T(8,128)(2,1)S(1)}, u32[]{:S(2)}, u32[]{:S(2)}) collective-permute-start(bf16[16,2944]{1,0:T(8,128)(2,1)S(1)} %get-tuple-element.26), channel_id=1, source_target_pairs={{0,96},{1,25},{8,104},{9,17},{16,112},{17,9},{24,120},{25,1},{32,6... | collective-permute-start | bytes 282632 | tf_op jit(solution)/shard_map/ppermute | solution.py:53
  62.5 4.9 %collective-permute-start.27 = (bf16[16,2944]{1,0:T(8,128)(2,1)S(1)}, bf16[16,2944]{1,0:T(8,128)(2,1)S(1)}, u32[]{:S(2)}, u32[]{:S(2)}) collective-permute-start(bf16[16,2944]{1,0:T(8,128)(2,1)S(1)} %get-tuple-element.26), channel_id=1, source_target_pairs={{0,64},{1,17},{8,72},{9,25},{16,80},{17,1},{24,88},{25,9},{32,96},... | collective-permute-start | bytes 282632 | tf_op jit(solution)/shard_map/ppermute | solution.py:53
  67.8 7.0 %collective-permute-start.32 = (bf16[16,256]{1,0:T(8,128)(2,1)S(1)}, bf16[16,256]{1,0:T(8,128)(2,1)S(1)}, u32[]{:S(2)}, u32[]{:S(2)}) collective-permute-start(bf16[16,256]{1,0:T(8,128)(2,1)S(1)} %shard_map.125), channel_id=1, source_target_pairs={{0,3},{1,2},{2,1},{3,0},{4,7},{5,6},{6,5},{7,4},{8,11},{9,10},{10,... | collective-permute-start | bytes 24584 | tf_op jit(solution)/shard_map/ppermute | solution.py:36
  72.3 4.3 %collective-permute-start.31 = (bf16[16,256]{1,0:T(8,128)(2,1)S(1)}, bf16[16,256]{1,0:T(8,128)(2,1)S(1)}, u32[]{:S(2)}, u32[]{:S(2)}) collective-permute-start(bf16[16,256]{1,0:T(8,128)(2,1)S(1)} %shard_map.125), channel_id=1, source_target_pairs={{0,7},{1,6},{2,5},{3,4},{4,3},{5,2},{6,1},{7,0},{8,15},{9,14},{10,... | collective-permute-start | bytes 24584 | tf_op jit(solution)/shard_map/ppermute | solution.py:36
  73.6 4.6 %collective-permute-start.30 = (bf16[16,256]{1,0:T(8,128)(2,1)S(1)}, bf16[16,256]{1,0:T(8,128)(2,1)S(1)}, u32[]{:S(2)}, u32[]{:S(2)}) collective-permute-start(bf16[16,256]{1,0:T(8,128)(2,1)S(1)} %shard_map.125), channel_id=1, source_target_pairs={{0,5},{1,4},{2,7},{3,6},{4,1},{5,0},{6,3},{7,2},{8,13},{9,12},{10,... | collective-permute-start | bytes 24584 | tf_op jit(solution)/shard_map/ppermute | solution.py:36
  78.2 1.8 %collective-permute-start.33 = (f32[16,256]{1,0:T(8,128)S(1)}, f32[16,256]{1,0:T(8,128)S(1)}, u32[]{:S(2)}, u32[]{:S(2)}) collective-permute-start(f32[16,256]{1,0:T(8,128)S(1)} %convert_add_fusion), channel_id=1, source_target_pairs={{0,1},{1,0},{2,3},{3,2},{4,5},{5,4},{6,7},{7,6},{8,9},{9,8},{10,11... | collective-permute-start | bytes 49160 | tf_op jit(solution)/shard_map/ppermute | solution.py:58

commit v9 on v8

--- a/solution.py
+++ b/solution.py
@@ -100,7 +100,7 @@
 
 
 def query_body(chip, own, a, b, c, gain, weight, packed, block, held):
-    batch = packed.shape[0]
+    batch = own.shape[0] - 8
     x = chip[0]
     held[x] = own[...]
     for s, ref in zip(SHIFTS, (a, b, c)):
@@ -111,19 +111,27 @@
     rows = block[:batch, :]
     gained = (rows * gain[...]).astype(BF16)
     width = weight.shape[1]
-    packed[:, :width] = jnp.dot(gained, weight[...], preferred_element_type=F32)
+    product = jnp.dot(gained, weight[...], preferred_element_type=F32)
+    for g in range(width // LANES):
+        packed[g * batch : (g + 1) * batch, :] = product[:, g * LANES : (g + 1) * LANES]
     squares = jnp.sum(rows * rows, axis=1, keepdims=True)
-    packed[:, width:] = jnp.broadcast_to(squares, (batch, LANES))
+    shape = (8, LANES)
+    packed[width // LANES * batch :, :] = jnp.where(
+        lane_of(shape) < LANES // 2,
+        jnp.broadcast_to(squares[:8], shape),
+        jnp.broadcast_to(squares[8:], shape),
+    )
 
 
 def attend_body(own, a, b, c, keys, values, out, sent, query, scores, weights):
     batch, _, _ = keys.shape
-    width = own.shape[1] - LANES
-    heads = width // LANES
+    heads = own.shape[0] // batch
     whole = own[...] + a[...] + b[...] + c[...]
-    inv = lax.rsqrt(whole[:, width:] / D + eps)
+    squares = whole[heads * batch :]
+    squares = jnp.concatenate([squares[:, :1], squares[:, LANES // 2 : LANES // 2 + 1]], axis=0)
+    inv = lax.rsqrt(squares / D + eps)
     for g in range(heads):
-        part = whole[:, g * LANES : (g + 1) * LANES] * inv
+        part = whole[g * batch : (g + 1) * batch] * inv
         query[g * batch : (g + 1) * batch, :] = part.astype(BF16).astype(F32)
     shape = (2 * heads, LANES)
     half = lane_of(shape) // HEAD_DIM
@@ -314,7 +322,7 @@
     pair = jnp.where(mine, own, partner(own))
     packed, block = kernel_call(
         query_body,
-        [shape((batch, width_q + LANES), F32), shape((own.shape[0], wide), F32)],
+        [shape((heads * batch + 8, LANES), F32), shape((own.shape[0], wide), F32)],
         [pltpu.VMEM((4, *own.shape), F32)],
         smem=1,
         n_in=7,

time: 80.8 us -> 80.7 us (level)
  no operation moved by 1% of the time
where the time goes in v9:
time: 80.7 us; the launch traced here: 80.6 us
  starting transfers between devices  43 us (53%)
  waiting for transfers between devices  32.3 us (40%)
  Pallas kernels  4.44 us (6%)
    ppermute x21, starting transfers between devices, peers(): got.append(lax.ppermute(shard, across, pairs))  31.6 us
    ppermute x21, waiting for transfers between devices, peers(): got.append(lax.ppermute(shard, across, pairs))  21.8 us
    ppermute x6, waiting for transfers between devices, kv_peers(): got.append(lax.ppermute(shard, (*KV, TP[1]), pairs))  7.77 us
    ppermute x6, starting transfers between devices, kv_peers(): got.append(lax.ppermute(shard, (*KV, TP[1]), pairs))  7.23 us
    ppermute x7, starting transfers between devices, partner(): return lax.ppermute(shard, TP[1], [(0, 1), (1, 0)])  4.2 us
    ppermute x7, waiting for transfers between devices, partner(): return lax.ppermute(shard, TP[1], [(0, 1), (1, 0)])  2.67 us
    pallas_call x1, Pallas kernels, per_device(): kernel_call(attend_body, states, [pltpu.VMEM((heads * batch, LANES), F32)...  1.89 us
  transfers between devices with their start and end apart: 34, of which 22 were waited for; matrix products, arithmetic and copies ran while one was open for 0% of the time, Pallas kernels for 0%

profile of v9, /device:TPU:1, one launch (start us, length us, event | category | flops | bytes accessed | tf_op | source)
XLA Modules:
  0.0 80.6 jit_solution(14223042916404290082)
XLA Ops:
  0.0 0.8 %shard_map.118 = f32[24,128]{1,0:T(8,128)S(1)} custom-call(bf16[16,32]{1,0:T(8,128)(2,1)} %hidden.1, f32[1,32]{1,0:T(1,128)} %bitcast.12), custom_call_target="tpu_custom_call" | custom-call | flops 1099511627776 | bytes 1099511627776 | tf_op jit(solution)/shard_map/pallas_call | solution.py:305
  0.8 1.5 %collective-permute-start = (f32[24,128]{1,0:T(8,128)S(1)}, f32[24,128]{1,0:T(8,128)S(1)}, u32[]{:S(2)}, u32[]{:S(2)}) collective-permute-start(f32[24,128]{1,0:T(8,128)S(1)} %shard_map.118), channel_id=1, source_target_pairs={{0,1},{1,0},{2,3},{3,2},{4,5},{5,4},{6,7},{7,6},{8,9},{9,8},{10,11... | collective-permute-start | bytes 36872 | tf_op jit(solution)/shard_map/ppermute | solution.py:58
  2.3 0.8 %collective-permute-done = f32[24,128]{1,0:T(8,128)S(1)} collective-permute-done((f32[24,128]{1,0:T(8,128)S(1)}, f32[24,128]{1,0:T(8,128)S(1)}, u32[]{:S(2)}, u32[]{:S(2)}) %collective-permute-start) | collective-permute-done | bytes 12320 | tf_op jit(solution)/shard_map/ppermute | solution.py:58
  3.1 1.6 %collective-permute-start.3 = (f32[24,128]{1,0:T(8,128)S(1)}, f32[24,128]{1,0:T(8,128)S(1)}, u32[]{:S(2)}, u32[]{:S(2)}) collective-permute-start(f32[24,128]{1,0:T(8,128)S(1)} %fusion.2.own), channel_id=1, source_target_pairs={{0,3},{1,2},{2,1},{3,0},{4,7},{5,6},{6,5},{7,4},{8,11},{9,10},{10,... | collective-permute-start | bytes 36872 | tf_op jit(solution)/shard_map/ppermute | solution.py:36
  4.8 1.9 %collective-permute-start.2 = (f32[24,128]{1,0:T(8,128)S(1)}, f32[24,128]{1,0:T(8,128)S(1)}, u32[]{:S(2)}, u32[]{:S(2)}) collective-permute-start(f32[24,128]{1,0:T(8,128)S(1)} %fusion.2.own), channel_id=1, source_target_pairs={{0,7},{1,6},{2,5},{3,4},{4,3},{5,2},{6,1},{7,0},{8,15},{9,14},{10,... | collective-permute-start | bytes 36872 | tf_op jit(solution)/shard_map/ppermute | solution.py:36
  6.6 0.6 collective-permute-start.1
  7.3 1.8 %collective-permute-done.2.b = f32[24,128]{1,0:T(8,128)S(1)} collective-permute-done((f32[24,128]{1,0:T(8,128)S(1)}, f32[24,128]{1,0:T(8,128)S(1)}, u32[]{:S(2)}, u32[]{:S(2)}) %collective-permute-start.2) | collective-permute-done | bytes 12320 | tf_op jit(solution)/shard_map/ppermute | solution.py:36
  9.1 2.2 %collective-permute-done.1.a = f32[24,128]{1,0:T(8,128)S(1)} collective-permute-done((f32[24,128]{1,0:T(8,128)S(1)}, f32[24,128]{1,0:T(8,128)S(1)}, u32[]{:S(2)}, u32[]{:S(2)}) %collective-permute-start.1) | collective-permute-done | bytes 12320 | tf_op jit(solution)/shard_map/ppermute | solution.py:36
  11.4 1.5 %collective-permute-start.7 = (f32[72,128]{1,0:T(8,128)S(1)}, f32[72,128]{1,0:T(8,128)S(1)}, u32[]{:S(2)}, u32[]{:S(2)}) collective-permute-start(f32[72,128]{1,0:T(8,128)S(1)} %get-tuple-element.16), channel_id=1, source_target_pairs={{0,9},{1,8},{8,1},{9,0},{16,25},{17,24},{24,17},{25,16},{2,11},{3,... | collective-permute-start | bytes 110600 | tf_op jit(solution)/shard_map/ppermute | solution.py:36
  13.0 2.0 %collective-permute-start.6 = (f32[72,128]{1,0:T(8,128)S(1)}, f32[72,128]{1,0:T(8,128)S(1)}, u32[]{:S(2)}, u32[]{:S(2)}) collective-permute-start(f32[72,128]{1,0:T(8,128)S(1)} %get-tuple-element.16), channel_id=1, source_target_pairs={{0,25},{1,24},{8,17},{9,16},{16,9},{17,8},{24,1},{25,0},{2,27},{3,... | collective-permute-start | bytes 110600 | tf_op jit(solution)/shard_map/ppermute | solution.py:36
  14.9 0.7 collective-permute-start.5
  15.6 0.3 collective-permute-start.4
  16.0 1.6 %collective-permute-done.6 = f32[72,128]{1,0:T(8,128)S(1)} collective-permute-done((f32[72,128]{1,0:T(8,128)S(1)}, f32[72,128]{1,0:T(8,128)S(1)}, u32[]{:S(2)}, u32[]{:S(2)}) %collective-permute-start.6) | collective-permute-done | bytes 36896 | tf_op jit(solution)/shard_map/ppermute | solution.py:36
  17.6 2.3 %collective-permute-done.5 = f32[72,128]{1,0:T(8,128)S(1)} collective-permute-done((f32[72,128]{1,0:T(8,128)S(1)}, f32[72,128]{1,0:T(8,128)S(1)}, u32[]{:S(2)}, u32[]{:S(2)}) %collective-permute-start.5) | collective-permute-done | bytes 36896 | tf_op jit(solution)/shard_map/ppermute | solution.py:36
  19.9 1.9 %collective-permute-start.11 = (f32[72,128]{1,0:T(8,128)S(1)}, f32[72,128]{1,0:T(8,128)S(1)}, u32[]{:S(2)}, u32[]{:S(2)}) collective-permute-start(f32[72,128]{1,0:T(8,128)S(1)} %add_add_fusion), channel_id=1, source_target_pairs={{0,33},{1,32},{32,1},{33,0},{64,97},{65,96},{96,65},{97,64},{2,35}... | collective-permute-start | bytes 110600 | tf_op jit(solution)/shard_map/ppermute | solution.py:36
  21.8 2.3 %collective-permute-start.10 = (f32[72,128]{1,0:T(8,128)S(1)}, f32[72,128]{1,0:T(8,128)S(1)}, u32[]{:S(2)}, u32[]{:S(2)}) collective-permute-start(f32[72,128]{1,0:T(8,128)S(1)} %add_add_fusion), channel_id=1, source_target_pairs={{0,97},{1,96},{32,65},{33,64},{64,33},{65,32},{96,1},{97,0},{2,99}... | collective-permute-start | bytes 110600 | tf_op jit(solution)/shard_map/ppermute | solution.py:36
  24.1 1.1 %collective-permute-start.9 = (f32[72,128]{1,0:T(8,128)S(1)}, f32[72,128]{1,0:T(8,128)S(1)}, u32[]{:S(2)}, u32[]{:S(2)}) collective-permute-start(f32[72,128]{1,0:T(8,128)S(1)} %add_add_fusion), channel_id=1, source_target_pairs={{0,65},{1,64},{32,97},{33,96},{64,1},{65,0},{96,33},{97,32},{2,67}... | collective-permute-start | bytes 110600 | tf_op jit(solution)/shard_map/ppermute | solution.py:36
  25.2 0.3 collective-permute-start.8
  25.5 0.9 %collective-permute-done.10.b = f32[72,128]{1,0:T(8,128)S(1)} collective-permute-done((f32[72,128]{1,0:T(8,128)S(1)}, f32[72,128]{1,0:T(8,128)S(1)}, u32[]{:S(2)}, u32[]{:S(2)}) %collective-permute-start.10) | collective-permute-done | bytes 36896 | tf_op jit(solution)/shard_map/ppermute | solution.py:36
  26.4 2.6 %collective-permute-done.9.a = f32[72,128]{1,0:T(8,128)S(1)} collective-permute-done((f32[72,128]{1,0:T(8,128)S(1)}, f32[72,128]{1,0:T(8,128)S(1)}, u32[]{:S(2)}, u32[]{:S(2)}) %collective-permute-start.9) | collective-permute-done | bytes 36896 | tf_op jit(solution)/shard_map/ppermute | solution.py:36
  29.1 1.9 %shard_map.120 = (f32[136,128]{1,0:T(8,128)S(1)}, bf16[144,128]{1,0:T(8,128)(2,1)S(1)}) custom-call(f32[72,128]{1,0:T(8,128)S(1)} %collective-permute-done.8.own, f32[72,128]{1,0:T(8,128)S(1)} %collective-permute-done.9.a, f32[72,128]{1,0:T(8,128)S(1)} %collective-permute-done.10.b, f32[72,128]{1,0:T(8,128)S(1)} %collective-permute-done.11.c, ...), custom_call_target="tpu_custom_call" | custom-call | tf_op jit(solution)/shard_map/pallas_call | solution.py:334
  31.0 0.4 collective-permute-start.12
  31.4 0.4 collective-permute-start.15
  31.9 0.5 collective-permute-start.14
  32.4 2.6 %collective-permute-start.13 = (bf16[144,128]{1,0:T(8,128)(2,1)S(1)}, bf16[144,128]{1,0:T(8,128)(2,1)S(1)}, u32[]{:S(2)}, u32[]{:S(2)}) collective-permute-start(bf16[144,128]{1,0:T(8,128)(2,1)S(1)} %get-tuple-element.18), channel_id=1, source_target_pairs={{0,17},{1,16},{8,25},{9,24},{16,1},{17,0},{24,9},{25,8},{2,19},{3,... | collective-permute-start | bytes 110600 | tf_op jit(solution)/shard_map/ppermute | solution.py:36
  35.0 1.5 %collective-permute-done.14.b = bf16[144,128]{1,0:T(8,128)(2,1)S(1)} collective-permute-done((bf16[144,128]{1,0:T(8,128)(2,1)S(1)}, bf16[144,128]{1,0:T(8,128)(2,1)S(1)}, u32[]{:S(2)}, u32[]{:S(2)}) %collective-permute-start.14) | collective-permute-done | bytes 36896 | tf_op jit(solution)/shard_map/ppermute | solution.py:36
  36.5 0.8 collective-permute-done.13.a
  37.3 0.3 shard_map.121
  37.6 0.4 collective-permute-start.16
  38.0 0.8 collective-permute-start.19
  38.8 0.6 collective-permute-start.18
  39.4 2.2 %collective-permute-start.17 = (bf16[144,128]{1,0:T(8,128)(2,1)S(1)}, bf16[144,128]{1,0:T(8,128)(2,1)S(1)}, u32[]{:S(2)}, u32[]{:S(2)}) collective-permute-start(bf16[144,128]{1,0:T(8,128)(2,1)S(1)} %get-tuple-element.20), channel_id=1, source_target_pairs={{0,65},{1,64},{32,97},{33,96},{64,1},{65,0},{96,33},{97,32},{2,67}... | collective-permute-start | bytes 110600 | tf_op jit(solution)/shard_map/ppermute | solution.py:36
  41.6 1.8 %collective-permute-done.18.b = bf16[144,128]{1,0:T(8,128)(2,1)S(1)} collective-permute-done((bf16[144,128]{1,0:T(8,128)(2,1)S(1)}, bf16[144,128]{1,0:T(8,128)(2,1)S(1)}, u32[]{:S(2)}, u32[]{:S(2)}) %collective-permute-start.18) | collective-permute-done | bytes 36896 | tf_op jit(solution)/shard_map/ppermute | solution.py:36
  43.5 0.9 %collective-permute-done.17.a = bf16[144,128]{1,0:T(8,128)(2,1)S(1)} collective-permute-done((bf16[144,128]{1,0:T(8,128)(2,1)S(1)}, bf16[144,128]{1,0:T(8,128)(2,1)S(1)}, u32[]{:S(2)}, u32[]{:S(2)}) %collective-permute-start.17) | collective-permute-done | bytes 36896 | tf_op jit(solution)/shard_map/ppermute | solution.py:36
  44.4 0.5 shard_map.122
  44.9 0.5 collective-permute-start.22
  45.4 0.6 collective-permute-start.21
  46.1 2.6 %collective-permute-start.20 = (bf16[16,256]{1,0:T(8,128)(2,1)S(1)}, bf16[16,256]{1,0:T(8,128)(2,1)S(1)}, u32[]{:S(2)}, u32[]{:S(2)}) collective-permute-start(bf16[16,256]{1,0:T(8,128)(2,1)S(1)} %shard_map.122), channel_id=1, source_target_pairs={{0,5},{1,4},{2,7},{3,6},{4,1},{5,0},{6,3},{7,2},{8,13},{9,12},{10,... | collective-permute-start | bytes 24584 | tf_op jit(solution)/shard_map/ppermute | solution.py:36
  48.7 1.4 %collective-permute-done.21 = bf16[16,256]{1,0:T(8,128)(2,1)S(1)} collective-permute-done((bf16[16,256]{1,0:T(8,128)(2,1)S(1)}, bf16[16,256]{1,0:T(8,128)(2,1)S(1)}, u32[]{:S(2)}, u32[]{:S(2)}) %collective-permute-start.21) | collective-permute-done | bytes 8224 | tf_op jit(solution)/shard_map/ppermute | solution.py:36
  50.0 0.6 collective-permute-done.20
  50.7 0.3 collective-permute-start.23
  50.9 1.0 %collective-permute-done.23.other = f32[16,256]{1,0:T(8,128)S(1)} collective-permute-done((f32[16,256]{1,0:T(8,128)S(1)}, f32[16,256]{1,0:T(8,128)S(1)}, u32[]{:S(2)}, u32[]{:S(2)}) %collective-permute-start.23) | collective-permute-done | bytes 16416 | tf_op jit(solution)/shard_map/ppermute | solution.py:58
  51.9 0.3 shard_map.123
  52.2 0.2 collective-permute-start.26
  52.4 2.2 %collective-permute-start.25 = (bf16[16,2944]{1,0:T(8,128)(2,1)S(1)}, bf16[16,2944]{1,0:T(8,128)(2,1)S(1)}, u32[]{:S(2)}, u32[]{:S(2)}) collective-permute-start(bf16[16,2944]{1,0:T(8,128)(2,1)S(1)} %get-tuple-element.24), channel_id=1, source_target_pairs={{0,24},{1,97},{8,16},{9,105},{16,8},{17,113},{24,0},{25,121},{32,5... | collective-permute-start | bytes 282632 | tf_op jit(solution)/shard_map/ppermute | solution.py:53
  54.6 1.1 %collective-permute-start.24 = (bf16[16,2944]{1,0:T(8,128)(2,1)S(1)}, bf16[16,2944]{1,0:T(8,128)(2,1)S(1)}, u32[]{:S(2)}, u32[]{:S(2)}) collective-permute-start(bf16[16,2944]{1,0:T(8,128)(2,1)S(1)} %get-tuple-element.24), channel_id=1, source_target_pairs={{0,16},{1,65},{8,24},{9,73},{16,0},{17,81},{24,8},{25,89},{32,48},... | collective-permute-start | bytes 282632 | tf_op jit(solution)/shard_map/ppermute | solution.py:53
  55.6 0.4 collective-permute-done.26.c
  56.0 1.0 %collective-permute-done.25.b = bf16[16,2944]{1,0:T(8,128)(2,1)S(1)} collective-permute-done((bf16[16,2944]{1,0:T(8,128)(2,1)S(1)}, bf16[16,2944]{1,0:T(8,128)(2,1)S(1)}, u32[]{:S(2)}, u32[]{:S(2)}) %collective-permute-start.25) | collective-permute-done | bytes 94240 | tf_op jit(solution)/shard_map/ppermute | solution.py:53
  57.0 2.5 %collective-permute-done.24.a = bf16[16,2944]{1,0:T(8,128)(2,1)S(1)} collective-permute-done((bf16[16,2944]{1,0:T(8,128)(2,1)S(1)}, bf16[16,2944]{1,0:T(8,128)(2,1)S(1)}, u32[]{:S(2)}, u32[]{:S(2)}) %collective-permute-start.24) | collective-permute-done | bytes 94240 | tf_op jit(solution)/shard_map/ppermute | solution.py:53
  59.5 0.2 shard_map.124
  59.7 0.9 %collective-permute-start.29 = (bf16[16,2944]{1,0:T(8,128)(2,1)S(1)}, bf16[16,2944]{1,0:T(8,128)(2,1)S(1)}, u32[]{:S(2)}, u32[]{:S(2)}) collective-permute-start(bf16[16,2944]{1,0:T(8,128)(2,1)S(1)} %get-tuple-element.26), channel_id=1, source_target_pairs={{0,32},{1,9},{8,40},{9,1},{16,48},{17,25},{24,56},{25,17},{32,0},{... | collective-permute-start | bytes 282632 | tf_op jit(solution)/shard_map/ppermute | solution.py:53
  60.6 1.9 %collective-permute-start.28 = (bf16[16,2944]{1,0:T(8,128)(2,1)S(1)}, bf16[16,2944]{1,0:T(8,128)(2,1)S(1)}, u32[]{:S(2)}, u32[]{:S(2)}) collective-permute-start(bf16[16,2944]{1,0:T(8,128)(2,1)S(1)} %get-tuple-element.26), channel_id=1, source_target_pairs={{0,96},{1,25},{8,104},{9,17},{16,112},{17,9},{24,120},{25,1},{32,6... | collective-permute-start | bytes 282632 | tf_op jit(solution)/shard_map/ppermute | solution.py:53
  62.5 1.0 %collective-permute-start.27 = (bf16[16,2944]{1,0:T(8,128)(2,1)S(1)}, bf16[16,2944]{1,0:T(8,128)(2,1)S(1)}, u32[]{:S(2)}, u32[]{:S(2)}) collective-permute-start(bf16[16,2944]{1,0:T(8,128)(2,1)S(1)} %get-tuple-element.26), channel_id=1, source_target_pairs={{0,64},{1,17},{8,72},{9,25},{16,80},{17,1},{24,88},{25,9},{32,96},... | collective-permute-start | bytes 282632 | tf_op jit(solution)/shard_map/ppermute | solution.py:53
  63.5 1.7 %collective-permute-done.28.b = bf16[16,2944]{1,0:T(8,128)(2,1)S(1)} collective-permute-done((bf16[16,2944]{1,0:T(8,128)(2,1)S(1)}, bf16[16,2944]{1,0:T(8,128)(2,1)S(1)}, u32[]{:S(2)}, u32[]{:S(2)}) %collective-permute-start.28) | collective-permute-done | bytes 94240 | tf_op jit(solution)/shard_map/ppermute | solution.py:53
  65.2 2.2 %collective-permute-done.27.a = bf16[16,2944]{1,0:T(8,128)(2,1)S(1)} collective-permute-done((bf16[16,2944]{1,0:T(8,128)(2,1)S(1)}, bf16[16,2944]{1,0:T(8,128)(2,1)S(1)}, u32[]{:S(2)}, u32[]{:S(2)}) %collective-permute-start.27) | collective-permute-done | bytes 94240 | tf_op jit(solution)/shard_map/ppermute | solution.py:53
  67.4 0.3 shard_map.125
  67.7 4.5 %collective-permute-start.32 = (bf16[16,256]{1,0:T(8,128)(2,1)S(1)}, bf16[16,256]{1,0:T(8,128)(2,1)S(1)}, u32[]{:S(2)}, u32[]{:S(2)}) collective-permute-start(bf16[16,256]{1,0:T(8,128)(2,1)S(1)} %shard_map.125), channel_id=1, source_target_pairs={{0,3},{1,2},{2,1},{3,0},{4,7},{5,6},{6,5},{7,4},{8,11},{9,10},{10,... | collective-permute-start | bytes 24584 | tf_op jit(solution)/shard_map/ppermute | solution.py:36
  72.2 1.3 %collective-permute-start.31 = (bf16[16,256]{1,0:T(8,128)(2,1)S(1)}, bf16[16,256]{1,0:T(8,128)(2,1)S(1)}, u32[]{:S(2)}, u32[]{:S(2)}) collective-permute-start(bf16[16,256]{1,0:T(8,128)(2,1)S(1)} %shard_map.125), channel_id=1, source_target_pairs={{0,7},{1,6},{2,5},{3,4},{4,3},{5,2},{6,1},{7,0},{8,15},{9,14},{10,... | collective-permute-start | bytes 24584 | tf_op jit(solution)/shard_map/ppermute | solution.py:36
  73.6 1.2 %collective-permute-start.30 = (bf16[16,256]{1,0:T(8,128)(2,1)S(1)}, bf16[16,256]{1,0:T(8,128)(2,1)S(1)}, u32[]{:S(2)}, u32[]{:S(2)}) collective-permute-start(bf16[16,256]{1,0:T(8,128)(2,1)S(1)} %shard_map.125), channel_id=1, source_target_pairs={{0,5},{1,4},{2,7},{3,6},{4,1},{5,0},{6,3},{7,2},{8,13},{9,12},{10,... | collective-permute-start | bytes 24584 | tf_op jit(solution)/shard_map/ppermute | solution.py:36
  74.8 1.8 %collective-permute-done.31 = bf16[16,256]{1,0:T(8,128)(2,1)S(1)} collective-permute-done((bf16[16,256]{1,0:T(8,128)(2,1)S(1)}, bf16[16,256]{1,0:T(8,128)(2,1)S(1)}, u32[]{:S(2)}, u32[]{:S(2)}) %collective-permute-start.31) | collective-permute-done | bytes 8224 | tf_op jit(solution)/shard_map/ppermute | solution.py:36
  76.5 1.6 %collective-permute-done.30 = bf16[16,256]{1,0:T(8,128)(2,1)S(1)} collective-permute-done((bf16[16,256]{1,0:T(8,128)(2,1)S(1)}, bf16[16,256]{1,0:T(8,128)(2,1)S(1)}, u32[]{:S(2)}, u32[]{:S(2)}) %collective-permute-start.30) | collective-permute-done | bytes 8224 | tf_op jit(solution)/shard_map/ppermute | solution.py:36
  78.2 1.0 %collective-permute-start.33 = (f32[16,256]{1,0:T(8,128)S(1)}, f32[16,256]{1,0:T(8,128)S(1)}, u32[]{:S(2)}, u32[]{:S(2)}) collective-permute-start(f32[16,256]{1,0:T(8,128)S(1)} %convert_add_fusion), channel_id=1, source_target_pairs={{0,1},{1,0},{2,3},{3,2},{4,5},{5,4},{6,7},{7,6},{8,9},{9,8},{10,11... | collective-permute-start | bytes 49160 | tf_op jit(solution)/shard_map/ppermute | solution.py:58
  79.1 0.8 %collective-permute-done.33 = f32[16,256]{1,0:T(8,128)S(1)} collective-permute-done((f32[16,256]{1,0:T(8,128)S(1)}, f32[16,256]{1,0:T(8,128)S(1)}, u32[]{:S(2)}, u32[]{:S(2)}) %collective-permute-start.33) | collective-permute-done | bytes 16416 | tf_op jit(solution)/shard_map/ppermute | solution.py:58
  80.0 0.7 fusion.3
  (39 shorter events, 0.3 us)
Async XLA Ops:
  0.0 11.3 %copy-start.8 = (bf16[256,512]{1,0:T(8,128)(2,1)S(1)}, bf16[256,512]{1,0:T(8,128)(2,1)}, u32[]{:S(2)}) copy-start(bf16[256,512]{1,0:T(8,128)(2,1)} %weight.3) | copy-start | bytes 786436
  0.0 11.3 %copy-start.9 = (f32[256]{0:T(256)S(1)}, f32[256]{0:T(256)}, u32[]{:S(2)}) copy-start(f32[256]{0:T(256)} %param.13) | copy-start | bytes 3076
  0.8 2.3 %collective-permute-start = (f32[24,128]{1,0:T(8,128)S(1)}, f32[24,128]{1,0:T(8,128)S(1)}, u32[]{:S(2)}, u32[]{:S(2)}) collective-permute-start(f32[24,128]{1,0:T(8,128)S(1)} %shard_map.118), channel_id=1, source_target_pairs={{0,1},{1,0},{2,3},{3,2},{4,5},{5,4},{6,7},{7,6},{8,9},{9,8},{10,11... | collective-permute-start | bytes 36872 | tf_op jit(solution)/shard_map/ppermute | solution.py:58
  3.1 4.1 %collective-permute-start.3 = (f32[24,128]{1,0:T(8,128)S(1)}, f32[24,128]{1,0:T(8,128)S(1)}, u32[]{:S(2)}, u32[]{:S(2)}) collective-permute-start(f32[24,128]{1,0:T(8,128)S(1)} %fusion.2.own), channel_id=1, source_target_pairs={{0,3},{1,2},{2,1},{3,0},{4,7},{5,6},{6,5},{7,4},{8,11},{9,10},{10,... | collective-permute-start | bytes 36872 | tf_op jit(solution)/shard_map/ppermute | solution.py:36
  4.8 4.3 %collective-permute-start.2 = (f32[24,128]{1,0:T(8,128)S(1)}, f32[24,128]{1,0:T(8,128)S(1)}, u32[]{:S(2)}, u32[]{:S(2)}) collective-permute-start(f32[24,128]{1,0:T(8,128)S(1)} %fusion.2.own), channel_id=1, source_target_pairs={{0,7},{1,6},{2,5},{3,4},{4,3},{5,2},{6,1},{7,0},{8,15},{9,14},{10,... | collective-permute-start | bytes 36872 | tf_op jit(solution)/shard_map/ppermute | solution.py:36
  6.6 4.6 %collective-permute-start.1 = (f32[24,128]{1,0:T(8,128)S(1)}, f32[24,128]{1,0:T(8,128)S(1)}, u32[]{:S(2)}, u32[]{:S(2)}) collective-permute-start(f32[24,128]{1,0:T(8,128)S(1)} %fusion.2.own), channel_id=1, source_target_pairs={{0,5},{1,4},{2,7},{3,6},{4,1},{5,0},{6,3},{7,2},{8,13},{9,12},{10,... | collective-permute-start | bytes 36872 | tf_op jit(solution)/shard_map/ppermute | solution.py:36
  11.3 17.8 %copy-start = (bf16[16,1024,1,128]{3,1,2,0:T(8,128)(2,1)S(1)}, bf16[16,1024,1,128]{3,1,2,0:T(8,128)(2,1)}, u32[]{:S(2)}) copy-start(bf16[16,1024,1,128]{3,1,2,0:T(8,128)(2,1)} %param.15) | copy-start | bytes 12582916
  11.3 17.8 %copy-start.1 = (bf16[16,1024,1,128]{3,1,2,0:T(8,128)(2,1)S(1)}, bf16[16,1024,1,128]{3,1,2,0:T(8,128)(2,1)}, u32[]{:S(2)}) copy-start(bf16[16,1024,1,128]{3,1,2,0:T(8,128)(2,1)} %param.16) | copy-start | bytes 12582916
  11.4 4.6 %collective-permute-start.7 = (f32[72,128]{1,0:T(8,128)S(1)}, f32[72,128]{1,0:T(8,128)S(1)}, u32[]{:S(2)}, u32[]{:S(2)}) collective-permute-start(f32[72,128]{1,0:T(8,128)S(1)} %get-tuple-element.16), channel_id=1, source_target_pairs={{0,9},{1,8},{8,1},{9,0},{16,25},{17,24},{24,17},{25,16},{2,11},{3,... | collective-permute-start | bytes 110600 | tf_op jit(solution)/shard_map/ppermute | solution.py:36
  13.0 4.6 %collective-permute-start.6 = (f32[72,128]{1,0:T(8,128)S(1)}, f32[72,128]{1,0:T(8,128)S(1)}, u32[]{:S(2)}, u32[]{:S(2)}) collective-permute-start(f32[72,128]{1,0:T(8,128)S(1)} %get-tuple-element.16), channel_id=1, source_target_pairs={{0,25},{1,24},{8,17},{9,16},{16,9},{17,8},{24,1},{25,0},{2,27},{3,... | collective-permute-start | bytes 110600 | tf_op jit(solution)/shard_map/ppermute | solution.py:36
  14.9 4.9 %collective-permute-start.5 = (f32[72,128]{1,0:T(8,128)S(1)}, f32[72,128]{1,0:T(8,128)S(1)}, u32[]{:S(2)}, u32[]{:S(2)}) collective-permute-start(f32[72,128]{1,0:T(8,128)S(1)} %get-tuple-element.16), channel_id=1, source_target_pairs={{0,17},{1,16},{8,25},{9,24},{16,1},{17,0},{24,9},{25,8},{2,19},{3,... | collective-permute-start | bytes 110600 | tf_op jit(solution)/shard_map/ppermute | solution.py:36
  15.6 4.2 %collective-permute-start.4 = (f32[72,128]{1,0:T(8,128)S(1)}, f32[72,128]{1,0:T(8,128)S(1)}, u32[]{:S(2)}, u32[]{:S(2)}) collective-permute-start(f32[72,128]{1,0:T(8,128)S(1)} %get-tuple-element.16), channel_id=1, source_target_pairs={{0,1},{1,0},{2,3},{3,2},{4,5},{5,4},{6,7},{7,6},{8,9},{9,8},{10,11... | collective-permute-start | bytes 110600 | tf_op jit(solution)/shard_map/ppermute | solution.py:58
  19.9 5.7 %collective-permute-start.11 = (f32[72,128]{1,0:T(8,128)S(1)}, f32[72,128]{1,0:T(8,128)S(1)}, u32[]{:S(2)}, u32[]{:S(2)}) collective-permute-start(f32[72,128]{1,0:T(8,128)S(1)} %add_add_fusion), channel_id=1, source_target_pairs={{0,33},{1,32},{32,1},{33,0},{64,97},{65,96},{96,65},{97,64},{2,35}... | collective-permute-start | bytes 110600 | tf_op jit(solution)/shard_map/ppermute | solution.py:36
  21.8 4.6 %collective-permute-start.10 = (f32[72,128]{1,0:T(8,128)S(1)}, f32[72,128]{1,0:T(8,128)S(1)}, u32[]{:S(2)}, u32[]{:S(2)}) collective-permute-start(f32[72,128]{1,0:T(8,128)S(1)} %add_add_fusion), channel_id=1, source_target_pairs={{0,97},{1,96},{32,65},{33,64},{64,33},{65,32},{96,1},{97,0},{2,99}... | collective-permute-start | bytes 110600 | tf_op jit(solution)/shard_map/ppermute | solution.py:36
  24.1 4.9 %collective-permute-start.9 = (f32[72,128]{1,0:T(8,128)S(1)}, f32[72,128]{1,0:T(8,128)S(1)}, u32[]{:S(2)}, u32[]{:S(2)}) collective-permute-start(f32[72,128]{1,0:T(8,128)S(1)} %add_add_fusion), channel_id=1, source_target_pairs={{0,65},{1,64},{32,97},{33,96},{64,1},{65,0},{96,33},{97,32},{2,67}... | collective-permute-start | bytes 110600 | tf_op jit(solution)/shard_map/ppermute | solution.py:36
  25.2 3.9 %collective-permute-start.8 = (f32[72,128]{1,0:T(8,128)S(1)}, f32[72,128]{1,0:T(8,128)S(1)}, u32[]{:S(2)}, u32[]{:S(2)}) collective-permute-start(f32[72,128]{1,0:T(8,128)S(1)} %add_add_fusion), channel_id=1, source_target_pairs={{0,1},{1,0},{2,3},{3,2},{4,5},{5,4},{6,7},{7,6},{8,9},{9,8},{10,11... | collective-permute-start | bytes 110600 | tf_op jit(solution)/shard_map/ppermute | solution.py:58
  29.1 15.3 %copy-start.5 = (bf16[512,256]{1,0:T(8,128)(2,1)S(1)}, bf16[512,256]{1,0:T(8,128)(2,1)}, u32[]{:S(2)}) copy-start(bf16[512,256]{1,0:T(8,128)(2,1)} %weight.4) | copy-start | bytes 786436
  29.1 15.3 %copy-start.6 = (f32[4]{0:T(128)S(1)}, f32[4]{0:T(128)}, u32[]{:S(2)}) copy-start(f32[4]{0:T(128)} %param.17) | copy-start | bytes 52
  29.1 15.3 %copy-start.7 = (f32[128]{0:T(128)S(1)}, f32[128]{0:T(128)}, u32[]{:S(2)}) copy-start(f32[128]{0:T(128)} %param.18) | copy-start | bytes 1540
  29.1 22.8 %copy-start.2 = (bf16[256,1408]{1,0:T(8,128)(2,1)S(1)}, bf16[256,1408]{1,0:T(8,128)(2,1)}, u32[]{:S(2)}) copy-start(bf16[256,1408]{1,0:T(8,128)(2,1)} %gate.1) | copy-start | bytes 2162692
  29.1 22.8 %copy-start.3 = (bf16[256,1408]{1,0:T(8,128)(2,1)S(1)}, bf16[256,1408]{1,0:T(8,128)(2,1)}, u32[]{:S(2)}) copy-start(bf16[256,1408]{1,0:T(8,128)(2,1)} %up.1) | copy-start | bytes 2162692
  29.1 38.3 %copy-start.4 = (bf16[1408,256]{1,0:T(8,128)(2,1)S(1)}, bf16[1408,256]{1,0:T(8,128)(2,1)}, u32[]{:S(2)}) copy-start(bf16[1408,256]{1,0:T(8,128)(2,1)} %weight.5) | copy-start | bytes 2162692
  31.0 6.3 %collective-permute-start.12 = (f32[136,128]{1,0:T(8,128)S(1)}, f32[136,128]{1,0:T(8,128)S(1)}, u32[]{:S(2)}, u32[]{:S(2)}) collective-permute-start(f32[136,128]{1,0:T(8,128)S(1)} %get-tuple-element.17), channel_id=1, source_target_pairs={{0,1},{1,0},{2,3},{3,2},{4,5},{5,4},{6,7},{7,6},{8,9},{9,8},{10,11... | collective-permute-start | bytes 208904 | tf_op jit(solution)/shard_map/ppermute | solution.py:58
  31.4 3.6 %collective-permute-start.15 = (bf16[144,128]{1,0:T(8,128)(2,1)S(1)}, bf16[144,128]{1,0:T(8,128)(2,1)S(1)}, u32[]{:S(2)}, u32[]{:S(2)}) collective-permute-start(bf16[144,128]{1,0:T(8,128)(2,1)S(1)} %get-tuple-element.18), channel_id=1, source_target_pairs={{0,9},{1,8},{8,1},{9,0},{16,25},{17,24},{24,17},{25,16},{2,11},{3,... | collective-permute-start | bytes 110600 | tf_op jit(solution)/shard_map/ppermute | solution.py:36
  31.9 4.6 %collective-permute-start.14 = (bf16[144,128]{1,0:T(8,128)(2,1)S(1)}, bf16[144,128]{1,0:T(8,128)(2,1)S(1)}, u32[]{:S(2)}, u32[]{:S(2)}) collective-permute-start(bf16[144,128]{1,0:T(8,128)(2,1)S(1)} %get-tuple-element.18), channel_id=1, source_target_pairs={{0,25},{1,24},{8,17},{9,16},{16,9},{17,8},{24,1},{25,0},{2,27},{3,... | collective-permute-start | bytes 110600 | tf_op jit(solution)/shard_map/ppermute | solution.py:36
  32.4 4.9 %collective-permute-start.13 = (bf16[144,128]{1,0:T(8,128)(2,1)S(1)}, bf16[144,128]{1,0:T(8,128)(2,1)S(1)}, u32[]{:S(2)}, u32[]{:S(2)}) collective-permute-start(bf16[144,128]{1,0:T(8,128)(2,1)S(1)} %get-tuple-element.18), channel_id=1, source_target_pairs={{0,17},{1,16},{8,25},{9,24},{16,1},{17,0},{24,9},{25,8},{2,19},{3,... | collective-permute-start | bytes 110600 | tf_op jit(solution)/shard_map/ppermute | solution.py:36
  37.6 6.8 %collective-permute-start.16 = (f32[136,128]{1,0:T(8,128)S(1)}, f32[136,128]{1,0:T(8,128)S(1)}, u32[]{:S(2)}, u32[]{:S(2)}) collective-permute-start(f32[136,128]{1,0:T(8,128)S(1)} %get-tuple-element.19), channel_id=1, source_target_pairs={{0,1},{1,0},{2,3},{3,2},{4,5},{5,4},{6,7},{7,6},{8,9},{9,8},{10,11... | collective-permute-start | bytes 208904 | tf_op jit(solution)/shard_map/ppermute | solution.py:58
  38.0 3.6 %collective-permute-start.19 = (bf16[144,128]{1,0:T(8,128)(2,1)S(1)}, bf16[144,128]{1,0:T(8,128)(2,1)S(1)}, u32[]{:S(2)}, u32[]{:S(2)}) collective-permute-start(bf16[144,128]{1,0:T(8,128)(2,1)S(1)} %get-tuple-element.20), channel_id=1, source_target_pairs={{0,33},{1,32},{32,1},{33,0},{64,97},{65,96},{96,65},{97,64},{2,35}... | collective-permute-start | bytes 110600 | tf_op jit(solution)/shard_map/ppermute | solution.py:36
  38.8 4.6 %collective-permute-start.18 = (bf16[144,128]{1,0:T(8,128)(2,1)S(1)}, bf16[144,128]{1,0:T(8,128)(2,1)S(1)}, u32[]{:S(2)}, u32[]{:S(2)}) collective-permute-start(bf16[144,128]{1,0:T(8,128)(2,1)S(1)} %get-tuple-element.20), channel_id=1, source_target_pairs={{0,97},{1,96},{32,65},{33,64},{64,33},{65,32},{96,1},{97,0},{2,99}... | collective-permute-start | bytes 110600 | tf_op jit(solution)/shard_map/ppermute | solution.py:36
  39.4 4.9 %collective-permute-start.17 = (bf16[144,128]{1,0:T(8,128)(2,1)S(1)}, bf16[144,128]{1,0:T(8,128)(2,1)S(1)}, u32[]{:S(2)}, u32[]{:S(2)}) collective-permute-start(bf16[144,128]{1,0:T(8,128)(2,1)S(1)} %get-tuple-element.20), channel_id=1, source_target_pairs={{0,65},{1,64},{32,97},{33,96},{64,1},{65,0},{96,33},{97,32},{2,67}... | collective-permute-start | bytes 110600 | tf_op jit(solution)/shard_map/ppermute | solution.py:36
  44.9 3.8 %collective-permute-start.22 = (bf16[16,256]{1,0:T(8,128)(2,1)S(1)}, bf16[16,256]{1,0:T(8,128)(2,1)S(1)}, u32[]{:S(2)}, u32[]{:S(2)}) collective-permute-start(bf16[16,256]{1,0:T(8,128)(2,1)S(1)} %shard_map.122), channel_id=1, source_target_pairs={{0,3},{1,2},{2,1},{3,0},{4,7},{5,6},{6,5},{7,4},{8,11},{9,10},{10,... | collective-permute-start | bytes 24584 | tf_op jit(solution)/shard_map/ppermute | solution.py:36
  45.4 4.6 %collective-permute-start.21 = (bf16[16,256]{1,0:T(8,128)(2,1)S(1)}, bf16[16,256]{1,0:T(8,128)(2,1)S(1)}, u32[]{:S(2)}, u32[]{:S(2)}) collective-permute-start(bf16[16,256]{1,0:T(8,128)(2,1)S(1)} %shard_map.122), channel_id=1, source_target_pairs={{0,7},{1,6},{2,5},{3,4},{4,3},{5,2},{6,1},{7,0},{8,15},{9,14},{10,... | collective-permute-start | bytes 24584 | tf_op jit(solution)/shard_map/ppermute | solution.py:36
  46.1 4.6 %collective-permute-start.20 = (bf16[16,256]{1,0:T(8,128)(2,1)S(1)}, bf16[16,256]{1,0:T(8,128)(2,1)S(1)}, u32[]{:S(2)}, u32[]{:S(2)}) collective-permute-start(bf16[16,256]{1,0:T(8,128)(2,1)S(1)} %shard_map.122), channel_id=1, source_target_pairs={{0,5},{1,4},{2,7},{3,6},{4,1},{5,0},{6,3},{7,2},{8,13},{9,12},{10,... | collective-permute-start | bytes 24584 | tf_op jit(solution)/shard_map/ppermute | solution.py:36
  50.7 1.3 %collective-permute-start.23 = (f32[16,256]{1,0:T(8,128)S(1)}, f32[16,256]{1,0:T(8,128)S(1)}, u32[]{:S(2)}, u32[]{:S(2)}) collective-permute-start(f32[16,256]{1,0:T(8,128)S(1)} %convert_add_fusion.1.attn), channel_id=1, source_target_pairs={{0,1},{1,0},{2,3},{3,2},{4,5},{5,4},{6,7},{7,6},{8,9},{9,8},{10,11... | collective-permute-start | bytes 49160 | tf_op jit(solution)/shard_map/ppermute | solution.py:58
  52.2 3.8 %collective-permute-start.26 = (bf16[16,2944]{1,0:T(8,128)(2,1)S(1)}, bf16[16,2944]{1,0:T(8,128)(2,1)S(1)}, u32[]{:S(2)}, u32[]{:S(2)}) collective-permute-start(bf16[16,2944]{1,0:T(8,128)(2,1)S(1)} %get-tuple-element.24), channel_id=1, source_target_pairs={{0,8},{1,33},{8,0},{9,41},{16,24},{17,49},{24,16},{25,57},{32,40},... | collective-permute-start | bytes 282632 | tf_op jit(solution)/shard_map/ppermute | solution.py:53
  52.4 4.6 %collective-permute-start.25 = (bf16[16,2944]{1,0:T(8,128)(2,1)S(1)}, bf16[16,2944]{1,0:T(8,128)(2,1)S(1)}, u32[]{:S(2)}, u32[]{:S(2)}) collective-permute-start(bf16[16,2944]{1,0:T(8,128)(2,1)S(1)} %get-tuple-element.24), channel_id=1, source_target_pairs={{0,24},{1,97},{8,16},{9,105},{16,8},{17,113},{24,0},{25,121},{32,5... | collective-permute-start | bytes 282632 | tf_op jit(solution)/shard_map/ppermute | solution.py:53
  54.6 4.9 %collective-permute-start.24 = (bf16[16,2944]{1,0:T(8,128)(2,1)S(1)}, bf16[16,2944]{1,0:T(8,128)(2,1)S(1)}, u32[]{:S(2)}, u32[]{:S(2)}) collective-permute-start(bf16[16,2944]{1,0:T(8,128)(2,1)S(1)} %get-tuple-element.24), channel_id=1, source_target_pairs={{0,16},{1,65},{8,24},{9,73},{16,0},{17,81},{24,8},{25,89},{32,48},... | collective-permute-start | bytes 282632 | tf_op jit(solution)/shard_map/ppermute | solution.py:53
  59.7 3.8 %collective-permute-start.29 = (bf16[16,2944]{1,0:T(8,128)(2,1)S(1)}, bf16[16,2944]{1,0:T(8,128)(2,1)S(1)}, u32[]{:S(2)}, u32[]{:S(2)}) collective-permute-start(bf16[16,2944]{1,0:T(8,128)(2,1)S(1)} %get-tuple-element.26), channel_id=1, source_target_pairs={{0,32},{1,9},{8,40},{9,1},{16,48},{17,25},{24,56},{25,17},{32,0},{... | collective-permute-start | bytes 282632 | tf_op jit(solution)/shard_map/ppermute | solution.py:53
  60.6 4.6 %collective-permute-start.28 = (bf16[16,2944]{1,0:T(8,128)(2,1)S(1)}, bf16[16,2944]{1,0:T(8,128)(2,1)S(1)}, u32[]{:S(2)}, u32[]{:S(2)}) collective-permute-start(bf16[16,2944]{1,0:T(8,128)(2,1)S(1)} %get-tuple-element.26), channel_id=1, source_target_pairs={{0,96},{1,25},{8,104},{9,17},{16,112},{17,9},{24,120},{25,1},{32,6... | collective-permute-start | bytes 282632 | tf_op jit(solution)/shard_map/ppermute | solution.py:53
  62.5 4.9 %collective-permute-start.27 = (bf16[16,2944]{1,0:T(8,128)(2,1)S(1)}, bf16[16,2944]{1,0:T(8,128)(2,1)S(1)}, u32[]{:S(2)}, u32[]{:S(2)}) collective-permute-start(bf16[16,2944]{1,0:T(8,128)(2,1)S(1)} %get-tuple-element.26), channel_id=1, source_target_pairs={{0,64},{1,17},{8,72},{9,25},{16,80},{17,1},{24,88},{25,9},{32,96},... | collective-permute-start | bytes 282632 | tf_op jit(solution)/shard_map/ppermute | solution.py:53
  67.7 7.0 %collective-permute-start.32 = (bf16[16,256]{1,0:T(8,128)(2,1)S(1)}, bf16[16,256]{1,0:T(8,128)(2,1)S(1)}, u32[]{:S(2)}, u32[]{:S(2)}) collective-permute-start(bf16[16,256]{1,0:T(8,128)(2,1)S(1)} %shard_map.125), channel_id=1, source_target_pairs={{0,3},{1,2},{2,1},{3,0},{4,7},{5,6},{6,5},{7,4},{8,11},{9,10},{10,... | collective-permute-start | bytes 24584 | tf_op jit(solution)/shard_map/ppermute | solution.py:36
  72.2 4.3 %collective-permute-start.31 = (bf16[16,256]{1,0:T(8,128)(2,1)S(1)}, bf16[16,256]{1,0:T(8,128)(2,1)S(1)}, u32[]{:S(2)}, u32[]{:S(2)}) collective-permute-start(bf16[16,256]{1,0:T(8,128)(2,1)S(1)} %shard_map.125), channel_id=1, source_target_pairs={{0,7},{1,6},{2,5},{3,4},{4,3},{5,2},{6,1},{7,0},{8,15},{9,14},{10,... | collective-permute-start | bytes 24584 | tf_op jit(solution)/shard_map/ppermute | solution.py:36
  73.6 4.6 %collective-permute-start.30 = (bf16[16,256]{1,0:T(8,128)(2,1)S(1)}, bf16[16,256]{1,0:T(8,128)(2,1)S(1)}, u32[]{:S(2)}, u32[]{:S(2)}) collective-permute-start(bf16[16,256]{1,0:T(8,128)(2,1)S(1)} %shard_map.125), channel_id=1, source_target_pairs={{0,5},{1,4},{2,7},{3,6},{4,1},{5,0},{6,3},{7,2},{8,13},{9,12},{10,... | collective-permute-start | bytes 24584 | tf_op jit(solution)/shard_map/ppermute | solution.py:36
  78.2 1.8 %collective-permute-start.33 = (f32[16,256]{1,0:T(8,128)S(1)}, f32[16,256]{1,0:T(8,128)S(1)}, u32[]{:S(2)}, u32[]{:S(2)}) collective-permute-start(f32[16,256]{1,0:T(8,128)S(1)} %convert_add_fusion), channel_id=1, source_target_pairs={{0,1},{1,0},{2,3},{3,2},{4,5},{5,4},{6,7},{7,6},{8,9},{9,8},{10,11... | collective-permute-start | bytes 49160 | tf_op jit(solution)/shard_map/ppermute | solution.py:58
